TPU v7x, 32 devices: a whole 2x2x4 slice. The times are simulated.
32 devices in a mesh: ep: 4 (over y, x), tp: 8 (over z, core).
Axes of the slice: x: 2, y: 2, z: 4, core: 2. Of those that a mesh axis runs over, the one named last changes fastest.
Arguments:
- queries: bfloat16 [3072, 2048], P('ep', 'tp'), may hold values from -6 to 6
- keys: bfloat16 [3072, 512], P('ep'), may hold values from -6 to 6
- values: bfloat16 [3072, 512], P('ep'), may hold values from -6 to 6
- query_gain: float32 [128], replicated, may hold values from 1 to 4.5
- key_gain: float32 [128], replicated, may hold values from 1 to 4.5
- out_weight: bfloat16 [2048, 2048], P('tp'), may hold values from -0.75 to 0.75
- tokens_b: bfloat16 [1536, 2048], P('ep'), may hold values from -6 to 6
- norm_gain: float32 [2048], replicated, may hold values from 0.1 to 1.9
- routes: int32 [1536, 2], P('ep'), may hold values from 0 to 15, all different within a row; in each aligned block of 48 rows (0 to 47, 48 to 95, ...) at most 8 rows name the same one
- route_weight: float32 [1536, 2], P('ep'), may hold values from 0.2 to 1
- gate_weight: bfloat16 [16, 2048, 4096], P('ep', None, 'tp'), may hold values from -0.125 to 0.125
- up_weight: bfloat16 [16, 2048, 4096], P('ep', None, 'tp'), may hold values from -0.125 to 0.125
- down_weight: bfloat16 [16, 4096, 2048], P('ep', 'tp'), may hold values from -0.09375 to 0.09375
Outputs:
- mixed_out: bfloat16 [3072, 2048], P(('ep', 'tp'))
- expert_out: bfloat16 [1536, 2048], P(('ep', 'tp'))
Inputs may be any that keep to these rules, and one draw needn't show every extreme that they name: `routes`: A row names 2 different experts. In each aligned block of 48 rows no expert is named more than 8 times, a bound that some block reaches.
All inputs are finite; a program needn't handle non-finite values.
Results may differ from a plain program's by a relative error of at most 0.019.
Values may be sent and summed in bfloat16 or wider, within the bound.
No kernel may reach another device: no remote copies, remote signals or barrier semaphores. Data moves between devices by JAX's collectives and lax.ppermute only.
A program may use at most 128 MiB of HBM per device.

v0:
```python
import jax
import jax.numpy as jnp
from jax import lax
from jax.sharding import PartitionSpec as P

D = 2048
HD = 128
HQ = 16
KVH = 4
EXPERTS = 16
TOPK = 2
GRID_W = 64
CAP = 8


EPS = 1e-06
THETA = 10000.0


def rotate(field, positions):
    n_freq = HD // 4
    row_pos = (positions // GRID_W).astype(jnp.float32)
    col_pos = (positions % GRID_W).astype(jnp.float32)
    inverse = THETA ** (-jnp.arange(n_freq, dtype=jnp.float32) / n_freq)
    angles = jnp.stack([row_pos[:, None] * inverse, col_pos[:, None] * inverse], axis=1)
    cosine = jnp.cos(angles)[:, None]
    sine = jnp.sin(angles)[:, None]
    length, n_heads = (field.shape[0], field.shape[1])
    halves = field.reshape(length, n_heads, 2, 2, n_freq)
    leading = halves[..., 0, :]
    second = halves[..., 1, :]
    turned = jnp.stack(
        [leading * cosine - second * sine, second * cosine + leading * sine], axis=-2
    )
    return turned.reshape(length, n_heads, HD)


def prepare(source, gain_vec, positions, n_heads):
    length = source.shape[0]
    field = source.astype(jnp.float32).reshape(length, n_heads, HD)
    field = field * lax.rsqrt(jnp.mean(field * field, axis=-1, keepdims=True) + EPS) * gain_vec
    return rotate(field, positions).astype(jnp.bfloat16)


def token_mixer(queries, keys, values, query_gain, key_gain, out_weight):
    n_rows = queries.shape[0]
    q_heads = queries.shape[1] // HD
    positions = lax.axis_index("ep") * n_rows + jnp.arange(n_rows, dtype=jnp.int32)
    query_n = prepare(queries, query_gain, positions, q_heads).reshape(n_rows * q_heads, HD)
    kv_index = lax.axis_index("tp") * q_heads // (HQ // KVH)
    own_keys = prepare(
        lax.dynamic_slice_in_dim(keys, kv_index * HD, HD, 1), key_gain, positions, 1
    ).reshape(n_rows, HD)
    own_values = lax.dynamic_slice_in_dim(values, kv_index * HD, HD, 1)
    score_scale = HD ** (-0.5)
    start_state = (
        jnp.full((n_rows * q_heads,), -1e30, jnp.float32),
        jnp.zeros((n_rows * q_heads,), jnp.float32),
        jnp.zeros((n_rows * q_heads, HD), jnp.float32),
    )
    key_piece = lax.all_gather(own_keys, "ep", axis=0, tiled=True)
    value_piece = lax.all_gather(own_values, "ep", axis=0, tiled=True)
    steps_n = key_piece.shape[0] // n_rows

    def one_block(index_b, state):
        running_max, totals, numerator = state
        key_blk = lax.dynamic_slice_in_dim(key_piece, index_b * n_rows, n_rows, 0)
        value_blk = lax.dynamic_slice_in_dim(value_piece, index_b * n_rows, n_rows, 0)
        scores = (
            jnp.einsum("qd,sd->qs", query_n, key_blk, preferred_element_type=jnp.float32)
            * score_scale
        )
        new_max = jnp.maximum(running_max, jnp.max(scores, axis=1))
        shrink = jnp.exp(running_max - new_max)
        weights = jnp.exp(scores - new_max[:, None])
        totals = totals * shrink + jnp.sum(weights, axis=1)
        numerator = numerator * shrink[:, None] + jnp.dot(
            weights.astype(jnp.bfloat16), value_blk, preferred_element_type=jnp.float32
        )
        return (new_max, totals, numerator)

    running_max, totals, numerator = lax.fori_loop(0, steps_n, one_block, start_state)
    attended = (numerator / totals[:, None]).astype(jnp.bfloat16).reshape(n_rows, q_heads * HD)
    return lax.psum_scatter(
        jnp.dot(attended, out_weight, preferred_element_type=jnp.float32).astype(jnp.bfloat16),
        "tp",
        scatter_dimension=0,
        tiled=True,
    )


def expert_half(tokens_b, norm_gain, routes, route_weight, gate_weight, up_weight, down_weight):
    n_tp = lax.axis_size("tp")
    n_ep = lax.axis_size("ep")
    tp_index = lax.axis_index("tp")
    local_rows = tokens_b.shape[0]
    block_rows = local_rows // n_tp
    picks = block_rows * TOPK
    local_experts = gate_weight.shape[0]
    assigned = routes.reshape(n_tp, picks)
    onehot = (assigned[:, :, None] == jnp.arange(EXPERTS, dtype=jnp.int32)[None, None, :]).astype(
        jnp.int32
    )
    slot_rank = jnp.sum((jnp.cumsum(onehot, axis=1) - onehot) * onehot, axis=-1)
    target = assigned * CAP + slot_rank
    target_hot = (
        target[:, :, None] == jnp.arange(EXPERTS * CAP, dtype=jnp.int32)[None, None, :]
    ).astype(jnp.float32)
    token_hot = (
        jnp.arange(picks, dtype=jnp.int32)[:, None] // TOPK
        == jnp.arange(block_rows, dtype=jnp.int32)[None, :]
    ).astype(jnp.float32)
    field = tokens_b.astype(jnp.float32)
    normed = (
        field * lax.rsqrt(jnp.mean(field * field, axis=-1, keepdims=True) + EPS) * norm_gain
    ).astype(jnp.bfloat16)
    dispatch_mat = jnp.einsum(
        "baj,at->bjt", target_hot, token_hot, precision=lax.Precision.HIGHEST
    ).astype(jnp.bfloat16)
    outgoing = jnp.einsum(
        "bjt,btd->bjd",
        dispatch_mat,
        normed.reshape(n_tp, block_rows, D),
        preferred_element_type=jnp.float32,
    )
    outgoing = outgoing.astype(jnp.bfloat16).reshape(n_tp, EXPERTS, CAP, D)
    arrived = lax.all_to_all(outgoing, "ep", split_axis=1, concat_axis=2, tiled=True)
    flat_rows = arrived.reshape(-1, D)
    share_rows = flat_rows.shape[0] // n_tp
    expert_slab_rows = flat_rows.reshape(
        share_rows * lax.axis_size("tp") // share_rows, local_experts, n_ep * CAP, D
    )
    gate_act = jnp.einsum(
        "blmd,ldf->blmf", expert_slab_rows, gate_weight, preferred_element_type=jnp.float32
    )
    up_act = jnp.einsum(
        "blmd,ldf->blmf", expert_slab_rows, up_weight, preferred_element_type=jnp.float32
    )
    hidden = (jax.nn.silu(gate_act) * up_act).astype(jnp.bfloat16)
    result = jnp.einsum("blmf,lfd->blmd", hidden, down_weight, preferred_element_type=jnp.float32)
    summed = lax.psum_scatter(
        result.reshape(-1, D).astype(jnp.bfloat16), "tp", scatter_dimension=0, tiled=True
    )
    returned = lax.all_to_all(
        summed.reshape(local_experts, n_ep, CAP, D), "ep", split_axis=1, concat_axis=0, tiled=True
    )
    returned = returned.reshape(EXPERTS * CAP, D)
    own_target = lax.dynamic_index_in_dim(target_hot, tp_index, 0, keepdims=False)
    shares = (route_weight / jnp.sum(route_weight, axis=-1, keepdims=True)).reshape(n_tp, picks)
    own_shares = lax.dynamic_index_in_dim(shares, tp_index, 0, keepdims=False)
    combine = jnp.einsum(
        "at,aj->tj", token_hot, own_target * own_shares[:, None], precision=lax.Precision.HIGHEST
    )
    return jnp.dot(combine, returned.astype(jnp.float32), precision=lax.Precision.HIGHEST).astype(
        jnp.bfloat16
    )


def on_device(
    queries,
    keys,
    values,
    query_gain,
    key_gain,
    out_weight,
    tokens_b,
    norm_gain,
    routes,
    route_weight,
    gate_weight,
    up_weight,
    down_weight,
):
    mixed_out = token_mixer(queries, keys, values, query_gain, key_gain, out_weight)
    expert_out = expert_half(
        tokens_b, norm_gain, routes, route_weight, gate_weight, up_weight, down_weight
    )
    return (mixed_out, expert_out)


def solution(mesh):
    placed = (
        P("ep", "tp"),
        P("ep", None),
        P("ep", None),
        P(),
        P(),
        P("tp", None),
        P("ep", None),
        P(),
        P("ep", None),
        P("ep", None),
        P("ep", None, "tp"),
        P("ep", None, "tp"),
        P("ep", "tp", None),
    )
    return jax.shard_map(
        on_device,
        mesh=mesh,
        in_specs=placed,
        out_specs=(P(("ep", "tp"), None), P(("ep", "tp"), None)),
        check_vma=False,
    )
```

profile of v0, /device:TPU:0, one launch (start us, length us, event | category | flops | bytes accessed | tf_op | source)
XLA Modules:
  0.0 199.7 jit_solution(16089087401707294677)
XLA Ops:
  7.2 1.9 fusion.24
  9.1 0.8 copy.47
  9.9 0.1 reshape.432
  10.1 1.9 select_reduce_fusion
  12.1 0.3 convolution_convert_fusion.2
  12.5 1.8 fusion.26
  14.3 1.3 convert_bitcast_fusion.1
  15.6 2.3 %copy.51 = bf16[8,16,8,2048]{3,2,0,1:T(8,128)(2,1)} copy(bf16[8,16,8,2048]{3,2,1,0:T(8,128)(2,1)S(1)} %convert_bitcast_fusion.1) | data formatting | bytes 8388608 | tf_op jit(solution)/shard_map/reshape | solution.py:126
  17.9 5.3 %all-to-all-start = ((bf16[8,16,8,2048]{3,2,0,1:T(8,128)(2,1)}), bf16[8,16,8,2048]{3,2,0,1:T(8,128)(2,1)}, u32[]{:S(2)}, u32[]{:S(2)}) async-start(bf16[8,16,8,2048]{3,2,0,1:T(8,128)(2,1)} %copy.51), calls=%async_computation.1 | async-start | bytes 8388608 | tf_op jit(solution)/shard_map/all_to_all | solution.py:127
  23.3 0.2 copy.44
  23.6 0.7 fusion.48
  24.7 47.1 %all-to-all-done = bf16[8,16,8,2048]{3,2,0,1:T(8,128)(2,1)} async-done(((bf16[8,16,8,2048]{3,2,0,1:T(8,128)(2,1)}), bf16[8,16,8,2048]{3,2,0,1:T(8,128)(2,1)}, u32[]{:S(2)}, u32[]{:S(2)}) %all-to-all-start) | async-done | bytes 4194336 | tf_op jit(solution)/shard_map/all_to_all | solution.py:127
  71.8 8.4 %fusion.16 = f32[4,8,32,512]{3,2,1,0:T(8,128)} fusion(bf16[4,2048,512]{2,1,0:T(8,128)(2,1)} %param.25, bf16[8,4,4,8,2048]{4,3,0,2,1:T(8,128)(2,1)} %bitcast.11), kind=kOutput, calls=%fused_computation.22 | convolution fusion | flops 2147483648 | bytes 14680064 | tf_op jit(solution)/shard_map/blmd,ldf->blmf/dot_general | solution.py:133
  80.2 14.2 %convert_bitcast_fusion = bf16[8,4,32,2048]{3,2,0,1:T(8,128)(2,1)} fusion(bf16[4,512,2048]{2,1,0:T(8,128)(2,1)} %param.27, f32[4,8,32,512]{3,2,1,0:T(8,128)} %fusion.16, bf16[4,2048,512]{2,1,0:T(8,128)(2,1)} %param.26, bf16[8,4,4,8,2048]{4,3,0,2,1:T(8,128)(2,1)} %bitcast.11), kind=kOutput, calls=%fused_computation.26 | convolution fusion | flops 4300210176 | bytes 27262976 | tf_op jit(solution)/shard_map/blmf,lfd->blmd/dot_general | solution.py:140
  94.4 4.7 %copy.53 = bf16[8,4,32,2048]{3,2,1,0:T(8,128)(2,1)} copy(bf16[8,4,32,2048]{3,2,0,1:T(8,128)(2,1)} %convert_bitcast_fusion) | data formatting | bytes 8388608 | tf_op jit(solution)/shard_map/convert_element_type | solution.py:142
  99.1 0.2 reduce-scatter.3.cloned.1.call-start
  99.3 0.9 constant_dynamic-slice_fusion.2
  100.3 0.1 copy.59
  100.5 2.9 %copy.45 = bf16[768,2,2,2,32]{4,3,2,1,0:T(2,128)(2,1)} copy(bf16[768,2,2,2,32]{0,4,3,2,1:T(8,128)(2,1)S(1)} %pad_maximum_fusion) | data formatting | bytes 786432 | tf_op jit(solution)/shard_map/stack | solution.py:32
  103.4 3.7 %convert_element_type.88 = bf16[1536,128]{1,0:T(8,128)(2,1)S(1)} reshape(bf16[768,2,2,2,32]{4,3,2,1,0:T(2,128)(2,1)} %copy.45) | data formatting | bytes 786432 | tf_op jit(solution)/shard_map/convert_element_type | solution.py:42
  107.1 0.9 constant_dynamic-slice_fusion.1
  108.2 0.7 subtract_convert_fusion.1
  109.0 12.7 %all_gather.6 = bf16[3072,128]{0,1:T(8,128)(2,1)S(1)} all-gather(bf16[768,128]{0,1:T(8,128)(2,1)S(1)} %bitcast.98), channel_id=1, replica_groups=mesh['ep'=4,'tp'=8] {'ep'}, dimensions={0}, use_global_device_ids=true | all-gather | bytes 983040 | tf_op jit(solution)/shard_map/all_gather | solution.py:61
  121.7 11.2 %all_gather.7 = bf16[3072,128]{1,0:T(8,128)(2,1)} all-gather(bf16[768,128]{1,0:T(8,128)(2,1)S(1)} %constant_dynamic-slice_fusion.1), channel_id=1, replica_groups=mesh['ep'=4,'tp'=8] {'ep'}, dimensions={0}, use_global_device_ids=true | all-gather | bytes 983040 | tf_op jit(solution)/shard_map/all_gather | solution.py:62
  132.9 15.4 %while.18 = (s32[]{:T(128)}, f32[1536]{0:T(1024)S(1)}, f32[1536]{0:T(1024)S(1)}, f32[1536,128]{1,0:T(8,128)S(1)}, bf16[3072,128]{0,1:T(8,128)(2,1)S(1)}, /*index...) while((s32[]{:T(128)}, f32[1536]{0:T(1024)S(1)}, ...), condition=%wide.region_5.6_spmd.clone, body=%wide.region_2.5_spmd.clone.sunk | while | flops 614014464 | bytes 16613559 | solution.py:82
  132.9 0.8 multiply_reduce_fusion.2
  133.8 0.8 fusion.86
  134.6 2.1 %convolution_add_fusion.2 = f32[1536,128]{1,0:T(8,128)S(1)} fusion(f32[768,1536]{1,0:T(8,128)S(1)} %get-tuple-element.254, f32[1536]{0:T(1024)S(1)} %select_maximum_fusion.2, f32[1536,128]{1,0:T(8,128)S(1)} %get-tuple-element.271, f32[1536]{0:T(1024)S(1)} %get-tuple-element.256, pred[]{:T(512)S(6)} %compare.22, ...), kind=kOutput, calls=%fused_computation.4.clone.1 | convolution fusion | flops 306118656 | bytes 6500357 | tf_op jit(solution)/shard_map/while/body/eval_jaxpr/dot_general | solution.py:77
  136.8 0.8 multiply_reduce_fusion.2
  137.6 0.8 fusion.86
  138.4 2.1 %convolution_add_fusion.2 = f32[1536,128]{1,0:T(8,128)S(1)} fusion(f32[768,1536]{1,0:T(8,128)S(1)} %get-tuple-element.254, f32[1536]{0:T(1024)S(1)} %select_maximum_fusion.2, f32[1536,128]{1,0:T(8,128)S(1)} %get-tuple-element.271, f32[1536]{0:T(1024)S(1)} %get-tuple-element.256, pred[]{:T(512)S(6)} %compare.22, ...), kind=kOutput, calls=%fused_computation.4.clone.1 | convolution fusion | flops 306118656 | bytes 6500357 | tf_op jit(solution)/shard_map/while/body/eval_jaxpr/dot_general | solution.py:77
  140.6 0.8 multiply_reduce_fusion.2
  141.5 0.8 fusion.86
  142.3 2.2 %convolution_add_fusion.2 = f32[1536,128]{1,0:T(8,128)S(1)} fusion(f32[768,1536]{1,0:T(8,128)S(1)} %get-tuple-element.254, f32[1536]{0:T(1024)S(1)} %select_maximum_fusion.2, f32[1536,128]{1,0:T(8,128)S(1)} %get-tuple-element.271, f32[1536]{0:T(1024)S(1)} %get-tuple-element.256, pred[]{:T(512)S(6)} %compare.22, ...), kind=kOutput, calls=%fused_computation.4.clone.1 | convolution fusion | flops 306118656 | bytes 6500357 | tf_op jit(solution)/shard_map/while/body/eval_jaxpr/dot_general | solution.py:77
  144.5 0.8 multiply_reduce_fusion.2
  145.3 0.8 fusion.86
  146.1 2.2 %convolution_add_fusion.2 = f32[1536,128]{1,0:T(8,128)S(1)} fusion(f32[768,1536]{1,0:T(8,128)S(1)} %get-tuple-element.254, f32[1536]{0:T(1024)S(1)} %select_maximum_fusion.2, f32[1536,128]{1,0:T(8,128)S(1)} %get-tuple-element.271, f32[1536]{0:T(1024)S(1)} %get-tuple-element.256, pred[]{:T(512)S(6)} %compare.22, ...), kind=kOutput, calls=%fused_computation.4.clone.1 | convolution fusion | flops 306118656 | bytes 6500357 | tf_op jit(solution)/shard_map/while/body/eval_jaxpr/dot_general | solution.py:77
  148.3 0.3 divide_convert_fusion
  148.8 2.7 %convolution_convert_fusion = bf16[768,2048]{1,0:T(8,128)(2,1)} fusion(bf16[768,256]{1,0:T(8,128)(2,1)S(1)} %reshape.431, bf16[256,2048]{1,0:T(8,128)(2,1)S(1)} %copy-done), kind=kOutput, calls=%fused_computation.32 | convolution fusion | flops 806879232 | bytes 4587520 | tf_op jit(solution)/shard_map/dot_general | solution.py:85
  151.5 0.2 iota_compare_fusion
  151.7 1.9 copy.54
  153.6 3.5 %all-to-all-start.1 = ((bf16[4,4,8,2048]{3,2,0,1:T(8,128)(2,1)}), bf16[4,4,8,2048]{3,2,0,1:T(8,128)(2,1)S(1)}, u32[]{:S(2)}, u32[]{:S(2)}) async-start(bf16[4,4,8,2048]{3,2,0,1:T(8,128)(2,1)} %copy.54), calls=%async_computation.3 | async-start | bytes 1048576 | tf_op jit(solution)/shard_map/all_to_all | solution.py:144
  157.1 0.1 copy.50
  157.2 0.1 reshape.433
  157.4 0.2 fusion.51
  157.6 6.0 %all-to-all-done.1 = bf16[4,4,8,2048]{3,2,0,1:T(8,128)(2,1)S(1)} async-done(((bf16[4,4,8,2048]{3,2,0,1:T(8,128)(2,1)}), bf16[4,4,8,2048]{3,2,0,1:T(8,128)(2,1)S(1)}, u32[]{:S(2)}, u32[]{:S(2)}) %all-to-all-start.1) | async-done | bytes 524320 | tf_op jit(solution)/shard_map/all_to_all | solution.py:144
  163.6 1.0 convolution_convert_fusion.1
  164.6 28.2 %reduce-scatter.3.cloned.1.call-done = bf16[96,2048]{1,0:T(8,128)(2,1)} async-done(((bf16[768,2048]{1,0:T(8,128)(2,1)}), bf16[96,2048]{1,0:T(8,128)(2,1)}) %reduce-scatter.3.cloned.1.call-update) | async-done | bytes 393232 | tf_op jit(solution)/shard_map/reduce_scatter | solution.py:84
  (51 shorter events, 1.3 us)
Async XLA Ops:
  7.2 141.6 %copy-start = (bf16[256,2048]{1,0:T(8,128)(2,1)S(1)}, bf16[256,2048]{1,0:T(8,128)(2,1)}, u32[]{:S(2)}) copy-start(bf16[256,2048]{1,0:T(8,128)(2,1)} %param.20) | copy-start | bytes 3145732
  17.9 5.3 %copy-start.3 = (f32[128]{0:T(128)S(1)}, f32[128]{0:T(128)}, u32[]{:S(2)}) copy-start(f32[128]{0:T(128)} %param.18) | copy-start | bytes 1540
  17.9 5.4 %copy-start.1 = (bf16[768,256]{1,0:T(8,128)(2,1)S(1)}, bf16[768,256]{1,0:T(8,128)(2,1)}, u32[]{:S(2)}) copy-start(bf16[768,256]{1,0:T(8,128)(2,1)} %param.15) | copy-start | bytes 1179652
  17.9 53.9 %all-to-all-start = ((bf16[8,16,8,2048]{3,2,0,1:T(8,128)(2,1)}), bf16[8,16,8,2048]{3,2,0,1:T(8,128)(2,1)}, u32[]{:S(2)}, u32[]{:S(2)}) async-start(bf16[8,16,8,2048]{3,2,0,1:T(8,128)(2,1)} %copy.51), calls=%async_computation.1 | async-start | bytes 8388608 | tf_op jit(solution)/shard_map/all_to_all | solution.py:127
  23.2 128.5 %reduce-scatter.5.cloned.1.call-start = ((), (), s32[]{:S(2)}) async-start(), calls=%async_computation.5 | async-start | bytes 4718592 | tf_op jit(solution)/shard_map/reduce_scatter | solution.py:141
  99.1 9.0 %copy-start.4 = (f32[128]{0:T(128)S(1)}, f32[128]{0:T(128)}, u32[]{:S(2)}) copy-start(f32[128]{0:T(128)} %param.19) | copy-start | bytes 1540
  99.1 93.7 %reduce-scatter.3.cloned.1.call-start = ((), (), s32[]{:S(2)}) async-start(), calls=%async_computation.4 | async-start | bytes 3538944 | tf_op jit(solution)/shard_map/reduce_scatter | solution.py:84
  148.7 2.7 %copy-start.2 = (f32[384,2]{0,1:T(2,128)S(1)}, f32[384,2]{0,1:T(2,128)}, u32[]{:S(2)}) copy-start(f32[384,2]{0,1:T(2,128)} %param.24) | copy-start | bytes 9220
  153.6 10.0 %all-to-all-start.1 = ((bf16[4,4,8,2048]{3,2,0,1:T(8,128)(2,1)}), bf16[4,4,8,2048]{3,2,0,1:T(8,128)(2,1)S(1)}, u32[]{:S(2)}, u32[]{:S(2)}) async-start(bf16[4,4,8,2048]{3,2,0,1:T(8,128)(2,1)} %copy.54), calls=%async_computation.3 | async-start | bytes 1048576 | tf_op jit(solution)/shard_map/all_to_all | solution.py:144
Sparse Core Ops, SparseCore 0:
  99.2 50.3 reduce-scatter.4
  152.6 40.2 reduce-scatter.2
where the time goes:
time: 200 us
  waiting for transfers between devices  81.4 us (41%)
  matrix products  40 us (20%)
  blocking collectives  23.9 us (12%)
  local copies, waits for them, and re-layouts  19.3 us (10%)
  between operations  14.3 us (7%)
  other arithmetic  11.5 us (6%)
  starting transfers between devices  9.02 us (5%)
    all_to_all x1, waiting for transfers between devices, expert_half(): lax.all_to_all(outgoing, 'ep', split_axis=1, concat_axis=2, tiled=True)  47.1 us
    reduce_scatter x1, waiting for transfers between devices, token_mixer(): lax.psum_scatter(jnp.dot(attended, out_weight, preferred_element_type=jnp...  28.2 us
    dot_general x1, matrix products, expert_half(): jnp.einsum('blmf,lfd->blmd', hidden, down_weight, preferred_element_type=...  14.2 us
    all_gather x1, blocking collectives, token_mixer(): key_piece = lax.all_gather(own_keys, 'ep', axis=0, tiled=True)  12.7 us
    all_gather x1, blocking collectives, token_mixer(): value_piece = lax.all_gather(own_values, 'ep', axis=0, tiled=True)  11.2 us
    dot_general x4, matrix products, one_block(): jnp.dot(weights.astype(jnp.bfloat16), value_blk, preferred_element_type=j...  8.6 us
    dot_general x1, matrix products, expert_half(): jnp.einsum('blmd,ldf->blmf', expert_slab_rows, gate_weight, preferred_ele...  8.38 us
    all_to_all x1, waiting for transfers between devices, expert_half(): lax.all_to_all(summed.reshape(local_experts, n_ep, CAP, D), 'ep', split_a...  6.01 us
  transfers between devices with their start and end apart: 4, of which 3 were waited for; matrix products, arithmetic and copies ran while one was open for 16% of the time, Pallas kernels for 0%

commit v1 on v0

v1 whole, which is shorter than its diff:
```python
import jax
import jax.numpy as jnp
from jax import lax
from jax.experimental import pallas as pl
from jax.experimental.pallas import tpu as pltpu
from jax.sharding import Mesh, PartitionSpec as P

HD = 128
KVH = 4
EXPERTS = 16
TOPK = 2
GRID_W = 64
CAP = 8
EPS = 1e-06
THETA = 10000.0
CORES = 2
MIB = 1024 * 1024

F32 = jnp.float32
BF16 = jnp.bfloat16


def rope_tables(positions):
    n_freq = HD // 4
    row_pos = (positions // GRID_W).astype(F32)[:, None]
    col_pos = (positions % GRID_W).astype(F32)[:, None]
    lane = jnp.arange(HD, dtype=jnp.int32)
    inverse = THETA ** (-(lane % n_freq).astype(F32) / n_freq)
    angle = jnp.where(lane < HD // 2, row_pos, col_pos) * inverse
    sign = jnp.where((lane // n_freq) % 2 == 0, -1.0, 1.0).astype(F32)
    return jnp.cos(angle), jnp.sin(angle) * sign


def norm_turn(field, gain, cosine, sine):
    quarter = HD // 4
    mean = jnp.mean(field * field, axis=-1, keepdims=True)
    field = field * lax.rsqrt(mean + EPS) * gain
    lane = lax.broadcasted_iota(jnp.int32, field.shape, 1)
    partner = jnp.where(
        (lane // quarter) % 2 == 0,
        pltpu.roll(field, HD - quarter, 1),
        pltpu.roll(field, quarter, 1),
    )
    return field * cosine + partner * sine


def kv_kernel(core_ref, head_ref, keys_ref, values_ref, gain_ref, cos_ref, sin_ref, out_ref):
    rows = cos_ref.shape[0]
    field = keys_ref[...].reshape(rows, HD).astype(F32)
    out_ref[0] = norm_turn(field, gain_ref[...], cos_ref[...], sin_ref[...]).astype(BF16)
    out_ref[1] = values_ref[...].reshape(rows, HD)


def prepare_kv(core, head, keys, values, gain, cosine, sine, n_z):
    rows = cosine.shape[0]
    part = rows // n_z
    view = lambda a: a.reshape(n_z, CORES, part, a.shape[-1])
    picked = pl.BlockSpec((n_z, 1, part, HD), lambda i, c, h: (0, c[0], 0, h[0]))
    whole = lambda shape: pl.BlockSpec(shape, lambda i, c, h: (0,) * len(shape))
    return pl.pallas_call(
        kv_kernel,
        grid_spec=pltpu.PrefetchScalarGridSpec(
            num_scalar_prefetch=2,
            grid=(1,),
            in_specs=[picked, picked, whole((1, HD)), whole((rows, HD)), whole((rows, HD))],
            out_specs=whole((2, rows, HD)),
        ),
        out_shape=jax.ShapeDtypeStruct((2, rows, HD), BF16),
        name="prepare_kv",
    )(core, head, view(keys), view(values), gain, cosine, sine)


def mix_kernel(n_pieces, core_ref, q_own, q_other, gain_ref, cos_ref, sin_ref, w_own, w_other, *rest):
    pieces = rest[:n_pieces]
    out_ref, att_ref, keys_ref, vals_ref = rest[n_pieces:]
    rows = cos_ref.shape[0]
    row = 0
    for piece in pieces:
        for n in range(piece.shape[0]):
            keys_ref[pl.ds(row, rows)] = piece[n, 0]
            vals_ref[pl.ds(row, rows)] = piece[n, 1]
            row += rows
    factor = HD ** (-0.5) * 1.4426950408889634
    heads = q_own.shape[-1] // HD
    for source, field_ref in enumerate((q_own, q_other)):
        for head in range(heads):
            field = field_ref[:, :, :, head * HD : (head + 1) * HD].reshape(rows, HD).astype(F32)
            query = norm_turn(field, gain_ref[...], cos_ref[...], sin_ref[...]).astype(BF16)
            scores = lax.dot_general(
                query, keys_ref[...], (((1,), (1,)), ((), ())), preferred_element_type=F32
            )
            top = jnp.max(scores, axis=1, keepdims=True)
            weights = jnp.exp2((scores - top) * factor)
            totals = jnp.sum(weights, axis=1, keepdims=True)
            merged = jnp.dot(weights.astype(BF16), vals_ref[...], preferred_element_type=F32)
            at = (source * heads + head) * HD
            att_ref[:, at : at + HD] = (merged / totals).astype(BF16)
    half = heads * HD
    mixed = jnp.dot(att_ref[:, :half], w_own[...], preferred_element_type=F32)
    mixed = mixed + jnp.dot(att_ref[:, half:], w_other[...], preferred_element_type=F32)
    out_ref[...] = mixed.astype(BF16)


def mix(core, queries, q_other, gain, cosine, sine, w_own, w_other, pieces, n_z):
    rows, width = cosine.shape[0], queries.shape[-1]
    part = rows // n_z
    view = queries.reshape(n_z, CORES, part, width)
    d_model = w_own.shape[-1]
    length = sum(p.shape[0] for p in pieces) * rows
    whole = lambda a: pl.BlockSpec(a.shape, lambda i, c: (0,) * a.ndim)
    others = [q_other.reshape(n_z, 1, part, width), gain, cosine, sine, w_own, w_other, *pieces]
    return pl.pallas_call(
        lambda *refs: mix_kernel(len(pieces), *refs),
        grid_spec=pltpu.PrefetchScalarGridSpec(
            num_scalar_prefetch=1,
            grid=(1,),
            in_specs=[pl.BlockSpec((n_z, 1, part, width), lambda i, c: (0, c[0], 0, 0))]
            + [whole(a) for a in others],
            out_specs=pl.BlockSpec((rows, d_model), lambda i, c: (0, 0)),
            scratch_shapes=[
                pltpu.VMEM((rows, 2 * width), BF16),
                pltpu.VMEM((length, HD), BF16),
                pltpu.VMEM((length, HD), BF16),
            ],
        ),
        out_shape=jax.ShapeDtypeStruct((rows, d_model), BF16),
        compiler_params=pltpu.CompilerParams(vmem_limit_bytes=56 * MIB),
        name="mix",
    )(core, view, *others)


def dispatch_kernel(core_ref, tokens_ref, gain_ref, slots_ref, out_ref):
    rows, d_model = slots_ref.shape[-1], tokens_ref.shape[-1]
    field = tokens_ref[...].reshape(rows, d_model).astype(F32)
    mean = jnp.mean(field * field, axis=-1, keepdims=True)
    normed = (field * lax.rsqrt(mean + EPS) * gain_ref[...]).astype(BF16)
    slot = lax.broadcasted_iota(jnp.int32, (out_ref.shape[0], rows), 0)
    hot = slot == slots_ref[0:1]
    for k in range(1, TOPK):
        hot = hot | (slot == slots_ref[k : k + 1])
    out_ref[...] = jnp.dot(
        hot.astype(F32).astype(BF16), normed, preferred_element_type=F32
    ).astype(BF16)


def dispatch(core, tokens, gain, slots, n_z):
    local_rows, d_model = tokens.shape
    part = local_rows // (n_z * CORES)
    n_slots = EXPERTS * n_z * CAP
    return pl.pallas_call(
        dispatch_kernel,
        grid_spec=pltpu.PrefetchScalarGridSpec(
            num_scalar_prefetch=1,
            grid=(1,),
            in_specs=[
                pl.BlockSpec((n_z, 1, part, d_model), lambda i, c: (0, c[0], 0, 0)),
                pl.BlockSpec((1, d_model), lambda i, c: (0, 0)),
                pl.BlockSpec(slots.shape, lambda i, c: (0, 0)),
            ],
            out_specs=pl.BlockSpec((n_slots, d_model), lambda i, c: (0, 0)),
        ),
        out_shape=jax.ShapeDtypeStruct((n_slots, d_model), BF16),
        name="dispatch",
    )(core, tokens.reshape(n_z, CORES, part, d_model), gain, slots)


def expert_kernel(own_ref, other_ref, gate_ref, up_ref, down_ref, keep_ref, send_ref, acc_ref):
    step = pl.program_id(1)
    n_src, _, rows, d_model = own_ref.shape
    half = n_src * rows
    field = jnp.concatenate(
        [own_ref[...].reshape(half, d_model), other_ref[...].reshape(half, d_model)], axis=0
    )
    gate = jnp.dot(field, gate_ref[0], preferred_element_type=F32)
    up = jnp.dot(field, up_ref[0], preferred_element_type=F32)
    hidden = (gate / (1.0 + jnp.exp(-gate)) * up).astype(BF16)
    result = jnp.dot(hidden, down_ref[0], preferred_element_type=F32)

    @pl.when(step == 0)
    def _():
        acc_ref[...] = result

    @pl.when(step > 0)
    def _():
        acc_ref[...] += result

    @pl.when(step == pl.num_programs(1) - 1)
    def _():
        keep_ref[...] = acc_ref[:half].astype(BF16).reshape(keep_ref.shape)
        send_ref[...] = acc_ref[half:].astype(BF16).reshape(send_ref.shape)


def experts(own, other, gate_weight, up_weight, down_weight):
    n_src, n_local, rows, d_model = own.shape
    width = gate_weight.shape[-1]
    steps = 2 if width % 512 == 0 else 1
    cut = width // steps
    act = pl.BlockSpec((n_src, 1, rows, d_model), lambda e, s: (0, e, 0, 0))
    return pl.pallas_call(
        expert_kernel,
        grid=(n_local, steps),
        in_specs=[
            act,
            act,
            pl.BlockSpec((1, d_model, cut), lambda e, s: (e, 0, s)),
            pl.BlockSpec((1, d_model, cut), lambda e, s: (e, 0, s)),
            pl.BlockSpec((1, cut, d_model), lambda e, s: (e, s, 0)),
        ],
        out_specs=[act, act],
        out_shape=[jax.ShapeDtypeStruct(own.shape, BF16)] * 2,
        scratch_shapes=[pltpu.VMEM((2 * n_src * rows, d_model), F32)],
        compiler_params=pltpu.CompilerParams(vmem_limit_bytes=40 * MIB),
        name="experts",
    )(own, other, gate_weight, up_weight, down_weight)


def combine_kernel(slots_ref, shares_ref, back_ref, out_ref):
    rows, n_slots = slots_ref.shape[0], back_ref.shape[0]
    slot = lax.broadcasted_iota(jnp.int32, (rows, n_slots), 1)
    matrix = jnp.zeros((rows, n_slots), F32)
    for k in range(TOPK):
        matrix = matrix + jnp.where(slot == slots_ref[:, k : k + 1], shares_ref[:, k : k + 1], 0.0)
    high = matrix.astype(BF16)
    low = (matrix - high.astype(F32)).astype(BF16)
    back = back_ref[...]
    out_ref[...] = (
        jnp.dot(high, back, preferred_element_type=F32)
        + jnp.dot(low, back, preferred_element_type=F32)
    ).astype(BF16)


def combine(slots, shares, back):
    return pl.pallas_call(
        combine_kernel,
        out_shape=jax.ShapeDtypeStruct((slots.shape[0], back.shape[-1]), BF16),
        name="combine",
    )(slots, shares, back)


def swap_cores(a):
    return lax.ppermute(a, "core", [(i, CORES - 1 - i) for i in range(CORES)])


def on_device(
    queries,
    keys,
    values,
    query_gain,
    key_gain,
    out_weight,
    tokens_b,
    norm_gain,
    routes,
    route_weight,
    gate_weight,
    up_weight,
    down_weight,
):
    n_ep, n_z = lax.axis_size("ep"), lax.axis_size("z")
    core, z_index = lax.axis_index("core"), lax.axis_index("z")
    core_arg = core.reshape(1).astype(jnp.int32)
    other_arg = 1 - core_arg
    n_rows, width = queries.shape
    d_model = tokens_b.shape[-1]
    heads = width // HD
    n_heads = heads * n_z * CORES

    part = n_rows // (n_z * CORES)
    offsets = (
        jnp.arange(n_z, dtype=jnp.int32)[:, None] * (CORES * part)
        + core * part
        + jnp.arange(part, dtype=jnp.int32)[None, :]
    ).reshape(-1)
    cosine, sine = rope_tables(lax.axis_index("ep") * n_rows + offsets)
    kv_head = ((z_index * CORES + core) * heads // (n_heads // KVH)).reshape(1).astype(jnp.int32)
    own_kv = prepare_kv(core_arg, kv_head, keys, values, key_gain[None], cosine, sine, n_z)
    if n_ep <= 4:
        mine = [own_kv[None]]
        for step in range(1, n_ep):
            mine.append(
                lax.ppermute(own_kv, "ep", [(i, (i + step) % n_ep) for i in range(n_ep)])[None]
            )
        gathered = jnp.concatenate(mine, axis=0)
    else:
        gathered = lax.all_gather(own_kv, "ep", axis=0, tiled=False)
    other_kv = swap_cores(gathered)

    q_view = queries.reshape(n_z, CORES, part, width)
    q_other = swap_cores(lax.dynamic_index_in_dim(q_view, 1 - core, 1, keepdims=False))
    w_other = swap_cores(out_weight)

    block_rows = tokens_b.shape[0] // (n_z * CORES)
    picks = block_rows * TOPK
    own_block = lambda a: lax.dynamic_index_in_dim(
        a.reshape(n_z, CORES, block_rows, TOPK), core, 1, keepdims=False
    )
    own_routes = own_block(routes)
    assigned = own_routes.reshape(n_z, picks)
    earlier = jnp.arange(picks)[:, None] > jnp.arange(picks)[None, :]
    same = (assigned[:, :, None] == assigned[:, None, :]) & earlier[None]
    rank = jnp.sum(same.astype(jnp.int32), axis=-1)
    block = jnp.arange(n_z, dtype=jnp.int32)[:, None]
    slots = ((assigned * n_z + block) * CAP + rank).reshape(n_z * block_rows, TOPK)
    own_weight = own_block(route_weight).reshape(n_z * block_rows, TOPK)
    shares = own_weight / jnp.sum(own_weight, axis=-1, keepdims=True)

    outgoing = dispatch(core_arg, tokens_b, norm_gain[None], slots.T, n_z)
    n_local = gate_weight.shape[0]
    outgoing = outgoing.reshape(n_ep, n_local, n_z * CAP, d_model)
    arrived = lax.all_to_all(outgoing, "ep", split_axis=0, concat_axis=0, tiled=True)
    arrived_other = swap_cores(arrived)

    mixed = mix(
        core_arg, queries, q_other, query_gain[None], cosine, sine, out_weight, w_other,
        [gathered, other_kv], n_z,
    )
    mixed = lax.all_to_all(
        mixed.reshape(n_z, part, d_model), "z", split_axis=0, concat_axis=0, tiled=True
    )
    mixed_out = jnp.sum(mixed.astype(F32), axis=0).astype(BF16)

    keep, send = experts(arrived, arrived_other, gate_weight, up_weight, down_weight)
    result = (keep.astype(F32) + swap_cores(send).astype(F32)).astype(BF16)
    back = lax.all_to_all(result, "ep", split_axis=0, concat_axis=0, tiled=True)
    rows = combine(slots, shares, back.reshape(-1, d_model))
    rows = lax.all_to_all(
        rows.reshape(n_z, block_rows, d_model), "z", split_axis=0, concat_axis=0, tiled=True
    )
    expert_out = jnp.sum(rows.astype(F32), axis=0).astype(BF16)
    return (mixed_out, expert_out)


def solution(mesh):
    n_ep, n_tp = mesh.shape["ep"], mesh.shape["tp"]
    fine = Mesh(mesh.devices.reshape(n_ep, n_tp // CORES, CORES), ("ep", "z", "core"))
    tp = ("z", "core")
    placed = (
        P("ep", tp),
        P("ep", None),
        P("ep", None),
        P(),
        P(),
        P(tp, None),
        P("ep", None),
        P(),
        P("ep", None),
        P("ep", None),
        P("ep", None, tp),
        P("ep", None, tp),
        P("ep", tp, None),
    )
    return jax.shard_map(
        on_device,
        mesh=fine,
        in_specs=placed,
        out_specs=(P(("ep", "z", "core"), None), P(("ep", "z", "core"), None)),
        check_vma=False,
    )
```

time: 200 us -> 187 us (0.935)
  matrix products: 40 us -> 0 us
  Pallas kernels: 0 us -> 38.3 us
  local copies, waits for them, and re-layouts: 19.3 us -> 3 us
  between operations: 14.3 us -> 0.8 us
  starting transfers between devices: 9.02 us -> 17.8 us
  blocking collectives: 23.9 us -> 30.6 us
  waiting for transfers between devices: 81.4 us -> 85.3 us
    dot_general x15 -> x0, matrix products: 40 us -> none  [the longest x1 14.2 us: expert_half(): jnp.einsum('blmf,lfd->blmd', hidden, down_weight, preferred_element_type=...]
    pallas_call x0 -> x5, Pallas kernels: none -> 38.3 us  [the longest x1 16.1 us: experts(): pl.pallas_call(expert_kernel, grid=(n_local, steps), in_specs=[act, act,...]
    ppermute x0 -> x8, waiting for transfers between devices: none -> 35.7 us  [the longest x3 25.4 us: on_device(): lax.ppermute(own_kv, 'ep', [(i, (i + step) % n_ep) for i in range(n_ep)])]
    all_to_all x0 -> x1, blocking collectives: none -> 30.6 us  [on_device(): lax.all_to_all(outgoing, 'ep', split_axis=0, concat_axis=0, tiled=True)]
    reduce_scatter x2 -> x0, waiting for transfers between devices: 28.2 us -> none  [the longest x1 28.2 us: token_mixer(): lax.psum_scatter(jnp.dot(attended, out_weight, preferred_element_type=jnp...]
    all_gather x2 -> x0, blocking collectives: 23.9 us -> none  [the longest x1 12.7 us: token_mixer(): key_piece = lax.all_gather(own_keys, 'ep', axis=0, tiled=True)]
    convert_element_type x2 -> x0, local copies, waits for them, and re-layouts: 8.41 us -> none  [the longest x1 4.7 us: expert_half(): result.reshape(-1, D).astype(jnp.bfloat16)]
    ppermute x0 -> x8, starting transfers between devices: none -> 5.65 us  [the longest x3 4.9 us: on_device(): lax.ppermute(own_kv, 'ep', [(i, (i + step) % n_ep) for i in range(n_ep)])]
  transfers between devices with their start and end apart: 4 -> 11, of which waited for: 3 -> 8; matrix products, arithmetic and copies ran while one was open for 16% -> 3% of each run, Pallas kernels for 0% -> 10%
where the time goes in v1:
time: 187 us
  waiting for transfers between devices  85.3 us (46%)
  Pallas kernels  38.3 us (20%)
  blocking collectives  30.6 us (16%)
  starting transfers between devices  17.8 us (10%)
  other arithmetic  10.8 us (6%)
  local copies, waits for them, and re-layouts  3 us (2%)
    all_to_all x1, waiting for transfers between devices, on_device(): lax.all_to_all(mixed.reshape(n_z, part, d_model), 'z', split_axis=0, conc...  32.5 us
    all_to_all x1, blocking collectives, on_device(): lax.all_to_all(outgoing, 'ep', split_axis=0, concat_axis=0, tiled=True)  30.6 us
    ppermute x3, waiting for transfers between devices, on_device(): lax.ppermute(own_kv, 'ep', [(i, (i + step) % n_ep) for i in range(n_ep)])  25.4 us
    all_to_all x1, waiting for transfers between devices, on_device(): lax.all_to_all(rows.reshape(n_z, block_rows, d_model), 'z', split_axis=0,...  17.1 us
    pallas_call x1, Pallas kernels, experts(): pl.pallas_call(expert_kernel, grid=(n_local, steps), in_specs=[act, act,...  16.1 us
    pallas_call x1, Pallas kernels, mix(): pl.pallas_call(lambda *refs: mix_kernel(len(pieces), *refs), grid_spec=pl...  12.9 us
    ppermute x5, waiting for transfers between devices, swap_cores(): return lax.ppermute(a, 'core', [(i, CORES - 1 - i) for i in range(CORES)])  10.3 us
    all_to_all x1, starting transfers between devices, on_device(): lax.all_to_all(mixed.reshape(n_z, part, d_model), 'z', split_axis=0, conc...  5.03 us
  transfers between devices with their start and end apart: 11, of which 8 were waited for; matrix products, arithmetic and copies ran while one was open for 3% of the time, Pallas kernels for 10%

profile of v1, /device:TPU:0, one launch (start us, length us, event | category | flops | bytes accessed | tf_op | source)
XLA Modules:
  0.0 186.6 jit_solution(8802360895786876675)
XLA Ops:
  0.7 0.8 reshape.180
  1.4 0.1 copy.38
  1.6 0.1 copy.39
  1.6 0.3 convert_reduce_fusion
  1.9 0.1 reduce_sum.46
  2.0 0.1 copy.37
  2.1 0.1 add.137
  2.2 0.1 fusion.2.slots_ref
  2.3 0.7 copy.42.slots_ref
  3.0 3.4 %dispatch.1 = bf16[512,2048]{1,0:T(8,128)(2,1)} custom-call(s32[1]{0:T(128)} %bitcast.core_ref.refs_0_, bf16[4,2,48,2048]{3,2,1,0:T(8,128)(2,1)} %bitcast.39, f32[1,2048]{1,0:T(1,128)} %bitcast.53, s32[2,192]{1,0:T(2,128)} %copy.42.slots_ref), custom_call_target="tpu_custom_call" | custom-call | tf_op jit(solution)/shard_map/dispatch/pallas_call | solution.py:150
  6.4 30.6 %all_to_all.20.own_ref = bf16[4,4,32,2048]{3,2,1,0:T(8,128)(2,1)S(1)} all-to-all(bf16[4,4,32,2048]{3,2,1,0:T(8,128)(2,1)} %bitcast.35), channel_id=1, replica_groups=mesh['ep'=4,'z'=4,'core'=2] {'ep'}, dimensions={0} | all-to-all | bytes 4194304 | tf_op jit(solution)/shard_map/all_to_all | solution.py:310
  37.0 0.0 collective-permute-start.6
  37.0 4.2 %collective-permute-done.6.other_ref = bf16[4,4,32,2048]{3,2,1,0:T(8,128)(2,1)S(1)} collective-permute-done((bf16[4,4,32,2048]{3,2,1,0:T(8,128)(2,1)S(1)}, bf16[4,4,32,2048]{3,2,1,0:T(8,128)(2,1)S(1)}, u32[]{:S(2)}, u32[]{:S(2)}) %collective-permute-start.6) | collective-permute-done | bytes 2097184 | tf_op jit(solution)/shard_map/ppermute | solution.py:241
  41.1 16.1 %experts.1 = (bf16[4,4,32,2048]{3,2,1,0:T(8,128)(2,1)S(1)}, bf16[4,4,32,2048]{3,2,1,0:T(8,128)(2,1)}) custom-call(bf16[4,4,32,2048]{3,2,1,0:T(8,128)(2,1)S(1)} %all_to_all.20.own_ref, bf16[4,4,32,2048]{3,2,1,0:T(8,128)(2,1)S(1)} %collective-permute-done.6.other_ref, bf16[4,2048,512]{2,1,0:T(8,128)(2,1)} %gate_ref.1, bf16[4,2048,512]{2,1,0:T(8,128)(2,1)} %up_ref.1, ...), custom_call_target="tpu_custom_call" | custom-call | tf_op jit(solution)/shard_map/experts/pallas_call | solution.py:199
  57.2 0.1 collective-permute-start.7
  57.4 0.1 add_add_fusion
  57.5 0.1 add.130
  57.6 4.2 %collective-permute-done.7 = bf16[4,4,32,2048]{3,2,1,0:T(8,128)(2,1)} collective-permute-done((bf16[4,4,32,2048]{3,2,1,0:T(8,128)(2,1)}, bf16[4,4,32,2048]{3,2,1,0:T(8,128)(2,1)}, u32[]{:S(2)}, u32[]{:S(2)}) %collective-permute-start.7) | collective-permute-done | bytes 2097184 | tf_op jit(solution)/shard_map/ppermute | solution.py:241
  61.7 3.7 %add_convert_fusion = bf16[4,4,32,2048]{3,2,1,0:T(8,128)(2,1)} fusion(bf16[4,4,32,2048]{3,2,1,0:T(8,128)(2,1)} %collective-permute-done.7, bf16[4,4,32,2048]{3,2,1,0:T(8,128)(2,1)S(1)} %get-tuple-element.4), kind=kLoop, calls=%fused_computation | loop fusion | flops 4194304 | bytes 6291456 | tf_op jit(solution)/shard_map/convert_element_type | solution.py:323
  65.4 3.6 %all-to-all-start.2 = ((bf16[4,4,32,2048]{3,2,1,0:T(8,128)(2,1)}), bf16[4,4,32,2048]{3,2,1,0:T(8,128)(2,1)S(1)}, u32[]{:S(2)}, u32[]{:S(2)}) async-start(bf16[4,4,32,2048]{3,2,1,0:T(8,128)(2,1)} %add_convert_fusion), calls=%async_computation.2 | async-start | bytes 4194304 | tf_op jit(solution)/shard_map/all_to_all | solution.py:324
  69.1 0.0 copy-start.3
  69.1 1.5 sine_multiply_fusion
  70.6 2.1 %prepare_kv.1 = bf16[2,384,128]{2,1,0:T(8,128)(2,1)} custom-call(s32[1]{0:T(128)} %bitcast.core_ref.refs_0_, s32[1]{0:T(128)} %bitcast.5.head_ref, bf16[4,2,96,512]{3,2,1,0:T(8,128)(2,1)} %bitcast.44, bf16[4,2,96,512]{3,2,1,0:T(8,128)(2,1)} %bitcast.45, f32[1,128]{1,0:T(1,128)} %bitcast.54, f32[384,128]{1,0:T(8,128)} %get-tuple-element.9.cos_ref.refs_4_, ...), custom_call_target="tpu_custom_call" | custom-call | tf_op jit(solution)/shard_map/prepare_kv/pallas_call | solution.py:60
  72.7 2.0 %collective-permute-start.2 = (bf16[2,384,128]{2,1,0:T(8,128)(2,1)}, bf16[2,384,128]{2,1,0:T(8,128)(2,1)S(1)}, u32[]{:S(2)}, u32[]{:S(2)}) collective-permute-start(bf16[2,384,128]{2,1,0:T(8,128)(2,1)} %prepare_kv.1), channel_id=1, source_target_pairs={{0,8},{8,16},{16,24},{24,0},{1,9},{9,17},{17,25},{25,1},{2,10},{10... | collective-permute-start | bytes 589832 | tf_op jit(solution)/shard_map/ppermute | solution.py:281
  74.7 1.5 collective-permute-start.3
  76.1 1.5 collective-permute-start.4
  77.6 0.0 collective-permute-start.1
  77.6 22.9 %collective-permute-done.2 = bf16[2,384,128]{2,1,0:T(8,128)(2,1)S(1)} collective-permute-done((bf16[2,384,128]{2,1,0:T(8,128)(2,1)}, bf16[2,384,128]{2,1,0:T(8,128)(2,1)S(1)}, u32[]{:S(2)}, u32[]{:S(2)}) %collective-permute-start.2) | collective-permute-done | bytes 196640 | tf_op jit(solution)/shard_map/ppermute | solution.py:281
  100.5 2.4 %collective-permute-done.3 = bf16[2,384,128]{2,1,0:T(8,128)(2,1)S(1)} collective-permute-done((bf16[2,384,128]{2,1,0:T(8,128)(2,1)}, bf16[2,384,128]{2,1,0:T(8,128)(2,1)S(1)}, u32[]{:S(2)}, u32[]{:S(2)}) %collective-permute-start.3) | collective-permute-done | bytes 196640 | tf_op jit(solution)/shard_map/ppermute | solution.py:281
  102.9 0.1 collective-permute-done.4
  102.9 1.0 pad_maximum_fusion.refs_8_
  104.0 0.1 collective-permute-start.5
  104.1 0.5 collective-permute-start
  104.6 2.0 %collective-permute-done = bf16[4,96,256]{2,1,0:T(8,128)(2,1)S(1)} collective-permute-done((bf16[4,96,256]{2,1,0:T(8,128)(2,1)S(1)}, bf16[4,96,256]{2,1,0:T(8,128)(2,1)S(1)}, u32[]{:S(2)}, u32[]{:S(2)}) %collective-permute-start) | collective-permute-done | bytes 196640 | tf_op jit(solution)/shard_map/ppermute | solution.py:241
  106.6 0.0 collective-permute-done.5.refs_9_
  106.6 0.7 copy-done.4
  107.3 12.9 %mix.1 = bf16[384,2048]{1,0:T(8,128)(2,1)} custom-call(s32[1]{0:T(128)} %bitcast.core_ref.refs_0_, bf16[4,2,96,256]{3,2,1,0:T(8,128)(2,1)} %bitcast.41, bf16[4,1,96,256]{3,2,1,0:T(8,128)(2,1)} %bitcast.46, f32[1,128]{1,0:T(1,128)} %bitcast.55, f32[384,128]{1,0:T(8,128)} %get-tuple-element.9.cos_ref.refs_4_, f32[384,128]{1,0:T(8,128)} %get-tuple-element.8.sin_ref.refs_5_, ...), custom_call_target="tpu_custom_call" | custom-call | tf_op jit(solution)/shard_map/mix/pallas_call | solution.py:112
  120.2 5.0 %all-to-all-start = ((bf16[4,96,2048]{2,1,0:T(8,128)(2,1)}), bf16[4,96,2048]{2,1,0:T(8,128)(2,1)}, u32[]{:S(2)}, u32[]{:S(2)}) async-start(bf16[4,96,2048]{2,1,0:T(8,128)(2,1)} %bitcast.37), calls=%async_computation | async-start | bytes 3145728 | tf_op jit(solution)/shard_map/all_to_all | solution.py:317
  125.3 0.1 reshape.181
  125.4 0.1 copy.44
  125.5 0.1 div.55
  125.6 0.8 bitcast_divide_fusion.shares_ref
  126.3 3.8 %combine.1 = bf16[192,2048]{1,0:T(8,128)(2,1)} custom-call(s32[192,2]{1,0:T(8,128)} %copy-done.2, f32[192,2]{1,0:T(8,128)} %bitcast_divide_fusion.shares_ref, bf16[512,2048]{1,0:T(8,128)(2,1)} %bitcast.36), custom_call_target="tpu_custom_call" | custom-call | tf_op jit(solution)/shard_map/combine/pallas_call | solution.py:233
  130.1 32.5 %all-to-all-done = bf16[4,96,2048]{2,1,0:T(8,128)(2,1)} async-done(((bf16[4,96,2048]{2,1,0:T(8,128)(2,1)}), bf16[4,96,2048]{2,1,0:T(8,128)(2,1)}, u32[]{:S(2)}, u32[]{:S(2)}) %all-to-all-start) | async-done | bytes 1572896 | tf_op jit(solution)/shard_map/all_to_all | solution.py:317
  162.6 3.5 %all-to-all-start.3 = ((bf16[4,48,2048]{2,1,0:T(8,128)(2,1)}), bf16[4,48,2048]{2,1,0:T(8,128)(2,1)S(1)}, u32[]{:S(2)}, u32[]{:S(2)}) async-start(bf16[4,48,2048]{2,1,0:T(8,128)(2,1)} %bitcast.38), calls=%async_computation.3 | async-start | bytes 1572864 | tf_op jit(solution)/shard_map/all_to_all | solution.py:326
  166.1 2.5 %reduce_sum.44 = bf16[96,2048]{1,0:T(8,128)(2,1)} reduce(bf16[4,96,2048]{2,1,0:T(8,128)(2,1)} %all-to-all-done, bf16[]{:T(256)} %constant.126.clone.1), dimensions={0}, to_apply=%region_0.1 | reduce | flops 589824 | bytes 1966082 | tf_op jit(solution)/shard_map/reduce_sum | solution.py:320
  168.7 17.1 %all-to-all-done.3 = bf16[4,48,2048]{2,1,0:T(8,128)(2,1)S(1)} async-done(((bf16[4,48,2048]{2,1,0:T(8,128)(2,1)}), bf16[4,48,2048]{2,1,0:T(8,128)(2,1)S(1)}, u32[]{:S(2)}, u32[]{:S(2)}) %all-to-all-start.3) | async-done | bytes 786464 | tf_op jit(solution)/shard_map/all_to_all | solution.py:326
  185.8 0.8 reduce_sum.48
  (22 shorter events, 0.1 us)
Async XLA Ops:
  2.3 34.6 %copy-start.2 = (s32[192,2]{1,0:T(8,128)}, s32[192,2]{1,0:T(8,128)S(1)}, u32[]{:S(2)}) copy-start(s32[192,2]{1,0:T(8,128)S(1)} %fusion.2.slots_ref) | copy-start | bytes 4612
  37.0 4.2 %collective-permute-start.6 = (bf16[4,4,32,2048]{3,2,1,0:T(8,128)(2,1)S(1)}, bf16[4,4,32,2048]{3,2,1,0:T(8,128)(2,1)S(1)}, u32[]{:S(2)}, u32[]{:S(2)}) collective-permute-start(bf16[4,4,32,2048]{3,2,1,0:T(8,128)(2,1)S(1)} %all_to_all.20.own_ref), channel_id=1, source_target_pairs={{0,1},{1,0},{2,3},{3,2},{4,5},{5,4},{6,7},{7,6},{8,9},{9,8},{10,11... | collective-permute-start | bytes 6291464 | tf_op jit(solution)/shard_map/ppermute | solution.py:241
  57.2 4.5 %collective-permute-start.7 = (bf16[4,4,32,2048]{3,2,1,0:T(8,128)(2,1)}, bf16[4,4,32,2048]{3,2,1,0:T(8,128)(2,1)}, u32[]{:S(2)}, u32[]{:S(2)}) collective-permute-start(bf16[4,4,32,2048]{3,2,1,0:T(8,128)(2,1)} %get-tuple-element.5), channel_id=1, source_target_pairs={{0,1},{1,0},{2,3},{3,2},{4,5},{5,4},{6,7},{7,6},{8,9},{9,8},{10,11... | collective-permute-start | bytes 6291464 | tf_op jit(solution)/shard_map/ppermute | solution.py:241
  65.4 54.8 %all-to-all-start.2 = ((bf16[4,4,32,2048]{3,2,1,0:T(8,128)(2,1)}), bf16[4,4,32,2048]{3,2,1,0:T(8,128)(2,1)S(1)}, u32[]{:S(2)}, u32[]{:S(2)}) async-start(bf16[4,4,32,2048]{3,2,1,0:T(8,128)(2,1)} %add_convert_fusion), calls=%async_computation.2 | async-start | bytes 4194304 | tf_op jit(solution)/shard_map/all_to_all | solution.py:324
  69.1 35.0 %copy-start.3 = (bf16[768,256]{1,0:T(8,128)(2,1)S(1)}, bf16[768,256]{1,0:T(8,128)(2,1)}, u32[]{:S(2)}) copy-start(bf16[768,256]{1,0:T(8,128)(2,1)} %param.13) | copy-start | bytes 1179652
  72.7 27.8 %collective-permute-start.2 = (bf16[2,384,128]{2,1,0:T(8,128)(2,1)}, bf16[2,384,128]{2,1,0:T(8,128)(2,1)S(1)}, u32[]{:S(2)}, u32[]{:S(2)}) collective-permute-start(bf16[2,384,128]{2,1,0:T(8,128)(2,1)} %prepare_kv.1), channel_id=1, source_target_pairs={{0,8},{8,16},{16,24},{24,0},{1,9},{9,17},{17,25},{25,1},{2,10},{10... | collective-permute-start | bytes 589832 | tf_op jit(solution)/shard_map/ppermute | solution.py:281
  74.7 28.2 %collective-permute-start.3 = (bf16[2,384,128]{2,1,0:T(8,128)(2,1)}, bf16[2,384,128]{2,1,0:T(8,128)(2,1)S(1)}, u32[]{:S(2)}, u32[]{:S(2)}) collective-permute-start(bf16[2,384,128]{2,1,0:T(8,128)(2,1)} %prepare_kv.1), channel_id=1, source_target_pairs={{0,16},{8,24},{16,0},{24,8},{1,17},{9,25},{17,1},{25,9},{2,18},{10... | collective-permute-start | bytes 589832 | tf_op jit(solution)/shard_map/ppermute | solution.py:281
  76.1 26.8 %collective-permute-start.4 = (bf16[2,384,128]{2,1,0:T(8,128)(2,1)}, bf16[2,384,128]{2,1,0:T(8,128)(2,1)S(1)}, u32[]{:S(2)}, u32[]{:S(2)}) collective-permute-start(bf16[2,384,128]{2,1,0:T(8,128)(2,1)} %prepare_kv.1), channel_id=1, source_target_pairs={{0,24},{8,0},{16,8},{24,16},{1,25},{9,1},{17,9},{25,17},{2,26},{10... | collective-permute-start | bytes 589832 | tf_op jit(solution)/shard_map/ppermute | solution.py:281
  77.6 29.0 %collective-permute-start.1 = (bf16[256,2048]{1,0:T(8,128)(2,1)}, bf16[256,2048]{1,0:T(8,128)(2,1)}, u32[]{:S(2)}, u32[]{:S(2)}) collective-permute-start(bf16[256,2048]{1,0:T(8,128)(2,1)} %refs_6_.1), channel_id=1, source_target_pairs={{0,1},{1,0},{2,3},{3,2},{4,5},{5,4},{6,7},{7,6},{8,9},{9,8},{10,11... | collective-permute-start | bytes 3145736 | tf_op jit(solution)/shard_map/ppermute | solution.py:241
  104.0 2.7 %copy-start.1 = (bf16[4,2,384,128]{3,2,1,0:T(8,128)(2,1)}, bf16[4,2,384,128]{3,2,1,0:T(8,128)(2,1)S(1)}, u32[]{:S(2)}) copy-start(bf16[4,2,384,128]{3,2,1,0:T(8,128)(2,1)S(1)} %pad_maximum_fusion.refs_8_) | copy-start | bytes 2359300
  104.0 2.6 %collective-permute-start.5 = (bf16[4,2,384,128]{3,2,1,0:T(8,128)(2,1)S(1)}, bf16[4,2,384,128]{3,2,1,0:T(8,128)(2,1)}, u32[]{:S(2)}, u32[]{:S(2)}) collective-permute-start(bf16[4,2,384,128]{3,2,1,0:T(8,128)(2,1)S(1)} %pad_maximum_fusion.refs_8_), channel_id=1, source_target_pairs={{0,1},{1,0},{2,3},{3,2},{4,5},{5,4},{6,7},{7,6},{8,9},{9,8},{10,11... | collective-permute-start | bytes 2359304 | tf_op jit(solution)/shard_map/ppermute | solution.py:241
  104.1 2.5 %collective-permute-start = (bf16[4,96,256]{2,1,0:T(8,128)(2,1)S(1)}, bf16[4,96,256]{2,1,0:T(8,128)(2,1)S(1)}, u32[]{:S(2)}, u32[]{:S(2)}) collective-permute-start(bf16[4,96,256]{2,1,0:T(8,128)(2,1)S(1)} %dynamic-slice_bitcast_fusion), channel_id=1, source_target_pairs={{0,1},{1,0},{2,3},{3,2},{4,5},{5,4},{6,7},{7,6},{8,9},{9,8},{10,11... | collective-permute-start | bytes 589832 | tf_op jit(solution)/shard_map/ppermute | solution.py:241
  106.6 0.7 copy-start.4
  120.2 5.0 %copy-start.5 = (f32[384,2]{0,1:T(2,128)S(1)}, f32[384,2]{0,1:T(2,128)}, u32[]{:S(2)}) copy-start(f32[384,2]{0,1:T(2,128)} %param.22) | copy-start | bytes 9220
  120.2 6.1 %copy-start = (bf16[4,4,32,2048]{3,2,1,0:T(8,128)(2,1)}, bf16[4,4,32,2048]{3,2,1,0:T(8,128)(2,1)S(1)}, u32[]{:S(2)}) copy-start(bf16[4,4,32,2048]{3,2,1,0:T(8,128)(2,1)S(1)} %all-to-all-done.2) | copy-start | bytes 6291460
  120.2 42.4 %all-to-all-start = ((bf16[4,96,2048]{2,1,0:T(8,128)(2,1)}), bf16[4,96,2048]{2,1,0:T(8,128)(2,1)}, u32[]{:S(2)}, u32[]{:S(2)}) async-start(bf16[4,96,2048]{2,1,0:T(8,128)(2,1)} %bitcast.37), calls=%async_computation | async-start | bytes 3145728 | tf_op jit(solution)/shard_map/all_to_all | solution.py:317
  162.6 23.1 %all-to-all-start.3 = ((bf16[4,48,2048]{2,1,0:T(8,128)(2,1)}), bf16[4,48,2048]{2,1,0:T(8,128)(2,1)S(1)}, u32[]{:S(2)}, u32[]{:S(2)}) async-start(bf16[4,48,2048]{2,1,0:T(8,128)(2,1)} %bitcast.38), calls=%async_computation.3 | async-start | bytes 1572864 | tf_op jit(solution)/shard_map/all_to_all | solution.py:326

commit v2 on v1

v2 whole, which is shorter than its diff:
```python
import jax
import jax.numpy as jnp
from jax import lax
from jax.experimental import pallas as pl
from jax.experimental.pallas import tpu as pltpu
from jax.sharding import Mesh, PartitionSpec as P


HD = 128
KVH = 4
EXPERTS = 16
TOPK = 2
GRID_W = 64
CAP = 8
EPS = 1e-06
THETA = 10000.0
CORES = 2
MIB = 1024 * 1024

F32 = jnp.float32
BF16 = jnp.bfloat16


def rope_tables(positions):
    n_freq = HD // 4
    row_pos = (positions // GRID_W).astype(F32)[:, None]
    col_pos = (positions % GRID_W).astype(F32)[:, None]
    lane = jnp.arange(HD, dtype=jnp.int32)
    inverse = THETA ** (-(lane % n_freq).astype(F32) / n_freq)
    angle = jnp.where(lane < HD // 2, row_pos, col_pos) * inverse
    sign = jnp.where((lane // n_freq) % 2 == 0, -1.0, 1.0).astype(F32)
    return jnp.cos(angle), jnp.sin(angle) * sign


def norm_turn(field, gain, cosine, sine):
    quarter = HD // 4
    mean = jnp.mean(field * field, axis=-1, keepdims=True)
    field = field * lax.rsqrt(mean + EPS) * gain
    lane = lax.broadcasted_iota(jnp.int32, field.shape, 1)
    partner = jnp.where(
        (lane // quarter) % 2 == 0,
        pltpu.roll(field, HD - quarter, 1),
        pltpu.roll(field, quarter, 1),
    )
    return field * cosine + partner * sine


def kv_kernel(core_ref, head_ref, keys_ref, values_ref, gain_ref, cos_ref, sin_ref, out_ref):
    rows = cos_ref.shape[0]
    field = keys_ref[...].reshape(rows, HD).astype(F32)
    out_ref[0] = norm_turn(field, gain_ref[...], cos_ref[...], sin_ref[...]).astype(BF16)
    out_ref[1] = values_ref[...].reshape(rows, HD)


def prepare_kv(core, head, keys, values, gain, cosine, sine, n_z):
    rows = cosine.shape[0]
    part = rows // n_z
    view = lambda a: a.reshape(n_z, CORES, part, a.shape[-1])
    picked = pl.BlockSpec((n_z, 1, part, HD), lambda i, c, h: (0, c[0], 0, h[0]))
    whole = lambda shape: pl.BlockSpec(shape, lambda i, c, h: (0,) * len(shape))
    return pl.pallas_call(
        kv_kernel,
        grid_spec=pltpu.PrefetchScalarGridSpec(
            num_scalar_prefetch=2,
            grid=(1,),
            in_specs=[picked, picked, whole((1, HD)), whole((rows, HD)), whole((rows, HD))],
            out_specs=whole((2, rows, HD)),
        ),
        out_shape=jax.ShapeDtypeStruct((2, rows, HD), BF16),
        name="prepare_kv",
    )(core, head, view(keys), view(values), gain, cosine, sine)


def mix_kernel(n_pieces, n_out, core_ref, z_ref, q_own, q_other, gain_ref, cos_ref, sin_ref, *rest):
    w_own, w_other = rest[:2]
    pieces = rest[2 : 2 + n_pieces]
    outs = rest[2 + n_pieces : 2 + n_pieces + n_out]
    keys_ref, vals_ref = rest[2 + n_pieces + n_out :]
    step = pl.program_id(0)

    @pl.when(step == 0)
    def _():
        row = 0
        for piece in pieces:
            rows = piece.shape[1]
            keys_ref[pl.ds(row, rows)] = piece[0]
            vals_ref[pl.ds(row, rows)] = piece[1]
            row += rows

    factor = HD ** (-0.5) * 1.4426950408889634
    part = cos_ref.shape[0]
    heads = q_own.shape[-1] // HD
    queries = []
    for field in (q_own[...].reshape(part, heads * HD), q_other[0]):
        for head in range(heads):
            one = field[:, head * HD : (head + 1) * HD].astype(F32)
            queries.append(norm_turn(one, gain_ref[...], cos_ref[...], sin_ref[...]).astype(BF16))
    query = jnp.concatenate(queries, axis=0)
    scores = lax.dot_general(
        query, keys_ref[...], (((1,), (1,)), ((), ())), preferred_element_type=F32
    )
    top = jnp.max(scores, axis=1, keepdims=True)
    weights = jnp.exp2((scores - top) * factor)
    totals = jnp.sum(weights, axis=1, keepdims=True)
    merged = jnp.dot(weights.astype(BF16), vals_ref[...], preferred_element_type=F32)
    merged = (merged / totals).astype(BF16)
    sides = []
    for side in range(2):
        picked = [merged[(side * heads + h) * part : (side * heads + h + 1) * part] for h in range(heads)]
        sides.append(jnp.concatenate(picked, axis=1) if heads > 1 else picked[0])
    mixed = jnp.dot(sides[0], w_own[...], preferred_element_type=F32)
    mixed = mixed + jnp.dot(sides[1], w_other[...], preferred_element_type=F32)
    mixed = mixed.astype(BF16)
    for n, out_ref in enumerate(outs):

        @pl.when(step == n)
        def _():
            out_ref[...] = mixed


def mix(core, z_index, queries, q_other, gain, cosine, sine, w_own, w_other, pieces, n_z):
    rows, width = cosine.shape[0], queries.shape[-1]
    part = rows // n_z
    d_model = w_own.shape[-1]
    length = sum(p.shape[1] for p in pieces)
    whole = lambda a: pl.BlockSpec(a.shape, lambda i, c, z: (0,) * a.ndim)
    turn = lambda i, z: lax.rem(i + z[0], n_z)
    table = pl.BlockSpec((part, HD), lambda i, c, z: (turn(i, z), 0))
    return pl.pallas_call(
        lambda *refs: mix_kernel(len(pieces), n_z, *refs),
        grid_spec=pltpu.PrefetchScalarGridSpec(
            num_scalar_prefetch=2,
            grid=(n_z,),
            in_specs=[
                pl.BlockSpec((1, 1, part, width), lambda i, c, z: (turn(i, z), c[0], 0, 0)),
                pl.BlockSpec((1, part, width), lambda i, c, z: (turn(i, z), 0, 0)),
                whole(gain),
                table,
                table,
                whole(w_own),
                whole(w_other),
            ]
            + [whole(p) for p in pieces],
            out_specs=[pl.BlockSpec((part, d_model), lambda i, c, z: (0, 0))] * n_z,
            scratch_shapes=[pltpu.VMEM((length, HD), BF16), pltpu.VMEM((length, HD), BF16)],
        ),
        out_shape=[jax.ShapeDtypeStruct((part, d_model), BF16)] * n_z,
        compiler_params=pltpu.CompilerParams(vmem_limit_bytes=56 * MIB),
        name="mix",
    )(
        core, z_index, queries.reshape(n_z, CORES, part, width), q_other, gain, cosine, sine,
        w_own, w_other, *pieces,
    )


def dispatch_kernel(core_ref, tokens_ref, gain_ref, slots_ref, *out_refs):
    rows, d_model = slots_ref.shape[-1], tokens_ref.shape[-1]
    field = tokens_ref[...].reshape(rows, d_model).astype(F32)
    mean = jnp.mean(field * field, axis=-1, keepdims=True)
    normed = (field * lax.rsqrt(mean + EPS) * gain_ref[...]).astype(BF16)
    for chunk, out_ref in enumerate(out_refs):
        n_slots = out_ref.shape[0]
        slot = lax.broadcasted_iota(jnp.int32, (n_slots, rows), 0) + chunk * n_slots
        hot = slot == slots_ref[0:1]
        for k in range(1, TOPK):
            hot = hot | (slot == slots_ref[k : k + 1])
        out_ref[...] = jnp.dot(
            hot.astype(F32).astype(BF16), normed, preferred_element_type=F32
        ).astype(BF16)


def dispatch(core, tokens, gain, slots, n_z, pieces):
    local_rows, d_model = tokens.shape
    part = local_rows // (n_z * CORES)
    n_slots = EXPERTS * n_z * CAP // pieces
    return pl.pallas_call(
        dispatch_kernel,
        grid_spec=pltpu.PrefetchScalarGridSpec(
            num_scalar_prefetch=1,
            grid=(1,),
            in_specs=[
                pl.BlockSpec((n_z, 1, part, d_model), lambda i, c: (0, c[0], 0, 0)),
                pl.BlockSpec((1, d_model), lambda i, c: (0, 0)),
                pl.BlockSpec(slots.shape, lambda i, c: (0, 0)),
            ],
            out_specs=[pl.BlockSpec((n_slots, d_model), lambda i, c: (0, 0))] * pieces,
        ),
        out_shape=[jax.ShapeDtypeStruct((n_slots, d_model), BF16)] * pieces,
        name="dispatch",
    )(core, tokens.reshape(n_z, CORES, part, d_model), gain, slots)


def expert_kernel(n_src, *refs):
    ins, (gate_ref, up_ref, down_ref) = refs[: 2 * n_src], refs[2 * n_src : 2 * n_src + 3]
    outs, (field_ref, acc_ref) = refs[2 * n_src + 3 : -2], refs[-2:]
    step = pl.program_id(1)
    rows = ins[0].shape[1]

    @pl.when(step == 0)
    def _():
        for n, ref in enumerate(ins):
            field_ref[n * rows : (n + 1) * rows] = ref[0]

    field = field_ref[...]
    gate = jnp.dot(field, gate_ref[0], preferred_element_type=F32)
    up = jnp.dot(field, up_ref[0], preferred_element_type=F32)
    hidden = (gate / (1.0 + jnp.exp(-gate)) * up).astype(BF16)
    result = jnp.dot(hidden, down_ref[0], preferred_element_type=F32)

    @pl.when(step == 0)
    def _():
        acc_ref[...] = result

    @pl.when(step > 0)
    def _():
        acc_ref[...] += result

    @pl.when(step == pl.num_programs(1) - 1)
    def _():
        for n, ref in enumerate(outs):
            ref[0] = acc_ref[n * rows : (n + 1) * rows].astype(BF16)


def experts(own, other, gate_weight, up_weight, down_weight, first):
    pieces = [*own, *other]
    per, rows, d_model = pieces[0].shape
    width = gate_weight.shape[-1]
    steps = 2 if width % 512 == 0 else 1
    cut = width // steps
    act = pl.BlockSpec((1, rows, d_model), lambda e, s: (e, 0, 0))
    outs = pl.pallas_call(
        lambda *refs: expert_kernel(len(own), *refs),
        grid=(per, steps),
        in_specs=[act] * len(pieces)
        + [
            pl.BlockSpec((1, d_model, cut), lambda e, s: (e + first, 0, s)),
            pl.BlockSpec((1, d_model, cut), lambda e, s: (e + first, 0, s)),
            pl.BlockSpec((1, cut, d_model), lambda e, s: (e + first, s, 0)),
        ],
        out_specs=[act] * len(pieces),
        out_shape=[jax.ShapeDtypeStruct((per, rows, d_model), BF16)] * len(pieces),
        scratch_shapes=[
            pltpu.VMEM((len(pieces) * rows, d_model), BF16),
            pltpu.VMEM((len(pieces) * rows, d_model), F32),
        ],
        compiler_params=pltpu.CompilerParams(vmem_limit_bytes=40 * MIB),
        name="experts",
    )(*pieces, gate_weight, up_weight, down_weight)
    return outs[: len(own)], outs[len(own) :]


def combine_kernel(n_back, z_ref, slots_ref, shares_ref, *rest):
    back_refs, out_refs, total_ref = rest[:n_back], rest[n_back:-1], rest[-1]
    rows = slots_ref.shape[0]
    total = jnp.zeros((rows, back_refs[0].shape[-1]), F32)
    for piece, back_ref in enumerate(back_refs):
        n_slots = back_ref.shape[0]
        slot = lax.broadcasted_iota(jnp.int32, (rows, n_slots), 1) + piece * n_slots
        matrix = jnp.zeros((rows, n_slots), F32)
        for k in range(TOPK):
            share = shares_ref[:, k : k + 1]
            matrix = matrix + jnp.where(slot == slots_ref[:, k : k + 1], share, 0.0)
        high = matrix.astype(BF16)
        low = (matrix - high.astype(F32)).astype(BF16)
        back = back_ref[...]
        total = total + jnp.dot(high, back, preferred_element_type=F32)
        total = total + jnp.dot(low, back, preferred_element_type=F32)
    total_ref[...] = total.reshape(total_ref.shape)
    n_z = len(out_refs)
    for n, out_ref in enumerate(out_refs):
        out_ref[...] = total_ref[lax.rem(z_ref[0] + n, n_z)].astype(BF16)


def combine(z_index, slots, shares, backs, n_z):
    rows, d_model = slots.shape[0], backs[0].shape[-1]
    whole = lambda a: pl.BlockSpec(a.shape, lambda i, z: (0,) * a.ndim)
    return pl.pallas_call(
        lambda *refs: combine_kernel(len(backs), *refs),
        grid_spec=pltpu.PrefetchScalarGridSpec(
            num_scalar_prefetch=1,
            grid=(1,),
            in_specs=[whole(a) for a in (slots, shares, *backs)],
            out_specs=[pl.BlockSpec((rows // n_z, d_model), lambda i, z: (0, 0))] * n_z,
            scratch_shapes=[pltpu.VMEM((n_z, rows // n_z, d_model), F32)],
        ),
        out_shape=[jax.ShapeDtypeStruct((rows // n_z, d_model), BF16)] * n_z,
        name="combine",
    )(z_index, slots, shares, *backs)


def shift(a, axis, step):
    n = lax.axis_size(axis)
    return lax.ppermute(a, axis, [(i, (i + step) % n) for i in range(n)])


def swap_cores(a):
    return lax.ppermute(a, "core", [(i, CORES - 1 - i) for i in range(CORES)])


def on_device(
    queries,
    keys,
    values,
    query_gain,
    key_gain,
    out_weight,
    tokens_b,
    norm_gain,
    routes,
    route_weight,
    gate_weight,
    up_weight,
    down_weight,
):
    n_ep, n_z = lax.axis_size("ep"), lax.axis_size("z")
    core, z_index = lax.axis_index("core"), lax.axis_index("z")
    core_arg = core.reshape(1).astype(jnp.int32)
    z_arg = z_index.reshape(1).astype(jnp.int32)
    n_rows, width = queries.shape
    d_model = tokens_b.shape[-1]
    heads = width // HD
    n_heads = heads * n_z * CORES

    part = n_rows // (n_z * CORES)
    offsets = (
        jnp.arange(n_z, dtype=jnp.int32)[:, None] * (CORES * part)
        + core * part
        + jnp.arange(part, dtype=jnp.int32)[None, :]
    ).reshape(-1)
    cosine, sine = rope_tables(lax.axis_index("ep") * n_rows + offsets)
    kv_head = ((z_index * CORES + core) * heads // (n_heads // KVH)).reshape(1).astype(jnp.int32)
    own_kv = prepare_kv(core_arg, kv_head, keys, values, key_gain[None], cosine, sine, n_z)
    pieces = [own_kv]
    for step in range(1, n_ep):
        pieces.append(shift(own_kv, "ep", step))
    pieces = pieces + [swap_cores(p) for p in pieces]

    q_view = queries.reshape(n_z, CORES, part, width)
    q_other = swap_cores(lax.dynamic_index_in_dim(q_view, 1 - core, 1, keepdims=False))
    w_other = swap_cores(out_weight)

    n_local = gate_weight.shape[0]
    chunks = 2 if n_local % 2 == 0 else 1
    per = n_local // chunks
    block_rows = tokens_b.shape[0] // (n_z * CORES)
    picks = block_rows * TOPK
    own_block = lambda a: lax.dynamic_index_in_dim(
        a.reshape(n_z, CORES, block_rows, TOPK), core, 1, keepdims=False
    )
    own_routes = own_block(routes)
    assigned = own_routes.reshape(n_z, picks)
    earlier = jnp.arange(picks)[:, None] > jnp.arange(picks)[None, :]
    same = (assigned[:, :, None] == assigned[:, None, :]) & earlier[None]
    rank = jnp.sum(same.astype(jnp.int32), axis=-1)
    block = jnp.arange(n_z, dtype=jnp.int32)[:, None]
    local = assigned % n_local
    ahead = lax.rem(assigned // n_local + n_ep - lax.axis_index("ep"), n_ep)
    place = ((local // per) * n_ep + ahead) * per + local % per
    slots = ((place * n_z + block) * CAP + rank).reshape(n_z * block_rows, TOPK)
    own_weight = own_block(route_weight).reshape(n_z * block_rows, TOPK)
    shares = own_weight / jnp.sum(own_weight, axis=-1, keepdims=True)

    outgoing = dispatch(core_arg, tokens_b, norm_gain[None], slots.T, n_z, chunks * n_ep)
    arrived = []
    for chunk in range(chunks):
        here = []
        for step in range(n_ep):
            piece = outgoing[chunk * n_ep + step].reshape(per, n_z * CAP, d_model)
            here.append(shift(piece, "ep", step) if step else piece)
        arrived.append((here, [swap_cores(p) for p in here]))

    mixed = mix(
        core_arg, z_arg, queries, q_other, query_gain[None], cosine, sine, out_weight, w_other,
        pieces, n_z,
    )
    gathered = [mixed[0].astype(F32)]
    for step in range(1, n_z):
        gathered.append(shift(mixed[step], "z", step).astype(F32))
    mixed_out = sum(gathered).astype(BF16)

    backs = []
    for chunk in range(chunks):
        keep, send = experts(
            *arrived[chunk], gate_weight, up_weight, down_weight, chunk * per
        )
        for step in range(n_ep):
            there = swap_cores(send[step])
            result = (keep[step].astype(F32) + there.astype(F32)).astype(BF16)
            result = shift(result, "ep", n_ep - step) if step else result
            backs.append(result.reshape(-1, d_model))
    rows = combine(z_arg, slots, shares, backs, n_z)
    gathered = [rows[0].astype(F32)]
    for step in range(1, n_z):
        gathered.append(shift(rows[step], "z", step).astype(F32))
    expert_out = sum(gathered).astype(BF16)
    return (mixed_out, expert_out)


def solution(mesh):
    n_ep, n_tp = mesh.shape["ep"], mesh.shape["tp"]
    fine = Mesh(mesh.devices.reshape(n_ep, n_tp // CORES, CORES), ("ep", "z", "core"))
    tp = ("z", "core")
    placed = (
        P("ep", tp),
        P("ep", None),
        P("ep", None),
        P(),
        P(),
        P(tp, None),
        P("ep", None),
        P(),
        P("ep", None),
        P("ep", None),
        P("ep", None, tp),
        P("ep", None, tp),
        P("ep", tp, None),
    )

    return jax.shard_map(
        on_device,
        mesh=fine,
        in_specs=placed,
        out_specs=(P(("ep", "z", "core"), None), P(("ep", "z", "core"), None)),
        check_vma=False,
    )
```

time: 187 us -> 187 us (level)
  the two profiles are of different devices: /device:TPU:0 before, /device:TPU:13 now
where the time goes in v2:
time: 187 us; the launch traced here: 186 us
  waiting for transfers between devices  76.2 us (41%)
  Pallas kernels  47.2 us (25%)
  starting transfers between devices  29 us (16%)
  local copies, waits for them, and re-layouts  23.1 us (12%)
  other arithmetic  9.51 us (5%)
    ppermute x21, waiting for transfers between devices, shift(): return lax.ppermute(a, axis, [(i, (i + step) % n) for i in range(n)])  71.7 us
    pallas_call x1, Pallas kernels, mix(): pl.pallas_call(lambda *refs: mix_kernel(len(pieces), n_z, *refs), grid_sp...  19.7 us
    unnamed x66, local copies, waits for them, and re-layouts  18.7 us
    ppermute x21, starting transfers between devices, shift(): return lax.ppermute(a, axis, [(i, (i + step) % n) for i in range(n)])  16.5 us
    pallas_call x2, Pallas kernels, experts(): pl.pallas_call(lambda *refs: expert_kernel(len(own), *refs), grid=(per, s...  15.7 us
    ppermute x22, starting transfers between devices, swap_cores(): return lax.ppermute(a, 'core', [(i, CORES - 1 - i) for i in range(CORES)])  12.6 us
    pallas_call x1, Pallas kernels, combine(): pl.pallas_call(lambda *refs: combine_kernel(len(backs), *refs), grid_spec...  6.28 us
    ppermute x22, waiting for transfers between devices, swap_cores(): return lax.ppermute(a, 'core', [(i, CORES - 1 - i) for i in range(CORES)])  4.57 us
  transfers between devices with their start and end apart: 43, of which 16 were waited for; matrix products, arithmetic and copies ran while one was open for 5% of the time, Pallas kernels for 24%

profile of v2, /device:TPU:13, one launch (start us, length us, event | category | flops | bytes accessed | tf_op | source)
XLA Modules:
  0.0 186.0 jit_solution(4703259286719805048)
XLA Ops:
  3.1 3.4 %dispatch.1 = (bf16[64,2048]{1,0:T(8,128)(2,1)}, bf16[64,2048]{1,0:T(8,128)(2,1)}, bf16[64,2048]{1,0:T(8,128)(2,1)}, bf16[64,2048]{1,0:T(8,128)(2,1)}, bf16[64,2...) custom-call(s32[1]{0:T(128)} %bitcast.core_ref.refs_0_, ...), custom_call_target="tpu_custom_call" | custom-call | tf_op jit(solution)/shard_map/dispatch/pallas_call | solution.py:176
  6.5 1.2 collective-permute-start.26
  7.9 1.2 collective-permute-start.28
  9.1 1.5 collective-permute-start.29
  11.0 1.6 dynamic-slice_bitcast_fusion
  12.7 2.1 %collective-permute-done.26.refs_1_ = bf16[2,32,2048]{2,1,0:T(8,128)(2,1)S(1)} collective-permute-done((bf16[2,32,2048]{2,1,0:T(8,128)(2,1)}, bf16[2,32,2048]{2,1,0:T(8,128)(2,1)S(1)}, u32[]{:S(2)}, u32[]{:S(2)}) %collective-permute-start.26) | collective-permute-done | bytes 262176 | tf_op jit(solution)/shard_map/ppermute | solution.py:293
  15.1 7.4 %collective-permute-done.27.refs_2_ = bf16[2,32,2048]{2,1,0:T(8,128)(2,1)S(1)} collective-permute-done((bf16[2,32,2048]{2,1,0:T(8,128)(2,1)}, bf16[2,32,2048]{2,1,0:T(8,128)(2,1)S(1)}, u32[]{:S(2)}, u32[]{:S(2)}) %collective-permute-start.27) | collective-permute-done | bytes 262176 | tf_op jit(solution)/shard_map/ppermute | solution.py:293
  22.5 1.1 collective-permute-start.30
  24.4 1.8 collective-permute-done.12.refs_1_
  26.1 2.7 %collective-permute-start.32 = (bf16[2,32,2048]{2,1,0:T(8,128)(2,1)S(1)}, bf16[2,32,2048]{2,1,0:T(8,128)(2,1)S(1)}, u32[]{:S(2)}, u32[]{:S(2)}) collective-permute-start(bf16[2,32,2048]{2,1,0:T(8,128)(2,1)S(1)} %collective-permute-done.28.refs_3_), channel_id=1, source_target_pairs={{0,1},{1,0},{2,3},{3,2},{4,5},{5,4},{6,7},{7,6},{8,9},{9,8},{10,11... | collective-permute-start | bytes 786440 | tf_op jit(solution)/shard_map/ppermute | solution.py:297
  29.6 1.6 sine_multiply_fusion
  31.1 1.6 collective-permute-done.13.refs_2_
  35.9 3.4 %copy-done = bf16[4,2048,512]{2,1,0:T(8,128)(2,1)S(1)} copy-done((bf16[4,2048,512]{2,1,0:T(8,128)(2,1)S(1)}, bf16[4,2048,512]{2,1,0:T(8,128)(2,1)}, u32[]{:S(2)}) %copy-start) | copy-done | bytes 8388632
  39.2 0.9 copy-done.3
  40.2 0.9 copy-done.5
  41.1 0.9 copy-done.7
  42.1 0.9 copy-done.9
  43.0 0.9 copy-done.11
  44.0 0.9 copy-done.13
  44.9 8.1 %experts.3 = (bf16[2,32,2048]{2,1,0:T(8,128)(2,1)S(1)}, bf16[2,32,2048]{2,1,0:T(8,128)(2,1)S(1)}, bf16[2,32,2048]{2,1,0:T(8,128)(2,1)S(1)}, bf16[2,32,2048]{2,1,...) custom-call(bf16[2,32,2048]{2,1,0:T(8,128)(2,1)S(1)} %bitcast.55, ...), custom_call_target="tpu_custom_call" | custom-call | tf_op jit(solution)/shard_map/experts/pallas_call | solution.py:231
  55.9 2.2 %prepare_kv.1.refs_9_ = bf16[2,384,128]{2,1,0:T(8,128)(2,1)} custom-call(s32[1]{0:T(128)} %bitcast.core_ref.refs_0_, s32[1]{0:T(128)} %bitcast.5.head_ref, bf16[4,2,96,512]{3,2,1,0:T(8,128)(2,1)} %bitcast.62, bf16[4,2,96,512]{3,2,1,0:T(8,128)(2,1)} %bitcast.63, f32[1,128]{1,0:T(1,128)} %bitcast.72, f32[384,128]{1,0:T(8,128)} %get-tuple-element.69.cos_ref.refs_5_, ...), custom_call_target="tpu_custom_call" | custom-call | tf_op jit(solution)/shard_map/prepare_kv/pallas_call | solution.py:61
  59.3 1.3 collective-permute-start.3
  61.4 1.0 collective-permute-start.5
  62.4 3.4 %copy-done.1 = bf16[4,2048,512]{2,1,0:T(8,128)(2,1)S(1)} copy-done((bf16[4,2048,512]{2,1,0:T(8,128)(2,1)S(1)}, bf16[4,2048,512]{2,1,0:T(8,128)(2,1)}, u32[]{:S(2)}) %copy-start.1) | copy-done | bytes 8388632
  65.8 7.5 %experts.2 = (bf16[2,32,2048]{2,1,0:T(8,128)(2,1)S(1)}, bf16[2,32,2048]{2,1,0:T(8,128)(2,1)S(1)}, bf16[2,32,2048]{2,1,0:T(8,128)(2,1)S(1)}, bf16[2,32,2048]{2,1,...) custom-call(bf16[2,32,2048]{2,1,0:T(8,128)(2,1)S(1)} %bitcast.53, ...), custom_call_target="tpu_custom_call" | custom-call | tf_op jit(solution)/shard_map/experts/pallas_call | solution.py:231
  73.4 1.0 add_convert_fusion.1
  75.2 1.3 collective-permute-done.34
  76.7 1.3 collective-permute-done.33
  82.5 2.6 %collective-permute-start.35 = (bf16[2,32,2048]{2,1,0:T(8,128)(2,1)S(1)}, bf16[2,32,2048]{2,1,0:T(8,128)(2,1)S(1)}, u32[]{:S(2)}, u32[]{:S(2)}) collective-permute-start(bf16[2,32,2048]{2,1,0:T(8,128)(2,1)S(1)} %add_convert_fusion.3), channel_id=1, source_target_pairs={{0,24},{8,0},{16,8},{24,16},{1,25},{9,1},{17,9},{25,17},{2,26},{10... | collective-permute-start | bytes 786440 | tf_op jit(solution)/shard_map/ppermute | solution.py:293
  85.2 4.6 %collective-permute-done.39 = bf16[2,32,2048]{2,1,0:T(8,128)(2,1)S(1)} collective-permute-done((bf16[2,32,2048]{2,1,0:T(8,128)(2,1)S(1)}, bf16[2,32,2048]{2,1,0:T(8,128)(2,1)S(1)}, u32[]{:S(2)}, u32[]{:S(2)}) %collective-permute-start.39) | collective-permute-done | bytes 262176 | tf_op jit(solution)/shard_map/ppermute | solution.py:293
  89.8 1.1 collective-permute-start.23
  91.0 5.4 %collective-permute-done.37 = bf16[2,32,2048]{2,1,0:T(8,128)(2,1)S(1)} collective-permute-done((bf16[2,32,2048]{2,1,0:T(8,128)(2,1)S(1)}, bf16[2,32,2048]{2,1,0:T(8,128)(2,1)S(1)}, u32[]{:S(2)}, u32[]{:S(2)}) %collective-permute-start.37) | collective-permute-done | bytes 262176 | tf_op jit(solution)/shard_map/ppermute | solution.py:293
  97.1 4.0 %collective-permute-done.25 = bf16[2,32,2048]{2,1,0:T(8,128)(2,1)S(1)} collective-permute-done((bf16[2,32,2048]{2,1,0:T(8,128)(2,1)S(1)}, bf16[2,32,2048]{2,1,0:T(8,128)(2,1)S(1)}, u32[]{:S(2)}, u32[]{:S(2)}) %collective-permute-start.25) | collective-permute-done | bytes 262176 | tf_op jit(solution)/shard_map/ppermute | solution.py:293
  101.1 1.0 collective-permute-start.7
  102.1 5.0 %collective-permute-done.23 = bf16[2,32,2048]{2,1,0:T(8,128)(2,1)S(1)} collective-permute-done((bf16[2,32,2048]{2,1,0:T(8,128)(2,1)S(1)}, bf16[2,32,2048]{2,1,0:T(8,128)(2,1)S(1)}, u32[]{:S(2)}, u32[]{:S(2)}) %collective-permute-start.23) | collective-permute-done | bytes 262176 | tf_op jit(solution)/shard_map/ppermute | solution.py:293
  107.9 6.6 %collective-permute-done.21 = bf16[2,32,2048]{2,1,0:T(8,128)(2,1)S(1)} collective-permute-done((bf16[2,32,2048]{2,1,0:T(8,128)(2,1)S(1)}, bf16[2,32,2048]{2,1,0:T(8,128)(2,1)S(1)}, u32[]{:S(2)}, u32[]{:S(2)}) %collective-permute-start.21) | collective-permute-done | bytes 262176 | tf_op jit(solution)/shard_map/ppermute | solution.py:293
  114.6 1.3 collective-permute-start.8
  115.9 6.3 %combine.1 = (bf16[48,2048]{1,0:T(8,128)(2,1)}, bf16[48,2048]{1,0:T(8,128)(2,1)}, bf16[48,2048]{1,0:T(8,128)(2,1)}, bf16[48,2048]{1,0:T(8,128)(2,1)}) custom-call(s32[1]{0:T(128)} %bitcast.1.refs_1_.refs_0_, s32[192,2]{1,0:T(8,128)} %copy-done.21, f32[192,2]{1,0:T(8,128)} %bitcast_divide_fusion.refs_2_, bf16[64,2048]{1,0:T(8,128)(2,1)} %bitcast.58, ...), custom_call_target="tpu_custom_call" | custom-call | tf_op jit(solution)/shard_map/combine/pallas_call | solution.py:277
  122.2 1.4 collective-permute-start.40
  123.6 1.1 collective-permute-start.41
  124.7 1.4 collective-permute-start.42
  127.1 19.7 %mix.1 = (bf16[96,2048]{1,0:T(8,128)(2,1)}, bf16[96,2048]{1,0:T(8,128)(2,1)}, bf16[96,2048]{1,0:T(8,128)(2,1)}, bf16[96,2048]{1,0:T(8,128)(2,1)}) custom-call(s32[1]{0:T(128)} %bitcast.core_ref.refs_0_, s32[1]{0:T(128)} %bitcast.1.refs_1_.refs_0_, bf16[4,2,96,256]{3,2,1,0:T(8,128)(2,1)} %bitcast.61, bf16[4,96,256]{2,1,0:T(8,128)(2,1)} %copy-done.29, ...), custom_call_target="tpu_custom_call" | custom-call | tf_op jit(solution)/shard_map/mix/pallas_call | solution.py:129
  146.9 1.2 collective-permute-start.11
  148.1 1.0 collective-permute-start.9
  149.1 1.7 add_convert_fusion.9
  150.8 21.2 %collective-permute-done.10 = bf16[96,2048]{1,0:T(8,128)(2,1)S(1)} collective-permute-done((bf16[96,2048]{1,0:T(8,128)(2,1)}, bf16[96,2048]{1,0:T(8,128)(2,1)S(1)}, u32[]{:S(2)}, u32[]{:S(2)}) %collective-permute-start.10) | collective-permute-done | bytes 393248 | tf_op jit(solution)/shard_map/ppermute | solution.py:293
  172.0 12.0 %collective-permute-done.11 = bf16[96,2048]{1,0:T(8,128)(2,1)S(1)} collective-permute-done((bf16[96,2048]{1,0:T(8,128)(2,1)}, bf16[96,2048]{1,0:T(8,128)(2,1)S(1)}, u32[]{:S(2)}, u32[]{:S(2)}) %collective-permute-start.11) | collective-permute-done | bytes 393248 | tf_op jit(solution)/shard_map/ppermute | solution.py:293
  184.0 2.0 %add_convert_fusion = bf16[96,2048]{1,0:T(8,128)(2,1)} fusion(bf16[96,2048]{1,0:T(8,128)(2,1)S(1)} %collective-permute-done.11, bf16[96,2048]{1,0:T(8,128)(2,1)S(1)} %collective-permute-done.10, bf16[96,2048]{1,0:T(8,128)(2,1)S(1)} %collective-permute-done.9, bf16[96,2048]{1,0:T(8,128)(2,1)} %get-tuple-element.34), kind=kLoop, calls=%fused_computation | loop fusion | flops 1572864 | bytes 1966080 | tf_op jit(solution)/shard_map/convert_element_type | solution.py:379
  (143 shorter events, 21.2 us)
Async XLA Ops:
  2.5 50.6 %copy-start.21 = (s32[192,2]{1,0:T(8,128)}, s32[192,2]{1,0:T(8,128)S(1)}, u32[]{:S(2)}) copy-start(s32[192,2]{1,0:T(8,128)S(1)} %fusion.8.refs_1_) | copy-start | bytes 4612
  6.5 8.3 %collective-permute-start.26 = (bf16[2,32,2048]{2,1,0:T(8,128)(2,1)}, bf16[2,32,2048]{2,1,0:T(8,128)(2,1)S(1)}, u32[]{:S(2)}, u32[]{:S(2)}) collective-permute-start(bf16[2,32,2048]{2,1,0:T(8,128)(2,1)} %bitcast.79), channel_id=1, source_target_pairs={{0,8},{8,16},{16,24},{24,0},{1,9},{9,17},{17,25},{25,1},{2,10},{10... | collective-permute-start | bytes 786440 | tf_op jit(solution)/shard_map/ppermute | solution.py:293
  7.7 14.7 %collective-permute-start.27 = (bf16[2,32,2048]{2,1,0:T(8,128)(2,1)}, bf16[2,32,2048]{2,1,0:T(8,128)(2,1)S(1)}, u32[]{:S(2)}, u32[]{:S(2)}) collective-permute-start(bf16[2,32,2048]{2,1,0:T(8,128)(2,1)} %bitcast.78), channel_id=1, source_target_pairs={{0,16},{8,24},{16,0},{24,8},{1,17},{9,25},{17,1},{25,9},{2,18},{10... | collective-permute-start | bytes 786440 | tf_op jit(solution)/shard_map/ppermute | solution.py:293
  7.9 14.5 %collective-permute-start.28 = (bf16[2,32,2048]{2,1,0:T(8,128)(2,1)}, bf16[2,32,2048]{2,1,0:T(8,128)(2,1)S(1)}, u32[]{:S(2)}, u32[]{:S(2)}) collective-permute-start(bf16[2,32,2048]{2,1,0:T(8,128)(2,1)} %bitcast.77), channel_id=1, source_target_pairs={{0,24},{8,0},{16,8},{24,16},{1,25},{9,1},{17,9},{25,17},{2,26},{10... | collective-permute-start | bytes 786440 | tf_op jit(solution)/shard_map/ppermute | solution.py:293
  9.1 14.5 %collective-permute-start.29 = (bf16[2,32,2048]{2,1,0:T(8,128)(2,1)}, bf16[2,32,2048]{2,1,0:T(8,128)(2,1)S(1)}, u32[]{:S(2)}, u32[]{:S(2)}) collective-permute-start(bf16[2,32,2048]{2,1,0:T(8,128)(2,1)} %bitcast.54), channel_id=1, source_target_pairs={{0,1},{1,0},{2,3},{3,2},{4,5},{5,4},{6,7},{7,6},{8,9},{9,8},{10,11... | collective-permute-start | bytes 786440 | tf_op jit(solution)/shard_map/ppermute | solution.py:297
  10.6 15.5 %collective-permute-start.12 = (bf16[2,32,2048]{2,1,0:T(8,128)(2,1)}, bf16[2,32,2048]{2,1,0:T(8,128)(2,1)S(1)}, u32[]{:S(2)}, u32[]{:S(2)}) collective-permute-start(bf16[2,32,2048]{2,1,0:T(8,128)(2,1)} %bitcast.76), channel_id=1, source_target_pairs={{0,8},{8,16},{16,24},{24,0},{1,9},{9,17},{17,25},{25,1},{2,10},{10... | collective-permute-start | bytes 786440 | tf_op jit(solution)/shard_map/ppermute | solution.py:293
  14.8 17.9 %collective-permute-start.13 = (bf16[2,32,2048]{2,1,0:T(8,128)(2,1)}, bf16[2,32,2048]{2,1,0:T(8,128)(2,1)S(1)}, u32[]{:S(2)}, u32[]{:S(2)}) collective-permute-start(bf16[2,32,2048]{2,1,0:T(8,128)(2,1)} %bitcast.75), channel_id=1, source_target_pairs={{0,16},{8,24},{16,0},{24,8},{1,17},{9,25},{17,1},{25,9},{2,18},{10... | collective-permute-start | bytes 786440 | tf_op jit(solution)/shard_map/ppermute | solution.py:293
  22.5 10.7 %collective-permute-start.14 = (bf16[2,32,2048]{2,1,0:T(8,128)(2,1)}, bf16[2,32,2048]{2,1,0:T(8,128)(2,1)S(1)}, u32[]{:S(2)}, u32[]{:S(2)}) collective-permute-start(bf16[2,32,2048]{2,1,0:T(8,128)(2,1)} %bitcast.74), channel_id=1, source_target_pairs={{0,24},{8,0},{16,8},{24,16},{1,25},{9,1},{17,9},{25,17},{2,26},{10... | collective-permute-start | bytes 786440 | tf_op jit(solution)/shard_map/ppermute | solution.py:293
  22.5 10.7 %collective-permute-start.30 = (bf16[2,32,2048]{2,1,0:T(8,128)(2,1)S(1)}, bf16[2,32,2048]{2,1,0:T(8,128)(2,1)S(1)}, u32[]{:S(2)}, u32[]{:S(2)}) collective-permute-start(bf16[2,32,2048]{2,1,0:T(8,128)(2,1)S(1)} %collective-permute-done.26.refs_1_), channel_id=1, source_target_pairs={{0,1},{1,0},{2,3},{3,2},{4,5},{5,4},{6,7},{7,6},{8,9},{9,8},{10,11... | collective-permute-start | bytes 786440 | tf_op jit(solution)/shard_map/ppermute | solution.py:297
  24.3 10.1 %collective-permute-start.31 = (bf16[2,32,2048]{2,1,0:T(8,128)(2,1)S(1)}, bf16[2,32,2048]{2,1,0:T(8,128)(2,1)S(1)}, u32[]{:S(2)}, u32[]{:S(2)}) collective-permute-start(bf16[2,32,2048]{2,1,0:T(8,128)(2,1)S(1)} %collective-permute-done.27.refs_2_), channel_id=1, source_target_pairs={{0,1},{1,0},{2,3},{3,2},{4,5},{5,4},{6,7},{7,6},{8,9},{9,8},{10,11... | collective-permute-start | bytes 786440 | tf_op jit(solution)/shard_map/ppermute | solution.py:297
  26.1 9.0 %collective-permute-start.32 = (bf16[2,32,2048]{2,1,0:T(8,128)(2,1)S(1)}, bf16[2,32,2048]{2,1,0:T(8,128)(2,1)S(1)}, u32[]{:S(2)}, u32[]{:S(2)}) collective-permute-start(bf16[2,32,2048]{2,1,0:T(8,128)(2,1)S(1)} %collective-permute-done.28.refs_3_), channel_id=1, source_target_pairs={{0,1},{1,0},{2,3},{3,2},{4,5},{5,4},{6,7},{7,6},{8,9},{9,8},{10,11... | collective-permute-start | bytes 786440 | tf_op jit(solution)/shard_map/ppermute | solution.py:297
  29.6 32.8 %copy-start.2 = (bf16[64,2048]{1,0:T(8,128)(2,1)S(1)}, bf16[64,2048]{1,0:T(8,128)(2,1)}, u32[]{:S(2)}) copy-start(bf16[64,2048]{1,0:T(8,128)(2,1)} %get-tuple-element.38) | copy-start | bytes 786436
  32.7 26.1 %collective-permute-start.15 = (bf16[2,32,2048]{2,1,0:T(8,128)(2,1)}, bf16[2,32,2048]{2,1,0:T(8,128)(2,1)S(1)}, u32[]{:S(2)}, u32[]{:S(2)}) collective-permute-start(bf16[2,32,2048]{2,1,0:T(8,128)(2,1)} %bitcast.52), channel_id=1, source_target_pairs={{0,1},{1,0},{2,3},{3,2},{4,5},{5,4},{6,7},{7,6},{8,9},{9,8},{10,11... | collective-permute-start | bytes 786440 | tf_op jit(solution)/shard_map/ppermute | solution.py:297
  33.2 26.1 %collective-permute-start.16 = (bf16[2,32,2048]{2,1,0:T(8,128)(2,1)S(1)}, bf16[2,32,2048]{2,1,0:T(8,128)(2,1)S(1)}, u32[]{:S(2)}, u32[]{:S(2)}) collective-permute-start(bf16[2,32,2048]{2,1,0:T(8,128)(2,1)S(1)} %collective-permute-done.12.refs_1_), channel_id=1, source_target_pairs={{0,1},{1,0},{2,3},{3,2},{4,5},{5,4},{6,7},{7,6},{8,9},{9,8},{10,11... | collective-permute-start | bytes 786440 | tf_op jit(solution)/shard_map/ppermute | solution.py:297
  33.9 26.7 %collective-permute-start.17 = (bf16[2,32,2048]{2,1,0:T(8,128)(2,1)S(1)}, bf16[2,32,2048]{2,1,0:T(8,128)(2,1)S(1)}, u32[]{:S(2)}, u32[]{:S(2)}) collective-permute-start(bf16[2,32,2048]{2,1,0:T(8,128)(2,1)S(1)} %collective-permute-done.13.refs_2_), channel_id=1, source_target_pairs={{0,1},{1,0},{2,3},{3,2},{4,5},{5,4},{6,7},{7,6},{8,9},{9,8},{10,11... | collective-permute-start | bytes 786440 | tf_op jit(solution)/shard_map/ppermute | solution.py:297
  35.1 26.3 %collective-permute-start.18 = (bf16[2,32,2048]{2,1,0:T(8,128)(2,1)S(1)}, bf16[2,32,2048]{2,1,0:T(8,128)(2,1)}, u32[]{:S(2)}, u32[]{:S(2)}) collective-permute-start(bf16[2,32,2048]{2,1,0:T(8,128)(2,1)S(1)} %collective-permute-done.14.refs_3_), channel_id=1, source_target_pairs={{0,1},{1,0},{2,3},{3,2},{4,5},{5,4},{6,7},{7,6},{8,9},{9,8},{10,11... | collective-permute-start | bytes 786440 | tf_op jit(solution)/shard_map/ppermute | solution.py:297
  55.2 18.1 %collective-permute-start.38 = (bf16[2,32,2048]{2,1,0:T(8,128)(2,1)}, bf16[2,32,2048]{2,1,0:T(8,128)(2,1)}, u32[]{:S(2)}, u32[]{:S(2)}) collective-permute-start(bf16[2,32,2048]{2,1,0:T(8,128)(2,1)} %get-tuple-element.61), channel_id=1, source_target_pairs={{0,1},{1,0},{2,3},{3,2},{4,5},{5,4},{6,7},{7,6},{8,9},{9,8},{10,11... | collective-permute-start | bytes 786440 | tf_op jit(solution)/shard_map/ppermute | solution.py:297
  55.9 20.6 %copy-start.15 = (bf16[2,32,2048]{2,1,0:T(8,128)(2,1)S(1)}, bf16[2,32,2048]{2,1,0:T(8,128)(2,1)}, u32[]{:S(2)}) copy-start(bf16[2,32,2048]{2,1,0:T(8,128)(2,1)} %copy-done.14) | copy-start | bytes 786436
  58.8 21.0 %collective-permute-start.2 = (bf16[2,384,128]{2,1,0:T(8,128)(2,1)}, bf16[2,384,128]{2,1,0:T(8,128)(2,1)}, u32[]{:S(2)}, u32[]{:S(2)}) collective-permute-start(bf16[2,384,128]{2,1,0:T(8,128)(2,1)} %prepare_kv.1.refs_9_), channel_id=1, source_target_pairs={{0,8},{8,16},{16,24},{24,0},{1,9},{9,17},{17,25},{25,1},{2,10},{10... | collective-permute-start | bytes 589832 | tf_op jit(solution)/shard_map/ppermute | solution.py:293
  59.3 20.9 %collective-permute-start.3 = (bf16[2,384,128]{2,1,0:T(8,128)(2,1)}, bf16[2,384,128]{2,1,0:T(8,128)(2,1)}, u32[]{:S(2)}, u32[]{:S(2)}) collective-permute-start(bf16[2,384,128]{2,1,0:T(8,128)(2,1)} %prepare_kv.1.refs_9_), channel_id=1, source_target_pairs={{0,16},{8,24},{16,0},{24,8},{1,17},{9,25},{17,1},{25,9},{2,18},{10... | collective-permute-start | bytes 589832 | tf_op jit(solution)/shard_map/ppermute | solution.py:293
  60.6 21.1 %collective-permute-start.4 = (bf16[2,384,128]{2,1,0:T(8,128)(2,1)}, bf16[2,384,128]{2,1,0:T(8,128)(2,1)}, u32[]{:S(2)}, u32[]{:S(2)}) collective-permute-start(bf16[2,384,128]{2,1,0:T(8,128)(2,1)} %prepare_kv.1.refs_9_), channel_id=1, source_target_pairs={{0,24},{8,0},{16,8},{24,16},{1,25},{9,1},{17,9},{25,17},{2,26},{10... | collective-permute-start | bytes 589832 | tf_op jit(solution)/shard_map/ppermute | solution.py:293
  61.4 20.8 %collective-permute-start.5 = (bf16[2,384,128]{2,1,0:T(8,128)(2,1)}, bf16[2,384,128]{2,1,0:T(8,128)(2,1)S(1)}, u32[]{:S(2)}, u32[]{:S(2)}) collective-permute-start(bf16[2,384,128]{2,1,0:T(8,128)(2,1)} %prepare_kv.1.refs_9_), channel_id=1, source_target_pairs={{0,1},{1,0},{2,3},{3,2},{4,5},{5,4},{6,7},{7,6},{8,9},{9,8},{10,11... | collective-permute-start | bytes 589832 | tf_op jit(solution)/shard_map/ppermute | solution.py:297
  73.4 1.6 collective-permute-start.36
  75.0 1.5 collective-permute-start.34
  76.5 1.5 collective-permute-start.33
  78.0 1.5 collective-permute-start.24
  79.6 1.5 collective-permute-start.22
  79.8 2.7 %collective-permute-start.20 = (bf16[2,32,2048]{2,1,0:T(8,128)(2,1)S(1)}, bf16[2,32,2048]{2,1,0:T(8,128)(2,1)S(1)}, u32[]{:S(2)}, u32[]{:S(2)}) collective-permute-start(bf16[2,32,2048]{2,1,0:T(8,128)(2,1)S(1)} %get-tuple-element.45), channel_id=1, source_target_pairs={{0,1},{1,0},{2,3},{3,2},{4,5},{5,4},{6,7},{7,6},{8,9},{9,8},{10,11... | collective-permute-start | bytes 786440 | tf_op jit(solution)/shard_map/ppermute | solution.py:297
  80.2 4.9 %collective-permute-start.19 = (bf16[2,32,2048]{2,1,0:T(8,128)(2,1)S(1)}, bf16[2,32,2048]{2,1,0:T(8,128)(2,1)S(1)}, u32[]{:S(2)}, u32[]{:S(2)}) collective-permute-start(bf16[2,32,2048]{2,1,0:T(8,128)(2,1)S(1)} %get-tuple-element.43), channel_id=1, source_target_pairs={{0,1},{1,0},{2,3},{3,2},{4,5},{5,4},{6,7},{7,6},{8,9},{9,8},{10,11... | collective-permute-start | bytes 786440 | tf_op jit(solution)/shard_map/ppermute | solution.py:297
  81.1 8.7 %collective-permute-start.39 = (bf16[2,32,2048]{2,1,0:T(8,128)(2,1)S(1)}, bf16[2,32,2048]{2,1,0:T(8,128)(2,1)S(1)}, u32[]{:S(2)}, u32[]{:S(2)}) collective-permute-start(bf16[2,32,2048]{2,1,0:T(8,128)(2,1)S(1)} %add_convert_fusion.1), channel_id=1, source_target_pairs={{0,8},{8,16},{16,24},{24,0},{1,9},{9,17},{17,25},{25,1},{2,10},{10... | collective-permute-start | bytes 786440 | tf_op jit(solution)/shard_map/ppermute | solution.py:293
  81.7 44.3 %collective-permute-start.1 = (bf16[256,2048]{1,0:T(8,128)(2,1)}, bf16[256,2048]{1,0:T(8,128)(2,1)S(1)}, u32[]{:S(2)}, u32[]{:S(2)}) collective-permute-start(bf16[256,2048]{1,0:T(8,128)(2,1)} %refs_7_.1), channel_id=1, source_target_pairs={{0,1},{1,0},{2,3},{3,2},{4,5},{5,4},{6,7},{7,6},{8,9},{9,8},{10,11... | collective-permute-start | bytes 3145736 | tf_op jit(solution)/shard_map/ppermute | solution.py:297
  82.2 32.4 %copy-start.28 = (bf16[2,384,128]{2,1,0:T(8,128)(2,1)}, bf16[2,384,128]{2,1,0:T(8,128)(2,1)S(1)}, u32[]{:S(2)}) copy-start(bf16[2,384,128]{2,1,0:T(8,128)(2,1)S(1)} %collective-permute-done.5.refs_13_) | copy-start | bytes 589828
  82.2 14.2 %collective-permute-start.37 = (bf16[2,32,2048]{2,1,0:T(8,128)(2,1)S(1)}, bf16[2,32,2048]{2,1,0:T(8,128)(2,1)S(1)}, u32[]{:S(2)}, u32[]{:S(2)}) collective-permute-start(bf16[2,32,2048]{2,1,0:T(8,128)(2,1)S(1)} %add_convert_fusion.2), channel_id=1, source_target_pairs={{0,16},{8,24},{16,0},{24,8},{1,17},{9,25},{17,1},{25,9},{2,18},{10... | collective-permute-start | bytes 786440 | tf_op jit(solution)/shard_map/ppermute | solution.py:293
  82.5 14.5 %collective-permute-start.35 = (bf16[2,32,2048]{2,1,0:T(8,128)(2,1)S(1)}, bf16[2,32,2048]{2,1,0:T(8,128)(2,1)S(1)}, u32[]{:S(2)}, u32[]{:S(2)}) collective-permute-start(bf16[2,32,2048]{2,1,0:T(8,128)(2,1)S(1)} %add_convert_fusion.3), channel_id=1, source_target_pairs={{0,24},{8,0},{16,8},{24,16},{1,25},{9,1},{17,9},{25,17},{2,26},{10... | collective-permute-start | bytes 786440 | tf_op jit(solution)/shard_map/ppermute | solution.py:293
  85.2 15.9 %collective-permute-start.25 = (bf16[2,32,2048]{2,1,0:T(8,128)(2,1)S(1)}, bf16[2,32,2048]{2,1,0:T(8,128)(2,1)S(1)}, u32[]{:S(2)}, u32[]{:S(2)}) collective-permute-start(bf16[2,32,2048]{2,1,0:T(8,128)(2,1)S(1)} %add_convert_fusion.5), channel_id=1, source_target_pairs={{0,8},{8,16},{16,24},{24,0},{1,9},{9,17},{17,25},{25,1},{2,10},{10... | collective-permute-start | bytes 786440 | tf_op jit(solution)/shard_map/ppermute | solution.py:293
  89.8 26.1 %copy-start.22 = (bf16[2,32,2048]{2,1,0:T(8,128)(2,1)}, bf16[2,32,2048]{2,1,0:T(8,128)(2,1)S(1)}, u32[]{:S(2)}) copy-start(bf16[2,32,2048]{2,1,0:T(8,128)(2,1)S(1)} %collective-permute-done.39) | copy-start | bytes 786436
  89.8 17.4 %collective-permute-start.23 = (bf16[2,32,2048]{2,1,0:T(8,128)(2,1)S(1)}, bf16[2,32,2048]{2,1,0:T(8,128)(2,1)S(1)}, u32[]{:S(2)}, u32[]{:S(2)}) collective-permute-start(bf16[2,32,2048]{2,1,0:T(8,128)(2,1)S(1)} %add_convert_fusion.6), channel_id=1, source_target_pairs={{0,16},{8,24},{16,0},{24,8},{1,17},{9,25},{17,1},{25,9},{2,18},{10... | collective-permute-start | bytes 786440 | tf_op jit(solution)/shard_map/ppermute | solution.py:293
  96.4 25.8 %collective-permute-start = (bf16[4,96,256]{2,1,0:T(8,128)(2,1)}, bf16[4,96,256]{2,1,0:T(8,128)(2,1)S(1)}, u32[]{:S(2)}, u32[]{:S(2)}) collective-permute-start(bf16[4,96,256]{2,1,0:T(8,128)(2,1)} %dynamic-slice_bitcast_fusion), channel_id=1, source_target_pairs={{0,1},{1,0},{2,3},{3,2},{4,5},{5,4},{6,7},{7,6},{8,9},{9,8},{10,11... | collective-permute-start | bytes 589832 | tf_op jit(solution)/shard_map/ppermute | solution.py:297
  97.0 26.5 %collective-permute-start.6 = (bf16[2,384,128]{2,1,0:T(8,128)(2,1)}, bf16[2,384,128]{2,1,0:T(8,128)(2,1)S(1)}, u32[]{:S(2)}, u32[]{:S(2)}) collective-permute-start(bf16[2,384,128]{2,1,0:T(8,128)(2,1)} %collective-permute-done.2.refs_10_), channel_id=1, source_target_pairs={{0,1},{1,0},{2,3},{3,2},{4,5},{5,4},{6,7},{7,6},{8,9},{9,8},{10,11... | collective-permute-start | bytes 589832 | tf_op jit(solution)/shard_map/ppermute | solution.py:297
  101.1 23.6 %collective-permute-start.7 = (bf16[2,384,128]{2,1,0:T(8,128)(2,1)}, bf16[2,384,128]{2,1,0:T(8,128)(2,1)}, u32[]{:S(2)}, u32[]{:S(2)}) collective-permute-start(bf16[2,384,128]{2,1,0:T(8,128)(2,1)} %collective-permute-done.3.refs_11_), channel_id=1, source_target_pairs={{0,1},{1,0},{2,3},{3,2},{4,5},{5,4},{6,7},{7,6},{8,9},{9,8},{10,11... | collective-permute-start | bytes 589832 | tf_op jit(solution)/shard_map/ppermute | solution.py:297
  107.1 7.4 %collective-permute-start.21 = (bf16[2,32,2048]{2,1,0:T(8,128)(2,1)S(1)}, bf16[2,32,2048]{2,1,0:T(8,128)(2,1)S(1)}, u32[]{:S(2)}, u32[]{:S(2)}) collective-permute-start(bf16[2,32,2048]{2,1,0:T(8,128)(2,1)S(1)} %add_convert_fusion.7), channel_id=1, source_target_pairs={{0,24},{8,0},{16,8},{24,16},{1,25},{9,1},{17,9},{25,17},{2,26},{10... | collective-permute-start | bytes 786440 | tf_op jit(solution)/shard_map/ppermute | solution.py:293
  114.6 11.5 %collective-permute-start.8 = (bf16[2,384,128]{2,1,0:T(8,128)(2,1)}, bf16[2,384,128]{2,1,0:T(8,128)(2,1)S(1)}, u32[]{:S(2)}, u32[]{:S(2)}) collective-permute-start(bf16[2,384,128]{2,1,0:T(8,128)(2,1)} %collective-permute-done.4.refs_12_), channel_id=1, source_target_pairs={{0,1},{1,0},{2,3},{3,2},{4,5},{5,4},{6,7},{7,6},{8,9},{9,8},{10,11... | collective-permute-start | bytes 589832 | tf_op jit(solution)/shard_map/ppermute | solution.py:297
  122.2 25.9 %collective-permute-start.40 = (bf16[48,2048]{1,0:T(8,128)(2,1)}, bf16[48,2048]{1,0:T(8,128)(2,1)S(1)}, u32[]{:S(2)}, u32[]{:S(2)}) collective-permute-start(bf16[48,2048]{1,0:T(8,128)(2,1)} %get-tuple-element.63), channel_id=1, source_target_pairs={{0,2},{2,4},{4,6},{6,0},{1,3},{3,5},{5,7},{7,1},{8,10},{10,12},{12... | collective-permute-start | bytes 589832 | tf_op jit(solution)/shard_map/ppermute | solution.py:293
  123.6 25.5 %collective-permute-start.41 = (bf16[48,2048]{1,0:T(8,128)(2,1)}, bf16[48,2048]{1,0:T(8,128)(2,1)S(1)}, u32[]{:S(2)}, u32[]{:S(2)}) collective-permute-start(bf16[48,2048]{1,0:T(8,128)(2,1)} %get-tuple-element.64), channel_id=1, source_target_pairs={{0,4},{2,6},{4,0},{6,2},{1,5},{3,7},{5,1},{7,3},{8,12},{10,14},{12... | collective-permute-start | bytes 589832 | tf_op jit(solution)/shard_map/ppermute | solution.py:293
  124.7 24.4 %collective-permute-start.42 = (bf16[48,2048]{1,0:T(8,128)(2,1)}, bf16[48,2048]{1,0:T(8,128)(2,1)S(1)}, u32[]{:S(2)}, u32[]{:S(2)}) collective-permute-start(bf16[48,2048]{1,0:T(8,128)(2,1)} %get-tuple-element.65), channel_id=1, source_target_pairs={{0,6},{2,0},{4,2},{6,4},{1,7},{3,1},{5,3},{7,5},{8,14},{10,8},{12,... | collective-permute-start | bytes 589832 | tf_op jit(solution)/shard_map/ppermute | solution.py:293
  146.8 25.2 %collective-permute-start.10 = (bf16[96,2048]{1,0:T(8,128)(2,1)}, bf16[96,2048]{1,0:T(8,128)(2,1)S(1)}, u32[]{:S(2)}, u32[]{:S(2)}) collective-permute-start(bf16[96,2048]{1,0:T(8,128)(2,1)} %get-tuple-element.36), channel_id=1, source_target_pairs={{0,4},{2,6},{4,0},{6,2},{1,5},{3,7},{5,1},{7,3},{8,12},{10,14},{12... | collective-permute-start | bytes 1179656 | tf_op jit(solution)/shard_map/ppermute | solution.py:293
  146.9 37.1 %collective-permute-start.11 = (bf16[96,2048]{1,0:T(8,128)(2,1)}, bf16[96,2048]{1,0:T(8,128)(2,1)S(1)}, u32[]{:S(2)}, u32[]{:S(2)}) collective-permute-start(bf16[96,2048]{1,0:T(8,128)(2,1)} %get-tuple-element.37), channel_id=1, source_target_pairs={{0,6},{2,0},{4,2},{6,4},{1,7},{3,1},{5,3},{7,5},{8,14},{10,8},{12,... | collective-permute-start | bytes 1179656 | tf_op jit(solution)/shard_map/ppermute | solution.py:293
  148.1 35.9 %collective-permute-start.9 = (bf16[96,2048]{1,0:T(8,128)(2,1)}, bf16[96,2048]{1,0:T(8,128)(2,1)S(1)}, u32[]{:S(2)}, u32[]{:S(2)}) collective-permute-start(bf16[96,2048]{1,0:T(8,128)(2,1)} %get-tuple-element.35), channel_id=1, source_target_pairs={{0,2},{2,4},{4,6},{6,0},{1,3},{3,5},{5,7},{7,1},{8,10},{10,12},{12... | collective-permute-start | bytes 1179656 | tf_op jit(solution)/shard_map/ppermute | solution.py:293
  (27 other events, 128.1 us)

commit v3 on v2

v3 whole, which is shorter than its diff:
```python
import jax
import jax.numpy as jnp
from jax import lax
from jax.experimental import pallas as pl
from jax.experimental.pallas import tpu as pltpu
from jax.sharding import Mesh, PartitionSpec as P


HD = 128
KVH = 4
EXPERTS = 16
TOPK = 2
GRID_W = 64
CAP = 8
EPS = 1e-06
THETA = 10000.0
CORES = 2
IN_VMEM = pl.BlockSpec(memory_space=pltpu.VMEM)
IN_SMEM = pl.BlockSpec(memory_space=pltpu.SMEM)
KEY_CHUNK = 1024
MIB = 1024 * 1024

F32 = jnp.float32
BF16 = jnp.bfloat16


def in_hbm(arrays):
    return [pltpu.with_memory_space_constraint(a, pltpu.HBM) for a in arrays]


def rope_tables(positions):
    n_freq = HD // 4
    row_pos = (positions // GRID_W).astype(F32)[:, None]
    col_pos = (positions % GRID_W).astype(F32)[:, None]
    lane = jnp.arange(HD, dtype=jnp.int32)
    inverse = THETA ** (-(lane % n_freq).astype(F32) / n_freq)
    angle = jnp.where(lane < HD // 2, row_pos, col_pos) * inverse
    sign = jnp.where((lane // n_freq) % 2 == 0, -1.0, 1.0).astype(F32)
    return jnp.cos(angle), jnp.sin(angle) * sign


def norm_turn(field, gain, cosine, sine):
    quarter = HD // 4
    mean = jnp.mean(field * field, axis=-1, keepdims=True)
    field = field * lax.rsqrt(mean + EPS) * gain
    lane = lax.broadcasted_iota(jnp.int32, field.shape, 1)
    partner = jnp.where(
        (lane // quarter) % 2 == 0,
        pltpu.roll(field, HD - quarter, 1),
        pltpu.roll(field, quarter, 1),
    )
    return field * cosine + partner * sine


def prepare_kernel(
    core_ref, head_ref, keys_ref, values_ref, q_ref, gain_ref, cos_ref, sin_ref, kv_ref, send_ref
):
    rows = cos_ref.shape[0]
    field = keys_ref[...].reshape(rows, HD).astype(F32)
    kv_ref[0] = norm_turn(field, gain_ref[...], cos_ref[...], sin_ref[...]).astype(BF16)
    kv_ref[1] = values_ref[...].reshape(rows, HD)
    send_ref[...] = q_ref[...].reshape(send_ref.shape)


def prepare(core, head, keys, values, queries, gain, cosine, sine, n_z):
    rows, width = cosine.shape[0], queries.shape[-1]
    part = rows // n_z
    view = lambda a: a.reshape(n_z, CORES, part, a.shape[-1])
    picked = pl.BlockSpec((n_z, 1, part, HD), lambda i, c, h: (0, c[0], 0, h[0]))
    whole = lambda shape: pl.BlockSpec(shape, lambda i, c, h: (0,) * len(shape))
    return pl.pallas_call(
        prepare_kernel,
        grid_spec=pltpu.PrefetchScalarGridSpec(
            num_scalar_prefetch=2,
            grid=(1,),
            in_specs=[
                picked,
                picked,
                pl.BlockSpec((n_z, 1, part, width), lambda i, c, h: (0, 1 - c[0], 0, 0)),
                whole((1, HD)),
                whole((rows, HD)),
                whole((rows, HD)),
            ],
            out_specs=[IN_VMEM, IN_VMEM],
        ),
        out_shape=[
            jax.ShapeDtypeStruct((2, rows, HD), BF16),
            jax.ShapeDtypeStruct((n_z, part, width), BF16),
        ],
        compiler_params=pltpu.CompilerParams(vmem_limit_bytes=8 * MIB),
        name="prepare",
    )(core, head, *in_hbm([view(keys), view(values), view(queries)]), gain, cosine, sine)


def add_kernel(*refs):
    total = refs[0][...].astype(F32)
    for ref in refs[1:-1]:
        total = total + ref[...].astype(F32)
    refs[-1][...] = total.astype(BF16)


def add(*arrays):
    return pl.pallas_call(
        add_kernel,
        in_specs=[IN_VMEM] * len(arrays),
        out_specs=IN_VMEM,
        out_shape=jax.ShapeDtypeStruct(arrays[0].shape, BF16),
        compiler_params=pltpu.CompilerParams(vmem_limit_bytes=8 * MIB),
        name="add",
    )(*arrays)


def mix_kernel(n_pieces, n_z, core_ref, z_ref, q_own, q_other, gain_ref, cos_ref, sin_ref, *rest):
    w_own, w_other = rest[:2]
    pieces = rest[2 : 2 + n_pieces]
    outs = rest[2 + n_pieces : 2 + n_pieces + n_z]
    keys_ref, vals_ref, mixed_ref = rest[2 + n_pieces + n_z :]
    row = 0
    for piece in pieces:
        rows = piece.shape[1]
        keys_ref[row : row + rows] = piece[0]
        vals_ref[row : row + rows, :HD] = piece[1]
        row += rows
    vals_ref[:, HD:] = jnp.ones((row, HD), BF16)
    factor = HD ** (-0.5) * 1.4426950408889634
    part = q_own.shape[2]
    heads = q_own.shape[-1] // HD
    n_chunks = max(1, row // KEY_CHUNK)
    cut = row // n_chunks
    tile = CORES * heads * part // 2

    def one(n, carry):
        block = lax.rem(z_ref[0] + n, n_z)
        at = pl.multiple_of(block * part, 16)
        cosine, sine = cos_ref[pl.ds(at, part)], sin_ref[pl.ds(at, part)]
        queries = []
        for field in (q_own[block, core_ref[0]], q_other[block]):
            for head in range(heads):
                vec = field[:, head * HD : (head + 1) * HD].astype(F32)
                queries.append(norm_turn(vec, gain_ref[...], cosine, sine).astype(BF16))
        query = jnp.concatenate(queries, axis=0)
        tiles = [query[:tile], query[tile:]]
        score = lambda side, c: lax.dot_general(
            tiles[side], keys_ref[c * cut : (c + 1) * cut],
            (((1,), (1,)), ((), ())), preferred_element_type=F32,
        )
        work = [(c, side) for c in range(n_chunks) for side in range(2)]
        top, total = [None] * 2, [None] * 2
        scores = score(0, 0)
        for step, (c, side) in enumerate(work):
            after = score(work[step + 1][1], work[step + 1][0]) if step + 1 < len(work) else None
            here = jnp.max(scores, axis=1, keepdims=True)
            if c:
                here = jnp.maximum(top[side], here)
                shrink = jnp.exp2((top[side] - here) * factor)
            weights = jnp.exp2((scores - here) * factor).astype(BF16)
            part_sum = jnp.dot(
                weights, vals_ref[c * cut : (c + 1) * cut], preferred_element_type=F32
            )
            total[side] = total[side] * shrink + part_sum if c else part_sum
            top[side] = here
            scores = after
        mixed = None
        for side, weight in enumerate((w_own, w_other)):
            merged = (total[side][:, :HD] / total[side][:, HD:]).astype(BF16)
            merged = jnp.concatenate(
                [merged[h * part : (h + 1) * part] for h in range(heads)], axis=1
            )
            out = jnp.dot(merged, weight[...], preferred_element_type=F32)
            mixed = out if mixed is None else mixed + out
        mixed_ref[n] = mixed.astype(BF16)
        return carry

    lax.fori_loop(0, n_z, one, 0)
    for n, out_ref in enumerate(outs):
        out_ref[...] = mixed_ref[n]


def mix(core, z_index, queries, q_other, gain, cosine, sine, w_own, w_other, pieces, n_z):
    rows, width = cosine.shape[0], queries.shape[-1]
    part = rows // n_z
    d_model = w_own.shape[-1]
    length = sum(p.shape[1] for p in pieces)
    return pl.pallas_call(
        lambda *refs: mix_kernel(len(pieces), n_z, *refs),
        in_specs=[IN_SMEM] * 2 + [IN_VMEM] * (7 + len(pieces)),
        out_specs=[IN_VMEM] * n_z,
        out_shape=[jax.ShapeDtypeStruct((part, d_model), BF16)] * n_z,
        scratch_shapes=[
            pltpu.VMEM((length, HD), BF16),
            pltpu.VMEM((length, 2 * HD), BF16),
            pltpu.VMEM((n_z, part, d_model), BF16),
        ],
        compiler_params=pltpu.CompilerParams(vmem_limit_bytes=32 * MIB),
        name="mix",
    )(
        core, z_index, queries.reshape(n_z, CORES, part, width), q_other, gain, cosine, sine,
        w_own, w_other, *pieces,
    )


def dispatch_kernel(core_ref, tokens_ref, gain_ref, slots_ref, *out_refs):
    rows, d_model = slots_ref.shape[-1], tokens_ref.shape[-1]
    field = tokens_ref[...].reshape(rows, d_model).astype(F32)
    mean = jnp.mean(field * field, axis=-1, keepdims=True)
    normed = (field * lax.rsqrt(mean + EPS) * gain_ref[...]).astype(BF16)
    for chunk, out_ref in enumerate(out_refs):
        n_slots = out_ref.shape[0]
        slot = lax.broadcasted_iota(jnp.int32, (n_slots, rows), 0) + chunk * n_slots
        hot = slot == slots_ref[0:1]
        for k in range(1, TOPK):
            hot = hot | (slot == slots_ref[k : k + 1])
        out_ref[...] = jnp.dot(
            hot.astype(F32).astype(BF16), normed, preferred_element_type=F32
        ).astype(BF16)


def dispatch(core, tokens, gain, slots, n_z, pieces):
    local_rows, d_model = tokens.shape
    part = local_rows // (n_z * CORES)
    n_slots = EXPERTS * n_z * CAP // pieces
    return pl.pallas_call(
        dispatch_kernel,
        grid_spec=pltpu.PrefetchScalarGridSpec(
            num_scalar_prefetch=1,
            grid=(1,),
            in_specs=[
                pl.BlockSpec((n_z, 1, part, d_model), lambda i, c: (0, c[0], 0, 0)),
                pl.BlockSpec((1, d_model), lambda i, c: (0, 0)),
                pl.BlockSpec(slots.shape, lambda i, c: (0, 0)),
            ],
            out_specs=[IN_VMEM] * pieces,
        ),
        out_shape=[jax.ShapeDtypeStruct((n_slots, d_model), BF16)] * pieces,
        compiler_params=pltpu.CompilerParams(vmem_limit_bytes=16 * MIB),
        name="dispatch",
    )(core, *in_hbm([tokens.reshape(n_z, CORES, part, d_model)]), gain, slots)


def expert_kernel(n_src, group, *refs):
    ins, (gate_ref, up_ref, down_ref) = refs[: 2 * n_src], refs[2 * n_src : 2 * n_src + 3]
    outs, acc_ref = refs[2 * n_src + 3 : -1], refs[-1]
    expert, step = pl.program_id(0), pl.program_id(1)
    last = pl.num_programs(1) - 1
    rows = ins[0].shape[1]
    for first in range(0, len(ins), group):
        field = jnp.concatenate([ref[expert] for ref in ins[first : first + group]], axis=0)
        gate = jnp.dot(field, gate_ref[0], preferred_element_type=F32)
        up = jnp.dot(field, up_ref[0], preferred_element_type=F32)
        hidden = (gate / (1.0 + jnp.exp(-gate)) * up).astype(BF16)
        result = jnp.dot(hidden, down_ref[0], preferred_element_type=F32)
        here = slice(first * rows, (first + group) * rows)

        def finish(whole):
            for n, ref in enumerate(outs[first : first + group]):
                ref[expert] = whole[n * rows : (n + 1) * rows].astype(BF16)

        if acc_ref.shape[0] < len(ins) * rows:
            finish(result)
            continue

        @pl.when(step == 0)
        def _():
            acc_ref[here] = result

        @pl.when((step > 0) & (step < last))
        def _():
            acc_ref[here] += result

        @pl.when(step == last)
        def _():
            finish(acc_ref[here] + result)


def experts(own, other, gate_weight, up_weight, down_weight, first):
    pieces = [*own, *other]
    per, rows, d_model = pieces[0].shape
    width = gate_weight.shape[-1]
    cut = min(width, 256)
    steps = width // cut
    group = min(len(pieces), max(1, 256 // rows))
    outs = pl.pallas_call(
        lambda *refs: expert_kernel(len(own), group, *refs),
        grid=(per, steps),
        in_specs=[IN_VMEM] * len(pieces)
        + [
            pl.BlockSpec((1, d_model, cut), lambda e, s: (e + first, 0, s)),
            pl.BlockSpec((1, d_model, cut), lambda e, s: (e + first, 0, s)),
            pl.BlockSpec((1, cut, d_model), lambda e, s: (e + first, s, 0)),
        ],
        out_specs=[IN_VMEM] * len(pieces),
        out_shape=[jax.ShapeDtypeStruct((per, rows, d_model), BF16)] * len(pieces),
        scratch_shapes=[pltpu.VMEM((len(pieces) * rows if steps > 1 else 8, d_model), F32)],
        compiler_params=pltpu.CompilerParams(vmem_limit_bytes=32 * MIB),
        name="experts",
    )(*pieces, *in_hbm([gate_weight, up_weight, down_weight]))
    return outs[: len(own)], outs[len(own) :]


def combine_kernel(n_back, z_ref, slots_ref, shares_ref, *rest):
    back_refs, out_refs, total_ref = rest[:n_back], rest[n_back:-1], rest[-1]
    rows = slots_ref.shape[0]
    back = jnp.concatenate([ref[...] for ref in back_refs], axis=0)
    slot = lax.broadcasted_iota(jnp.int32, (rows, back.shape[0]), 1)
    matrix = jnp.zeros(slot.shape, F32)
    for k in range(TOPK):
        share = shares_ref[:, k : k + 1]
        matrix = matrix + jnp.where(slot == slots_ref[:, k : k + 1], share, 0.0)
    high = matrix.astype(BF16)
    low = (matrix - high.astype(F32)).astype(BF16)
    both = jnp.dot(jnp.concatenate([high, low], axis=0), back, preferred_element_type=F32)
    total_ref[...] = (both[:rows] + both[rows:]).reshape(total_ref.shape)
    n_z = len(out_refs)
    for n, out_ref in enumerate(out_refs):
        out_ref[...] = total_ref[lax.rem(z_ref[0] + n, n_z)].astype(BF16)


def combine(z_index, slots, shares, backs, n_z):
    rows, d_model = slots.shape[0], backs[0].shape[-1]
    return pl.pallas_call(
        lambda *refs: combine_kernel(len(backs), *refs),
        in_specs=[IN_SMEM] + [IN_VMEM] * (2 + len(backs)),
        out_specs=[IN_VMEM] * n_z,
        out_shape=[jax.ShapeDtypeStruct((rows // n_z, d_model), BF16)] * n_z,
        scratch_shapes=[pltpu.VMEM((n_z, rows // n_z, d_model), F32)],
        compiler_params=pltpu.CompilerParams(vmem_limit_bytes=24 * MIB),
        name="combine",
    )(z_index, slots, shares, *backs)


def shift(a, axis, step):
    n = lax.axis_size(axis)
    return lax.ppermute(a, axis, [(i, (i + step) % n) for i in range(n)])


def swap_cores(a):
    return lax.ppermute(a, "core", [(i, CORES - 1 - i) for i in range(CORES)])


def on_device(
    queries,
    keys,
    values,
    query_gain,
    key_gain,
    out_weight,
    tokens_b,
    norm_gain,
    routes,
    route_weight,
    gate_weight,
    up_weight,
    down_weight,
):
    n_ep, n_z = lax.axis_size("ep"), lax.axis_size("z")
    core, z_index = lax.axis_index("core"), lax.axis_index("z")
    core_arg = core.reshape(1).astype(jnp.int32)
    z_arg = z_index.reshape(1).astype(jnp.int32)
    n_rows, width = queries.shape
    d_model = tokens_b.shape[-1]
    heads = width // HD
    n_heads = heads * n_z * CORES

    part = n_rows // (n_z * CORES)
    offsets = (
        jnp.arange(n_z, dtype=jnp.int32)[:, None] * (CORES * part)
        + core * part
        + jnp.arange(part, dtype=jnp.int32)[None, :]
    ).reshape(-1)
    cosine, sine = rope_tables(lax.axis_index("ep") * n_rows + offsets)
    kv_head = ((z_index * CORES + core) * heads // (n_heads // KVH)).reshape(1).astype(jnp.int32)
    own_kv, q_send = prepare(
        core_arg, kv_head, keys, values, queries, key_gain[None], cosine, sine, n_z
    )
    pieces = [own_kv]
    for step in range(1, n_ep):
        pieces.append(shift(own_kv, "ep", step))
    pieces = pieces + [swap_cores(p) for p in pieces]

    q_other = swap_cores(q_send)
    w_other = swap_cores(out_weight)

    n_local = gate_weight.shape[0]
    chunks = 2 if n_local % 2 == 0 else 1
    per = n_local // chunks
    block_rows = tokens_b.shape[0] // (n_z * CORES)
    picks = block_rows * TOPK
    own_block = lambda a: lax.dynamic_index_in_dim(
        a.reshape(n_z, CORES, block_rows, TOPK), core, 1, keepdims=False
    )
    own_routes = own_block(routes)
    assigned = own_routes.reshape(n_z, picks)
    earlier = jnp.arange(picks)[:, None] > jnp.arange(picks)[None, :]
    same = (assigned[:, :, None] == assigned[:, None, :]) & earlier[None]
    rank = jnp.sum(same.astype(jnp.int32), axis=-1)
    block = jnp.arange(n_z, dtype=jnp.int32)[:, None]
    local = assigned % n_local
    ahead = lax.rem(assigned // n_local + n_ep - lax.axis_index("ep"), n_ep)
    place = ((local // per) * n_ep + ahead) * per + local % per
    slots = ((place * n_z + block) * CAP + rank).reshape(n_z * block_rows, TOPK)
    own_weight = own_block(route_weight).reshape(n_z * block_rows, TOPK)
    shares = own_weight / jnp.sum(own_weight, axis=-1, keepdims=True)
    slots, shares = lax.optimization_barrier((slots, shares))

    outgoing = dispatch(core_arg, tokens_b, norm_gain[None], slots.T, n_z, chunks * n_ep)
    arrived = []
    for chunk in range(chunks):
        here = []
        for step in range(n_ep):
            piece = outgoing[chunk * n_ep + step].reshape(per, n_z * CAP, d_model)
            here.append(shift(piece, "ep", step) if step else piece)
        arrived.append((here, [swap_cores(p) for p in here]))

    mixed = mix(
        core_arg, z_arg, queries, q_other, query_gain[None], cosine, sine, out_weight, w_other,
        pieces, n_z,
    )
    gathered = [mixed[0]]
    for step in range(1, n_z):
        gathered.append(shift(mixed[step], "z", step))
    mixed_out = add(*gathered)

    backs = []
    for chunk in range(chunks):
        keep, send = experts(
            *arrived[chunk], gate_weight, up_weight, down_weight, chunk * per
        )
        for step in range(n_ep):
            there = swap_cores(send[step])
            result = add(keep[step], there)
            result = shift(result, "ep", n_ep - step) if step else result
            backs.append(result.reshape(-1, d_model))
    rows = combine(z_arg, slots, shares, backs, n_z)
    gathered = [rows[0]]
    for step in range(1, n_z):
        gathered.append(shift(rows[step], "z", step))
    expert_out = add(*gathered)
    return (mixed_out, expert_out)


def solution(mesh):
    n_ep, n_tp = mesh.shape["ep"], mesh.shape["tp"]
    fine = Mesh(mesh.devices.reshape(n_ep, n_tp // CORES, CORES), ("ep", "z", "core"))
    tp = ("z", "core")
    placed = (
        P("ep", tp),
        P("ep", None),
        P("ep", None),
        P(),
        P(),
        P(tp, None),
        P("ep", None),
        P(),
        P("ep", None),
        P("ep", None),
        P("ep", None, tp),
        P("ep", None, tp),
        P("ep", tp, None),
    )

    return jax.shard_map(
        on_device,
        mesh=fine,
        in_specs=placed,
        out_specs=(P(("ep", "z", "core"), None), P(("ep", "z", "core"), None)),
        check_vma=False,
    )
```

time: 187 us -> 150 us (0.80)
  the two profiles are of different devices: /device:TPU:13 before, /device:TPU:0 now
where the time goes in v3:
time: 150 us; the launch traced here: 149 us
  waiting for transfers between devices  76.6 us (51%)
  starting transfers between devices  33.5 us (22%)
  Pallas kernels  32.3 us (22%)
  local copies, waits for them, and re-layouts  3.78 us (3%)
  other arithmetic  1.51 us (1%)
    ppermute x21, waiting for transfers between devices, shift(): return lax.ppermute(a, axis, [(i, (i + step) % n) for i in range(n)])  75.6 us
    ppermute x21, starting transfers between devices, shift(): return lax.ppermute(a, axis, [(i, (i + step) % n) for i in range(n)])  29.4 us
    pallas_call x2, Pallas kernels, experts(): pl.pallas_call(lambda *refs: expert_kernel(len(own), group, *refs), grid=...  15.3 us
    pallas_call x1, Pallas kernels, mix(): pl.pallas_call(lambda *refs: mix_kernel(len(pieces), n_z, *refs), in_spec...  9.58 us
    ppermute x22, starting transfers between devices, swap_cores(): return lax.ppermute(a, 'core', [(i, CORES - 1 - i) for i in range(CORES)])  4.17 us
  transfers between devices with their start and end apart: 43, of which 14 were waited for; matrix products, arithmetic and copies ran while one was open for 1% of the time, Pallas kernels for 19%

profile of v3, /device:TPU:0, one launch (start us, length us, event | category | flops | bytes accessed | tf_op | source)
XLA Modules:
  0.0 148.7 jit_solution(18335467064403437136)
XLA Ops:
  0.7 0.8 reshape.215
  2.2 0.8 reshape.217
  3.7 0.7 copy-done.2
  4.4 2.6 %dispatch.1 = (bf16[64,2048]{1,0:T(8,128)(2,1)S(1)}, bf16[64,2048]{1,0:T(8,128)(2,1)S(1)}, bf16[64,2048]{1,0:T(8,128)(2,1)S(1)}, bf16[64,2048]{1,0:T(8,128)(2,1)...) custom-call(s32[1]{0:T(128)} %bitcast.core_ref.refs_0_, ...), custom_call_target="tpu_custom_call" | custom-call | tf_op jit(solution)/shard_map/dispatch/pallas_call | solution.py:222
  7.0 3.0 %collective-permute-start.26 = (bf16[2,32,2048]{2,1,0:T(8,128)(2,1)S(1)}, bf16[2,32,2048]{2,1,0:T(8,128)(2,1)S(1)}, u32[]{:S(2)}, u32[]{:S(2)}) collective-permute-start(bf16[2,32,2048]{2,1,0:T(8,128)(2,1)S(1)} %bitcast.73), channel_id=1, source_target_pairs={{0,8},{8,16},{16,24},{24,0},{1,9},{9,17},{17,25},{25,1},{2,10},{10... | collective-permute-start | bytes 786440 | tf_op jit(solution)/shard_map/ppermute | solution.py:333
  10.3 0.8 sine_multiply_fusion
  11.1 0.6 copy-done.3
  11.7 1.3 prepare.1
  13.0 1.5 %collective-permute-start.2 = (bf16[2,384,128]{2,1,0:T(8,128)(2,1)S(1)}, bf16[2,384,128]{2,1,0:T(8,128)(2,1)S(1)}, u32[]{:S(2)}, u32[]{:S(2)}) collective-permute-start(bf16[2,384,128]{2,1,0:T(8,128)(2,1)S(1)} %get-tuple-element.39.refs_9_), channel_id=1, source_target_pairs={{0,8},{8,16},{16,24},{24,0},{1,9},{9,17},{17,25},{25,1},{2,10},{10... | collective-permute-start | bytes 589832 | tf_op jit(solution)/shard_map/ppermute | solution.py:333
  14.7 2.8 %collective-permute-start.28 = (bf16[2,32,2048]{2,1,0:T(8,128)(2,1)S(1)}, bf16[2,32,2048]{2,1,0:T(8,128)(2,1)S(1)}, u32[]{:S(2)}, u32[]{:S(2)}) collective-permute-start(bf16[2,32,2048]{2,1,0:T(8,128)(2,1)S(1)} %bitcast.71), channel_id=1, source_target_pairs={{0,24},{8,0},{16,8},{24,16},{1,25},{9,1},{17,9},{25,17},{2,26},{10... | collective-permute-start | bytes 786440 | tf_op jit(solution)/shard_map/ppermute | solution.py:333
  17.5 4.9 %collective-permute-done.2.refs_10_ = bf16[2,384,128]{2,1,0:T(8,128)(2,1)S(1)} collective-permute-done((bf16[2,384,128]{2,1,0:T(8,128)(2,1)S(1)}, bf16[2,384,128]{2,1,0:T(8,128)(2,1)S(1)}, u32[]{:S(2)}, u32[]{:S(2)}) %collective-permute-start.2) | collective-permute-done | bytes 196640 | tf_op jit(solution)/shard_map/ppermute | solution.py:333
  22.4 1.0 collective-permute-start.12
  23.4 1.5 %collective-permute-start.13 = (bf16[2,32,2048]{2,1,0:T(8,128)(2,1)S(1)}, bf16[2,32,2048]{2,1,0:T(8,128)(2,1)S(1)}, u32[]{:S(2)}, u32[]{:S(2)}) collective-permute-start(bf16[2,32,2048]{2,1,0:T(8,128)(2,1)S(1)} %bitcast.69), channel_id=1, source_target_pairs={{0,16},{8,24},{16,0},{24,8},{1,17},{9,25},{17,1},{25,9},{2,18},{10... | collective-permute-start | bytes 786440 | tf_op jit(solution)/shard_map/ppermute | solution.py:333
  24.9 3.1 %collective-permute-done.27.refs_2_ = bf16[2,32,2048]{2,1,0:T(8,128)(2,1)S(1)} collective-permute-done((bf16[2,32,2048]{2,1,0:T(8,128)(2,1)S(1)}, bf16[2,32,2048]{2,1,0:T(8,128)(2,1)S(1)}, u32[]{:S(2)}, u32[]{:S(2)}) %collective-permute-start.27) | collective-permute-done | bytes 262176 | tf_op jit(solution)/shard_map/ppermute | solution.py:333
  28.1 0.5 collective-permute-start.14
  28.6 0.5 collective-permute-start.31
  29.1 4.6 %collective-permute-done.12.refs_1_ = bf16[2,32,2048]{2,1,0:T(8,128)(2,1)S(1)} collective-permute-done((bf16[2,32,2048]{2,1,0:T(8,128)(2,1)S(1)}, bf16[2,32,2048]{2,1,0:T(8,128)(2,1)S(1)}, u32[]{:S(2)}, u32[]{:S(2)}) %collective-permute-start.12) | collective-permute-done | bytes 262176 | tf_op jit(solution)/shard_map/ppermute | solution.py:333
  33.7 4.7 %collective-permute-done.13.refs_2_ = bf16[2,32,2048]{2,1,0:T(8,128)(2,1)S(1)} collective-permute-done((bf16[2,32,2048]{2,1,0:T(8,128)(2,1)S(1)}, bf16[2,32,2048]{2,1,0:T(8,128)(2,1)S(1)}, u32[]{:S(2)}, u32[]{:S(2)}) %collective-permute-start.13) | collective-permute-done | bytes 262176 | tf_op jit(solution)/shard_map/ppermute | solution.py:333
  38.9 0.3 collective-permute-start.17
  39.2 1.5 collective-permute-start.3
  40.8 7.7 %experts.3 = (bf16[2,32,2048]{2,1,0:T(8,128)(2,1)S(1)}, bf16[2,32,2048]{2,1,0:T(8,128)(2,1)S(1)}, bf16[2,32,2048]{2,1,0:T(8,128)(2,1)S(1)}, bf16[2,32,2048]{2,1,...) custom-call(bf16[2,32,2048]{2,1,0:T(8,128)(2,1)S(1)} %bitcast.64, ...), custom_call_target="tpu_custom_call" | custom-call | tf_op jit(solution)/shard_map/experts/pallas_call | solution.py:282
  48.5 0.4 collective-permute-start.38
  49.1 1.8 %collective-permute-start.4 = (bf16[2,384,128]{2,1,0:T(8,128)(2,1)S(1)}, bf16[2,384,128]{2,1,0:T(8,128)(2,1)S(1)}, u32[]{:S(2)}, u32[]{:S(2)}) collective-permute-start(bf16[2,384,128]{2,1,0:T(8,128)(2,1)S(1)} %get-tuple-element.39.refs_9_), channel_id=1, source_target_pairs={{0,24},{8,0},{16,8},{24,16},{1,25},{9,1},{17,9},{25,17},{2,26},{10... | collective-permute-start | bytes 589832 | tf_op jit(solution)/shard_map/ppermute | solution.py:333
  51.0 0.4 collective-permute-start.1
  51.4 7.7 %experts.2 = (bf16[2,32,2048]{2,1,0:T(8,128)(2,1)S(1)}, bf16[2,32,2048]{2,1,0:T(8,128)(2,1)S(1)}, bf16[2,32,2048]{2,1,0:T(8,128)(2,1)S(1)}, bf16[2,32,2048]{2,1,...) custom-call(bf16[2,32,2048]{2,1,0:T(8,128)(2,1)S(1)} %bitcast.62, ...), custom_call_target="tpu_custom_call" | custom-call | tf_op jit(solution)/shard_map/experts/pallas_call | solution.py:282
  59.3 0.4 collective-permute-start.24
  59.8 0.4 collective-permute-start.20
  60.4 0.4 collective-permute-done.34.refs_1_
  61.9 0.5 collective-permute-start.37
  62.7 2.6 %collective-permute-start.35 = (bf16[2,32,2048]{2,1,0:T(8,128)(2,1)S(1)}, bf16[2,32,2048]{2,1,0:T(8,128)(2,1)S(1)}, u32[]{:S(2)}, u32[]{:S(2)}) collective-permute-start(bf16[2,32,2048]{2,1,0:T(8,128)(2,1)S(1)} %add.245), channel_id=1, source_target_pairs={{0,24},{8,0},{16,8},{24,16},{1,25},{9,1},{17,9},{25,17},{2,26},{10... | collective-permute-start | bytes 786440 | tf_op jit(solution)/shard_map/ppermute | solution.py:333
  65.4 6.2 %collective-permute-done.39 = bf16[2,32,2048]{2,1,0:T(8,128)(2,1)S(1)} collective-permute-done((bf16[2,32,2048]{2,1,0:T(8,128)(2,1)S(1)}, bf16[2,32,2048]{2,1,0:T(8,128)(2,1)S(1)}, u32[]{:S(2)}, u32[]{:S(2)}) %collective-permute-start.39) | collective-permute-done | bytes 262176 | tf_op jit(solution)/shard_map/ppermute | solution.py:333
  71.6 0.5 collective-permute-start.23
  72.1 5.2 %collective-permute-done.37 = bf16[2,32,2048]{2,1,0:T(8,128)(2,1)S(1)} collective-permute-done((bf16[2,32,2048]{2,1,0:T(8,128)(2,1)S(1)}, bf16[2,32,2048]{2,1,0:T(8,128)(2,1)S(1)}, u32[]{:S(2)}, u32[]{:S(2)}) %collective-permute-start.37) | collective-permute-done | bytes 262176 | tf_op jit(solution)/shard_map/ppermute | solution.py:333
  77.3 1.9 %collective-permute-start.21 = (bf16[2,32,2048]{2,1,0:T(8,128)(2,1)S(1)}, bf16[2,32,2048]{2,1,0:T(8,128)(2,1)S(1)}, u32[]{:S(2)}, u32[]{:S(2)}) collective-permute-start(bf16[2,32,2048]{2,1,0:T(8,128)(2,1)S(1)} %add.241), channel_id=1, source_target_pairs={{0,24},{8,0},{16,8},{24,16},{1,25},{9,1},{17,9},{25,17},{2,26},{10... | collective-permute-start | bytes 786440 | tf_op jit(solution)/shard_map/ppermute | solution.py:333
  79.2 3.7 %collective-permute-done.25 = bf16[2,32,2048]{2,1,0:T(8,128)(2,1)S(1)} collective-permute-done((bf16[2,32,2048]{2,1,0:T(8,128)(2,1)S(1)}, bf16[2,32,2048]{2,1,0:T(8,128)(2,1)S(1)}, u32[]{:S(2)}, u32[]{:S(2)}) %collective-permute-start.25) | collective-permute-done | bytes 262176 | tf_op jit(solution)/shard_map/ppermute | solution.py:333
  82.9 4.2 %collective-permute-done.23 = bf16[2,32,2048]{2,1,0:T(8,128)(2,1)S(1)} collective-permute-done((bf16[2,32,2048]{2,1,0:T(8,128)(2,1)S(1)}, bf16[2,32,2048]{2,1,0:T(8,128)(2,1)S(1)}, u32[]{:S(2)}, u32[]{:S(2)}) %collective-permute-start.23) | collective-permute-done | bytes 262176 | tf_op jit(solution)/shard_map/ppermute | solution.py:333
  87.1 0.5 collective-permute-start.8
  87.7 1.2 combine.1
  89.0 1.8 %collective-permute-start.40 = (bf16[48,2048]{1,0:T(8,128)(2,1)S(1)}, bf16[48,2048]{1,0:T(8,128)(2,1)S(1)}, u32[]{:S(2)}, u32[]{:S(2)}) collective-permute-start(bf16[48,2048]{1,0:T(8,128)(2,1)S(1)} %get-tuple-element.71), channel_id=1, source_target_pairs={{0,2},{2,4},{4,6},{6,0},{1,3},{3,5},{5,7},{7,1},{8,10},{10,12},{12... | collective-permute-start | bytes 589832 | tf_op jit(solution)/shard_map/ppermute | solution.py:333
  90.8 9.6 %mix.1 = (bf16[96,2048]{1,0:T(8,128)(2,1)S(1)}, bf16[96,2048]{1,0:T(8,128)(2,1)S(1)}, bf16[96,2048]{1,0:T(8,128)(2,1)S(1)}, bf16[96,2048]{1,0:T(8,128)(2,1)S(1)}) custom-call(s32[1]{0:T(128)} %bitcast.core_ref.refs_0_, s32[1]{0:T(128)} %bitcast.1.refs_1_.refs_0_, bf16[4,2,96,256]{3,2,1,0:T(8,128)(2,1)S(1)} %bitcast.51, ...), custom_call_target="tpu_custom_call" | custom-call | tf_op jit(solution)/shard_map/mix/pallas_call | solution.py:184
  100.4 2.7 %collective-permute-start.10 = (bf16[96,2048]{1,0:T(8,128)(2,1)S(1)}, bf16[96,2048]{1,0:T(8,128)(2,1)S(1)}, u32[]{:S(2)}, u32[]{:S(2)}) collective-permute-start(bf16[96,2048]{1,0:T(8,128)(2,1)S(1)} %get-tuple-element.42), channel_id=1, source_target_pairs={{0,4},{2,6},{4,0},{6,2},{1,5},{3,7},{5,1},{7,3},{8,12},{10,14},{12... | collective-permute-start | bytes 1179656 | tf_op jit(solution)/shard_map/ppermute | solution.py:333
  103.1 1.3 collective-permute-start.11
  104.4 0.7 collective-permute-start.9
  105.1 0.3 collective-permute-start.41
  105.4 2.8 %collective-permute-start.42 = (bf16[48,2048]{1,0:T(8,128)(2,1)S(1)}, bf16[48,2048]{1,0:T(8,128)(2,1)S(1)}, u32[]{:S(2)}, u32[]{:S(2)}) collective-permute-start(bf16[48,2048]{1,0:T(8,128)(2,1)S(1)} %get-tuple-element.73), channel_id=1, source_target_pairs={{0,6},{2,0},{4,2},{6,4},{1,7},{3,1},{5,3},{7,5},{8,14},{10,8},{12,... | collective-permute-start | bytes 589832 | tf_op jit(solution)/shard_map/ppermute | solution.py:333
  108.2 38.7 %collective-permute-done.41.refs_2_ = bf16[48,2048]{1,0:T(8,128)(2,1)S(1)} collective-permute-done((bf16[48,2048]{1,0:T(8,128)(2,1)S(1)}, bf16[48,2048]{1,0:T(8,128)(2,1)S(1)}, u32[]{:S(2)}, u32[]{:S(2)}) %collective-permute-start.41) | collective-permute-done | bytes 196640 | tf_op jit(solution)/shard_map/ppermute | solution.py:333
  147.0 0.8 add.248
  147.8 0.9 add.239
  (88 shorter events, 4.7 us)
Async XLA Ops:
  3.6 0.7 copy-start.2
  7.0 16.4 %collective-permute-start.26 = (bf16[2,32,2048]{2,1,0:T(8,128)(2,1)S(1)}, bf16[2,32,2048]{2,1,0:T(8,128)(2,1)S(1)}, u32[]{:S(2)}, u32[]{:S(2)}) collective-permute-start(bf16[2,32,2048]{2,1,0:T(8,128)(2,1)S(1)} %bitcast.73), channel_id=1, source_target_pairs={{0,8},{8,16},{16,24},{24,0},{1,9},{9,17},{17,25},{25,1},{2,10},{10... | collective-permute-start | bytes 786440 | tf_op jit(solution)/shard_map/ppermute | solution.py:333
  11.0 0.7 copy-start.3
  13.0 9.4 %collective-permute-start.2 = (bf16[2,384,128]{2,1,0:T(8,128)(2,1)S(1)}, bf16[2,384,128]{2,1,0:T(8,128)(2,1)S(1)}, u32[]{:S(2)}, u32[]{:S(2)}) collective-permute-start(bf16[2,384,128]{2,1,0:T(8,128)(2,1)S(1)} %get-tuple-element.39.refs_9_), channel_id=1, source_target_pairs={{0,8},{8,16},{16,24},{24,0},{1,9},{9,17},{17,25},{25,1},{2,10},{10... | collective-permute-start | bytes 589832 | tf_op jit(solution)/shard_map/ppermute | solution.py:333
  14.6 13.5 %collective-permute-start.27 = (bf16[2,32,2048]{2,1,0:T(8,128)(2,1)S(1)}, bf16[2,32,2048]{2,1,0:T(8,128)(2,1)S(1)}, u32[]{:S(2)}, u32[]{:S(2)}) collective-permute-start(bf16[2,32,2048]{2,1,0:T(8,128)(2,1)S(1)} %bitcast.72), channel_id=1, source_target_pairs={{0,16},{8,24},{16,0},{24,8},{1,17},{9,25},{17,1},{25,9},{2,18},{10... | collective-permute-start | bytes 786440 | tf_op jit(solution)/shard_map/ppermute | solution.py:333
  14.7 13.9 %collective-permute-start.28 = (bf16[2,32,2048]{2,1,0:T(8,128)(2,1)S(1)}, bf16[2,32,2048]{2,1,0:T(8,128)(2,1)S(1)}, u32[]{:S(2)}, u32[]{:S(2)}) collective-permute-start(bf16[2,32,2048]{2,1,0:T(8,128)(2,1)S(1)} %bitcast.71), channel_id=1, source_target_pairs={{0,24},{8,0},{16,8},{24,16},{1,25},{9,1},{17,9},{25,17},{2,26},{10... | collective-permute-start | bytes 786440 | tf_op jit(solution)/shard_map/ppermute | solution.py:333
  17.5 11.1 %collective-permute-start.29 = (bf16[2,32,2048]{2,1,0:T(8,128)(2,1)S(1)}, bf16[2,32,2048]{2,1,0:T(8,128)(2,1)S(1)}, u32[]{:S(2)}, u32[]{:S(2)}) collective-permute-start(bf16[2,32,2048]{2,1,0:T(8,128)(2,1)S(1)} %bitcast.63), channel_id=1, source_target_pairs={{0,1},{1,0},{2,3},{3,2},{4,5},{5,4},{6,7},{7,6},{8,9},{9,8},{10,11... | collective-permute-start | bytes 786440 | tf_op jit(solution)/shard_map/ppermute | solution.py:337
  22.4 11.3 %collective-permute-start.12 = (bf16[2,32,2048]{2,1,0:T(8,128)(2,1)S(1)}, bf16[2,32,2048]{2,1,0:T(8,128)(2,1)S(1)}, u32[]{:S(2)}, u32[]{:S(2)}) collective-permute-start(bf16[2,32,2048]{2,1,0:T(8,128)(2,1)S(1)} %bitcast.70), channel_id=1, source_target_pairs={{0,8},{8,16},{16,24},{24,0},{1,9},{9,17},{17,25},{25,1},{2,10},{10... | collective-permute-start | bytes 786440 | tf_op jit(solution)/shard_map/ppermute | solution.py:333
  23.4 14.9 %collective-permute-start.13 = (bf16[2,32,2048]{2,1,0:T(8,128)(2,1)S(1)}, bf16[2,32,2048]{2,1,0:T(8,128)(2,1)S(1)}, u32[]{:S(2)}, u32[]{:S(2)}) collective-permute-start(bf16[2,32,2048]{2,1,0:T(8,128)(2,1)S(1)} %bitcast.69), channel_id=1, source_target_pairs={{0,16},{8,24},{16,0},{24,8},{1,17},{9,25},{17,1},{25,9},{2,18},{10... | collective-permute-start | bytes 786440 | tf_op jit(solution)/shard_map/ppermute | solution.py:333
  28.1 10.6 %collective-permute-start.14 = (bf16[2,32,2048]{2,1,0:T(8,128)(2,1)S(1)}, bf16[2,32,2048]{2,1,0:T(8,128)(2,1)S(1)}, u32[]{:S(2)}, u32[]{:S(2)}) collective-permute-start(bf16[2,32,2048]{2,1,0:T(8,128)(2,1)S(1)} %bitcast.68), channel_id=1, source_target_pairs={{0,24},{8,0},{16,8},{24,16},{1,25},{9,1},{17,9},{25,17},{2,26},{10... | collective-permute-start | bytes 786440 | tf_op jit(solution)/shard_map/ppermute | solution.py:333
  28.6 10.3 %collective-permute-start.30 = (bf16[2,32,2048]{2,1,0:T(8,128)(2,1)S(1)}, bf16[2,32,2048]{2,1,0:T(8,128)(2,1)S(1)}, u32[]{:S(2)}, u32[]{:S(2)}) collective-permute-start(bf16[2,32,2048]{2,1,0:T(8,128)(2,1)S(1)} %collective-permute-done.26.refs_1_), channel_id=1, source_target_pairs={{0,1},{1,0},{2,3},{3,2},{4,5},{5,4},{6,7},{7,6},{8,9},{9,8},{10,11... | collective-permute-start | bytes 786440 | tf_op jit(solution)/shard_map/ppermute | solution.py:337
  28.6 10.6 %collective-permute-start.31 = (bf16[2,32,2048]{2,1,0:T(8,128)(2,1)S(1)}, bf16[2,32,2048]{2,1,0:T(8,128)(2,1)S(1)}, u32[]{:S(2)}, u32[]{:S(2)}) collective-permute-start(bf16[2,32,2048]{2,1,0:T(8,128)(2,1)S(1)} %collective-permute-done.27.refs_2_), channel_id=1, source_target_pairs={{0,1},{1,0},{2,3},{3,2},{4,5},{5,4},{6,7},{7,6},{8,9},{9,8},{10,11... | collective-permute-start | bytes 786440 | tf_op jit(solution)/shard_map/ppermute | solution.py:337
  33.7 7.0 %collective-permute-start.32 = (bf16[2,32,2048]{2,1,0:T(8,128)(2,1)S(1)}, bf16[2,32,2048]{2,1,0:T(8,128)(2,1)S(1)}, u32[]{:S(2)}, u32[]{:S(2)}) collective-permute-start(bf16[2,32,2048]{2,1,0:T(8,128)(2,1)S(1)} %collective-permute-done.28.refs_3_), channel_id=1, source_target_pairs={{0,1},{1,0},{2,3},{3,2},{4,5},{5,4},{6,7},{7,6},{8,9},{9,8},{10,11... | collective-permute-start | bytes 786440 | tf_op jit(solution)/shard_map/ppermute | solution.py:337
  38.4 12.6 %copy-start.1 = (bf16[256,2048]{1,0:T(8,128)(2,1)S(1)}, bf16[256,2048]{1,0:T(8,128)(2,1)}, u32[]{:S(2)}) copy-start(bf16[256,2048]{1,0:T(8,128)(2,1)} %refs_7_.1) | copy-start | bytes 3145732
  38.4 10.6 %collective-permute-start.15 = (bf16[2,32,2048]{2,1,0:T(8,128)(2,1)S(1)}, bf16[2,32,2048]{2,1,0:T(8,128)(2,1)S(1)}, u32[]{:S(2)}, u32[]{:S(2)}) collective-permute-start(bf16[2,32,2048]{2,1,0:T(8,128)(2,1)S(1)} %bitcast.61), channel_id=1, source_target_pairs={{0,1},{1,0},{2,3},{3,2},{4,5},{5,4},{6,7},{7,6},{8,9},{9,8},{10,11... | collective-permute-start | bytes 786440 | tf_op jit(solution)/shard_map/ppermute | solution.py:337
  38.7 10.4 %collective-permute-start.16 = (bf16[2,32,2048]{2,1,0:T(8,128)(2,1)S(1)}, bf16[2,32,2048]{2,1,0:T(8,128)(2,1)S(1)}, u32[]{:S(2)}, u32[]{:S(2)}) collective-permute-start(bf16[2,32,2048]{2,1,0:T(8,128)(2,1)S(1)} %collective-permute-done.12.refs_1_), channel_id=1, source_target_pairs={{0,1},{1,0},{2,3},{3,2},{4,5},{5,4},{6,7},{7,6},{8,9},{9,8},{10,11... | collective-permute-start | bytes 786440 | tf_op jit(solution)/shard_map/ppermute | solution.py:337
  38.9 12.0 %collective-permute-start.17 = (bf16[2,32,2048]{2,1,0:T(8,128)(2,1)S(1)}, bf16[2,32,2048]{2,1,0:T(8,128)(2,1)S(1)}, u32[]{:S(2)}, u32[]{:S(2)}) collective-permute-start(bf16[2,32,2048]{2,1,0:T(8,128)(2,1)S(1)} %collective-permute-done.13.refs_2_), channel_id=1, source_target_pairs={{0,1},{1,0},{2,3},{3,2},{4,5},{5,4},{6,7},{7,6},{8,9},{9,8},{10,11... | collective-permute-start | bytes 786440 | tf_op jit(solution)/shard_map/ppermute | solution.py:337
  39.2 9.3 %collective-permute-start.3 = (bf16[2,384,128]{2,1,0:T(8,128)(2,1)S(1)}, bf16[2,384,128]{2,1,0:T(8,128)(2,1)S(1)}, u32[]{:S(2)}, u32[]{:S(2)}) collective-permute-start(bf16[2,384,128]{2,1,0:T(8,128)(2,1)S(1)} %get-tuple-element.39.refs_9_), channel_id=1, source_target_pairs={{0,16},{8,24},{16,0},{24,8},{1,17},{9,25},{17,1},{25,9},{2,18},{10... | collective-permute-start | bytes 589832 | tf_op jit(solution)/shard_map/ppermute | solution.py:333
  40.7 10.3 %collective-permute-start.18 = (bf16[2,32,2048]{2,1,0:T(8,128)(2,1)S(1)}, bf16[2,32,2048]{2,1,0:T(8,128)(2,1)S(1)}, u32[]{:S(2)}, u32[]{:S(2)}) collective-permute-start(bf16[2,32,2048]{2,1,0:T(8,128)(2,1)S(1)} %collective-permute-done.14.refs_3_), channel_id=1, source_target_pairs={{0,1},{1,0},{2,3},{3,2},{4,5},{5,4},{6,7},{7,6},{8,9},{9,8},{10,11... | collective-permute-start | bytes 786440 | tf_op jit(solution)/shard_map/ppermute | solution.py:337
  48.5 11.2 %collective-permute-start.38 = (bf16[2,32,2048]{2,1,0:T(8,128)(2,1)S(1)}, bf16[2,32,2048]{2,1,0:T(8,128)(2,1)S(1)}, u32[]{:S(2)}, u32[]{:S(2)}) collective-permute-start(bf16[2,32,2048]{2,1,0:T(8,128)(2,1)S(1)} %get-tuple-element.69), channel_id=1, source_target_pairs={{0,1},{1,0},{2,3},{3,2},{4,5},{5,4},{6,7},{7,6},{8,9},{9,8},{10,11... | collective-permute-start | bytes 786440 | tf_op jit(solution)/shard_map/ppermute | solution.py:337
  48.9 10.9 %collective-permute-start.36 = (bf16[2,32,2048]{2,1,0:T(8,128)(2,1)S(1)}, bf16[2,32,2048]{2,1,0:T(8,128)(2,1)S(1)}, u32[]{:S(2)}, u32[]{:S(2)}) collective-permute-start(bf16[2,32,2048]{2,1,0:T(8,128)(2,1)S(1)} %get-tuple-element.67), channel_id=1, source_target_pairs={{0,1},{1,0},{2,3},{3,2},{4,5},{5,4},{6,7},{7,6},{8,9},{9,8},{10,11... | collective-permute-start | bytes 786440 | tf_op jit(solution)/shard_map/ppermute | solution.py:337
  49.1 10.0 %collective-permute-start.4 = (bf16[2,384,128]{2,1,0:T(8,128)(2,1)S(1)}, bf16[2,384,128]{2,1,0:T(8,128)(2,1)S(1)}, u32[]{:S(2)}, u32[]{:S(2)}) collective-permute-start(bf16[2,384,128]{2,1,0:T(8,128)(2,1)S(1)} %get-tuple-element.39.refs_9_), channel_id=1, source_target_pairs={{0,24},{8,0},{16,8},{24,16},{1,25},{9,1},{17,9},{25,17},{2,26},{10... | collective-permute-start | bytes 589832 | tf_op jit(solution)/shard_map/ppermute | solution.py:333
  50.9 8.4 %collective-permute-start = (bf16[4,96,256]{2,1,0:T(8,128)(2,1)S(1)}, bf16[4,96,256]{2,1,0:T(8,128)(2,1)S(1)}, u32[]{:S(2)}, u32[]{:S(2)}) collective-permute-start(bf16[4,96,256]{2,1,0:T(8,128)(2,1)S(1)} %get-tuple-element.38), channel_id=1, source_target_pairs={{0,1},{1,0},{2,3},{3,2},{4,5},{5,4},{6,7},{7,6},{8,9},{9,8},{10,11... | collective-permute-start | bytes 589832 | tf_op jit(solution)/shard_map/ppermute | solution.py:337
  51.0 39.8 %collective-permute-start.1 = (bf16[256,2048]{1,0:T(8,128)(2,1)S(1)}, bf16[256,2048]{1,0:T(8,128)(2,1)S(1)}, u32[]{:S(2)}, u32[]{:S(2)}) collective-permute-start(bf16[256,2048]{1,0:T(8,128)(2,1)S(1)} %copy-done.1), channel_id=1, source_target_pairs={{0,1},{1,0},{2,3},{3,2},{4,5},{5,4},{6,7},{7,6},{8,9},{9,8},{10,11... | collective-permute-start | bytes 3145736 | tf_op jit(solution)/shard_map/ppermute | solution.py:337
  59.1 31.7 %copy-start = (bf16[768,256]{1,0:T(8,128)(2,1)S(1)}, bf16[768,256]{1,0:T(8,128)(2,1)}, u32[]{:S(2)}) copy-start(bf16[768,256]{1,0:T(8,128)(2,1)} %param.13) | copy-start | bytes 1179652
  59.1 31.7 %copy-start.4 = (f32[128]{0:T(128)S(1)}, f32[128]{0:T(128)}, u32[]{:S(2)}) copy-start(f32[128]{0:T(128)} %param.16) | copy-start | bytes 1540
  59.1 1.6 %collective-permute-start.34 = (bf16[2,32,2048]{2,1,0:T(8,128)(2,1)S(1)}, bf16[2,32,2048]{2,1,0:T(8,128)(2,1)S(1)}, u32[]{:S(2)}, u32[]{:S(2)}) collective-permute-start(bf16[2,32,2048]{2,1,0:T(8,128)(2,1)S(1)} %get-tuple-element.65), channel_id=1, source_target_pairs={{0,1},{1,0},{2,3},{3,2},{4,5},{5,4},{6,7},{7,6},{8,9},{9,8},{10,11... | collective-permute-start | bytes 786440 | tf_op jit(solution)/shard_map/ppermute | solution.py:337
  59.3 1.8 %collective-permute-start.24 = (bf16[2,32,2048]{2,1,0:T(8,128)(2,1)S(1)}, bf16[2,32,2048]{2,1,0:T(8,128)(2,1)S(1)}, u32[]{:S(2)}, u32[]{:S(2)}) collective-permute-start(bf16[2,32,2048]{2,1,0:T(8,128)(2,1)S(1)} %get-tuple-element.57), channel_id=1, source_target_pairs={{0,1},{1,0},{2,3},{3,2},{4,5},{5,4},{6,7},{7,6},{8,9},{9,8},{10,11... | collective-permute-start | bytes 786440 | tf_op jit(solution)/shard_map/ppermute | solution.py:337
  59.7 1.8 %collective-permute-start.22 = (bf16[2,32,2048]{2,1,0:T(8,128)(2,1)S(1)}, bf16[2,32,2048]{2,1,0:T(8,128)(2,1)S(1)}, u32[]{:S(2)}, u32[]{:S(2)}) collective-permute-start(bf16[2,32,2048]{2,1,0:T(8,128)(2,1)S(1)} %get-tuple-element.55), channel_id=1, source_target_pairs={{0,1},{1,0},{2,3},{3,2},{4,5},{5,4},{6,7},{7,6},{8,9},{9,8},{10,11... | collective-permute-start | bytes 786440 | tf_op jit(solution)/shard_map/ppermute | solution.py:337
  59.8 2.1 %collective-permute-start.20 = (bf16[2,32,2048]{2,1,0:T(8,128)(2,1)S(1)}, bf16[2,32,2048]{2,1,0:T(8,128)(2,1)S(1)}, u32[]{:S(2)}, u32[]{:S(2)}) collective-permute-start(bf16[2,32,2048]{2,1,0:T(8,128)(2,1)S(1)} %get-tuple-element.53), channel_id=1, source_target_pairs={{0,1},{1,0},{2,3},{3,2},{4,5},{5,4},{6,7},{7,6},{8,9},{9,8},{10,11... | collective-permute-start | bytes 786440 | tf_op jit(solution)/shard_map/ppermute | solution.py:337
  60.7 1.9 %collective-permute-start.33 = (bf16[2,32,2048]{2,1,0:T(8,128)(2,1)S(1)}, bf16[2,32,2048]{2,1,0:T(8,128)(2,1)S(1)}, u32[]{:S(2)}, u32[]{:S(2)}) collective-permute-start(bf16[2,32,2048]{2,1,0:T(8,128)(2,1)S(1)} %get-tuple-element.63), channel_id=1, source_target_pairs={{0,1},{1,0},{2,3},{3,2},{4,5},{5,4},{6,7},{7,6},{8,9},{9,8},{10,11... | collective-permute-start | bytes 786440 | tf_op jit(solution)/shard_map/ppermute | solution.py:337
  61.1 4.2 %collective-permute-start.19 = (bf16[2,32,2048]{2,1,0:T(8,128)(2,1)S(1)}, bf16[2,32,2048]{2,1,0:T(8,128)(2,1)S(1)}, u32[]{:S(2)}, u32[]{:S(2)}) collective-permute-start(bf16[2,32,2048]{2,1,0:T(8,128)(2,1)S(1)} %get-tuple-element.51), channel_id=1, source_target_pairs={{0,1},{1,0},{2,3},{3,2},{4,5},{5,4},{6,7},{7,6},{8,9},{9,8},{10,11... | collective-permute-start | bytes 786440 | tf_op jit(solution)/shard_map/ppermute | solution.py:337
  61.5 10.1 %collective-permute-start.39 = (bf16[2,32,2048]{2,1,0:T(8,128)(2,1)S(1)}, bf16[2,32,2048]{2,1,0:T(8,128)(2,1)S(1)}, u32[]{:S(2)}, u32[]{:S(2)}) collective-permute-start(bf16[2,32,2048]{2,1,0:T(8,128)(2,1)S(1)} %add.247), channel_id=1, source_target_pairs={{0,8},{8,16},{16,24},{24,0},{1,9},{9,17},{17,25},{25,1},{2,10},{10... | collective-permute-start | bytes 786440 | tf_op jit(solution)/shard_map/ppermute | solution.py:333
  61.9 15.4 %collective-permute-start.37 = (bf16[2,32,2048]{2,1,0:T(8,128)(2,1)S(1)}, bf16[2,32,2048]{2,1,0:T(8,128)(2,1)S(1)}, u32[]{:S(2)}, u32[]{:S(2)}) collective-permute-start(bf16[2,32,2048]{2,1,0:T(8,128)(2,1)S(1)} %add.246), channel_id=1, source_target_pairs={{0,16},{8,24},{16,0},{24,8},{1,17},{9,25},{17,1},{25,9},{2,18},{10... | collective-permute-start | bytes 786440 | tf_op jit(solution)/shard_map/ppermute | solution.py:333
  62.7 16.6 %collective-permute-start.35 = (bf16[2,32,2048]{2,1,0:T(8,128)(2,1)S(1)}, bf16[2,32,2048]{2,1,0:T(8,128)(2,1)S(1)}, u32[]{:S(2)}, u32[]{:S(2)}) collective-permute-start(bf16[2,32,2048]{2,1,0:T(8,128)(2,1)S(1)} %add.245), channel_id=1, source_target_pairs={{0,24},{8,0},{16,8},{24,16},{1,25},{9,1},{17,9},{25,17},{2,26},{10... | collective-permute-start | bytes 786440 | tf_op jit(solution)/shard_map/ppermute | solution.py:333
  65.3 17.6 %collective-permute-start.25 = (bf16[2,32,2048]{2,1,0:T(8,128)(2,1)S(1)}, bf16[2,32,2048]{2,1,0:T(8,128)(2,1)S(1)}, u32[]{:S(2)}, u32[]{:S(2)}) collective-permute-start(bf16[2,32,2048]{2,1,0:T(8,128)(2,1)S(1)} %add.243), channel_id=1, source_target_pairs={{0,8},{8,16},{16,24},{24,0},{1,9},{9,17},{17,25},{25,1},{2,10},{10... | collective-permute-start | bytes 786440 | tf_op jit(solution)/shard_map/ppermute | solution.py:333
  71.6 15.5 %collective-permute-start.23 = (bf16[2,32,2048]{2,1,0:T(8,128)(2,1)S(1)}, bf16[2,32,2048]{2,1,0:T(8,128)(2,1)S(1)}, u32[]{:S(2)}, u32[]{:S(2)}) collective-permute-start(bf16[2,32,2048]{2,1,0:T(8,128)(2,1)S(1)} %add.242), channel_id=1, source_target_pairs={{0,16},{8,24},{16,0},{24,8},{1,17},{9,25},{17,1},{25,9},{2,18},{10... | collective-permute-start | bytes 786440 | tf_op jit(solution)/shard_map/ppermute | solution.py:333
  77.3 9.8 %collective-permute-start.21 = (bf16[2,32,2048]{2,1,0:T(8,128)(2,1)S(1)}, bf16[2,32,2048]{2,1,0:T(8,128)(2,1)S(1)}, u32[]{:S(2)}, u32[]{:S(2)}) collective-permute-start(bf16[2,32,2048]{2,1,0:T(8,128)(2,1)S(1)} %add.241), channel_id=1, source_target_pairs={{0,24},{8,0},{16,8},{24,16},{1,25},{9,1},{17,9},{25,17},{2,26},{10... | collective-permute-start | bytes 786440 | tf_op jit(solution)/shard_map/ppermute | solution.py:333
  79.2 9.7 %collective-permute-start.5 = (bf16[2,384,128]{2,1,0:T(8,128)(2,1)S(1)}, bf16[2,384,128]{2,1,0:T(8,128)(2,1)S(1)}, u32[]{:S(2)}, u32[]{:S(2)}) collective-permute-start(bf16[2,384,128]{2,1,0:T(8,128)(2,1)S(1)} %get-tuple-element.39.refs_9_), channel_id=1, source_target_pairs={{0,1},{1,0},{2,3},{3,2},{4,5},{5,4},{6,7},{7,6},{8,9},{9,8},{10,11... | collective-permute-start | bytes 589832 | tf_op jit(solution)/shard_map/ppermute | solution.py:337
  82.9 7.9 %collective-permute-start.6 = (bf16[2,384,128]{2,1,0:T(8,128)(2,1)S(1)}, bf16[2,384,128]{2,1,0:T(8,128)(2,1)S(1)}, u32[]{:S(2)}, u32[]{:S(2)}) collective-permute-start(bf16[2,384,128]{2,1,0:T(8,128)(2,1)S(1)} %collective-permute-done.2.refs_10_), channel_id=1, source_target_pairs={{0,1},{1,0},{2,3},{3,2},{4,5},{5,4},{6,7},{7,6},{8,9},{9,8},{10,11... | collective-permute-start | bytes 589832 | tf_op jit(solution)/shard_map/ppermute | solution.py:337
  87.1 3.7 %collective-permute-start.7 = (bf16[2,384,128]{2,1,0:T(8,128)(2,1)S(1)}, bf16[2,384,128]{2,1,0:T(8,128)(2,1)S(1)}, u32[]{:S(2)}, u32[]{:S(2)}) collective-permute-start(bf16[2,384,128]{2,1,0:T(8,128)(2,1)S(1)} %collective-permute-done.3.refs_11_), channel_id=1, source_target_pairs={{0,1},{1,0},{2,3},{3,2},{4,5},{5,4},{6,7},{7,6},{8,9},{9,8},{10,11... | collective-permute-start | bytes 589832 | tf_op jit(solution)/shard_map/ppermute | solution.py:337
  87.1 3.7 %collective-permute-start.8 = (bf16[2,384,128]{2,1,0:T(8,128)(2,1)S(1)}, bf16[2,384,128]{2,1,0:T(8,128)(2,1)S(1)}, u32[]{:S(2)}, u32[]{:S(2)}) collective-permute-start(bf16[2,384,128]{2,1,0:T(8,128)(2,1)S(1)} %collective-permute-done.4.refs_12_), channel_id=1, source_target_pairs={{0,1},{1,0},{2,3},{3,2},{4,5},{5,4},{6,7},{7,6},{8,9},{9,8},{10,11... | collective-permute-start | bytes 589832 | tf_op jit(solution)/shard_map/ppermute | solution.py:337
  89.0 16.5 %collective-permute-start.40 = (bf16[48,2048]{1,0:T(8,128)(2,1)S(1)}, bf16[48,2048]{1,0:T(8,128)(2,1)S(1)}, u32[]{:S(2)}, u32[]{:S(2)}) collective-permute-start(bf16[48,2048]{1,0:T(8,128)(2,1)S(1)} %get-tuple-element.71), channel_id=1, source_target_pairs={{0,2},{2,4},{4,6},{6,0},{1,3},{3,5},{5,7},{7,1},{8,10},{10,12},{12... | collective-permute-start | bytes 589832 | tf_op jit(solution)/shard_map/ppermute | solution.py:333
  100.4 47.4 %collective-permute-start.10 = (bf16[96,2048]{1,0:T(8,128)(2,1)S(1)}, bf16[96,2048]{1,0:T(8,128)(2,1)S(1)}, u32[]{:S(2)}, u32[]{:S(2)}) collective-permute-start(bf16[96,2048]{1,0:T(8,128)(2,1)S(1)} %get-tuple-element.42), channel_id=1, source_target_pairs={{0,4},{2,6},{4,0},{6,2},{1,5},{3,7},{5,1},{7,3},{8,12},{10,14},{12... | collective-permute-start | bytes 1179656 | tf_op jit(solution)/shard_map/ppermute | solution.py:333
  103.1 44.7 %collective-permute-start.11 = (bf16[96,2048]{1,0:T(8,128)(2,1)S(1)}, bf16[96,2048]{1,0:T(8,128)(2,1)S(1)}, u32[]{:S(2)}, u32[]{:S(2)}) collective-permute-start(bf16[96,2048]{1,0:T(8,128)(2,1)S(1)} %get-tuple-element.43), channel_id=1, source_target_pairs={{0,6},{2,0},{4,2},{6,4},{1,7},{3,1},{5,3},{7,5},{8,14},{10,8},{12,... | collective-permute-start | bytes 1179656 | tf_op jit(solution)/shard_map/ppermute | solution.py:333
  104.4 43.4 %collective-permute-start.9 = (bf16[96,2048]{1,0:T(8,128)(2,1)S(1)}, bf16[96,2048]{1,0:T(8,128)(2,1)S(1)}, u32[]{:S(2)}, u32[]{:S(2)}) collective-permute-start(bf16[96,2048]{1,0:T(8,128)(2,1)S(1)} %get-tuple-element.41), channel_id=1, source_target_pairs={{0,2},{2,4},{4,6},{6,0},{1,3},{3,5},{5,7},{7,1},{8,10},{10,12},{12... | collective-permute-start | bytes 1179656 | tf_op jit(solution)/shard_map/ppermute | solution.py:333
  105.1 41.9 %collective-permute-start.41 = (bf16[48,2048]{1,0:T(8,128)(2,1)S(1)}, bf16[48,2048]{1,0:T(8,128)(2,1)S(1)}, u32[]{:S(2)}, u32[]{:S(2)}) collective-permute-start(bf16[48,2048]{1,0:T(8,128)(2,1)S(1)} %get-tuple-element.72), channel_id=1, source_target_pairs={{0,4},{2,6},{4,0},{6,2},{1,5},{3,7},{5,1},{7,3},{8,12},{10,14},{12... | collective-permute-start | bytes 589832 | tf_op jit(solution)/shard_map/ppermute | solution.py:333
  105.4 41.6 %collective-permute-start.42 = (bf16[48,2048]{1,0:T(8,128)(2,1)S(1)}, bf16[48,2048]{1,0:T(8,128)(2,1)S(1)}, u32[]{:S(2)}, u32[]{:S(2)}) collective-permute-start(bf16[48,2048]{1,0:T(8,128)(2,1)S(1)} %get-tuple-element.73), channel_id=1, source_target_pairs={{0,6},{2,0},{4,2},{6,4},{1,7},{3,1},{5,3},{7,5},{8,14},{10,8},{12,... | collective-permute-start | bytes 589832 | tf_op jit(solution)/shard_map/ppermute | solution.py:333

commit v4 on v3

v4 whole, which is shorter than its diff:
```python
import jax
import jax.numpy as jnp
from jax import lax
from jax.experimental import pallas as pl
from jax.experimental.pallas import tpu as pltpu
from jax.sharding import Mesh, PartitionSpec as P


HD = 128
KVH = 4
EXPERTS = 16
TOPK = 2
GRID_W = 64
CAP = 8
EPS = 1e-06
THETA = 10000.0
CORES = 2
IN_VMEM = pl.BlockSpec(memory_space=pltpu.VMEM)
IN_SMEM = pl.BlockSpec(memory_space=pltpu.SMEM)
KEY_CHUNK = 1024
MIB = 1024 * 1024

F32 = jnp.float32
BF16 = jnp.bfloat16


def in_hbm(arrays):
    return [pltpu.with_memory_space_constraint(a, pltpu.HBM) for a in arrays]


def rope_tables(positions):
    n_freq = HD // 4
    row_pos = (positions // GRID_W).astype(F32)[:, None]
    col_pos = (positions % GRID_W).astype(F32)[:, None]
    lane = jnp.arange(HD, dtype=jnp.int32)
    inverse = THETA ** (-(lane % n_freq).astype(F32) / n_freq)
    angle = jnp.where(lane < HD // 2, row_pos, col_pos) * inverse
    sign = jnp.where((lane // n_freq) % 2 == 0, -1.0, 1.0).astype(F32)
    return jnp.cos(angle), jnp.sin(angle) * sign


def norm_turn(field, gain, cosine, sine):
    quarter = HD // 4
    mean = jnp.mean(field * field, axis=-1, keepdims=True)
    field = field * lax.rsqrt(mean + EPS) * gain
    lane = lax.broadcasted_iota(jnp.int32, field.shape, 1)
    partner = jnp.where(
        (lane // quarter) % 2 == 0,
        pltpu.roll(field, HD - quarter, 1),
        pltpu.roll(field, quarter, 1),
    )
    return field * cosine + partner * sine


def prepare_kernel(
    core_ref, head_ref, keys_ref, values_ref, q_ref, own_ref, gain_ref, cos_ref, sin_ref,
    kv_ref, send_ref, keep_ref,
):
    rows = cos_ref.shape[0]
    field = keys_ref[...].reshape(rows, HD).astype(F32)
    kv_ref[0] = norm_turn(field, gain_ref[...], cos_ref[...], sin_ref[...]).astype(BF16)
    kv_ref[1] = values_ref[...].reshape(rows, HD)
    send_ref[...] = q_ref[...].reshape(send_ref.shape)
    keep_ref[...] = own_ref[...].reshape(keep_ref.shape)


def prepare(core, head, keys, values, queries, gain, cosine, sine, n_z):
    rows, width = cosine.shape[0], queries.shape[-1]
    part = rows // n_z
    view = lambda a: a.reshape(n_z, CORES, part, a.shape[-1])
    picked = pl.BlockSpec((n_z, 1, part, HD), lambda i, c, h: (0, c[0], 0, h[0]))
    whole = lambda shape: pl.BlockSpec(shape, lambda i, c, h: (0,) * len(shape))
    return pl.pallas_call(
        prepare_kernel,
        grid_spec=pltpu.PrefetchScalarGridSpec(
            num_scalar_prefetch=2,
            grid=(1,),
            in_specs=[
                picked,
                picked,
                pl.BlockSpec((n_z, 1, part, width), lambda i, c, h: (0, 1 - c[0], 0, 0)),
                pl.BlockSpec((n_z, 1, part, width), lambda i, c, h: (0, c[0], 0, 0)),
                whole((1, HD)),
                whole((rows, HD)),
                whole((rows, HD)),
            ],
            out_specs=[IN_VMEM] * 3,
        ),
        out_shape=[
            jax.ShapeDtypeStruct((2, rows, HD), BF16),
            jax.ShapeDtypeStruct((n_z, part, width), BF16),
            jax.ShapeDtypeStruct((n_z, part, width), BF16),
        ],
        compiler_params=pltpu.CompilerParams(vmem_limit_bytes=8 * MIB),
        name="prepare",
    )(
        core, head, *in_hbm([view(keys), view(values), view(queries), view(queries), gain]),
        cosine, sine,
    )


def add_kernel(*refs):
    total = refs[0][...].astype(F32)
    for ref in refs[1:-1]:
        total = total + ref[...].astype(F32)
    refs[-1][...] = total.astype(BF16)


def add(*arrays):
    return pl.pallas_call(
        add_kernel,
        in_specs=[IN_VMEM] * len(arrays),
        out_specs=IN_VMEM,
        out_shape=jax.ShapeDtypeStruct(arrays[0].shape, BF16),
        compiler_params=pltpu.CompilerParams(vmem_limit_bytes=8 * MIB),
        name="add",
    )(*arrays)


def mix_kernel(n_pieces, n_z, z_ref, q_own, q_other, gain_hbm, cos_ref, sin_ref, w_other, *rest):
    sources = [gain_hbm, rest[0], *[w.at[pl.ds(0, o.shape[0])] for w, o in zip(
        rest[1:4], rest[4 + n_pieces + n_z : 7 + n_pieces + n_z])]]
    pieces = rest[4 : 4 + n_pieces]
    outs = rest[4 + n_pieces : 4 + n_pieces + n_z]
    loaded = rest[4 + n_pieces + n_z : 7 + n_pieces + n_z]
    keys_ref, vals_ref, mixed_ref, w_own, gain_ref, sems = rest[7 + n_pieces + n_z :]
    copies = [
        pltpu.make_async_copy(source, target, sems.at[n])
        for n, (source, target) in enumerate(zip(sources, (gain_ref, w_own, *loaded)))
    ]
    for copy in copies:
        copy.start()
    row = 0
    for piece in pieces:
        rows = piece.shape[1]
        keys_ref[row : row + rows] = piece[0]
        vals_ref[row : row + rows, :HD] = piece[1]
        row += rows
    vals_ref[:, HD:] = jnp.ones((row, HD), BF16)
    factor = HD ** (-0.5) * 1.4426950408889634
    part = q_own.shape[1]
    heads = q_own.shape[-1] // HD
    n_chunks = max(1, row // KEY_CHUNK)
    cut = row // n_chunks
    tile = CORES * heads * part // 2

    copies[0].wait()
    copies[1].wait()

    def one(n, carry):
        block = lax.rem(z_ref[0] + n, n_z)
        at = pl.multiple_of(block * part, 16)
        cosine, sine = cos_ref[pl.ds(at, part)], sin_ref[pl.ds(at, part)]
        queries = []
        for field in (q_own[block], q_other[block]):
            for head in range(heads):
                vec = field[:, head * HD : (head + 1) * HD].astype(F32)
                queries.append(norm_turn(vec, gain_ref[...], cosine, sine).astype(BF16))
        query = jnp.concatenate(queries, axis=0)
        tiles = [query[:tile], query[tile:]]
        score = lambda side, c: lax.dot_general(
            tiles[side], keys_ref[c * cut : (c + 1) * cut],
            (((1,), (1,)), ((), ())), preferred_element_type=F32,
        )
        work = [(c, side) for c in range(n_chunks) for side in range(2)]
        top, total = [None] * 2, [None] * 2
        scores = score(0, 0)
        for step, (c, side) in enumerate(work):
            after = score(work[step + 1][1], work[step + 1][0]) if step + 1 < len(work) else None
            here = jnp.max(scores, axis=1, keepdims=True)
            if c:
                here = jnp.maximum(top[side], here)
                shrink = jnp.exp2((top[side] - here) * factor)
            weights = jnp.exp2((scores - here) * factor).astype(BF16)
            part_sum = jnp.dot(
                weights, vals_ref[c * cut : (c + 1) * cut], preferred_element_type=F32
            )
            total[side] = total[side] * shrink + part_sum if c else part_sum
            top[side] = here
            scores = after
        mixed = None
        for side, weight in enumerate((w_own, w_other)):
            merged = (total[side][:, :HD] / total[side][:, HD:]).astype(BF16)
            merged = jnp.concatenate(
                [merged[h * part : (h + 1) * part] for h in range(heads)], axis=1
            )
            out = jnp.dot(merged, weight[...], preferred_element_type=F32)
            mixed = out if mixed is None else mixed + out
        mixed_ref[n] = mixed.astype(BF16)
        return carry

    lax.fori_loop(0, n_z, one, 0)
    for n, out_ref in enumerate(outs):
        out_ref[...] = mixed_ref[n]
    for copy in copies[2:]:
        copy.wait()


def mix(z_index, q_own, q_other, gain, cosine, sine, w_own, w_other, weights, per, pieces):
    n_z, part, _ = q_own.shape
    d_model = w_own.shape[-1]
    length = sum(p.shape[1] for p in pieces)
    any_space = pl.BlockSpec(memory_space=pl.ANY)
    outs = pl.pallas_call(
        lambda *refs: mix_kernel(len(pieces), n_z, *refs),
        in_specs=[IN_SMEM, IN_VMEM, IN_VMEM, any_space, IN_VMEM, IN_VMEM, IN_VMEM]
        + [any_space] * 4
        + [IN_VMEM] * len(pieces),
        out_specs=[IN_VMEM] * (n_z + 3),
        out_shape=[jax.ShapeDtypeStruct((part, d_model), BF16)] * n_z
        + [jax.ShapeDtypeStruct((per, *w.shape[1:]), BF16) for w in weights],
        scratch_shapes=[
            pltpu.VMEM((length, HD), BF16),
            pltpu.VMEM((length, 2 * HD), BF16),
            pltpu.VMEM((n_z, part, d_model), BF16),
            pltpu.VMEM(w_own.shape, BF16),
            pltpu.VMEM(gain.shape, F32),
            pltpu.SemaphoreType.DMA((5,)),
        ],
        compiler_params=pltpu.CompilerParams(vmem_limit_bytes=20 * MIB),
        name="mix",
    )(
        z_index, q_own, q_other, *in_hbm([gain]), cosine, sine, w_other,
        *in_hbm([w_own, *weights]), *pieces,
    )
    return outs[:n_z], outs[n_z:]


def block_of(index, block, count):
    found = jnp.zeros_like(index)
    for n in range(1, count):
        found = found + (index >= n * block).astype(jnp.int32)
    return found


def dispatch_kernel(
    n_ep, n_local, core_ref, ep_ref, tokens_ref, gain_ref, routes_ref, weight_ref, *rest
):
    out_refs, cols_ref = rest[:n_ep], rest[n_ep]
    n_z, _, block, d_model = tokens_ref.shape
    rows, local_rows = n_z * block, routes_ref.shape[1]
    iota = lambda shape, dim: lax.broadcasted_iota(jnp.int32, shape, dim)
    exact = dict(preferred_element_type=F32, precision=lax.Precision.HIGHEST)

    lane = iota((local_rows, rows), 1)
    lane_block = block_of(lane, block, n_z)
    source = lane + (lane_block * (CORES - 1) + core_ref[0]) * block
    select = (iota((local_rows, rows), 0) == source).astype(F32)
    chosen = jnp.dot(routes_ref[...].astype(F32), select, **exact)
    chosen = (chosen + 0.5).astype(jnp.int32)
    weight = jnp.dot(weight_ref[...], select, **exact)

    shape = (EXPERTS, rows)
    expert = iota(shape, 0)
    hot = [expert == chosen[k : k + 1] for k in range(TOPK)]
    either = hot[0]
    for one in hot[1:]:
        either = either | one
    square = (rows, rows)
    above, across = iota(square, 0), iota(square, 1)
    first = block_of(across, block, n_z) * block
    earlier = ((above < across) & (above >= first)).astype(F32).astype(BF16)
    count = jnp.dot(either.astype(F32).astype(BF16), earlier, preferred_element_type=F32)
    owner = block_of(expert, n_local, n_ep)
    ahead = owner - ep_ref[0]
    ahead = jnp.where(ahead < 0, ahead + n_ep, ahead)
    place = (ahead * n_local + expert - owner * n_local) * (n_z * CAP)
    place = place + block_of(iota(shape, 1), block, n_z) * CAP + (count + 0.5).astype(jnp.int32)
    slots = [jnp.sum(jnp.where(h, place, 0), axis=0, keepdims=True) for h in hot]

    total = jnp.sum(weight, axis=0, keepdims=True)
    table = [s.astype(F32) for s in slots] + [weight[k : k + 1] / total for k in range(TOPK)]
    lines = iota((8, rows), 0)
    stacked = jnp.zeros((8, rows), F32)
    for n, line in enumerate(table):
        stacked = jnp.where(lines == n, line, stacked)
    same = (above == across).astype(F32)
    cols_ref[...] = lax.dot_general(same, stacked, (((1,), (1,)), ((), ())), **exact)

    field = tokens_ref[...].reshape(rows, d_model).astype(F32)
    mean = jnp.mean(field * field, axis=-1, keepdims=True)
    normed = (field * lax.rsqrt(mean + EPS) * gain_ref[...]).astype(BF16)
    n_slots = out_refs[0].shape[0]
    for piece, out_ref in enumerate(out_refs):
        slot = iota((n_slots, rows), 0) + piece * n_slots
        picked = slot == slots[0]
        for one in slots[1:]:
            picked = picked | (slot == one)
        picked = picked.astype(F32).astype(BF16)
        out_ref[...] = jnp.dot(picked, normed, preferred_element_type=F32).astype(BF16)


def dispatch(core, ep, tokens, gain, routes, weight, n_z, n_ep, n_local):
    local_rows, d_model = tokens.shape
    block = local_rows // (n_z * CORES)
    n_slots = n_local * n_z * CAP
    whole = lambda a: pl.BlockSpec(a.shape, lambda i, c, e: (0,) * a.ndim)
    outs = pl.pallas_call(
        lambda *refs: dispatch_kernel(n_ep, n_local, *refs),
        grid_spec=pltpu.PrefetchScalarGridSpec(
            num_scalar_prefetch=2,
            grid=(1,),
            in_specs=[
                pl.BlockSpec((n_z, 1, block, d_model), lambda i, c, e: (0, c[0], 0, 0)),
                whole(gain),
                whole(routes),
                whole(weight),
            ],
            out_specs=[IN_VMEM] * (n_ep + 1),
        ),
        out_shape=[jax.ShapeDtypeStruct((n_slots, d_model), BF16)] * n_ep
        + [jax.ShapeDtypeStruct((n_z * block, 8), F32)],
        compiler_params=pltpu.CompilerParams(vmem_limit_bytes=16 * MIB),
        name="dispatch",
    )(core, ep, *in_hbm([tokens.reshape(n_z, CORES, block, d_model), gain]), routes, weight)
    return outs[:n_ep], outs[n_ep]


def expert_kernel(n_in, group, first, n_next, *refs):
    ins, (gate_ref, up_ref, down_ref) = refs[:n_in], refs[n_in : n_in + 3]
    sources, outs = refs[n_in + 3 : n_in + 3 + n_next], refs[n_in + 3 + n_next : 2 * n_in + 3 + n_next]
    per, rows, _ = outs[0].shape
    copies = []
    if n_next:
        targets, sems = refs[2 * n_in + 3 + n_next : -1], refs[-1]
        for n, (source, target) in enumerate(zip(sources, targets)):
            part = source.at[pl.ds(first + per, per)]
            copies.append(pltpu.make_async_copy(part, target, sems.at[n]))
    for copy in copies:
        copy.start()
    for expert in range(per):
        for start in range(0, len(ins), group):
            field = [ref[first + expert] for ref in ins[start : start + group]]
            field = jnp.concatenate(field, axis=0)
            gate = jnp.dot(field, gate_ref[expert], preferred_element_type=F32)
            up = jnp.dot(field, up_ref[expert], preferred_element_type=F32)
            hidden = (gate / (1.0 + jnp.exp(-gate)) * up).astype(BF16)
            result = jnp.dot(hidden, down_ref[expert], preferred_element_type=F32)
            for n, ref in enumerate(outs[start : start + group]):
                ref[expert] = result[n * rows : (n + 1) * rows].astype(BF16)
    for copy in copies:
        copy.wait()


def experts(own, other, weights, first, all_weights):
    pieces = [*own, *other]
    _, rows, d_model = pieces[0].shape
    per = weights[0].shape[0]
    more = in_hbm(all_weights) if first + per < all_weights[0].shape[0] else []
    group = min(len(pieces), max(1, 256 // rows))
    outs = pl.pallas_call(
        lambda *refs: expert_kernel(len(pieces), group, first, len(more), *refs),
        in_specs=[IN_VMEM] * (len(pieces) + 3) + [pl.BlockSpec(memory_space=pl.ANY)] * len(more),
        out_specs=[IN_VMEM] * (len(pieces) + len(more)),
        out_shape=[jax.ShapeDtypeStruct((per, rows, d_model), BF16)] * len(pieces)
        + [jax.ShapeDtypeStruct((per, *w.shape[1:]), BF16) for w in more],
        scratch_shapes=[pltpu.SemaphoreType.DMA((len(more),))] if more else [],
        compiler_params=pltpu.CompilerParams(vmem_limit_bytes=16 * MIB),
        name="experts",
    )(*pieces, *weights, *more)
    return outs[: len(own)], outs[len(own) : len(pieces)], outs[len(pieces) :]


def combine_kernel(n_back, z_ref, cols_ref, *rest):
    back_refs, out_refs, total_ref = rest[:n_back], rest[n_back:-1], rest[-1]
    rows = cols_ref.shape[0]
    back = jnp.concatenate([ref[...] for ref in back_refs], axis=0)
    slot = lax.broadcasted_iota(jnp.int32, (rows, back.shape[0]), 1)
    matrix = jnp.zeros(slot.shape, F32)
    for k in range(TOPK):
        own = (cols_ref[:, k : k + 1] + 0.5).astype(jnp.int32)
        share = cols_ref[:, TOPK + k : TOPK + k + 1]
        matrix = matrix + jnp.where(slot == own, share, 0.0)
    high = matrix.astype(BF16)
    low = (matrix - high.astype(F32)).astype(BF16)
    both = jnp.dot(jnp.concatenate([high, low], axis=0), back, preferred_element_type=F32)
    total_ref[...] = (both[:rows] + both[rows:]).reshape(total_ref.shape)
    n_z = len(out_refs)
    for n, out_ref in enumerate(out_refs):
        out_ref[...] = total_ref[lax.rem(z_ref[0] + n, n_z)].astype(BF16)


def combine(z_index, cols, backs, n_z):
    rows, d_model = cols.shape[0], backs[0].shape[-1]
    return pl.pallas_call(
        lambda *refs: combine_kernel(len(backs), *refs),
        in_specs=[IN_SMEM] + [IN_VMEM] * (1 + len(backs)),
        out_specs=[IN_VMEM] * n_z,
        out_shape=[jax.ShapeDtypeStruct((rows // n_z, d_model), BF16)] * n_z,
        scratch_shapes=[pltpu.VMEM((n_z, rows // n_z, d_model), F32)],
        compiler_params=pltpu.CompilerParams(vmem_limit_bytes=24 * MIB),
        name="combine",
    )(z_index, cols, *backs)


def shift(a, axis, step):
    n = lax.axis_size(axis)
    return lax.ppermute(a, axis, [(i, (i + step) % n) for i in range(n)])


def swap_cores(a):
    return lax.ppermute(a, "core", [(i, CORES - 1 - i) for i in range(CORES)])


def on_device(
    queries,
    keys,
    values,
    query_gain,
    key_gain,
    out_weight,
    tokens_b,
    norm_gain,
    routes,
    route_weight,
    gate_weight,
    up_weight,
    down_weight,
):
    n_ep, n_z = lax.axis_size("ep"), lax.axis_size("z")
    core, z_index = lax.axis_index("core"), lax.axis_index("z")
    core_arg = core.reshape(1).astype(jnp.int32)
    z_arg = z_index.reshape(1).astype(jnp.int32)
    n_rows, width = queries.shape
    d_model = tokens_b.shape[-1]
    heads = width // HD
    n_heads = heads * n_z * CORES

    part = n_rows // (n_z * CORES)
    offsets = (
        jnp.arange(n_z, dtype=jnp.int32)[:, None] * (CORES * part)
        + core * part
        + jnp.arange(part, dtype=jnp.int32)[None, :]
    ).reshape(-1)
    cosine, sine = rope_tables(lax.axis_index("ep") * n_rows + offsets)
    kv_head = ((z_index * CORES + core) * heads // (n_heads // KVH)).reshape(1).astype(jnp.int32)
    own_kv, q_send, q_own = prepare(
        core_arg, kv_head, keys, values, queries, key_gain[None], cosine, sine, n_z
    )
    pieces = [own_kv]
    for step in range(1, n_ep):
        pieces.append(shift(own_kv, "ep", step))
    pieces = pieces + [swap_cores(p) for p in pieces]

    q_other = swap_cores(q_send)
    w_other = swap_cores(out_weight)

    n_local = gate_weight.shape[0]
    chunks = 2 if n_local % 2 == 0 else 1
    per = n_local // chunks
    ep_arg = lax.axis_index("ep").reshape(1).astype(jnp.int32)
    outgoing, cols = dispatch(
        core_arg, ep_arg, tokens_b, norm_gain[None], routes.T, route_weight.T, n_z, n_ep, n_local
    )
    here = []
    for step in range(n_ep):
        piece = outgoing[step].reshape(n_local, n_z * CAP, d_model)
        here.append(shift(piece, "ep", step) if step else piece)
    there = [swap_cores(p) for p in here]

    all_weights = [gate_weight, up_weight, down_weight]
    mixed, weights = mix(
        z_arg, q_own, q_other, query_gain[None], cosine, sine, out_weight, w_other,
        all_weights, per, pieces,
    )
    gathered = [mixed[0]]
    for step in range(1, n_z):
        gathered.append(shift(mixed[step], "z", step))
    mixed_out = add(*gathered)

    backs = [[] for _ in range(n_ep)]
    for chunk in range(chunks):
        keep, send, weights = experts(here, there, weights, chunk * per, all_weights)
        for step in range(n_ep):
            result = add(keep[step], swap_cores(send[step]))
            result = shift(result, "ep", n_ep - step) if step else result
            backs[step].append(result.reshape(-1, d_model))
    rows = combine(z_arg, cols, [b for step in backs for b in step], n_z)
    gathered = [rows[0]]
    for step in range(1, n_z):
        gathered.append(shift(rows[step], "z", step))
    expert_out = add(*gathered)
    return (mixed_out, expert_out)


def solution(mesh):
    n_ep, n_tp = mesh.shape["ep"], mesh.shape["tp"]
    fine = Mesh(mesh.devices.reshape(n_ep, n_tp // CORES, CORES), ("ep", "z", "core"))
    tp = ("z", "core")
    placed = (
        P("ep", tp),
        P("ep", None),
        P("ep", None),
        P(),
        P(),
        P(tp, None),
        P("ep", None),
        P(),
        P("ep", None),
        P("ep", None),
        P("ep", None, tp),
        P("ep", None, tp),
        P("ep", tp, None),
    )

    return jax.shard_map(
        on_device,
        mesh=fine,
        in_specs=placed,
        out_specs=(P(("ep", "z", "core"), None), P(("ep", "z", "core"), None)),
        check_vma=False,
    )
```

time: 150 us -> 129 us (0.86)
  waiting for transfers between devices: 76.6 us -> 60.5 us
  Pallas kernels: 32.3 us -> 29.2 us
  local copies, waits for them, and re-layouts: 3.78 us -> 1.46 us
    ppermute x21 -> x18, waiting for transfers between devices: 75.6 us -> 57.6 us  [shift(): return lax.ppermute(a, axis, [(i, (i + step) % n) for i in range(n)])]
    pallas_call x3, Pallas kernels: 18 us -> 13.6 us  [the longest x2 11 us: experts(): pl.pallas_call(lambda *refs: expert_kernel(len(pieces), group, first, len...]
    ppermute x22 -> x18, waiting for transfers between devices: 1.03 us -> 2.92 us  [swap_cores(): return lax.ppermute(a, 'core', [(i, CORES - 1 - i) for i in range(CORES)])]
    reshape x2 -> x0, local copies, waits for them, and re-layouts: 1.54 us -> none  [on_device(): a.reshape(n_z, CORES, block_rows, TOPK)]
    ppermute x21 -> x18, starting transfers between devices: 29.4 us -> 29.7 us  [shift(): return lax.ppermute(a, axis, [(i, (i + step) % n) for i in range(n)])]
    ppermute x22 -> x18, starting transfers between devices: 4.17 us -> 4.27 us  [swap_cores(): return lax.ppermute(a, 'core', [(i, CORES - 1 - i) for i in range(CORES)])]
  transfers between devices with their start and end apart: 43 -> 36, of which waited for: 14 -> 13; matrix products, arithmetic and copies ran while one was open for 1% -> 0% of each run, Pallas kernels for 19% -> 15%
where the time goes in v4:
time: 129 us; the launch traced here: 127 us
  waiting for transfers between devices  60.5 us (47%)
  starting transfers between devices  34 us (26%)
  Pallas kernels  29.2 us (23%)
  local copies, waits for them, and re-layouts  1.46 us (1%)
    ppermute x18, waiting for transfers between devices, shift(): return lax.ppermute(a, axis, [(i, (i + step) % n) for i in range(n)])  57.6 us
    ppermute x18, starting transfers between devices, shift(): return lax.ppermute(a, axis, [(i, (i + step) % n) for i in range(n)])  29.7 us
    pallas_call x2, Pallas kernels, experts(): pl.pallas_call(lambda *refs: expert_kernel(len(pieces), group, first, len...  11 us
    pallas_call x1, Pallas kernels, mix(): pl.pallas_call(lambda *refs: mix_kernel(len(pieces), n_z, *refs), in_spec...  10.6 us
    ppermute x18, starting transfers between devices, swap_cores(): return lax.ppermute(a, 'core', [(i, CORES - 1 - i) for i in range(CORES)])  4.27 us
    ppermute x18, waiting for transfers between devices, swap_cores(): return lax.ppermute(a, 'core', [(i, CORES - 1 - i) for i in range(CORES)])  2.92 us
  transfers between devices with their start and end apart: 36, of which 13 were waited for; matrix products, arithmetic and copies ran while one was open for 0% of the time, Pallas kernels for 15%

profile of v4, /device:TPU:0, one launch (start us, length us, event | category | flops | bytes accessed | tf_op | source)
XLA Modules:
  0.0 126.9 jit_solution(11544260287603772364)
XLA Ops:
  0.9 0.8 sine_multiply_fusion
  1.7 1.4 %prepare.1 = (bf16[2,384,128]{2,1,0:T(8,128)(2,1)S(1)}, bf16[4,96,256]{2,1,0:T(8,128)(2,1)S(1)}, bf16[4,96,256]{2,1,0:T(8,128)(2,1)S(1)}) custom-call(s32[1]{0:T(128)} %bitcast.1.core_ref.refs_0_, s32[1]{0:T(128)} %bitcast.2.head_ref, bf16[4,2,96,512]{3,2,1,0:T(8,128)(2,1)} %bitcast.44, bf16[4,2,96,512]{3,2,1,0:T(8,128)(2,1)} %bitcast.45, ...), custom_call_target="tpu_custom_call" | custom-call | tf_op jit(solution)/shard_map/prepare/pallas_call | solution.py:73
  3.1 4.0 %collective-permute-start.4 = (bf16[2,384,128]{2,1,0:T(8,128)(2,1)S(1)}, bf16[2,384,128]{2,1,0:T(8,128)(2,1)S(1)}, u32[]{:S(2)}, u32[]{:S(2)}) collective-permute-start(bf16[2,384,128]{2,1,0:T(8,128)(2,1)S(1)} %get-tuple-element.42.refs_11_), channel_id=1, source_target_pairs={{0,24},{8,0},{16,8},{24,16},{1,25},{9,1},{17,9},{25,17},{2,26},{10... | collective-permute-start | bytes 589832 | tf_op jit(solution)/shard_map/ppermute | solution.py:398
  7.1 0.5 collective-permute-start.5
  7.6 0.5 collective-permute-start.3
  8.1 0.6 collective-permute-start.2
  8.7 3.7 %collective-permute-done.4.refs_14_ = bf16[2,384,128]{2,1,0:T(8,128)(2,1)S(1)} collective-permute-done((bf16[2,384,128]{2,1,0:T(8,128)(2,1)S(1)}, bf16[2,384,128]{2,1,0:T(8,128)(2,1)S(1)}, u32[]{:S(2)}, u32[]{:S(2)}) %collective-permute-start.4) | collective-permute-done | bytes 196640 | tf_op jit(solution)/shard_map/ppermute | solution.py:398
  12.4 0.7 copy-done
  13.1 0.7 copy-done.1
  13.8 2.6 %dispatch.1 = (bf16[128,2048]{1,0:T(8,128)(2,1)S(1)}, bf16[128,2048]{1,0:T(8,128)(2,1)S(1)}, bf16[128,2048]{1,0:T(8,128)(2,1)S(1)}, bf16[128,2048]{1,0:T(8,128)(2,1)S(1)}, f32[192,8]{1,0:T(8,128)S(1)}) custom-call(s32[1]{0:T(128)} %bitcast.1.core_ref.refs_0_, s32[1]{0:T(128)} %bitcast.8.refs_1_, bf16[4,2,48,2048]{3,2,1,0:T(8,128)(2,1)} %bitcast.41, ...), custom_call_target="tpu_custom_call" | custom-call | tf_op jit(solution)/shard_map/dispatch/pallas_call | solution.py:298
  16.4 0.6 collective-permute-start.1
  17.0 2.4 %collective-permute-start.12 = (bf16[4,32,2048]{2,1,0:T(8,128)(2,1)S(1)}, bf16[4,32,2048]{2,1,0:T(8,128)(2,1)S(1)}, u32[]{:S(2)}, u32[]{:S(2)}) collective-permute-start(bf16[4,32,2048]{2,1,0:T(8,128)(2,1)S(1)} %bitcast.40), channel_id=1, source_target_pairs={{0,8},{8,16},{16,24},{24,0},{1,9},{9,17},{17,25},{25,1},{2,10},{10... | collective-permute-start | bytes 1572872 | tf_op jit(solution)/shard_map/ppermute | solution.py:398
  19.4 1.5 %collective-permute-start.13 = (bf16[4,32,2048]{2,1,0:T(8,128)(2,1)S(1)}, bf16[4,32,2048]{2,1,0:T(8,128)(2,1)S(1)}, u32[]{:S(2)}, u32[]{:S(2)}) collective-permute-start(bf16[4,32,2048]{2,1,0:T(8,128)(2,1)S(1)} %bitcast.39), channel_id=1, source_target_pairs={{0,16},{8,24},{16,0},{24,8},{1,17},{9,25},{17,1},{25,9},{2,18},{10... | collective-permute-start | bytes 1572872 | tf_op jit(solution)/shard_map/ppermute | solution.py:398
  20.9 0.3 collective-permute-start.14
  21.2 1.4 %collective-permute-done.7.refs_17_ = bf16[2,384,128]{2,1,0:T(8,128)(2,1)S(1)} collective-permute-done((bf16[2,384,128]{2,1,0:T(8,128)(2,1)S(1)}, bf16[2,384,128]{2,1,0:T(8,128)(2,1)S(1)}, u32[]{:S(2)}, u32[]{:S(2)}) %collective-permute-start.7) | collective-permute-done | bytes 196640 | tf_op jit(solution)/shard_map/ppermute | solution.py:402
  22.8 1.3 %collective-permute-done.6.refs_16_ = bf16[2,384,128]{2,1,0:T(8,128)(2,1)S(1)} collective-permute-done((bf16[2,384,128]{2,1,0:T(8,128)(2,1)S(1)}, bf16[2,384,128]{2,1,0:T(8,128)(2,1)S(1)}, u32[]{:S(2)}, u32[]{:S(2)}) %collective-permute-start.6) | collective-permute-done | bytes 196640 | tf_op jit(solution)/shard_map/ppermute | solution.py:402
  24.2 8.9 %collective-permute-done.12.refs_1_ = bf16[4,32,2048]{2,1,0:T(8,128)(2,1)S(1)} collective-permute-done((bf16[4,32,2048]{2,1,0:T(8,128)(2,1)S(1)}, bf16[4,32,2048]{2,1,0:T(8,128)(2,1)S(1)}, u32[]{:S(2)}, u32[]{:S(2)}) %collective-permute-start.12) | collective-permute-done | bytes 524320 | tf_op jit(solution)/shard_map/ppermute | solution.py:398
  33.2 10.6 %collective-permute-done.13.refs_2_ = bf16[4,32,2048]{2,1,0:T(8,128)(2,1)S(1)} collective-permute-done((bf16[4,32,2048]{2,1,0:T(8,128)(2,1)S(1)}, bf16[4,32,2048]{2,1,0:T(8,128)(2,1)S(1)}, u32[]{:S(2)}, u32[]{:S(2)}) %collective-permute-start.13) | collective-permute-done | bytes 524320 | tf_op jit(solution)/shard_map/ppermute | solution.py:398
  43.8 0.5 collective-permute-start.18
  44.3 10.6 %mix.1 = (bf16[96,2048]{1,0:T(8,128)(2,1)S(1)}, bf16[96,2048]{1,0:T(8,128)(2,1)S(1)}, bf16[96,2048]{1,0:T(8,128)(2,1)S(1)}, bf16[96,2048]{1,0:T(8,128)(2,1)S(1)}...) custom-call(s32[1]{0:T(128)} %bitcast.refs_0_, ...), custom_call_target="tpu_custom_call" | custom-call | tf_op jit(solution)/shard_map/mix/pallas_call | solution.py:204
  55.0 7.5 %experts.2 = (bf16[2,32,2048]{2,1,0:T(8,128)(2,1)S(1)}, bf16[2,32,2048]{2,1,0:T(8,128)(2,1)S(1)}, bf16[2,32,2048]{2,1,0:T(8,128)(2,1)S(1)}, bf16[2,32,2048]{2,1,...) custom-call(bf16[4,32,2048]{2,1,0:T(8,128)(2,1)S(1)} %bitcast.26, ...), custom_call_target="tpu_custom_call" | custom-call | tf_op jit(solution)/shard_map/experts/pallas_call | solution.py:351
  62.5 3.6 %experts.3 = (bf16[2,32,2048]{2,1,0:T(8,128)(2,1)S(1)}, bf16[2,32,2048]{2,1,0:T(8,128)(2,1)S(1)}, bf16[2,32,2048]{2,1,0:T(8,128)(2,1)S(1)}, bf16[2,32,2048]{2,1,...) custom-call(bf16[4,32,2048]{2,1,0:T(8,128)(2,1)S(1)} %bitcast.27, ...), custom_call_target="tpu_custom_call" | custom-call | tf_op jit(solution)/shard_map/experts/pallas_call | solution.py:351
  66.1 0.6 collective-permute-start.23
  66.7 0.4 collective-permute-start.20
  67.2 0.4 collective-permute-start.21
  67.8 0.4 collective-permute-start.25
  68.2 0.4 collective-permute-start.29
  68.7 1.9 %collective-permute-start.24 = (bf16[2,32,2048]{2,1,0:T(8,128)(2,1)S(1)}, bf16[2,32,2048]{2,1,0:T(8,128)(2,1)S(1)}, u32[]{:S(2)}, u32[]{:S(2)}) collective-permute-start(bf16[2,32,2048]{2,1,0:T(8,128)(2,1)S(1)} %add.139), channel_id=1, source_target_pairs={{0,24},{8,0},{16,8},{24,16},{1,25},{9,1},{17,9},{25,17},{2,26},{10... | collective-permute-start | bytes 786440 | tf_op jit(solution)/shard_map/ppermute | solution.py:398
  70.6 1.0 collective-permute-start.28
  71.9 3.0 %collective-permute-start.22 = (bf16[2,32,2048]{2,1,0:T(8,128)(2,1)S(1)}, bf16[2,32,2048]{2,1,0:T(8,128)(2,1)S(1)}, u32[]{:S(2)}, u32[]{:S(2)}) collective-permute-start(bf16[2,32,2048]{2,1,0:T(8,128)(2,1)S(1)} %add.138), channel_id=1, source_target_pairs={{0,24},{8,0},{16,8},{24,16},{1,25},{9,1},{17,9},{25,17},{2,26},{10... | collective-permute-start | bytes 786440 | tf_op jit(solution)/shard_map/ppermute | solution.py:398
  74.8 1.6 %collective-permute-start.9 = (bf16[96,2048]{1,0:T(8,128)(2,1)S(1)}, bf16[96,2048]{1,0:T(8,128)(2,1)S(1)}, u32[]{:S(2)}, u32[]{:S(2)}) collective-permute-start(bf16[96,2048]{1,0:T(8,128)(2,1)S(1)} %get-tuple-element.44), channel_id=1, source_target_pairs={{0,2},{2,4},{4,6},{6,0},{1,3},{3,5},{5,7},{7,1},{8,10},{10,12},{12... | collective-permute-start | bytes 1179656 | tf_op jit(solution)/shard_map/ppermute | solution.py:398
  76.5 1.4 %collective-permute-done.24 = bf16[2,32,2048]{2,1,0:T(8,128)(2,1)S(1)} collective-permute-done((bf16[2,32,2048]{2,1,0:T(8,128)(2,1)S(1)}, bf16[2,32,2048]{2,1,0:T(8,128)(2,1)S(1)}, u32[]{:S(2)}, u32[]{:S(2)}) %collective-permute-start.24) | collective-permute-done | bytes 262176 | tf_op jit(solution)/shard_map/ppermute | solution.py:398
  77.9 0.6 collective-permute-start.26
  78.5 6.9 %collective-permute-done.28 = bf16[2,32,2048]{2,1,0:T(8,128)(2,1)S(1)} collective-permute-done((bf16[2,32,2048]{2,1,0:T(8,128)(2,1)S(1)}, bf16[2,32,2048]{2,1,0:T(8,128)(2,1)S(1)}, u32[]{:S(2)}, u32[]{:S(2)}) %collective-permute-start.28) | collective-permute-done | bytes 262176 | tf_op jit(solution)/shard_map/ppermute | solution.py:398
  85.4 0.6 collective-permute-start.30
  86.0 2.6 %collective-permute-start.10 = (bf16[96,2048]{1,0:T(8,128)(2,1)S(1)}, bf16[96,2048]{1,0:T(8,128)(2,1)S(1)}, u32[]{:S(2)}, u32[]{:S(2)}) collective-permute-start(bf16[96,2048]{1,0:T(8,128)(2,1)S(1)} %get-tuple-element.45), channel_id=1, source_target_pairs={{0,4},{2,6},{4,0},{6,2},{1,5},{3,7},{5,1},{7,3},{8,12},{10,14},{12... | collective-permute-start | bytes 1179656 | tf_op jit(solution)/shard_map/ppermute | solution.py:398
  88.6 0.7 collective-permute-done.22
  89.2 3.6 %collective-permute-start.11 = (bf16[96,2048]{1,0:T(8,128)(2,1)S(1)}, bf16[96,2048]{1,0:T(8,128)(2,1)S(1)}, u32[]{:S(2)}, u32[]{:S(2)}) collective-permute-start(bf16[96,2048]{1,0:T(8,128)(2,1)S(1)} %get-tuple-element.46), channel_id=1, source_target_pairs={{0,6},{2,0},{4,2},{6,4},{1,7},{3,1},{5,3},{7,5},{8,14},{10,8},{12,... | collective-permute-start | bytes 1179656 | tf_op jit(solution)/shard_map/ppermute | solution.py:398
  93.0 2.6 %collective-permute-done.26 = bf16[2,32,2048]{2,1,0:T(8,128)(2,1)S(1)} collective-permute-done((bf16[2,32,2048]{2,1,0:T(8,128)(2,1)S(1)}, bf16[2,32,2048]{2,1,0:T(8,128)(2,1)S(1)}, u32[]{:S(2)}, u32[]{:S(2)}) %collective-permute-start.26) | collective-permute-done | bytes 262176 | tf_op jit(solution)/shard_map/ppermute | solution.py:398
  95.6 1.2 combine.1
  96.8 1.6 %collective-permute-start.33 = (bf16[48,2048]{1,0:T(8,128)(2,1)S(1)}, bf16[48,2048]{1,0:T(8,128)(2,1)S(1)}, u32[]{:S(2)}, u32[]{:S(2)}) collective-permute-start(bf16[48,2048]{1,0:T(8,128)(2,1)S(1)} %get-tuple-element.75), channel_id=1, source_target_pairs={{0,2},{2,4},{4,6},{6,0},{1,3},{3,5},{5,7},{7,1},{8,10},{10,12},{12... | collective-permute-start | bytes 589832 | tf_op jit(solution)/shard_map/ppermute | solution.py:398
  98.4 2.6 %collective-permute-start.34 = (bf16[48,2048]{1,0:T(8,128)(2,1)S(1)}, bf16[48,2048]{1,0:T(8,128)(2,1)S(1)}, u32[]{:S(2)}, u32[]{:S(2)}) collective-permute-start(bf16[48,2048]{1,0:T(8,128)(2,1)S(1)} %get-tuple-element.76), channel_id=1, source_target_pairs={{0,4},{2,6},{4,0},{6,2},{1,5},{3,7},{5,1},{7,3},{8,12},{10,14},{12... | collective-permute-start | bytes 589832 | tf_op jit(solution)/shard_map/ppermute | solution.py:398
  101.0 1.3 %collective-permute-start.35 = (bf16[48,2048]{1,0:T(8,128)(2,1)S(1)}, bf16[48,2048]{1,0:T(8,128)(2,1)S(1)}, u32[]{:S(2)}, u32[]{:S(2)}) collective-permute-start(bf16[48,2048]{1,0:T(8,128)(2,1)S(1)} %get-tuple-element.77), channel_id=1, source_target_pairs={{0,6},{2,0},{4,2},{6,4},{1,7},{3,1},{5,3},{7,5},{8,14},{10,8},{12,... | collective-permute-start | bytes 589832 | tf_op jit(solution)/shard_map/ppermute | solution.py:398
  102.4 6.0 %collective-permute-done.10.refs_2_ = bf16[96,2048]{1,0:T(8,128)(2,1)S(1)} collective-permute-done((bf16[96,2048]{1,0:T(8,128)(2,1)S(1)}, bf16[96,2048]{1,0:T(8,128)(2,1)S(1)}, u32[]{:S(2)}, u32[]{:S(2)}) %collective-permute-start.10) | collective-permute-done | bytes 393248 | tf_op jit(solution)/shard_map/ppermute | solution.py:398
  108.4 3.8 %collective-permute-done.11.refs_3_ = bf16[96,2048]{1,0:T(8,128)(2,1)S(1)} collective-permute-done((bf16[96,2048]{1,0:T(8,128)(2,1)S(1)}, bf16[96,2048]{1,0:T(8,128)(2,1)S(1)}, u32[]{:S(2)}, u32[]{:S(2)}) %collective-permute-start.11) | collective-permute-done | bytes 393248 | tf_op jit(solution)/shard_map/ppermute | solution.py:398
  112.2 1.0 add.135
  113.1 13.0 %collective-permute-done.34.refs_2_ = bf16[48,2048]{1,0:T(8,128)(2,1)S(1)} collective-permute-done((bf16[48,2048]{1,0:T(8,128)(2,1)S(1)}, bf16[48,2048]{1,0:T(8,128)(2,1)S(1)}, u32[]{:S(2)}, u32[]{:S(2)}) %collective-permute-start.34) | collective-permute-done | bytes 196640 | tf_op jit(solution)/shard_map/ppermute | solution.py:398
  126.1 0.8 add.144
  (53 shorter events, 1.5 us)
Async XLA Ops:
  0.6 15.8 %copy-start.2 = (bf16[256,2048]{1,0:T(8,128)(2,1)S(1)}, bf16[256,2048]{1,0:T(8,128)(2,1)}, u32[]{:S(2)}) copy-start(bf16[256,2048]{1,0:T(8,128)(2,1)} %refs_7_.1) | copy-start | bytes 3145732
  3.1 9.3 %collective-permute-start.4 = (bf16[2,384,128]{2,1,0:T(8,128)(2,1)S(1)}, bf16[2,384,128]{2,1,0:T(8,128)(2,1)S(1)}, u32[]{:S(2)}, u32[]{:S(2)}) collective-permute-start(bf16[2,384,128]{2,1,0:T(8,128)(2,1)S(1)} %get-tuple-element.42.refs_11_), channel_id=1, source_target_pairs={{0,24},{8,0},{16,8},{24,16},{1,25},{9,1},{17,9},{25,17},{2,26},{10... | collective-permute-start | bytes 589832 | tf_op jit(solution)/shard_map/ppermute | solution.py:398
  7.1 9.3 %collective-permute-start = (bf16[4,96,256]{2,1,0:T(8,128)(2,1)S(1)}, bf16[4,96,256]{2,1,0:T(8,128)(2,1)S(1)}, u32[]{:S(2)}, u32[]{:S(2)}) collective-permute-start(bf16[4,96,256]{2,1,0:T(8,128)(2,1)S(1)} %get-tuple-element.41), channel_id=1, source_target_pairs={{0,1},{1,0},{2,3},{3,2},{4,5},{5,4},{6,7},{7,6},{8,9},{9,8},{10,11... | collective-permute-start | bytes 589832 | tf_op jit(solution)/shard_map/ppermute | solution.py:402
  7.1 9.9 %collective-permute-start.5 = (bf16[2,384,128]{2,1,0:T(8,128)(2,1)S(1)}, bf16[2,384,128]{2,1,0:T(8,128)(2,1)S(1)}, u32[]{:S(2)}, u32[]{:S(2)}) collective-permute-start(bf16[2,384,128]{2,1,0:T(8,128)(2,1)S(1)} %get-tuple-element.42.refs_11_), channel_id=1, source_target_pairs={{0,1},{1,0},{2,3},{3,2},{4,5},{5,4},{6,7},{7,6},{8,9},{9,8},{10,11... | collective-permute-start | bytes 589832 | tf_op jit(solution)/shard_map/ppermute | solution.py:402
  7.6 11.8 %collective-permute-start.3 = (bf16[2,384,128]{2,1,0:T(8,128)(2,1)S(1)}, bf16[2,384,128]{2,1,0:T(8,128)(2,1)S(1)}, u32[]{:S(2)}, u32[]{:S(2)}) collective-permute-start(bf16[2,384,128]{2,1,0:T(8,128)(2,1)S(1)} %get-tuple-element.42.refs_11_), channel_id=1, source_target_pairs={{0,16},{8,24},{16,0},{24,8},{1,17},{9,25},{17,1},{25,9},{2,18},{10... | collective-permute-start | bytes 589832 | tf_op jit(solution)/shard_map/ppermute | solution.py:398
  8.1 12.8 %collective-permute-start.2 = (bf16[2,384,128]{2,1,0:T(8,128)(2,1)S(1)}, bf16[2,384,128]{2,1,0:T(8,128)(2,1)S(1)}, u32[]{:S(2)}, u32[]{:S(2)}) collective-permute-start(bf16[2,384,128]{2,1,0:T(8,128)(2,1)S(1)} %get-tuple-element.42.refs_11_), channel_id=1, source_target_pairs={{0,8},{8,16},{16,24},{24,0},{1,9},{9,17},{17,25},{25,1},{2,10},{10... | collective-permute-start | bytes 589832 | tf_op jit(solution)/shard_map/ppermute | solution.py:398
  12.4 8.8 %collective-permute-start.8 = (bf16[2,384,128]{2,1,0:T(8,128)(2,1)S(1)}, bf16[2,384,128]{2,1,0:T(8,128)(2,1)S(1)}, u32[]{:S(2)}, u32[]{:S(2)}) collective-permute-start(bf16[2,384,128]{2,1,0:T(8,128)(2,1)S(1)} %collective-permute-done.4.refs_14_), channel_id=1, source_target_pairs={{0,1},{1,0},{2,3},{3,2},{4,5},{5,4},{6,7},{7,6},{8,9},{9,8},{10,11... | collective-permute-start | bytes 589832 | tf_op jit(solution)/shard_map/ppermute | solution.py:402
  12.4 0.7 copy-start
  13.1 0.7 copy-start.1
  16.4 27.9 %collective-permute-start.1 = (bf16[256,2048]{1,0:T(8,128)(2,1)S(1)}, bf16[256,2048]{1,0:T(8,128)(2,1)S(1)}, u32[]{:S(2)}, u32[]{:S(2)}) collective-permute-start(bf16[256,2048]{1,0:T(8,128)(2,1)S(1)} %copy-done.2), channel_id=1, source_target_pairs={{0,1},{1,0},{2,3},{3,2},{4,5},{5,4},{6,7},{7,6},{8,9},{9,8},{10,11... | collective-permute-start | bytes 3145736 | tf_op jit(solution)/shard_map/ppermute | solution.py:402
  17.0 16.2 %collective-permute-start.12 = (bf16[4,32,2048]{2,1,0:T(8,128)(2,1)S(1)}, bf16[4,32,2048]{2,1,0:T(8,128)(2,1)S(1)}, u32[]{:S(2)}, u32[]{:S(2)}) collective-permute-start(bf16[4,32,2048]{2,1,0:T(8,128)(2,1)S(1)} %bitcast.40), channel_id=1, source_target_pairs={{0,8},{8,16},{16,24},{24,0},{1,9},{9,17},{17,25},{25,1},{2,10},{10... | collective-permute-start | bytes 1572872 | tf_op jit(solution)/shard_map/ppermute | solution.py:398
  19.4 24.3 %collective-permute-start.13 = (bf16[4,32,2048]{2,1,0:T(8,128)(2,1)S(1)}, bf16[4,32,2048]{2,1,0:T(8,128)(2,1)S(1)}, u32[]{:S(2)}, u32[]{:S(2)}) collective-permute-start(bf16[4,32,2048]{2,1,0:T(8,128)(2,1)S(1)} %bitcast.39), channel_id=1, source_target_pairs={{0,16},{8,24},{16,0},{24,8},{1,17},{9,25},{17,1},{25,9},{2,18},{10... | collective-permute-start | bytes 1572872 | tf_op jit(solution)/shard_map/ppermute | solution.py:398
  20.9 22.8 %collective-permute-start.14 = (bf16[4,32,2048]{2,1,0:T(8,128)(2,1)S(1)}, bf16[4,32,2048]{2,1,0:T(8,128)(2,1)S(1)}, u32[]{:S(2)}, u32[]{:S(2)}) collective-permute-start(bf16[4,32,2048]{2,1,0:T(8,128)(2,1)S(1)} %bitcast.38), channel_id=1, source_target_pairs={{0,24},{8,0},{16,8},{24,16},{1,25},{9,1},{17,9},{25,17},{2,26},{10... | collective-permute-start | bytes 1572872 | tf_op jit(solution)/shard_map/ppermute | solution.py:398
  21.2 1.4 %collective-permute-start.7 = (bf16[2,384,128]{2,1,0:T(8,128)(2,1)S(1)}, bf16[2,384,128]{2,1,0:T(8,128)(2,1)S(1)}, u32[]{:S(2)}, u32[]{:S(2)}) collective-permute-start(bf16[2,384,128]{2,1,0:T(8,128)(2,1)S(1)} %collective-permute-done.3.refs_13_), channel_id=1, source_target_pairs={{0,1},{1,0},{2,3},{3,2},{4,5},{5,4},{6,7},{7,6},{8,9},{9,8},{10,11... | collective-permute-start | bytes 589832 | tf_op jit(solution)/shard_map/ppermute | solution.py:402
  22.7 1.4 %collective-permute-start.6 = (bf16[2,384,128]{2,1,0:T(8,128)(2,1)S(1)}, bf16[2,384,128]{2,1,0:T(8,128)(2,1)S(1)}, u32[]{:S(2)}, u32[]{:S(2)}) collective-permute-start(bf16[2,384,128]{2,1,0:T(8,128)(2,1)S(1)} %collective-permute-done.2.refs_12_), channel_id=1, source_target_pairs={{0,1},{1,0},{2,3},{3,2},{4,5},{5,4},{6,7},{7,6},{8,9},{9,8},{10,11... | collective-permute-start | bytes 589832 | tf_op jit(solution)/shard_map/ppermute | solution.py:402
  24.1 30.8 %collective-permute-start.15 = (bf16[4,32,2048]{2,1,0:T(8,128)(2,1)S(1)}, bf16[4,32,2048]{2,1,0:T(8,128)(2,1)S(1)}, u32[]{:S(2)}, u32[]{:S(2)}) collective-permute-start(bf16[4,32,2048]{2,1,0:T(8,128)(2,1)S(1)} %bitcast.25), channel_id=1, source_target_pairs={{0,1},{1,0},{2,3},{3,2},{4,5},{5,4},{6,7},{7,6},{8,9},{9,8},{10,11... | collective-permute-start | bytes 1572872 | tf_op jit(solution)/shard_map/ppermute | solution.py:402
  33.2 21.8 %collective-permute-start.16 = (bf16[4,32,2048]{2,1,0:T(8,128)(2,1)S(1)}, bf16[4,32,2048]{2,1,0:T(8,128)(2,1)S(1)}, u32[]{:S(2)}, u32[]{:S(2)}) collective-permute-start(bf16[4,32,2048]{2,1,0:T(8,128)(2,1)S(1)} %collective-permute-done.12.refs_1_), channel_id=1, source_target_pairs={{0,1},{1,0},{2,3},{3,2},{4,5},{5,4},{6,7},{7,6},{8,9},{9,8},{10,11... | collective-permute-start | bytes 1572872 | tf_op jit(solution)/shard_map/ppermute | solution.py:402
  43.8 11.2 %collective-permute-start.17 = (bf16[4,32,2048]{2,1,0:T(8,128)(2,1)S(1)}, bf16[4,32,2048]{2,1,0:T(8,128)(2,1)S(1)}, u32[]{:S(2)}, u32[]{:S(2)}) collective-permute-start(bf16[4,32,2048]{2,1,0:T(8,128)(2,1)S(1)} %collective-permute-done.13.refs_2_), channel_id=1, source_target_pairs={{0,1},{1,0},{2,3},{3,2},{4,5},{5,4},{6,7},{7,6},{8,9},{9,8},{10,11... | collective-permute-start | bytes 1572872 | tf_op jit(solution)/shard_map/ppermute | solution.py:402
  43.8 11.2 %collective-permute-start.18 = (bf16[4,32,2048]{2,1,0:T(8,128)(2,1)S(1)}, bf16[4,32,2048]{2,1,0:T(8,128)(2,1)S(1)}, u32[]{:S(2)}, u32[]{:S(2)}) collective-permute-start(bf16[4,32,2048]{2,1,0:T(8,128)(2,1)S(1)} %collective-permute-done.14.refs_3_), channel_id=1, source_target_pairs={{0,1},{1,0},{2,3},{3,2},{4,5},{5,4},{6,7},{7,6},{8,9},{9,8},{10,11... | collective-permute-start | bytes 1572872 | tf_op jit(solution)/shard_map/ppermute | solution.py:402
  62.4 4.8 %collective-permute-start.19 = (bf16[2,32,2048]{2,1,0:T(8,128)(2,1)S(1)}, bf16[2,32,2048]{2,1,0:T(8,128)(2,1)S(1)}, u32[]{:S(2)}, u32[]{:S(2)}) collective-permute-start(bf16[2,32,2048]{2,1,0:T(8,128)(2,1)S(1)} %get-tuple-element.56), channel_id=1, source_target_pairs={{0,1},{1,0},{2,3},{3,2},{4,5},{5,4},{6,7},{7,6},{8,9},{9,8},{10,11... | collective-permute-start | bytes 786440 | tf_op jit(solution)/shard_map/ppermute | solution.py:402
  66.1 1.7 %collective-permute-start.23 = (bf16[2,32,2048]{2,1,0:T(8,128)(2,1)S(1)}, bf16[2,32,2048]{2,1,0:T(8,128)(2,1)S(1)}, u32[]{:S(2)}, u32[]{:S(2)}) collective-permute-start(bf16[2,32,2048]{2,1,0:T(8,128)(2,1)S(1)} %get-tuple-element.65), channel_id=1, source_target_pairs={{0,1},{1,0},{2,3},{3,2},{4,5},{5,4},{6,7},{7,6},{8,9},{9,8},{10,11... | collective-permute-start | bytes 786440 | tf_op jit(solution)/shard_map/ppermute | solution.py:402
  66.6 1.5 %collective-permute-start.27 = (bf16[2,32,2048]{2,1,0:T(8,128)(2,1)S(1)}, bf16[2,32,2048]{2,1,0:T(8,128)(2,1)S(1)}, u32[]{:S(2)}, u32[]{:S(2)}) collective-permute-start(bf16[2,32,2048]{2,1,0:T(8,128)(2,1)S(1)} %get-tuple-element.69), channel_id=1, source_target_pairs={{0,1},{1,0},{2,3},{3,2},{4,5},{5,4},{6,7},{7,6},{8,9},{9,8},{10,11... | collective-permute-start | bytes 786440 | tf_op jit(solution)/shard_map/ppermute | solution.py:402
  66.7 2.0 %collective-permute-start.20 = (bf16[2,32,2048]{2,1,0:T(8,128)(2,1)S(1)}, bf16[2,32,2048]{2,1,0:T(8,128)(2,1)S(1)}, u32[]{:S(2)}, u32[]{:S(2)}) collective-permute-start(bf16[2,32,2048]{2,1,0:T(8,128)(2,1)S(1)} %get-tuple-element.61), channel_id=1, source_target_pairs={{0,1},{1,0},{2,3},{3,2},{4,5},{5,4},{6,7},{7,6},{8,9},{9,8},{10,11... | collective-permute-start | bytes 786440 | tf_op jit(solution)/shard_map/ppermute | solution.py:402
  67.2 3.4 %collective-permute-start.31 = (bf16[2,32,2048]{2,1,0:T(8,128)(2,1)S(1)}, bf16[2,32,2048]{2,1,0:T(8,128)(2,1)S(1)}, u32[]{:S(2)}, u32[]{:S(2)}) collective-permute-start(bf16[2,32,2048]{2,1,0:T(8,128)(2,1)S(1)} %get-tuple-element.73), channel_id=1, source_target_pairs={{0,1},{1,0},{2,3},{3,2},{4,5},{5,4},{6,7},{7,6},{8,9},{9,8},{10,11... | collective-permute-start | bytes 786440 | tf_op jit(solution)/shard_map/ppermute | solution.py:402
  67.2 4.5 %collective-permute-start.21 = (bf16[2,32,2048]{2,1,0:T(8,128)(2,1)S(1)}, bf16[2,32,2048]{2,1,0:T(8,128)(2,1)S(1)}, u32[]{:S(2)}, u32[]{:S(2)}) collective-permute-start(bf16[2,32,2048]{2,1,0:T(8,128)(2,1)S(1)} %get-tuple-element.63), channel_id=1, source_target_pairs={{0,1},{1,0},{2,3},{3,2},{4,5},{5,4},{6,7},{7,6},{8,9},{9,8},{10,11... | collective-permute-start | bytes 786440 | tf_op jit(solution)/shard_map/ppermute | solution.py:402
  67.8 4.0 %collective-permute-start.25 = (bf16[2,32,2048]{2,1,0:T(8,128)(2,1)S(1)}, bf16[2,32,2048]{2,1,0:T(8,128)(2,1)S(1)}, u32[]{:S(2)}, u32[]{:S(2)}) collective-permute-start(bf16[2,32,2048]{2,1,0:T(8,128)(2,1)S(1)} %get-tuple-element.67), channel_id=1, source_target_pairs={{0,1},{1,0},{2,3},{3,2},{4,5},{5,4},{6,7},{7,6},{8,9},{9,8},{10,11... | collective-permute-start | bytes 786440 | tf_op jit(solution)/shard_map/ppermute | solution.py:402
  68.2 6.6 %collective-permute-start.29 = (bf16[2,32,2048]{2,1,0:T(8,128)(2,1)S(1)}, bf16[2,32,2048]{2,1,0:T(8,128)(2,1)S(1)}, u32[]{:S(2)}, u32[]{:S(2)}) collective-permute-start(bf16[2,32,2048]{2,1,0:T(8,128)(2,1)S(1)} %get-tuple-element.71), channel_id=1, source_target_pairs={{0,1},{1,0},{2,3},{3,2},{4,5},{5,4},{6,7},{7,6},{8,9},{9,8},{10,11... | collective-permute-start | bytes 786440 | tf_op jit(solution)/shard_map/ppermute | solution.py:402
  68.7 9.2 %collective-permute-start.24 = (bf16[2,32,2048]{2,1,0:T(8,128)(2,1)S(1)}, bf16[2,32,2048]{2,1,0:T(8,128)(2,1)S(1)}, u32[]{:S(2)}, u32[]{:S(2)}) collective-permute-start(bf16[2,32,2048]{2,1,0:T(8,128)(2,1)S(1)} %add.139), channel_id=1, source_target_pairs={{0,24},{8,0},{16,8},{24,16},{1,25},{9,1},{17,9},{25,17},{2,26},{10... | collective-permute-start | bytes 786440 | tf_op jit(solution)/shard_map/ppermute | solution.py:398
  70.6 14.8 %collective-permute-start.28 = (bf16[2,32,2048]{2,1,0:T(8,128)(2,1)S(1)}, bf16[2,32,2048]{2,1,0:T(8,128)(2,1)S(1)}, u32[]{:S(2)}, u32[]{:S(2)}) collective-permute-start(bf16[2,32,2048]{2,1,0:T(8,128)(2,1)S(1)} %add.141), channel_id=1, source_target_pairs={{0,16},{8,24},{16,0},{24,8},{1,17},{9,25},{17,1},{25,9},{2,18},{10... | collective-permute-start | bytes 786440 | tf_op jit(solution)/shard_map/ppermute | solution.py:398
  71.7 14.3 %collective-permute-start.32 = (bf16[2,32,2048]{2,1,0:T(8,128)(2,1)S(1)}, bf16[2,32,2048]{2,1,0:T(8,128)(2,1)S(1)}, u32[]{:S(2)}, u32[]{:S(2)}) collective-permute-start(bf16[2,32,2048]{2,1,0:T(8,128)(2,1)S(1)} %add.143), channel_id=1, source_target_pairs={{0,8},{8,16},{16,24},{24,0},{1,9},{9,17},{17,25},{25,1},{2,10},{10... | collective-permute-start | bytes 786440 | tf_op jit(solution)/shard_map/ppermute | solution.py:398
  71.9 17.4 %collective-permute-start.22 = (bf16[2,32,2048]{2,1,0:T(8,128)(2,1)S(1)}, bf16[2,32,2048]{2,1,0:T(8,128)(2,1)S(1)}, u32[]{:S(2)}, u32[]{:S(2)}) collective-permute-start(bf16[2,32,2048]{2,1,0:T(8,128)(2,1)S(1)} %add.138), channel_id=1, source_target_pairs={{0,24},{8,0},{16,8},{24,16},{1,25},{9,1},{17,9},{25,17},{2,26},{10... | collective-permute-start | bytes 786440 | tf_op jit(solution)/shard_map/ppermute | solution.py:398
  74.8 26.2 %collective-permute-start.9 = (bf16[96,2048]{1,0:T(8,128)(2,1)S(1)}, bf16[96,2048]{1,0:T(8,128)(2,1)S(1)}, u32[]{:S(2)}, u32[]{:S(2)}) collective-permute-start(bf16[96,2048]{1,0:T(8,128)(2,1)S(1)} %get-tuple-element.44), channel_id=1, source_target_pairs={{0,2},{2,4},{4,6},{6,0},{1,3},{3,5},{5,7},{7,1},{8,10},{10,12},{12... | collective-permute-start | bytes 1179656 | tf_op jit(solution)/shard_map/ppermute | solution.py:398
  77.9 17.6 %collective-permute-start.26 = (bf16[2,32,2048]{2,1,0:T(8,128)(2,1)S(1)}, bf16[2,32,2048]{2,1,0:T(8,128)(2,1)S(1)}, u32[]{:S(2)}, u32[]{:S(2)}) collective-permute-start(bf16[2,32,2048]{2,1,0:T(8,128)(2,1)S(1)} %add.140), channel_id=1, source_target_pairs={{0,16},{8,24},{16,0},{24,8},{1,17},{9,25},{17,1},{25,9},{2,18},{10... | collective-permute-start | bytes 786440 | tf_op jit(solution)/shard_map/ppermute | solution.py:398
  85.4 10.2 %collective-permute-start.30 = (bf16[2,32,2048]{2,1,0:T(8,128)(2,1)S(1)}, bf16[2,32,2048]{2,1,0:T(8,128)(2,1)S(1)}, u32[]{:S(2)}, u32[]{:S(2)}) collective-permute-start(bf16[2,32,2048]{2,1,0:T(8,128)(2,1)S(1)} %add.142), channel_id=1, source_target_pairs={{0,8},{8,16},{16,24},{24,0},{1,9},{9,17},{17,25},{25,1},{2,10},{10... | collective-permute-start | bytes 786440 | tf_op jit(solution)/shard_map/ppermute | solution.py:398
  86.0 22.4 %collective-permute-start.10 = (bf16[96,2048]{1,0:T(8,128)(2,1)S(1)}, bf16[96,2048]{1,0:T(8,128)(2,1)S(1)}, u32[]{:S(2)}, u32[]{:S(2)}) collective-permute-start(bf16[96,2048]{1,0:T(8,128)(2,1)S(1)} %get-tuple-element.45), channel_id=1, source_target_pairs={{0,4},{2,6},{4,0},{6,2},{1,5},{3,7},{5,1},{7,3},{8,12},{10,14},{12... | collective-permute-start | bytes 1179656 | tf_op jit(solution)/shard_map/ppermute | solution.py:398
  89.2 23.0 %collective-permute-start.11 = (bf16[96,2048]{1,0:T(8,128)(2,1)S(1)}, bf16[96,2048]{1,0:T(8,128)(2,1)S(1)}, u32[]{:S(2)}, u32[]{:S(2)}) collective-permute-start(bf16[96,2048]{1,0:T(8,128)(2,1)S(1)} %get-tuple-element.46), channel_id=1, source_target_pairs={{0,6},{2,0},{4,2},{6,4},{1,7},{3,1},{5,3},{7,5},{8,14},{10,8},{12,... | collective-permute-start | bytes 1179656 | tf_op jit(solution)/shard_map/ppermute | solution.py:398
  96.8 16.3 %collective-permute-start.33 = (bf16[48,2048]{1,0:T(8,128)(2,1)S(1)}, bf16[48,2048]{1,0:T(8,128)(2,1)S(1)}, u32[]{:S(2)}, u32[]{:S(2)}) collective-permute-start(bf16[48,2048]{1,0:T(8,128)(2,1)S(1)} %get-tuple-element.75), channel_id=1, source_target_pairs={{0,2},{2,4},{4,6},{6,0},{1,3},{3,5},{5,7},{7,1},{8,10},{10,12},{12... | collective-permute-start | bytes 589832 | tf_op jit(solution)/shard_map/ppermute | solution.py:398
  98.4 27.7 %collective-permute-start.34 = (bf16[48,2048]{1,0:T(8,128)(2,1)S(1)}, bf16[48,2048]{1,0:T(8,128)(2,1)S(1)}, u32[]{:S(2)}, u32[]{:S(2)}) collective-permute-start(bf16[48,2048]{1,0:T(8,128)(2,1)S(1)} %get-tuple-element.76), channel_id=1, source_target_pairs={{0,4},{2,6},{4,0},{6,2},{1,5},{3,7},{5,1},{7,3},{8,12},{10,14},{12... | collective-permute-start | bytes 589832 | tf_op jit(solution)/shard_map/ppermute | solution.py:398
  101.0 25.1 %collective-permute-start.35 = (bf16[48,2048]{1,0:T(8,128)(2,1)S(1)}, bf16[48,2048]{1,0:T(8,128)(2,1)S(1)}, u32[]{:S(2)}, u32[]{:S(2)}) collective-permute-start(bf16[48,2048]{1,0:T(8,128)(2,1)S(1)} %get-tuple-element.77), channel_id=1, source_target_pairs={{0,6},{2,0},{4,2},{6,4},{1,7},{3,1},{5,3},{7,5},{8,14},{10,8},{12,... | collective-permute-start | bytes 589832 | tf_op jit(solution)/shard_map/ppermute | solution.py:398

commit v5 on v4

--- a/solution.py
+++ b/solution.py
@@ -17,6 +17,7 @@
 CORES = 2
 IN_VMEM = pl.BlockSpec(memory_space=pltpu.VMEM)
 IN_SMEM = pl.BlockSpec(memory_space=pltpu.SMEM)
+SPLIT = 2
 KEY_CHUNK = 1024
 MIB = 1024 * 1024
 
@@ -117,16 +118,32 @@
     )(*arrays)
 
 
+def weight_copies(sources, targets, first, sems, sem):
+    copies = []
+    for source, target in zip(sources, targets):
+        per, rows, _ = target.shape
+        cut = rows // SPLIT
+        for expert in range(per):
+            for n in range(SPLIT):
+                part = pl.ds(n * cut, cut)
+                copies.append(
+                    pltpu.make_async_copy(
+                        source.at[first + expert, part], target.at[expert, part], sems.at[sem]
+                    )
+                )
+                sem += 1
+    return copies
+
+
 def mix_kernel(n_pieces, n_z, z_ref, q_own, q_other, gain_hbm, cos_ref, sin_ref, w_other, *rest):
-    sources = [gain_hbm, rest[0], *[w.at[pl.ds(0, o.shape[0])] for w, o in zip(
-        rest[1:4], rest[4 + n_pieces + n_z : 7 + n_pieces + n_z])]]
     pieces = rest[4 : 4 + n_pieces]
     outs = rest[4 + n_pieces : 4 + n_pieces + n_z]
     loaded = rest[4 + n_pieces + n_z : 7 + n_pieces + n_z]
     keys_ref, vals_ref, mixed_ref, w_own, gain_ref, sems = rest[7 + n_pieces + n_z :]
     copies = [
-        pltpu.make_async_copy(source, target, sems.at[n])
-        for n, (source, target) in enumerate(zip(sources, (gain_ref, w_own, *loaded)))
+        pltpu.make_async_copy(gain_hbm, gain_ref, sems.at[0]),
+        pltpu.make_async_copy(rest[0], w_own, sems.at[1]),
+        *weight_copies(rest[1:4], loaded, 0, sems, 2),
     ]
     for copy in copies:
         copy.start()
@@ -148,7 +165,7 @@
     copies[1].wait()
 
     def one(n, carry):
-        block = lax.rem(z_ref[0] + n, n_z)
+        block = peer(z_ref[0], n, n_z)
         at = pl.multiple_of(block * part, 16)
         cosine, sine = cos_ref[pl.ds(at, part)], sin_ref[pl.ds(at, part)]
         queries = []
@@ -215,7 +232,7 @@
             pltpu.VMEM((n_z, part, d_model), BF16),
             pltpu.VMEM(w_own.shape, BF16),
             pltpu.VMEM(gain.shape, F32),
-            pltpu.SemaphoreType.DMA((5,)),
+            pltpu.SemaphoreType.DMA((2 + 3 * per * SPLIT,)),
         ],
         compiler_params=pltpu.CompilerParams(vmem_limit_bytes=20 * MIB),
         name="mix",
@@ -234,9 +251,9 @@
 
 
 def dispatch_kernel(
-    n_ep, n_local, core_ref, ep_ref, tokens_ref, gain_ref, routes_ref, weight_ref, *rest
+    n_ep, n_local, per, core_ref, ep_ref, tokens_ref, gain_ref, routes_ref, weight_ref, *rest
 ):
-    out_refs, cols_ref = rest[:n_ep], rest[n_ep]
+    out_refs, cols_ref = rest[:-1], rest[-1]
     n_z, _, block, d_model = tokens_ref.shape
     rows, local_rows = n_z * block, routes_ref.shape[1]
     iota = lambda shape, dim: lax.broadcasted_iota(jnp.int32, shape, dim)
@@ -262,9 +279,14 @@
     earlier = ((above < across) & (above >= first)).astype(F32).astype(BF16)
     count = jnp.dot(either.astype(F32).astype(BF16), earlier, preferred_element_type=F32)
     owner = block_of(expert, n_local, n_ep)
-    ahead = owner - ep_ref[0]
-    ahead = jnp.where(ahead < 0, ahead + n_ep, ahead)
-    place = (ahead * n_local + expert - owner * n_local) * (n_z * CAP)
+    if n_ep & (n_ep - 1) == 0:
+        ahead = owner ^ ep_ref[0]
+    else:
+        ahead = owner - ep_ref[0]
+        ahead = jnp.where(ahead < 0, ahead + n_ep, ahead)
+    local = expert - owner * n_local
+    turn = block_of(local, per, n_local // per)
+    place = ((turn * n_ep + ahead) * per + local - turn * per) * (n_z * CAP)
     place = place + block_of(iota(shape, 1), block, n_z) * CAP + (count + 0.5).astype(jnp.int32)
     slots = [jnp.sum(jnp.where(h, place, 0), axis=0, keepdims=True) for h in hot]
 
@@ -290,13 +312,14 @@
         out_ref[...] = jnp.dot(picked, normed, preferred_element_type=F32).astype(BF16)
 
 
-def dispatch(core, ep, tokens, gain, routes, weight, n_z, n_ep, n_local):
+def dispatch(core, ep, tokens, gain, routes, weight, n_z, n_ep, n_local, per):
     local_rows, d_model = tokens.shape
     block = local_rows // (n_z * CORES)
-    n_slots = n_local * n_z * CAP
+    n_slots = per * n_z * CAP
+    n_out = n_ep * (n_local // per)
     whole = lambda a: pl.BlockSpec(a.shape, lambda i, c, e: (0,) * a.ndim)
     outs = pl.pallas_call(
-        lambda *refs: dispatch_kernel(n_ep, n_local, *refs),
+        lambda *refs: dispatch_kernel(n_ep, n_local, per, *refs),
         grid_spec=pltpu.PrefetchScalarGridSpec(
             num_scalar_prefetch=2,
             grid=(1,),
@@ -306,14 +329,14 @@
                 whole(routes),
                 whole(weight),
             ],
-            out_specs=[IN_VMEM] * (n_ep + 1),
+            out_specs=[IN_VMEM] * (n_out + 1),
         ),
-        out_shape=[jax.ShapeDtypeStruct((n_slots, d_model), BF16)] * n_ep
+        out_shape=[jax.ShapeDtypeStruct((n_slots, d_model), BF16)] * n_out
         + [jax.ShapeDtypeStruct((n_z * block, 8), F32)],
         compiler_params=pltpu.CompilerParams(vmem_limit_bytes=16 * MIB),
         name="dispatch",
-    )(core, ep, *in_hbm([tokens.reshape(n_z, CORES, block, d_model), gain]), routes, weight)
-    return outs[:n_ep], outs[n_ep]
+    )(core, ep, *in_hbm([tokens.reshape(n_z, CORES, block, d_model), gain, routes, weight]))
+    return outs[:n_out], outs[n_out]
 
 
 def expert_kernel(n_in, group, first, n_next, *refs):
@@ -322,15 +345,12 @@
     per, rows, _ = outs[0].shape
     copies = []
     if n_next:
-        targets, sems = refs[2 * n_in + 3 + n_next : -1], refs[-1]
-        for n, (source, target) in enumerate(zip(sources, targets)):
-            part = source.at[pl.ds(first + per, per)]
-            copies.append(pltpu.make_async_copy(part, target, sems.at[n]))
+        copies = weight_copies(sources, refs[2 * n_in + 3 + n_next : -1], first + per, refs[-1], 0)
     for copy in copies:
         copy.start()
     for expert in range(per):
         for start in range(0, len(ins), group):
-            field = [ref[first + expert] for ref in ins[start : start + group]]
+            field = [ref[expert] for ref in ins[start : start + group]]
             field = jnp.concatenate(field, axis=0)
             gate = jnp.dot(field, gate_ref[expert], preferred_element_type=F32)
             up = jnp.dot(field, up_ref[expert], preferred_element_type=F32)
@@ -354,7 +374,7 @@
         out_specs=[IN_VMEM] * (len(pieces) + len(more)),
         out_shape=[jax.ShapeDtypeStruct((per, rows, d_model), BF16)] * len(pieces)
         + [jax.ShapeDtypeStruct((per, *w.shape[1:]), BF16) for w in more],
-        scratch_shapes=[pltpu.SemaphoreType.DMA((len(more),))] if more else [],
+        scratch_shapes=[pltpu.SemaphoreType.DMA((3 * per * SPLIT,))] if more else [],
         compiler_params=pltpu.CompilerParams(vmem_limit_bytes=16 * MIB),
         name="experts",
     )(*pieces, *weights, *more)
@@ -377,7 +397,7 @@
     total_ref[...] = (both[:rows] + both[rows:]).reshape(total_ref.shape)
     n_z = len(out_refs)
     for n, out_ref in enumerate(out_refs):
-        out_ref[...] = total_ref[lax.rem(z_ref[0] + n, n_z)].astype(BF16)
+        out_ref[...] = total_ref[peer(z_ref[0], n, n_z)].astype(BF16)
 
 
 def combine(z_index, cols, backs, n_z):
@@ -393,9 +413,17 @@
     )(z_index, cols, *backs)
 
 
-def shift(a, axis, step):
+def peer(own, step, n):
+    return own ^ step if n & (n - 1) == 0 else lax.rem(own + step, n)
+
+
+def shift(a, axis, step, back=False):
     n = lax.axis_size(axis)
-    return lax.ppermute(a, axis, [(i, (i + step) % n) for i in range(n)])
+    if n & (n - 1) == 0:
+        pairs = [(i, i ^ step) for i in range(n)]
+    else:
+        pairs = [(i, (i - step if back else i + step) % n) for i in range(n)]
+    return lax.ppermute(a, axis, pairs)
 
 
 def swap_cores(a):
@@ -450,13 +478,16 @@
     per = n_local // chunks
     ep_arg = lax.axis_index("ep").reshape(1).astype(jnp.int32)
     outgoing, cols = dispatch(
-        core_arg, ep_arg, tokens_b, norm_gain[None], routes.T, route_weight.T, n_z, n_ep, n_local
-    )
-    here = []
-    for step in range(n_ep):
-        piece = outgoing[step].reshape(n_local, n_z * CAP, d_model)
-        here.append(shift(piece, "ep", step) if step else piece)
-    there = [swap_cores(p) for p in here]
+        core_arg, ep_arg, tokens_b, norm_gain[None], routes.T, route_weight.T, n_z, n_ep, n_local,
+        per,
+    )
+    arrived = []
+    for chunk in range(chunks):
+        here = []
+        for step in range(n_ep):
+            piece = outgoing[chunk * n_ep + step].reshape(per, n_z * CAP, d_model)
+            here.append(shift(piece, "ep", step) if step else piece)
+        arrived.append((here, [swap_cores(p) for p in here]))
 
     all_weights = [gate_weight, up_weight, down_weight]
     mixed, weights = mix(
@@ -468,14 +499,14 @@
         gathered.append(shift(mixed[step], "z", step))
     mixed_out = add(*gathered)
 
-    backs = [[] for _ in range(n_ep)]
+    backs = []
     for chunk in range(chunks):
-        keep, send, weights = experts(here, there, weights, chunk * per, all_weights)
+        keep, send, weights = experts(*arrived[chunk], weights, chunk * per, all_weights)
         for step in range(n_ep):
             result = add(keep[step], swap_cores(send[step]))
-            result = shift(result, "ep", n_ep - step) if step else result
-            backs[step].append(result.reshape(-1, d_model))
-    rows = combine(z_arg, cols, [b for step in backs for b in step], n_z)
+            result = shift(result, "ep", step, back=True) if step else result
+            backs.append(result.reshape(-1, d_model))
+    rows = combine(z_arg, cols, backs, n_z)
     gathered = [rows[0]]
     for step in range(1, n_z):
         gathered.append(shift(rows[step], "z", step))

time: 129 us -> 139 us (1.078)
  waiting for transfers between devices: 60.5 us -> 67.1 us
  starting transfers between devices: 34 us -> 38.3 us
    ppermute x18 -> x21, waiting for transfers between devices: 57.6 us -> 66 us  [shift(): return lax.ppermute(a, axis, pairs)]
    ppermute x18 -> x21, starting transfers between devices: 29.7 us -> 33.1 us  [shift(): return lax.ppermute(a, axis, pairs)]
    ppermute x18 -> x22, waiting for transfers between devices: 2.92 us -> 1.09 us  [swap_cores(): return lax.ppermute(a, 'core', [(i, CORES - 1 - i) for i in range(CORES)])]
    ppermute x18 -> x22, starting transfers between devices: 4.27 us -> 5.19 us  [swap_cores(): return lax.ppermute(a, 'core', [(i, CORES - 1 - i) for i in range(CORES)])]
  transfers between devices with their start and end apart: 36 -> 43, of which waited for: 13 -> 17; matrix products, arithmetic and copies ran while one was open for 0% -> 0% of each run, Pallas kernels for 15% -> 20%
where the time goes in v5:
time: 139 us; the launch traced here: 137 us
  waiting for transfers between devices  67.1 us (48%)
  starting transfers between devices  38.3 us (28%)
  Pallas kernels  29.7 us (21%)
    ppermute x21, waiting for transfers between devices, shift(): return lax.ppermute(a, axis, pairs)  66 us
    ppermute x21, starting transfers between devices, shift(): return lax.ppermute(a, axis, pairs)  33.1 us
    pallas_call x2, Pallas kernels, experts(): pl.pallas_call(lambda *refs: expert_kernel(len(pieces), group, first, len...  11.3 us
    pallas_call x1, Pallas kernels, mix(): pl.pallas_call(lambda *refs: mix_kernel(len(pieces), n_z, *refs), in_spec...  10.7 us
    ppermute x22, starting transfers between devices, swap_cores(): return lax.ppermute(a, 'core', [(i, CORES - 1 - i) for i in range(CORES)])  5.19 us
    pallas_call x1, Pallas kernels, dispatch(): pl.pallas_call(lambda *refs: dispatch_kernel(n_ep, n_local, per, *refs),...  2.84 us
  transfers between devices with their start and end apart: 43, of which 17 were waited for; matrix products, arithmetic and copies ran while one was open for 0% of the time, Pallas kernels for 20%

profile of v5, /device:TPU:0, one launch (start us, length us, event | category | flops | bytes accessed | tf_op | source)
XLA Modules:
  0.0 136.9 jit_solution(993138854860463971)
XLA Ops:
  0.9 0.8 sine_multiply_fusion
  1.7 1.4 %prepare.1 = (bf16[2,384,128]{2,1,0:T(8,128)(2,1)S(1)}, bf16[4,96,256]{2,1,0:T(8,128)(2,1)S(1)}, bf16[4,96,256]{2,1,0:T(8,128)(2,1)S(1)}) custom-call(s32[1]{0:T(128)} %bitcast.1.core_ref.refs_0_, s32[1]{0:T(128)} %bitcast.2.head_ref, bf16[4,2,96,512]{3,2,1,0:T(8,128)(2,1)} %bitcast.50, bf16[4,2,96,512]{3,2,1,0:T(8,128)(2,1)} %bitcast.51, ...), custom_call_target="tpu_custom_call" | custom-call | tf_op jit(solution)/shard_map/prepare/pallas_call | solution.py:74
  3.1 0.6 collective-permute-start
  3.7 2.6 %collective-permute-start.2 = (bf16[2,384,128]{2,1,0:T(8,128)(2,1)S(1)}, bf16[2,384,128]{2,1,0:T(8,128)(2,1)S(1)}, u32[]{:S(2)}, u32[]{:S(2)}) collective-permute-start(bf16[2,384,128]{2,1,0:T(8,128)(2,1)S(1)} %get-tuple-element.46.refs_11_), channel_id=1, source_target_pairs={{0,8},{8,0},{16,24},{24,16},{1,9},{9,1},{17,25},{25,17},{2,10},{10... | collective-permute-start | bytes 589832 | tf_op jit(solution)/shard_map/ppermute | solution.py:426
  6.2 1.5 %collective-permute-start.3 = (bf16[2,384,128]{2,1,0:T(8,128)(2,1)S(1)}, bf16[2,384,128]{2,1,0:T(8,128)(2,1)S(1)}, u32[]{:S(2)}, u32[]{:S(2)}) collective-permute-start(bf16[2,384,128]{2,1,0:T(8,128)(2,1)S(1)} %get-tuple-element.46.refs_11_), channel_id=1, source_target_pairs={{0,16},{8,24},{16,0},{24,8},{1,17},{9,25},{17,1},{25,9},{2,18},{10... | collective-permute-start | bytes 589832 | tf_op jit(solution)/shard_map/ppermute | solution.py:426
  7.8 0.5 collective-permute-start.5
  8.3 2.8 %dispatch.1 = (bf16[64,2048]{1,0:T(8,128)(2,1)S(1)}, bf16[64,2048]{1,0:T(8,128)(2,1)S(1)}, bf16[64,2048]{1,0:T(8,128)(2,1)S(1)}, bf16[64,2048]{1,0:T(8,128)(2,1)...) custom-call(s32[1]{0:T(128)} %bitcast.1.core_ref.refs_0_, ...), custom_call_target="tpu_custom_call" | custom-call | tf_op jit(solution)/shard_map/dispatch/pallas_call | solution.py:321
  11.1 0.8 collective-permute-done.2.refs_12_
  12.0 2.0 %collective-permute-start.12 = (bf16[2,32,2048]{2,1,0:T(8,128)(2,1)S(1)}, bf16[2,32,2048]{2,1,0:T(8,128)(2,1)S(1)}, u32[]{:S(2)}, u32[]{:S(2)}) collective-permute-start(bf16[2,32,2048]{2,1,0:T(8,128)(2,1)S(1)} %bitcast.46), channel_id=1, source_target_pairs={{0,8},{8,0},{16,24},{24,16},{1,9},{9,1},{17,25},{25,17},{2,10},{10... | collective-permute-start | bytes 786440 | tf_op jit(solution)/shard_map/ppermute | solution.py:426
  14.0 3.1 %collective-permute-done.3.refs_13_ = bf16[2,384,128]{2,1,0:T(8,128)(2,1)S(1)} collective-permute-done((bf16[2,384,128]{2,1,0:T(8,128)(2,1)S(1)}, bf16[2,384,128]{2,1,0:T(8,128)(2,1)S(1)}, u32[]{:S(2)}, u32[]{:S(2)}) %collective-permute-start.3) | collective-permute-done | bytes 196640 | tf_op jit(solution)/shard_map/ppermute | solution.py:426
  17.1 1.9 %collective-permute-start.13 = (bf16[2,32,2048]{2,1,0:T(8,128)(2,1)S(1)}, bf16[2,32,2048]{2,1,0:T(8,128)(2,1)S(1)}, u32[]{:S(2)}, u32[]{:S(2)}) collective-permute-start(bf16[2,32,2048]{2,1,0:T(8,128)(2,1)S(1)} %bitcast.45), channel_id=1, source_target_pairs={{0,16},{8,24},{16,0},{24,8},{1,17},{9,25},{17,1},{25,9},{2,18},{10... | collective-permute-start | bytes 786440 | tf_op jit(solution)/shard_map/ppermute | solution.py:426
  19.2 2.7 %collective-permute-done.12.refs_1_ = bf16[2,32,2048]{2,1,0:T(8,128)(2,1)S(1)} collective-permute-done((bf16[2,32,2048]{2,1,0:T(8,128)(2,1)S(1)}, bf16[2,32,2048]{2,1,0:T(8,128)(2,1)S(1)}, u32[]{:S(2)}, u32[]{:S(2)}) %collective-permute-start.12) | collective-permute-done | bytes 262176 | tf_op jit(solution)/shard_map/ppermute | solution.py:426
  21.8 2.0 %collective-permute-start.26 = (bf16[2,32,2048]{2,1,0:T(8,128)(2,1)S(1)}, bf16[2,32,2048]{2,1,0:T(8,128)(2,1)S(1)}, u32[]{:S(2)}, u32[]{:S(2)}) collective-permute-start(bf16[2,32,2048]{2,1,0:T(8,128)(2,1)S(1)} %bitcast.43), channel_id=1, source_target_pairs={{0,8},{8,0},{16,24},{24,16},{1,9},{9,1},{17,25},{25,17},{2,10},{10... | collective-permute-start | bytes 786440 | tf_op jit(solution)/shard_map/ppermute | solution.py:426
  23.9 6.4 %collective-permute-done.13.refs_2_ = bf16[2,32,2048]{2,1,0:T(8,128)(2,1)S(1)} collective-permute-done((bf16[2,32,2048]{2,1,0:T(8,128)(2,1)S(1)}, bf16[2,32,2048]{2,1,0:T(8,128)(2,1)S(1)}, u32[]{:S(2)}, u32[]{:S(2)}) %collective-permute-start.13) | collective-permute-done | bytes 262176 | tf_op jit(solution)/shard_map/ppermute | solution.py:426
  30.3 1.7 %collective-permute-start.27 = (bf16[2,32,2048]{2,1,0:T(8,128)(2,1)S(1)}, bf16[2,32,2048]{2,1,0:T(8,128)(2,1)S(1)}, u32[]{:S(2)}, u32[]{:S(2)}) collective-permute-start(bf16[2,32,2048]{2,1,0:T(8,128)(2,1)S(1)} %bitcast.42), channel_id=1, source_target_pairs={{0,16},{8,24},{16,0},{24,8},{1,17},{9,25},{17,1},{25,9},{2,18},{10... | collective-permute-start | bytes 786440 | tf_op jit(solution)/shard_map/ppermute | solution.py:426
  32.1 1.1 collective-permute-done.26.refs_1_
  33.2 9.3 %collective-permute-done.27.refs_2_ = bf16[2,32,2048]{2,1,0:T(8,128)(2,1)S(1)} collective-permute-done((bf16[2,32,2048]{2,1,0:T(8,128)(2,1)S(1)}, bf16[2,32,2048]{2,1,0:T(8,128)(2,1)S(1)}, u32[]{:S(2)}, u32[]{:S(2)}) %collective-permute-start.27) | collective-permute-done | bytes 262176 | tf_op jit(solution)/shard_map/ppermute | solution.py:426
  42.6 0.5 collective-permute-start.16
  43.1 0.4 collective-permute-start.18
  43.6 0.4 collective-permute-done.8.refs_18_
  45.3 10.7 %mix.1 = (bf16[96,2048]{1,0:T(8,128)(2,1)S(1)}, bf16[96,2048]{1,0:T(8,128)(2,1)S(1)}, bf16[96,2048]{1,0:T(8,128)(2,1)S(1)}, bf16[96,2048]{1,0:T(8,128)(2,1)S(1)}...) custom-call(s32[1]{0:T(128)} %bitcast.refs_0_, ...), custom_call_target="tpu_custom_call" | custom-call | tf_op jit(solution)/shard_map/mix/pallas_call | solution.py:221
  56.0 7.6 %experts.2 = (bf16[2,32,2048]{2,1,0:T(8,128)(2,1)S(1)}, bf16[2,32,2048]{2,1,0:T(8,128)(2,1)S(1)}, bf16[2,32,2048]{2,1,0:T(8,128)(2,1)S(1)}, bf16[2,32,2048]{2,1,...) custom-call(bf16[2,32,2048]{2,1,0:T(8,128)(2,1)S(1)} %bitcast.34, ...), custom_call_target="tpu_custom_call" | custom-call | tf_op jit(solution)/shard_map/experts/pallas_call | solution.py:371
  63.7 0.3 collective-permute-start.19
  64.0 0.3 collective-permute-start.20
  64.5 0.3 collective-permute-start.24
  64.8 3.6 %experts.3 = (bf16[2,32,2048]{2,1,0:T(8,128)(2,1)S(1)}, bf16[2,32,2048]{2,1,0:T(8,128)(2,1)S(1)}, bf16[2,32,2048]{2,1,0:T(8,128)(2,1)S(1)}, bf16[2,32,2048]{2,1,...) custom-call(bf16[2,32,2048]{2,1,0:T(8,128)(2,1)S(1)} %bitcast.32, ...), custom_call_target="tpu_custom_call" | custom-call | tf_op jit(solution)/shard_map/experts/pallas_call | solution.py:371
  68.4 0.3 collective-permute-start.33
  68.7 0.3 collective-permute-start.34
  70.0 1.7 %collective-permute-start.23 = (bf16[2,32,2048]{2,1,0:T(8,128)(2,1)S(1)}, bf16[2,32,2048]{2,1,0:T(8,128)(2,1)S(1)}, u32[]{:S(2)}, u32[]{:S(2)}) collective-permute-start(bf16[2,32,2048]{2,1,0:T(8,128)(2,1)S(1)} %add.138), channel_id=1, source_target_pairs={{0,16},{8,24},{16,0},{24,8},{1,17},{9,25},{17,1},{25,9},{2,18},{10... | collective-permute-start | bytes 786440 | tf_op jit(solution)/shard_map/ppermute | solution.py:426
  71.8 1.5 %collective-permute-start.25 = (bf16[2,32,2048]{2,1,0:T(8,128)(2,1)S(1)}, bf16[2,32,2048]{2,1,0:T(8,128)(2,1)S(1)}, u32[]{:S(2)}, u32[]{:S(2)}) collective-permute-start(bf16[2,32,2048]{2,1,0:T(8,128)(2,1)S(1)} %add.139), channel_id=1, source_target_pairs={{0,24},{8,16},{16,8},{24,0},{1,25},{9,17},{17,9},{25,1},{2,26},{10... | collective-permute-start | bytes 786440 | tf_op jit(solution)/shard_map/ppermute | solution.py:426
  73.4 0.4 collective-permute-start.35
  73.8 1.3 collective-permute-start.9
  75.2 3.6 %collective-permute-done.21 = bf16[2,32,2048]{2,1,0:T(8,128)(2,1)S(1)} collective-permute-done((bf16[2,32,2048]{2,1,0:T(8,128)(2,1)S(1)}, bf16[2,32,2048]{2,1,0:T(8,128)(2,1)S(1)}, u32[]{:S(2)}, u32[]{:S(2)}) %collective-permute-start.21) | collective-permute-done | bytes 262176 | tf_op jit(solution)/shard_map/ppermute | solution.py:426
  78.9 1.7 %collective-permute-start.37 = (bf16[2,32,2048]{2,1,0:T(8,128)(2,1)S(1)}, bf16[2,32,2048]{2,1,0:T(8,128)(2,1)S(1)}, u32[]{:S(2)}, u32[]{:S(2)}) collective-permute-start(bf16[2,32,2048]{2,1,0:T(8,128)(2,1)S(1)} %add.142), channel_id=1, source_target_pairs={{0,16},{8,24},{16,0},{24,8},{1,17},{9,25},{17,1},{25,9},{2,18},{10... | collective-permute-start | bytes 786440 | tf_op jit(solution)/shard_map/ppermute | solution.py:426
  80.6 2.9 %collective-permute-done.23 = bf16[2,32,2048]{2,1,0:T(8,128)(2,1)S(1)} collective-permute-done((bf16[2,32,2048]{2,1,0:T(8,128)(2,1)S(1)}, bf16[2,32,2048]{2,1,0:T(8,128)(2,1)S(1)}, u32[]{:S(2)}, u32[]{:S(2)}) %collective-permute-start.23) | collective-permute-done | bytes 262176 | tf_op jit(solution)/shard_map/ppermute | solution.py:426
  83.5 4.2 %collective-permute-start.39 = (bf16[2,32,2048]{2,1,0:T(8,128)(2,1)S(1)}, bf16[2,32,2048]{2,1,0:T(8,128)(2,1)S(1)}, u32[]{:S(2)}, u32[]{:S(2)}) collective-permute-start(bf16[2,32,2048]{2,1,0:T(8,128)(2,1)S(1)} %add.143), channel_id=1, source_target_pairs={{0,24},{8,16},{16,8},{24,0},{1,25},{9,17},{17,9},{25,1},{2,26},{10... | collective-permute-start | bytes 786440 | tf_op jit(solution)/shard_map/ppermute | solution.py:426
  87.7 2.3 %collective-permute-start.10 = (bf16[96,2048]{1,0:T(8,128)(2,1)S(1)}, bf16[96,2048]{1,0:T(8,128)(2,1)S(1)}, u32[]{:S(2)}, u32[]{:S(2)}) collective-permute-start(bf16[96,2048]{1,0:T(8,128)(2,1)S(1)} %get-tuple-element.49), channel_id=1, source_target_pairs={{0,4},{2,6},{4,0},{6,2},{1,5},{3,7},{5,1},{7,3},{8,12},{10,14},{12... | collective-permute-start | bytes 1179656 | tf_op jit(solution)/shard_map/ppermute | solution.py:426
  90.2 3.3 %collective-permute-start.11 = (bf16[96,2048]{1,0:T(8,128)(2,1)S(1)}, bf16[96,2048]{1,0:T(8,128)(2,1)S(1)}, u32[]{:S(2)}, u32[]{:S(2)}) collective-permute-start(bf16[96,2048]{1,0:T(8,128)(2,1)S(1)} %get-tuple-element.50), channel_id=1, source_target_pairs={{0,6},{2,4},{4,2},{6,0},{1,7},{3,5},{5,3},{7,1},{8,14},{10,12},{12... | collective-permute-start | bytes 1179656 | tf_op jit(solution)/shard_map/ppermute | solution.py:426
  93.6 1.0 collective-permute-done.37
  94.6 1.6 %collective-permute-done.39 = bf16[2,32,2048]{2,1,0:T(8,128)(2,1)S(1)} collective-permute-done((bf16[2,32,2048]{2,1,0:T(8,128)(2,1)S(1)}, bf16[2,32,2048]{2,1,0:T(8,128)(2,1)S(1)}, u32[]{:S(2)}, u32[]{:S(2)}) %collective-permute-start.39) | collective-permute-done | bytes 262176 | tf_op jit(solution)/shard_map/ppermute | solution.py:426
  96.2 1.2 combine.1
  97.4 1.4 collective-permute-start.40
  98.8 2.6 %collective-permute-start.41 = (bf16[48,2048]{1,0:T(8,128)(2,1)S(1)}, bf16[48,2048]{1,0:T(8,128)(2,1)S(1)}, u32[]{:S(2)}, u32[]{:S(2)}) collective-permute-start(bf16[48,2048]{1,0:T(8,128)(2,1)S(1)} %get-tuple-element.84), channel_id=1, source_target_pairs={{0,4},{2,6},{4,0},{6,2},{1,5},{3,7},{5,1},{7,3},{8,12},{10,14},{12... | collective-permute-start | bytes 589832 | tf_op jit(solution)/shard_map/ppermute | solution.py:426
  101.4 0.5 collective-permute-start.42
  101.9 21.6 %collective-permute-done.10.refs_2_ = bf16[96,2048]{1,0:T(8,128)(2,1)S(1)} collective-permute-done((bf16[96,2048]{1,0:T(8,128)(2,1)S(1)}, bf16[96,2048]{1,0:T(8,128)(2,1)S(1)}, u32[]{:S(2)}, u32[]{:S(2)}) %collective-permute-start.10) | collective-permute-done | bytes 393248 | tf_op jit(solution)/shard_map/ppermute | solution.py:426
  123.5 0.9 add.135
  124.4 11.7 %collective-permute-done.41.refs_2_ = bf16[48,2048]{1,0:T(8,128)(2,1)S(1)} collective-permute-done((bf16[48,2048]{1,0:T(8,128)(2,1)S(1)}, bf16[48,2048]{1,0:T(8,128)(2,1)S(1)}, u32[]{:S(2)}, u32[]{:S(2)}) %collective-permute-start.41) | collective-permute-done | bytes 196640 | tf_op jit(solution)/shard_map/ppermute | solution.py:426
  136.1 0.8 add.144
  (61 shorter events, 3.7 us)
Async XLA Ops:
  3.1 4.7 %collective-permute-start = (bf16[4,96,256]{2,1,0:T(8,128)(2,1)S(1)}, bf16[4,96,256]{2,1,0:T(8,128)(2,1)S(1)}, u32[]{:S(2)}, u32[]{:S(2)}) collective-permute-start(bf16[4,96,256]{2,1,0:T(8,128)(2,1)S(1)} %get-tuple-element.45), channel_id=1, source_target_pairs={{0,1},{1,0},{2,3},{3,2},{4,5},{5,4},{6,7},{7,6},{8,9},{9,8},{10,11... | collective-permute-start | bytes 589832 | tf_op jit(solution)/shard_map/ppermute | solution.py:430
  3.7 8.3 %collective-permute-start.2 = (bf16[2,384,128]{2,1,0:T(8,128)(2,1)S(1)}, bf16[2,384,128]{2,1,0:T(8,128)(2,1)S(1)}, u32[]{:S(2)}, u32[]{:S(2)}) collective-permute-start(bf16[2,384,128]{2,1,0:T(8,128)(2,1)S(1)} %get-tuple-element.46.refs_11_), channel_id=1, source_target_pairs={{0,8},{8,0},{16,24},{24,16},{1,9},{9,1},{17,25},{25,17},{2,10},{10... | collective-permute-start | bytes 589832 | tf_op jit(solution)/shard_map/ppermute | solution.py:426
  6.2 10.8 %collective-permute-start.3 = (bf16[2,384,128]{2,1,0:T(8,128)(2,1)S(1)}, bf16[2,384,128]{2,1,0:T(8,128)(2,1)S(1)}, u32[]{:S(2)}, u32[]{:S(2)}) collective-permute-start(bf16[2,384,128]{2,1,0:T(8,128)(2,1)S(1)} %get-tuple-element.46.refs_11_), channel_id=1, source_target_pairs={{0,16},{8,24},{16,0},{24,8},{1,17},{9,25},{17,1},{25,9},{2,18},{10... | collective-permute-start | bytes 589832 | tf_op jit(solution)/shard_map/ppermute | solution.py:426
  7.7 11.2 %collective-permute-start.4 = (bf16[2,384,128]{2,1,0:T(8,128)(2,1)S(1)}, bf16[2,384,128]{2,1,0:T(8,128)(2,1)S(1)}, u32[]{:S(2)}, u32[]{:S(2)}) collective-permute-start(bf16[2,384,128]{2,1,0:T(8,128)(2,1)S(1)} %get-tuple-element.46.refs_11_), channel_id=1, source_target_pairs={{0,24},{8,16},{16,8},{24,0},{1,25},{9,17},{17,9},{25,1},{2,26},{10... | collective-permute-start | bytes 589832 | tf_op jit(solution)/shard_map/ppermute | solution.py:426
  7.8 37.2 %collective-permute-start.1 = (bf16[256,2048]{1,0:T(8,128)(2,1)}, bf16[256,2048]{1,0:T(8,128)(2,1)S(1)}, u32[]{:S(2)}, u32[]{:S(2)}) collective-permute-start(bf16[256,2048]{1,0:T(8,128)(2,1)} %refs_7_.1), channel_id=1, source_target_pairs={{0,1},{1,0},{2,3},{3,2},{4,5},{5,4},{6,7},{7,6},{8,9},{9,8},{10,11... | collective-permute-start | bytes 3145736 | tf_op jit(solution)/shard_map/ppermute | solution.py:430
  7.8 11.4 %collective-permute-start.5 = (bf16[2,384,128]{2,1,0:T(8,128)(2,1)S(1)}, bf16[2,384,128]{2,1,0:T(8,128)(2,1)S(1)}, u32[]{:S(2)}, u32[]{:S(2)}) collective-permute-start(bf16[2,384,128]{2,1,0:T(8,128)(2,1)S(1)} %get-tuple-element.46.refs_11_), channel_id=1, source_target_pairs={{0,1},{1,0},{2,3},{3,2},{4,5},{5,4},{6,7},{7,6},{8,9},{9,8},{10,11... | collective-permute-start | bytes 589832 | tf_op jit(solution)/shard_map/ppermute | solution.py:430
  12.0 9.9 %collective-permute-start.12 = (bf16[2,32,2048]{2,1,0:T(8,128)(2,1)S(1)}, bf16[2,32,2048]{2,1,0:T(8,128)(2,1)S(1)}, u32[]{:S(2)}, u32[]{:S(2)}) collective-permute-start(bf16[2,32,2048]{2,1,0:T(8,128)(2,1)S(1)} %bitcast.46), channel_id=1, source_target_pairs={{0,8},{8,0},{16,24},{24,16},{1,9},{9,1},{17,25},{25,17},{2,10},{10... | collective-permute-start | bytes 786440 | tf_op jit(solution)/shard_map/ppermute | solution.py:426
  17.1 13.2 %collective-permute-start.13 = (bf16[2,32,2048]{2,1,0:T(8,128)(2,1)S(1)}, bf16[2,32,2048]{2,1,0:T(8,128)(2,1)S(1)}, u32[]{:S(2)}, u32[]{:S(2)}) collective-permute-start(bf16[2,32,2048]{2,1,0:T(8,128)(2,1)S(1)} %bitcast.45), channel_id=1, source_target_pairs={{0,16},{8,24},{16,0},{24,8},{1,17},{9,25},{17,1},{25,9},{2,18},{10... | collective-permute-start | bytes 786440 | tf_op jit(solution)/shard_map/ppermute | solution.py:426
  18.9 13.1 %collective-permute-start.14 = (bf16[2,32,2048]{2,1,0:T(8,128)(2,1)S(1)}, bf16[2,32,2048]{2,1,0:T(8,128)(2,1)S(1)}, u32[]{:S(2)}, u32[]{:S(2)}) collective-permute-start(bf16[2,32,2048]{2,1,0:T(8,128)(2,1)S(1)} %bitcast.44), channel_id=1, source_target_pairs={{0,24},{8,16},{16,8},{24,0},{1,25},{9,17},{17,9},{25,1},{2,26},{10... | collective-permute-start | bytes 786440 | tf_op jit(solution)/shard_map/ppermute | solution.py:426
  19.2 12.9 %collective-permute-start.15 = (bf16[2,32,2048]{2,1,0:T(8,128)(2,1)S(1)}, bf16[2,32,2048]{2,1,0:T(8,128)(2,1)S(1)}, u32[]{:S(2)}, u32[]{:S(2)}) collective-permute-start(bf16[2,32,2048]{2,1,0:T(8,128)(2,1)S(1)} %bitcast.33), channel_id=1, source_target_pairs={{0,1},{1,0},{2,3},{3,2},{4,5},{5,4},{6,7},{7,6},{8,9},{9,8},{10,11... | collective-permute-start | bytes 786440 | tf_op jit(solution)/shard_map/ppermute | solution.py:430
  21.8 11.4 %collective-permute-start.26 = (bf16[2,32,2048]{2,1,0:T(8,128)(2,1)S(1)}, bf16[2,32,2048]{2,1,0:T(8,128)(2,1)S(1)}, u32[]{:S(2)}, u32[]{:S(2)}) collective-permute-start(bf16[2,32,2048]{2,1,0:T(8,128)(2,1)S(1)} %bitcast.43), channel_id=1, source_target_pairs={{0,8},{8,0},{16,24},{24,16},{1,9},{9,1},{17,25},{25,17},{2,10},{10... | collective-permute-start | bytes 786440 | tf_op jit(solution)/shard_map/ppermute | solution.py:426
  30.3 12.3 %collective-permute-start.27 = (bf16[2,32,2048]{2,1,0:T(8,128)(2,1)S(1)}, bf16[2,32,2048]{2,1,0:T(8,128)(2,1)S(1)}, u32[]{:S(2)}, u32[]{:S(2)}) collective-permute-start(bf16[2,32,2048]{2,1,0:T(8,128)(2,1)S(1)} %bitcast.42), channel_id=1, source_target_pairs={{0,16},{8,24},{16,0},{24,8},{1,17},{9,25},{17,1},{25,9},{2,18},{10... | collective-permute-start | bytes 786440 | tf_op jit(solution)/shard_map/ppermute | solution.py:426
  32.0 10.5 %collective-permute-start.28 = (bf16[2,32,2048]{2,1,0:T(8,128)(2,1)S(1)}, bf16[2,32,2048]{2,1,0:T(8,128)(2,1)S(1)}, u32[]{:S(2)}, u32[]{:S(2)}) collective-permute-start(bf16[2,32,2048]{2,1,0:T(8,128)(2,1)S(1)} %bitcast.41), channel_id=1, source_target_pairs={{0,24},{8,16},{16,8},{24,0},{1,25},{9,17},{17,9},{25,1},{2,26},{10... | collective-permute-start | bytes 786440 | tf_op jit(solution)/shard_map/ppermute | solution.py:426
  32.1 11.0 %collective-permute-start.6 = (bf16[2,384,128]{2,1,0:T(8,128)(2,1)S(1)}, bf16[2,384,128]{2,1,0:T(8,128)(2,1)S(1)}, u32[]{:S(2)}, u32[]{:S(2)}) collective-permute-start(bf16[2,384,128]{2,1,0:T(8,128)(2,1)S(1)} %collective-permute-done.2.refs_12_), channel_id=1, source_target_pairs={{0,1},{1,0},{2,3},{3,2},{4,5},{5,4},{6,7},{7,6},{8,9},{9,8},{10,11... | collective-permute-start | bytes 589832 | tf_op jit(solution)/shard_map/ppermute | solution.py:430
  33.2 9.9 %collective-permute-start.7 = (bf16[2,384,128]{2,1,0:T(8,128)(2,1)S(1)}, bf16[2,384,128]{2,1,0:T(8,128)(2,1)S(1)}, u32[]{:S(2)}, u32[]{:S(2)}) collective-permute-start(bf16[2,384,128]{2,1,0:T(8,128)(2,1)S(1)} %collective-permute-done.3.refs_13_), channel_id=1, source_target_pairs={{0,1},{1,0},{2,3},{3,2},{4,5},{5,4},{6,7},{7,6},{8,9},{9,8},{10,11... | collective-permute-start | bytes 589832 | tf_op jit(solution)/shard_map/ppermute | solution.py:430
  42.6 1.4 %collective-permute-start.8 = (bf16[2,384,128]{2,1,0:T(8,128)(2,1)S(1)}, bf16[2,384,128]{2,1,0:T(8,128)(2,1)S(1)}, u32[]{:S(2)}, u32[]{:S(2)}) collective-permute-start(bf16[2,384,128]{2,1,0:T(8,128)(2,1)S(1)} %collective-permute-done.4.refs_14_), channel_id=1, source_target_pairs={{0,1},{1,0},{2,3},{3,2},{4,5},{5,4},{6,7},{7,6},{8,9},{9,8},{10,11... | collective-permute-start | bytes 589832 | tf_op jit(solution)/shard_map/ppermute | solution.py:430
  42.6 1.8 %collective-permute-start.16 = (bf16[2,32,2048]{2,1,0:T(8,128)(2,1)S(1)}, bf16[2,32,2048]{2,1,0:T(8,128)(2,1)S(1)}, u32[]{:S(2)}, u32[]{:S(2)}) collective-permute-start(bf16[2,32,2048]{2,1,0:T(8,128)(2,1)S(1)} %collective-permute-done.12.refs_1_), channel_id=1, source_target_pairs={{0,1},{1,0},{2,3},{3,2},{4,5},{5,4},{6,7},{7,6},{8,9},{9,8},{10,11... | collective-permute-start | bytes 786440 | tf_op jit(solution)/shard_map/ppermute | solution.py:430
  43.1 1.7 %collective-permute-start.17 = (bf16[2,32,2048]{2,1,0:T(8,128)(2,1)S(1)}, bf16[2,32,2048]{2,1,0:T(8,128)(2,1)S(1)}, u32[]{:S(2)}, u32[]{:S(2)}) collective-permute-start(bf16[2,32,2048]{2,1,0:T(8,128)(2,1)S(1)} %collective-permute-done.13.refs_2_), channel_id=1, source_target_pairs={{0,1},{1,0},{2,3},{3,2},{4,5},{5,4},{6,7},{7,6},{8,9},{9,8},{10,11... | collective-permute-start | bytes 786440 | tf_op jit(solution)/shard_map/ppermute | solution.py:430
  43.1 12.9 %collective-permute-start.18 = (bf16[2,32,2048]{2,1,0:T(8,128)(2,1)S(1)}, bf16[2,32,2048]{2,1,0:T(8,128)(2,1)S(1)}, u32[]{:S(2)}, u32[]{:S(2)}) collective-permute-start(bf16[2,32,2048]{2,1,0:T(8,128)(2,1)S(1)} %collective-permute-done.14.refs_3_), channel_id=1, source_target_pairs={{0,1},{1,0},{2,3},{3,2},{4,5},{5,4},{6,7},{7,6},{8,9},{9,8},{10,11... | collective-permute-start | bytes 786440 | tf_op jit(solution)/shard_map/ppermute | solution.py:430
  44.0 20.0 %collective-permute-start.29 = (bf16[2,32,2048]{2,1,0:T(8,128)(2,1)S(1)}, bf16[2,32,2048]{2,1,0:T(8,128)(2,1)S(1)}, u32[]{:S(2)}, u32[]{:S(2)}) collective-permute-start(bf16[2,32,2048]{2,1,0:T(8,128)(2,1)S(1)} %bitcast.31), channel_id=1, source_target_pairs={{0,1},{1,0},{2,3},{3,2},{4,5},{5,4},{6,7},{7,6},{8,9},{9,8},{10,11... | collective-permute-start | bytes 786440 | tf_op jit(solution)/shard_map/ppermute | solution.py:430
  44.4 19.9 %collective-permute-start.30 = (bf16[2,32,2048]{2,1,0:T(8,128)(2,1)S(1)}, bf16[2,32,2048]{2,1,0:T(8,128)(2,1)S(1)}, u32[]{:S(2)}, u32[]{:S(2)}) collective-permute-start(bf16[2,32,2048]{2,1,0:T(8,128)(2,1)S(1)} %collective-permute-done.26.refs_1_), channel_id=1, source_target_pairs={{0,1},{1,0},{2,3},{3,2},{4,5},{5,4},{6,7},{7,6},{8,9},{9,8},{10,11... | collective-permute-start | bytes 786440 | tf_op jit(solution)/shard_map/ppermute | solution.py:430
  44.7 19.7 %collective-permute-start.31 = (bf16[2,32,2048]{2,1,0:T(8,128)(2,1)S(1)}, bf16[2,32,2048]{2,1,0:T(8,128)(2,1)S(1)}, u32[]{:S(2)}, u32[]{:S(2)}) collective-permute-start(bf16[2,32,2048]{2,1,0:T(8,128)(2,1)S(1)} %collective-permute-done.27.refs_2_), channel_id=1, source_target_pairs={{0,1},{1,0},{2,3},{3,2},{4,5},{5,4},{6,7},{7,6},{8,9},{9,8},{10,11... | collective-permute-start | bytes 786440 | tf_op jit(solution)/shard_map/ppermute | solution.py:430
  45.0 19.8 %collective-permute-start.32 = (bf16[2,32,2048]{2,1,0:T(8,128)(2,1)S(1)}, bf16[2,32,2048]{2,1,0:T(8,128)(2,1)S(1)}, u32[]{:S(2)}, u32[]{:S(2)}) collective-permute-start(bf16[2,32,2048]{2,1,0:T(8,128)(2,1)S(1)} %collective-permute-done.28.refs_3_), channel_id=1, source_target_pairs={{0,1},{1,0},{2,3},{3,2},{4,5},{5,4},{6,7},{7,6},{8,9},{9,8},{10,11... | collective-permute-start | bytes 786440 | tf_op jit(solution)/shard_map/ppermute | solution.py:430
  63.7 5.0 %collective-permute-start.19 = (bf16[2,32,2048]{2,1,0:T(8,128)(2,1)S(1)}, bf16[2,32,2048]{2,1,0:T(8,128)(2,1)S(1)}, u32[]{:S(2)}, u32[]{:S(2)}) collective-permute-start(bf16[2,32,2048]{2,1,0:T(8,128)(2,1)S(1)} %get-tuple-element.60), channel_id=1, source_target_pairs={{0,1},{1,0},{2,3},{3,2},{4,5},{5,4},{6,7},{7,6},{8,9},{9,8},{10,11... | collective-permute-start | bytes 786440 | tf_op jit(solution)/shard_map/ppermute | solution.py:430
  64.0 5.0 %collective-permute-start.20 = (bf16[2,32,2048]{2,1,0:T(8,128)(2,1)S(1)}, bf16[2,32,2048]{2,1,0:T(8,128)(2,1)S(1)}, u32[]{:S(2)}, u32[]{:S(2)}) collective-permute-start(bf16[2,32,2048]{2,1,0:T(8,128)(2,1)S(1)} %get-tuple-element.62), channel_id=1, source_target_pairs={{0,1},{1,0},{2,3},{3,2},{4,5},{5,4},{6,7},{7,6},{8,9},{9,8},{10,11... | collective-permute-start | bytes 786440 | tf_op jit(solution)/shard_map/ppermute | solution.py:430
  64.3 5.0 %collective-permute-start.22 = (bf16[2,32,2048]{2,1,0:T(8,128)(2,1)S(1)}, bf16[2,32,2048]{2,1,0:T(8,128)(2,1)S(1)}, u32[]{:S(2)}, u32[]{:S(2)}) collective-permute-start(bf16[2,32,2048]{2,1,0:T(8,128)(2,1)S(1)} %get-tuple-element.64), channel_id=1, source_target_pairs={{0,1},{1,0},{2,3},{3,2},{4,5},{5,4},{6,7},{7,6},{8,9},{9,8},{10,11... | collective-permute-start | bytes 786440 | tf_op jit(solution)/shard_map/ppermute | solution.py:430
  64.5 5.2 %collective-permute-start.24 = (bf16[2,32,2048]{2,1,0:T(8,128)(2,1)S(1)}, bf16[2,32,2048]{2,1,0:T(8,128)(2,1)S(1)}, u32[]{:S(2)}, u32[]{:S(2)}) collective-permute-start(bf16[2,32,2048]{2,1,0:T(8,128)(2,1)S(1)} %get-tuple-element.66), channel_id=1, source_target_pairs={{0,1},{1,0},{2,3},{3,2},{4,5},{5,4},{6,7},{7,6},{8,9},{9,8},{10,11... | collective-permute-start | bytes 786440 | tf_op jit(solution)/shard_map/ppermute | solution.py:430
  68.4 1.6 %collective-permute-start.33 = (bf16[2,32,2048]{2,1,0:T(8,128)(2,1)S(1)}, bf16[2,32,2048]{2,1,0:T(8,128)(2,1)S(1)}, u32[]{:S(2)}, u32[]{:S(2)}) collective-permute-start(bf16[2,32,2048]{2,1,0:T(8,128)(2,1)S(1)} %get-tuple-element.75), channel_id=1, source_target_pairs={{0,1},{1,0},{2,3},{3,2},{4,5},{5,4},{6,7},{7,6},{8,9},{9,8},{10,11... | collective-permute-start | bytes 786440 | tf_op jit(solution)/shard_map/ppermute | solution.py:430
  68.7 3.1 %collective-permute-start.34 = (bf16[2,32,2048]{2,1,0:T(8,128)(2,1)S(1)}, bf16[2,32,2048]{2,1,0:T(8,128)(2,1)S(1)}, u32[]{:S(2)}, u32[]{:S(2)}) collective-permute-start(bf16[2,32,2048]{2,1,0:T(8,128)(2,1)S(1)} %get-tuple-element.77), channel_id=1, source_target_pairs={{0,1},{1,0},{2,3},{3,2},{4,5},{5,4},{6,7},{7,6},{8,9},{9,8},{10,11... | collective-permute-start | bytes 786440 | tf_op jit(solution)/shard_map/ppermute | solution.py:430
  69.0 4.4 %collective-permute-start.36 = (bf16[2,32,2048]{2,1,0:T(8,128)(2,1)S(1)}, bf16[2,32,2048]{2,1,0:T(8,128)(2,1)S(1)}, u32[]{:S(2)}, u32[]{:S(2)}) collective-permute-start(bf16[2,32,2048]{2,1,0:T(8,128)(2,1)S(1)} %get-tuple-element.79), channel_id=1, source_target_pairs={{0,1},{1,0},{2,3},{3,2},{4,5},{5,4},{6,7},{7,6},{8,9},{9,8},{10,11... | collective-permute-start | bytes 786440 | tf_op jit(solution)/shard_map/ppermute | solution.py:430
  69.2 4.6 %collective-permute-start.38 = (bf16[2,32,2048]{2,1,0:T(8,128)(2,1)S(1)}, bf16[2,32,2048]{2,1,0:T(8,128)(2,1)S(1)}, u32[]{:S(2)}, u32[]{:S(2)}) collective-permute-start(bf16[2,32,2048]{2,1,0:T(8,128)(2,1)S(1)} %get-tuple-element.81), channel_id=1, source_target_pairs={{0,1},{1,0},{2,3},{3,2},{4,5},{5,4},{6,7},{7,6},{8,9},{9,8},{10,11... | collective-permute-start | bytes 786440 | tf_op jit(solution)/shard_map/ppermute | solution.py:430
  69.7 9.2 %collective-permute-start.21 = (bf16[2,32,2048]{2,1,0:T(8,128)(2,1)S(1)}, bf16[2,32,2048]{2,1,0:T(8,128)(2,1)S(1)}, u32[]{:S(2)}, u32[]{:S(2)}) collective-permute-start(bf16[2,32,2048]{2,1,0:T(8,128)(2,1)S(1)} %add.137), channel_id=1, source_target_pairs={{0,8},{8,0},{16,24},{24,16},{1,9},{9,1},{17,25},{25,17},{2,10},{10... | collective-permute-start | bytes 786440 | tf_op jit(solution)/shard_map/ppermute | solution.py:426
  70.0 13.5 %collective-permute-start.23 = (bf16[2,32,2048]{2,1,0:T(8,128)(2,1)S(1)}, bf16[2,32,2048]{2,1,0:T(8,128)(2,1)S(1)}, u32[]{:S(2)}, u32[]{:S(2)}) collective-permute-start(bf16[2,32,2048]{2,1,0:T(8,128)(2,1)S(1)} %add.138), channel_id=1, source_target_pairs={{0,16},{8,24},{16,0},{24,8},{1,17},{9,25},{17,1},{25,9},{2,18},{10... | collective-permute-start | bytes 786440 | tf_op jit(solution)/shard_map/ppermute | solution.py:426
  71.8 15.9 %collective-permute-start.25 = (bf16[2,32,2048]{2,1,0:T(8,128)(2,1)S(1)}, bf16[2,32,2048]{2,1,0:T(8,128)(2,1)S(1)}, u32[]{:S(2)}, u32[]{:S(2)}) collective-permute-start(bf16[2,32,2048]{2,1,0:T(8,128)(2,1)S(1)} %add.139), channel_id=1, source_target_pairs={{0,24},{8,16},{16,8},{24,0},{1,25},{9,17},{17,9},{25,1},{2,26},{10... | collective-permute-start | bytes 786440 | tf_op jit(solution)/shard_map/ppermute | solution.py:426
  73.4 16.7 %collective-permute-start.35 = (bf16[2,32,2048]{2,1,0:T(8,128)(2,1)S(1)}, bf16[2,32,2048]{2,1,0:T(8,128)(2,1)S(1)}, u32[]{:S(2)}, u32[]{:S(2)}) collective-permute-start(bf16[2,32,2048]{2,1,0:T(8,128)(2,1)S(1)} %add.141), channel_id=1, source_target_pairs={{0,8},{8,0},{16,24},{24,16},{1,9},{9,1},{17,25},{25,17},{2,10},{10... | collective-permute-start | bytes 786440 | tf_op jit(solution)/shard_map/ppermute | solution.py:426
  73.8 27.6 %collective-permute-start.9 = (bf16[96,2048]{1,0:T(8,128)(2,1)S(1)}, bf16[96,2048]{1,0:T(8,128)(2,1)S(1)}, u32[]{:S(2)}, u32[]{:S(2)}) collective-permute-start(bf16[96,2048]{1,0:T(8,128)(2,1)S(1)} %get-tuple-element.48), channel_id=1, source_target_pairs={{0,2},{2,0},{4,6},{6,4},{1,3},{3,1},{5,7},{7,5},{8,10},{10,8},{12,... | collective-permute-start | bytes 1179656 | tf_op jit(solution)/shard_map/ppermute | solution.py:426
  78.9 15.7 %collective-permute-start.37 = (bf16[2,32,2048]{2,1,0:T(8,128)(2,1)S(1)}, bf16[2,32,2048]{2,1,0:T(8,128)(2,1)S(1)}, u32[]{:S(2)}, u32[]{:S(2)}) collective-permute-start(bf16[2,32,2048]{2,1,0:T(8,128)(2,1)S(1)} %add.142), channel_id=1, source_target_pairs={{0,16},{8,24},{16,0},{24,8},{1,17},{9,25},{17,1},{25,9},{2,18},{10... | collective-permute-start | bytes 786440 | tf_op jit(solution)/shard_map/ppermute | solution.py:426
  83.5 12.7 %collective-permute-start.39 = (bf16[2,32,2048]{2,1,0:T(8,128)(2,1)S(1)}, bf16[2,32,2048]{2,1,0:T(8,128)(2,1)S(1)}, u32[]{:S(2)}, u32[]{:S(2)}) collective-permute-start(bf16[2,32,2048]{2,1,0:T(8,128)(2,1)S(1)} %add.143), channel_id=1, source_target_pairs={{0,24},{8,16},{16,8},{24,0},{1,25},{9,17},{17,9},{25,1},{2,26},{10... | collective-permute-start | bytes 786440 | tf_op jit(solution)/shard_map/ppermute | solution.py:426
  87.7 35.7 %collective-permute-start.10 = (bf16[96,2048]{1,0:T(8,128)(2,1)S(1)}, bf16[96,2048]{1,0:T(8,128)(2,1)S(1)}, u32[]{:S(2)}, u32[]{:S(2)}) collective-permute-start(bf16[96,2048]{1,0:T(8,128)(2,1)S(1)} %get-tuple-element.49), channel_id=1, source_target_pairs={{0,4},{2,6},{4,0},{6,2},{1,5},{3,7},{5,1},{7,3},{8,12},{10,14},{12... | collective-permute-start | bytes 1179656 | tf_op jit(solution)/shard_map/ppermute | solution.py:426
  90.2 33.3 %collective-permute-start.11 = (bf16[96,2048]{1,0:T(8,128)(2,1)S(1)}, bf16[96,2048]{1,0:T(8,128)(2,1)S(1)}, u32[]{:S(2)}, u32[]{:S(2)}) collective-permute-start(bf16[96,2048]{1,0:T(8,128)(2,1)S(1)} %get-tuple-element.50), channel_id=1, source_target_pairs={{0,6},{2,4},{4,2},{6,0},{1,7},{3,5},{5,3},{7,1},{8,14},{10,12},{12... | collective-permute-start | bytes 1179656 | tf_op jit(solution)/shard_map/ppermute | solution.py:426
  97.4 27.0 %collective-permute-start.40 = (bf16[48,2048]{1,0:T(8,128)(2,1)S(1)}, bf16[48,2048]{1,0:T(8,128)(2,1)S(1)}, u32[]{:S(2)}, u32[]{:S(2)}) collective-permute-start(bf16[48,2048]{1,0:T(8,128)(2,1)S(1)} %get-tuple-element.83), channel_id=1, source_target_pairs={{0,2},{2,0},{4,6},{6,4},{1,3},{3,1},{5,7},{7,5},{8,10},{10,8},{12,... | collective-permute-start | bytes 589832 | tf_op jit(solution)/shard_map/ppermute | solution.py:426
  98.8 37.3 %collective-permute-start.41 = (bf16[48,2048]{1,0:T(8,128)(2,1)S(1)}, bf16[48,2048]{1,0:T(8,128)(2,1)S(1)}, u32[]{:S(2)}, u32[]{:S(2)}) collective-permute-start(bf16[48,2048]{1,0:T(8,128)(2,1)S(1)} %get-tuple-element.84), channel_id=1, source_target_pairs={{0,4},{2,6},{4,0},{6,2},{1,5},{3,7},{5,1},{7,3},{8,12},{10,14},{12... | collective-permute-start | bytes 589832 | tf_op jit(solution)/shard_map/ppermute | solution.py:426
  101.4 34.7 %collective-permute-start.42 = (bf16[48,2048]{1,0:T(8,128)(2,1)S(1)}, bf16[48,2048]{1,0:T(8,128)(2,1)S(1)}, u32[]{:S(2)}, u32[]{:S(2)}) collective-permute-start(bf16[48,2048]{1,0:T(8,128)(2,1)S(1)} %get-tuple-element.85), channel_id=1, source_target_pairs={{0,6},{2,4},{4,2},{6,0},{1,7},{3,5},{5,3},{7,1},{8,14},{10,12},{12... | collective-permute-start | bytes 589832 | tf_op jit(solution)/shard_map/ppermute | solution.py:426

commit v6 on v5

--- a/solution.py
+++ b/solution.py
@@ -133,6 +133,28 @@
                 )
                 sem += 1
     return copies
+
+
+def load_kernel(first, after_ref, *refs):
+    sources, targets, sems = refs[:3], refs[3:6], refs[6]
+    copies = weight_copies(sources, targets, first, sems, 0)
+    for copy in copies:
+        copy.start()
+    for copy in copies:
+        copy.wait()
+
+
+def load(weights, first, per, after):
+    any_space = pl.BlockSpec(memory_space=pl.ANY)
+    return pl.pallas_call(
+        lambda *refs: load_kernel(first, *refs),
+        in_specs=[any_space] * 4,
+        out_specs=[IN_VMEM] * 3,
+        out_shape=[jax.ShapeDtypeStruct((per, *w.shape[1:]), BF16) for w in weights],
+        scratch_shapes=[pltpu.SemaphoreType.DMA((3 * per * SPLIT,))],
+        compiler_params=pltpu.CompilerParams(vmem_limit_bytes=2 * MIB),
+        name="load",
+    )(after, *in_hbm(weights))
 
 
 def mix_kernel(n_pieces, n_z, z_ref, q_own, q_other, gain_hbm, cos_ref, sin_ref, w_other, *rest):
@@ -234,7 +256,7 @@
             pltpu.VMEM(gain.shape, F32),
             pltpu.SemaphoreType.DMA((2 + 3 * per * SPLIT,)),
         ],
-        compiler_params=pltpu.CompilerParams(vmem_limit_bytes=20 * MIB),
+        compiler_params=pltpu.CompilerParams(vmem_limit_bytes=8 * MIB + length * HD * 6),
         name="mix",
     )(
         z_index, q_own, q_other, *in_hbm([gain]), cosine, sine, w_other,
@@ -339,15 +361,10 @@
     return outs[:n_out], outs[n_out]
 
 
-def expert_kernel(n_in, group, first, n_next, *refs):
+def expert_kernel(n_in, group, *refs):
     ins, (gate_ref, up_ref, down_ref) = refs[:n_in], refs[n_in : n_in + 3]
-    sources, outs = refs[n_in + 3 : n_in + 3 + n_next], refs[n_in + 3 + n_next : 2 * n_in + 3 + n_next]
+    outs = refs[n_in + 3 :]
     per, rows, _ = outs[0].shape
-    copies = []
-    if n_next:
-        copies = weight_copies(sources, refs[2 * n_in + 3 + n_next : -1], first + per, refs[-1], 0)
-    for copy in copies:
-        copy.start()
     for expert in range(per):
         for start in range(0, len(ins), group):
             field = [ref[expert] for ref in ins[start : start + group]]
@@ -358,27 +375,22 @@
             result = jnp.dot(hidden, down_ref[expert], preferred_element_type=F32)
             for n, ref in enumerate(outs[start : start + group]):
                 ref[expert] = result[n * rows : (n + 1) * rows].astype(BF16)
-    for copy in copies:
-        copy.wait()
-
-
-def experts(own, other, weights, first, all_weights):
+
+
+def experts(own, other, weights):
     pieces = [*own, *other]
     _, rows, d_model = pieces[0].shape
     per = weights[0].shape[0]
-    more = in_hbm(all_weights) if first + per < all_weights[0].shape[0] else []
     group = min(len(pieces), max(1, 256 // rows))
     outs = pl.pallas_call(
-        lambda *refs: expert_kernel(len(pieces), group, first, len(more), *refs),
-        in_specs=[IN_VMEM] * (len(pieces) + 3) + [pl.BlockSpec(memory_space=pl.ANY)] * len(more),
-        out_specs=[IN_VMEM] * (len(pieces) + len(more)),
-        out_shape=[jax.ShapeDtypeStruct((per, rows, d_model), BF16)] * len(pieces)
-        + [jax.ShapeDtypeStruct((per, *w.shape[1:]), BF16) for w in more],
-        scratch_shapes=[pltpu.SemaphoreType.DMA((3 * per * SPLIT,))] if more else [],
-        compiler_params=pltpu.CompilerParams(vmem_limit_bytes=16 * MIB),
+        lambda *refs: expert_kernel(len(pieces), group, *refs),
+        in_specs=[IN_VMEM] * (len(pieces) + 3),
+        out_specs=[IN_VMEM] * len(pieces),
+        out_shape=[jax.ShapeDtypeStruct((per, rows, d_model), BF16)] * len(pieces),
+        compiler_params=pltpu.CompilerParams(vmem_limit_bytes=10 * MIB),
         name="experts",
-    )(*pieces, *weights, *more)
-    return outs[: len(own)], outs[len(own) : len(pieces)], outs[len(pieces) :]
+    )(*pieces, *weights)
+    return outs[: len(own)], outs[len(own) :]
 
 
 def combine_kernel(n_back, z_ref, cols_ref, *rest):
@@ -490,10 +502,12 @@
         arrived.append((here, [swap_cores(p) for p in here]))
 
     all_weights = [gate_weight, up_weight, down_weight]
-    mixed, weights = mix(
+    weights = [load(all_weights, chunk * per, per, cols) for chunk in range(1, chunks)]
+    mixed, first_weights = mix(
         z_arg, q_own, q_other, query_gain[None], cosine, sine, out_weight, w_other,
         all_weights, per, pieces,
     )
+    weights = [first_weights, *weights]
     gathered = [mixed[0]]
     for step in range(1, n_z):
         gathered.append(shift(mixed[step], "z", step))
@@ -501,7 +515,7 @@
 
     backs = []
     for chunk in range(chunks):
-        keep, send, weights = experts(*arrived[chunk], weights, chunk * per, all_weights)
+        keep, send = experts(*arrived[chunk], weights[chunk])
         for step in range(n_ep):
             result = add(keep[step], swap_cores(send[step]))
             result = shift(result, "ep", step, back=True) if step else result

time: 139 us -> 140 us (level)
  starting transfers between devices: 38.3 us -> 35.9 us
  waiting for transfers between devices: 67.1 us -> 69.4 us
    ppermute x21, starting transfers between devices: 33.1 us -> 30.9 us  [shift(): return lax.ppermute(a, axis, pairs)]
    ppermute x21, waiting for transfers between devices: 66 us -> 68.1 us  [shift(): return lax.ppermute(a, axis, pairs)]
    pallas_call x2 -> x3, Pallas kernels: 11.3 us -> 11.9 us  [the longest x2 7.2 us: experts(): pl.pallas_call(lambda *refs: expert_kernel(len(pieces), group, *refs), in...]
  transfers between devices with their start and end apart: 43 -> 43, of which waited for: 17 -> 12; matrix products, arithmetic and copies ran while one was open for 0% -> 0% of each run, Pallas kernels for 20% -> 20%
where the time goes in v6:
time: 140 us; the launch traced here: 137 us
  waiting for transfers between devices  69.4 us (50%)
  starting transfers between devices  35.9 us (26%)
  Pallas kernels  30.3 us (22%)
    ppermute x21, waiting for transfers between devices, shift(): return lax.ppermute(a, axis, pairs)  68.1 us
    ppermute x21, starting transfers between devices, shift(): return lax.ppermute(a, axis, pairs)  30.9 us
    pallas_call x1, Pallas kernels, mix(): pl.pallas_call(lambda *refs: mix_kernel(len(pieces), n_z, *refs), in_spec...  10.7 us
    pallas_call x2, Pallas kernels, experts(): pl.pallas_call(lambda *refs: expert_kernel(len(pieces), group, *refs), in...  7.2 us
    ppermute x22, starting transfers between devices, swap_cores(): return lax.ppermute(a, 'core', [(i, CORES - 1 - i) for i in range(CORES)])  4.99 us
    pallas_call x1, Pallas kernels, load(): pl.pallas_call(lambda *refs: load_kernel(first, *refs), in_specs=[any_spa...  4.7 us
    pallas_call x1, Pallas kernels, dispatch(): pl.pallas_call(lambda *refs: dispatch_kernel(n_ep, n_local, per, *refs),...  2.85 us
  transfers between devices with their start and end apart: 43, of which 12 were waited for; matrix products, arithmetic and copies ran while one was open for 0% of the time, Pallas kernels for 20%

profile of v6, /device:TPU:0, one launch (start us, length us, event | category | flops | bytes accessed | tf_op | source)
XLA Modules:
  0.0 137.5 jit_solution(5127238954985990859)
XLA Ops:
  0.9 0.8 sine_multiply_fusion
  1.7 1.4 %prepare.1 = (bf16[2,384,128]{2,1,0:T(8,128)(2,1)S(1)}, bf16[4,96,256]{2,1,0:T(8,128)(2,1)S(1)}, bf16[4,96,256]{2,1,0:T(8,128)(2,1)S(1)}) custom-call(s32[1]{0:T(128)} %bitcast.1.core_ref.refs_0_, s32[1]{0:T(128)} %bitcast.2.head_ref, bf16[4,2,96,512]{3,2,1,0:T(8,128)(2,1)} %bitcast.50, bf16[4,2,96,512]{3,2,1,0:T(8,128)(2,1)} %bitcast.51, ...), custom_call_target="tpu_custom_call" | custom-call | tf_op jit(solution)/shard_map/prepare/pallas_call | solution.py:74
  3.1 0.6 collective-permute-start
  3.7 2.6 %collective-permute-start.2 = (bf16[2,384,128]{2,1,0:T(8,128)(2,1)S(1)}, bf16[2,384,128]{2,1,0:T(8,128)(2,1)S(1)}, u32[]{:S(2)}, u32[]{:S(2)}) collective-permute-start(bf16[2,384,128]{2,1,0:T(8,128)(2,1)S(1)} %get-tuple-element.46.refs_11_), channel_id=1, source_target_pairs={{0,8},{8,0},{16,24},{24,16},{1,9},{9,1},{17,25},{25,17},{2,10},{10... | collective-permute-start | bytes 589832 | tf_op jit(solution)/shard_map/ppermute | solution.py:438
  6.2 1.5 %collective-permute-start.3 = (bf16[2,384,128]{2,1,0:T(8,128)(2,1)S(1)}, bf16[2,384,128]{2,1,0:T(8,128)(2,1)S(1)}, u32[]{:S(2)}, u32[]{:S(2)}) collective-permute-start(bf16[2,384,128]{2,1,0:T(8,128)(2,1)S(1)} %get-tuple-element.46.refs_11_), channel_id=1, source_target_pairs={{0,16},{8,24},{16,0},{24,8},{1,17},{9,25},{17,1},{25,9},{2,18},{10... | collective-permute-start | bytes 589832 | tf_op jit(solution)/shard_map/ppermute | solution.py:438
  7.8 2.8 %dispatch.1 = (bf16[64,2048]{1,0:T(8,128)(2,1)S(1)}, bf16[64,2048]{1,0:T(8,128)(2,1)S(1)}, bf16[64,2048]{1,0:T(8,128)(2,1)S(1)}, bf16[64,2048]{1,0:T(8,128)(2,1)...) custom-call(s32[1]{0:T(128)} %bitcast.1.core_ref.refs_0_, ...), custom_call_target="tpu_custom_call" | custom-call | tf_op jit(solution)/shard_map/dispatch/pallas_call | solution.py:343
  10.6 2.0 %collective-permute-start.12 = (bf16[2,32,2048]{2,1,0:T(8,128)(2,1)S(1)}, bf16[2,32,2048]{2,1,0:T(8,128)(2,1)S(1)}, u32[]{:S(2)}, u32[]{:S(2)}) collective-permute-start(bf16[2,32,2048]{2,1,0:T(8,128)(2,1)S(1)} %bitcast.46), channel_id=1, source_target_pairs={{0,8},{8,0},{16,24},{24,16},{1,9},{9,1},{17,25},{25,17},{2,10},{10... | collective-permute-start | bytes 786440 | tf_op jit(solution)/shard_map/ppermute | solution.py:438
  12.6 1.6 %collective-permute-start.13 = (bf16[2,32,2048]{2,1,0:T(8,128)(2,1)S(1)}, bf16[2,32,2048]{2,1,0:T(8,128)(2,1)S(1)}, u32[]{:S(2)}, u32[]{:S(2)}) collective-permute-start(bf16[2,32,2048]{2,1,0:T(8,128)(2,1)S(1)} %bitcast.45), channel_id=1, source_target_pairs={{0,16},{8,24},{16,0},{24,8},{1,17},{9,25},{17,1},{25,9},{2,18},{10... | collective-permute-start | bytes 786440 | tf_op jit(solution)/shard_map/ppermute | solution.py:438
  14.2 3.1 %collective-permute-done.3.refs_13_ = bf16[2,384,128]{2,1,0:T(8,128)(2,1)S(1)} collective-permute-done((bf16[2,384,128]{2,1,0:T(8,128)(2,1)S(1)}, bf16[2,384,128]{2,1,0:T(8,128)(2,1)S(1)}, u32[]{:S(2)}, u32[]{:S(2)}) %collective-permute-start.3) | collective-permute-done | bytes 196640 | tf_op jit(solution)/shard_map/ppermute | solution.py:438
  17.4 1.7 %collective-permute-start.14 = (bf16[2,32,2048]{2,1,0:T(8,128)(2,1)S(1)}, bf16[2,32,2048]{2,1,0:T(8,128)(2,1)S(1)}, u32[]{:S(2)}, u32[]{:S(2)}) collective-permute-start(bf16[2,32,2048]{2,1,0:T(8,128)(2,1)S(1)} %bitcast.44), channel_id=1, source_target_pairs={{0,24},{8,16},{16,8},{24,0},{1,25},{9,17},{17,9},{25,1},{2,26},{10... | collective-permute-start | bytes 786440 | tf_op jit(solution)/shard_map/ppermute | solution.py:438
  19.1 0.5 collective-permute-start.1
  19.6 2.3 %collective-permute-done.12.refs_1_ = bf16[2,32,2048]{2,1,0:T(8,128)(2,1)S(1)} collective-permute-done((bf16[2,32,2048]{2,1,0:T(8,128)(2,1)S(1)}, bf16[2,32,2048]{2,1,0:T(8,128)(2,1)S(1)}, u32[]{:S(2)}, u32[]{:S(2)}) %collective-permute-start.12) | collective-permute-done | bytes 262176 | tf_op jit(solution)/shard_map/ppermute | solution.py:438
  21.9 2.0 %collective-permute-start.26 = (bf16[2,32,2048]{2,1,0:T(8,128)(2,1)S(1)}, bf16[2,32,2048]{2,1,0:T(8,128)(2,1)S(1)}, u32[]{:S(2)}, u32[]{:S(2)}) collective-permute-start(bf16[2,32,2048]{2,1,0:T(8,128)(2,1)S(1)} %bitcast.43), channel_id=1, source_target_pairs={{0,8},{8,0},{16,24},{24,16},{1,9},{9,1},{17,25},{25,17},{2,10},{10... | collective-permute-start | bytes 786440 | tf_op jit(solution)/shard_map/ppermute | solution.py:438
  23.9 4.4 %collective-permute-done.13.refs_2_ = bf16[2,32,2048]{2,1,0:T(8,128)(2,1)S(1)} collective-permute-done((bf16[2,32,2048]{2,1,0:T(8,128)(2,1)S(1)}, bf16[2,32,2048]{2,1,0:T(8,128)(2,1)S(1)}, u32[]{:S(2)}, u32[]{:S(2)}) %collective-permute-start.13) | collective-permute-done | bytes 262176 | tf_op jit(solution)/shard_map/ppermute | solution.py:438
  28.3 1.9 %collective-permute-start.27 = (bf16[2,32,2048]{2,1,0:T(8,128)(2,1)S(1)}, bf16[2,32,2048]{2,1,0:T(8,128)(2,1)S(1)}, u32[]{:S(2)}, u32[]{:S(2)}) collective-permute-start(bf16[2,32,2048]{2,1,0:T(8,128)(2,1)S(1)} %bitcast.42), channel_id=1, source_target_pairs={{0,16},{8,24},{16,0},{24,8},{1,17},{9,25},{17,1},{25,9},{2,18},{10... | collective-permute-start | bytes 786440 | tf_op jit(solution)/shard_map/ppermute | solution.py:438
  30.5 3.6 %collective-permute-done.26.refs_1_ = bf16[2,32,2048]{2,1,0:T(8,128)(2,1)S(1)} collective-permute-done((bf16[2,32,2048]{2,1,0:T(8,128)(2,1)S(1)}, bf16[2,32,2048]{2,1,0:T(8,128)(2,1)S(1)}, u32[]{:S(2)}, u32[]{:S(2)}) %collective-permute-start.26) | collective-permute-done | bytes 262176 | tf_op jit(solution)/shard_map/ppermute | solution.py:438
  34.0 7.0 %collective-permute-done.27.refs_2_ = bf16[2,32,2048]{2,1,0:T(8,128)(2,1)S(1)} collective-permute-done((bf16[2,32,2048]{2,1,0:T(8,128)(2,1)S(1)}, bf16[2,32,2048]{2,1,0:T(8,128)(2,1)S(1)}, u32[]{:S(2)}, u32[]{:S(2)}) %collective-permute-start.27) | collective-permute-done | bytes 262176 | tf_op jit(solution)/shard_map/ppermute | solution.py:438
  41.0 0.5 collective-permute-start.32
  41.6 0.4 collective-permute-start.7
  42.0 0.5 collective-permute-done.31.refs_6_
  43.1 4.7 %load.1 = (bf16[2,2048,512]{2,1,0:T(8,128)(2,1)S(1)}, bf16[2,2048,512]{2,1,0:T(8,128)(2,1)S(1)}, bf16[2,512,2048]{2,1,0:T(8,128)(2,1)S(1)}) custom-call(f32[192,8]{1,0:T(8,128)S(1)} %get-tuple-element.51.refs_0_.refs_1_, bf16[4,2048,512]{2,1,0:T(8,128)(2,1)} %refs_1_.1, bf16[4,2048,512]{2,1,0:T(8,128)(2,1)} %refs_2_.1, bf16[4,512,2048]{2,1,0:T(8,128)(2,1)} %refs_3_.1), custom_call_target="tpu_custom_call" | custom-call | tf_op jit(solution)/shard_map/load/pallas_call | solution.py:149
  47.8 3.6 %experts.3 = (bf16[2,32,2048]{2,1,0:T(8,128)(2,1)S(1)}, bf16[2,32,2048]{2,1,0:T(8,128)(2,1)S(1)}, bf16[2,32,2048]{2,1,0:T(8,128)(2,1)S(1)}, bf16[2,32,2048]{2,1,...) custom-call(bf16[2,32,2048]{2,1,0:T(8,128)(2,1)S(1)} %bitcast.34, ...), custom_call_target="tpu_custom_call" | custom-call | tf_op jit(solution)/shard_map/experts/pallas_call | solution.py:385
  51.4 0.4 collective-permute-start.34
  52.0 0.4 collective-permute-start.18
  52.5 0.5 collective-permute-done.34.refs_1_
  53.0 0.4 collective-permute-start.38
  53.4 0.3 collective-permute-start.33
  53.7 10.7 %mix.1 = (bf16[96,2048]{1,0:T(8,128)(2,1)S(1)}, bf16[96,2048]{1,0:T(8,128)(2,1)S(1)}, bf16[96,2048]{1,0:T(8,128)(2,1)S(1)}, bf16[96,2048]{1,0:T(8,128)(2,1)S(1)}...) custom-call(s32[1]{0:T(128)} %bitcast.refs_0_, ...), custom_call_target="tpu_custom_call" | custom-call | tf_op jit(solution)/shard_map/mix/pallas_call | solution.py:243
  64.5 3.6 %experts.2 = (bf16[2,32,2048]{2,1,0:T(8,128)(2,1)S(1)}, bf16[2,32,2048]{2,1,0:T(8,128)(2,1)S(1)}, bf16[2,32,2048]{2,1,0:T(8,128)(2,1)S(1)}, bf16[2,32,2048]{2,1,...) custom-call(bf16[2,32,2048]{2,1,0:T(8,128)(2,1)S(1)} %bitcast.32, ...), custom_call_target="tpu_custom_call" | custom-call | tf_op jit(solution)/shard_map/experts/pallas_call | solution.py:385
  68.1 0.4 collective-permute-start.20
  68.7 0.3 collective-permute-start.24
  69.1 1.8 %collective-permute-start.37 = (bf16[2,32,2048]{2,1,0:T(8,128)(2,1)S(1)}, bf16[2,32,2048]{2,1,0:T(8,128)(2,1)S(1)}, u32[]{:S(2)}, u32[]{:S(2)}) collective-permute-start(bf16[2,32,2048]{2,1,0:T(8,128)(2,1)S(1)} %add.142), channel_id=1, source_target_pairs={{0,16},{8,24},{16,0},{24,8},{1,17},{9,25},{17,1},{25,9},{2,18},{10... | collective-permute-start | bytes 786440 | tf_op jit(solution)/shard_map/ppermute | solution.py:438
  70.9 1.6 %collective-permute-start.39 = (bf16[2,32,2048]{2,1,0:T(8,128)(2,1)S(1)}, bf16[2,32,2048]{2,1,0:T(8,128)(2,1)S(1)}, u32[]{:S(2)}, u32[]{:S(2)}) collective-permute-start(bf16[2,32,2048]{2,1,0:T(8,128)(2,1)S(1)} %add.143), channel_id=1, source_target_pairs={{0,24},{8,16},{16,8},{24,0},{1,25},{9,17},{17,9},{25,1},{2,26},{10... | collective-permute-start | bytes 786440 | tf_op jit(solution)/shard_map/ppermute | solution.py:438
  72.5 0.6 collective-permute-start.21
  73.1 1.6 %collective-permute-start.9 = (bf16[96,2048]{1,0:T(8,128)(2,1)S(1)}, bf16[96,2048]{1,0:T(8,128)(2,1)S(1)}, u32[]{:S(2)}, u32[]{:S(2)}) collective-permute-start(bf16[96,2048]{1,0:T(8,128)(2,1)S(1)} %get-tuple-element.48), channel_id=1, source_target_pairs={{0,2},{2,0},{4,6},{6,4},{1,3},{3,1},{5,7},{7,5},{8,10},{10,8},{12,... | collective-permute-start | bytes 1179656 | tf_op jit(solution)/shard_map/ppermute | solution.py:438
  74.8 8.4 %collective-permute-done.37 = bf16[2,32,2048]{2,1,0:T(8,128)(2,1)S(1)} collective-permute-done((bf16[2,32,2048]{2,1,0:T(8,128)(2,1)S(1)}, bf16[2,32,2048]{2,1,0:T(8,128)(2,1)S(1)}, u32[]{:S(2)}, u32[]{:S(2)}) %collective-permute-start.37) | collective-permute-done | bytes 262176 | tf_op jit(solution)/shard_map/ppermute | solution.py:438
  83.2 1.7 %collective-permute-start.23 = (bf16[2,32,2048]{2,1,0:T(8,128)(2,1)S(1)}, bf16[2,32,2048]{2,1,0:T(8,128)(2,1)S(1)}, u32[]{:S(2)}, u32[]{:S(2)}) collective-permute-start(bf16[2,32,2048]{2,1,0:T(8,128)(2,1)S(1)} %add.138), channel_id=1, source_target_pairs={{0,16},{8,24},{16,0},{24,8},{1,17},{9,25},{17,1},{25,9},{2,18},{10... | collective-permute-start | bytes 786440 | tf_op jit(solution)/shard_map/ppermute | solution.py:438
  85.0 1.7 %collective-permute-start.25 = (bf16[2,32,2048]{2,1,0:T(8,128)(2,1)S(1)}, bf16[2,32,2048]{2,1,0:T(8,128)(2,1)S(1)}, u32[]{:S(2)}, u32[]{:S(2)}) collective-permute-start(bf16[2,32,2048]{2,1,0:T(8,128)(2,1)S(1)} %add.139), channel_id=1, source_target_pairs={{0,24},{8,16},{16,8},{24,0},{1,25},{9,17},{17,9},{25,1},{2,26},{10... | collective-permute-start | bytes 786440 | tf_op jit(solution)/shard_map/ppermute | solution.py:438
  86.7 2.6 %collective-permute-start.10 = (bf16[96,2048]{1,0:T(8,128)(2,1)S(1)}, bf16[96,2048]{1,0:T(8,128)(2,1)S(1)}, u32[]{:S(2)}, u32[]{:S(2)}) collective-permute-start(bf16[96,2048]{1,0:T(8,128)(2,1)S(1)} %get-tuple-element.49), channel_id=1, source_target_pairs={{0,4},{2,6},{4,0},{6,2},{1,5},{3,7},{5,1},{7,3},{8,12},{10,14},{12... | collective-permute-start | bytes 1179656 | tf_op jit(solution)/shard_map/ppermute | solution.py:438
  89.3 1.3 collective-permute-start.11
  90.8 5.6 %collective-permute-done.23 = bf16[2,32,2048]{2,1,0:T(8,128)(2,1)S(1)} collective-permute-done((bf16[2,32,2048]{2,1,0:T(8,128)(2,1)S(1)}, bf16[2,32,2048]{2,1,0:T(8,128)(2,1)S(1)}, u32[]{:S(2)}, u32[]{:S(2)}) %collective-permute-start.23) | collective-permute-done | bytes 262176 | tf_op jit(solution)/shard_map/ppermute | solution.py:438
  96.4 1.2 combine.1
  97.6 1.6 %collective-permute-start.40 = (bf16[48,2048]{1,0:T(8,128)(2,1)S(1)}, bf16[48,2048]{1,0:T(8,128)(2,1)S(1)}, u32[]{:S(2)}, u32[]{:S(2)}) collective-permute-start(bf16[48,2048]{1,0:T(8,128)(2,1)S(1)} %get-tuple-element.83), channel_id=1, source_target_pairs={{0,2},{2,0},{4,6},{6,4},{1,3},{3,1},{5,7},{7,5},{8,10},{10,8},{12,... | collective-permute-start | bytes 589832 | tf_op jit(solution)/shard_map/ppermute | solution.py:438
  99.3 2.6 %collective-permute-start.41 = (bf16[48,2048]{1,0:T(8,128)(2,1)S(1)}, bf16[48,2048]{1,0:T(8,128)(2,1)S(1)}, u32[]{:S(2)}, u32[]{:S(2)}) collective-permute-start(bf16[48,2048]{1,0:T(8,128)(2,1)S(1)} %get-tuple-element.84), channel_id=1, source_target_pairs={{0,4},{2,6},{4,0},{6,2},{1,5},{3,7},{5,1},{7,3},{8,12},{10,14},{12... | collective-permute-start | bytes 589832 | tf_op jit(solution)/shard_map/ppermute | solution.py:438
  102.1 22.0 %collective-permute-done.10.refs_2_ = bf16[96,2048]{1,0:T(8,128)(2,1)S(1)} collective-permute-done((bf16[96,2048]{1,0:T(8,128)(2,1)S(1)}, bf16[96,2048]{1,0:T(8,128)(2,1)S(1)}, u32[]{:S(2)}, u32[]{:S(2)}) %collective-permute-start.10) | collective-permute-done | bytes 393248 | tf_op jit(solution)/shard_map/ppermute | solution.py:438
  124.1 0.9 add.135
  125.0 11.7 %collective-permute-done.41.refs_2_ = bf16[48,2048]{1,0:T(8,128)(2,1)S(1)} collective-permute-done((bf16[48,2048]{1,0:T(8,128)(2,1)S(1)}, bf16[48,2048]{1,0:T(8,128)(2,1)S(1)}, u32[]{:S(2)}, u32[]{:S(2)}) %collective-permute-start.41) | collective-permute-done | bytes 196640 | tf_op jit(solution)/shard_map/ppermute | solution.py:438
  136.7 0.8 add.144
  (64 shorter events, 2.4 us)
Async XLA Ops:
  0.6 18.4 %copy-start = (bf16[256,2048]{1,0:T(8,128)(2,1)S(1)}, bf16[256,2048]{1,0:T(8,128)(2,1)}, u32[]{:S(2)}) copy-start(bf16[256,2048]{1,0:T(8,128)(2,1)} %refs_7_.1) | copy-start | bytes 3145732
  3.1 9.5 %collective-permute-start = (bf16[4,96,256]{2,1,0:T(8,128)(2,1)S(1)}, bf16[4,96,256]{2,1,0:T(8,128)(2,1)S(1)}, u32[]{:S(2)}, u32[]{:S(2)}) collective-permute-start(bf16[4,96,256]{2,1,0:T(8,128)(2,1)S(1)} %get-tuple-element.45), channel_id=1, source_target_pairs={{0,1},{1,0},{2,3},{3,2},{4,5},{5,4},{6,7},{7,6},{8,9},{9,8},{10,11... | collective-permute-start | bytes 589832 | tf_op jit(solution)/shard_map/ppermute | solution.py:442
  3.7 9.0 %collective-permute-start.2 = (bf16[2,384,128]{2,1,0:T(8,128)(2,1)S(1)}, bf16[2,384,128]{2,1,0:T(8,128)(2,1)S(1)}, u32[]{:S(2)}, u32[]{:S(2)}) collective-permute-start(bf16[2,384,128]{2,1,0:T(8,128)(2,1)S(1)} %get-tuple-element.46.refs_11_), channel_id=1, source_target_pairs={{0,8},{8,0},{16,24},{24,16},{1,9},{9,1},{17,25},{25,17},{2,10},{10... | collective-permute-start | bytes 589832 | tf_op jit(solution)/shard_map/ppermute | solution.py:438
  6.2 11.1 %collective-permute-start.3 = (bf16[2,384,128]{2,1,0:T(8,128)(2,1)S(1)}, bf16[2,384,128]{2,1,0:T(8,128)(2,1)S(1)}, u32[]{:S(2)}, u32[]{:S(2)}) collective-permute-start(bf16[2,384,128]{2,1,0:T(8,128)(2,1)S(1)} %get-tuple-element.46.refs_11_), channel_id=1, source_target_pairs={{0,16},{8,24},{16,0},{24,8},{1,17},{9,25},{17,1},{25,9},{2,18},{10... | collective-permute-start | bytes 589832 | tf_op jit(solution)/shard_map/ppermute | solution.py:438
  7.7 11.3 %collective-permute-start.4 = (bf16[2,384,128]{2,1,0:T(8,128)(2,1)S(1)}, bf16[2,384,128]{2,1,0:T(8,128)(2,1)S(1)}, u32[]{:S(2)}, u32[]{:S(2)}) collective-permute-start(bf16[2,384,128]{2,1,0:T(8,128)(2,1)S(1)} %get-tuple-element.46.refs_11_), channel_id=1, source_target_pairs={{0,24},{8,16},{16,8},{24,0},{1,25},{9,17},{17,9},{25,1},{2,26},{10... | collective-permute-start | bytes 589832 | tf_op jit(solution)/shard_map/ppermute | solution.py:438
  10.6 11.2 %collective-permute-start.12 = (bf16[2,32,2048]{2,1,0:T(8,128)(2,1)S(1)}, bf16[2,32,2048]{2,1,0:T(8,128)(2,1)S(1)}, u32[]{:S(2)}, u32[]{:S(2)}) collective-permute-start(bf16[2,32,2048]{2,1,0:T(8,128)(2,1)S(1)} %bitcast.46), channel_id=1, source_target_pairs={{0,8},{8,0},{16,24},{24,16},{1,9},{9,1},{17,25},{25,17},{2,10},{10... | collective-permute-start | bytes 786440 | tf_op jit(solution)/shard_map/ppermute | solution.py:438
  12.6 6.4 %collective-permute-start.5 = (bf16[2,384,128]{2,1,0:T(8,128)(2,1)S(1)}, bf16[2,384,128]{2,1,0:T(8,128)(2,1)S(1)}, u32[]{:S(2)}, u32[]{:S(2)}) collective-permute-start(bf16[2,384,128]{2,1,0:T(8,128)(2,1)S(1)} %get-tuple-element.46.refs_11_), channel_id=1, source_target_pairs={{0,1},{1,0},{2,3},{3,2},{4,5},{5,4},{6,7},{7,6},{8,9},{9,8},{10,11... | collective-permute-start | bytes 589832 | tf_op jit(solution)/shard_map/ppermute | solution.py:442
  12.6 15.6 %collective-permute-start.13 = (bf16[2,32,2048]{2,1,0:T(8,128)(2,1)S(1)}, bf16[2,32,2048]{2,1,0:T(8,128)(2,1)S(1)}, u32[]{:S(2)}, u32[]{:S(2)}) collective-permute-start(bf16[2,32,2048]{2,1,0:T(8,128)(2,1)S(1)} %bitcast.45), channel_id=1, source_target_pairs={{0,16},{8,24},{16,0},{24,8},{1,17},{9,25},{17,1},{25,9},{2,18},{10... | collective-permute-start | bytes 786440 | tf_op jit(solution)/shard_map/ppermute | solution.py:438
  17.4 12.8 %collective-permute-start.14 = (bf16[2,32,2048]{2,1,0:T(8,128)(2,1)S(1)}, bf16[2,32,2048]{2,1,0:T(8,128)(2,1)S(1)}, u32[]{:S(2)}, u32[]{:S(2)}) collective-permute-start(bf16[2,32,2048]{2,1,0:T(8,128)(2,1)S(1)} %bitcast.44), channel_id=1, source_target_pairs={{0,24},{8,16},{16,8},{24,0},{1,25},{9,17},{17,9},{25,1},{2,26},{10... | collective-permute-start | bytes 786440 | tf_op jit(solution)/shard_map/ppermute | solution.py:438
  19.0 11.4 %collective-permute-start.15 = (bf16[2,32,2048]{2,1,0:T(8,128)(2,1)S(1)}, bf16[2,32,2048]{2,1,0:T(8,128)(2,1)S(1)}, u32[]{:S(2)}, u32[]{:S(2)}) collective-permute-start(bf16[2,32,2048]{2,1,0:T(8,128)(2,1)S(1)} %bitcast.31), channel_id=1, source_target_pairs={{0,1},{1,0},{2,3},{3,2},{4,5},{5,4},{6,7},{7,6},{8,9},{9,8},{10,11... | collective-permute-start | bytes 786440 | tf_op jit(solution)/shard_map/ppermute | solution.py:442
  19.1 34.7 %collective-permute-start.1 = (bf16[256,2048]{1,0:T(8,128)(2,1)S(1)}, bf16[256,2048]{1,0:T(8,128)(2,1)S(1)}, u32[]{:S(2)}, u32[]{:S(2)}) collective-permute-start(bf16[256,2048]{1,0:T(8,128)(2,1)S(1)} %copy-done), channel_id=1, source_target_pairs={{0,1},{1,0},{2,3},{3,2},{4,5},{5,4},{6,7},{7,6},{8,9},{9,8},{10,11... | collective-permute-start | bytes 3145736 | tf_op jit(solution)/shard_map/ppermute | solution.py:442
  21.9 12.2 %collective-permute-start.26 = (bf16[2,32,2048]{2,1,0:T(8,128)(2,1)S(1)}, bf16[2,32,2048]{2,1,0:T(8,128)(2,1)S(1)}, u32[]{:S(2)}, u32[]{:S(2)}) collective-permute-start(bf16[2,32,2048]{2,1,0:T(8,128)(2,1)S(1)} %bitcast.43), channel_id=1, source_target_pairs={{0,8},{8,0},{16,24},{24,16},{1,9},{9,1},{17,25},{25,17},{2,10},{10... | collective-permute-start | bytes 786440 | tf_op jit(solution)/shard_map/ppermute | solution.py:438
  28.3 12.7 %collective-permute-start.27 = (bf16[2,32,2048]{2,1,0:T(8,128)(2,1)S(1)}, bf16[2,32,2048]{2,1,0:T(8,128)(2,1)S(1)}, u32[]{:S(2)}, u32[]{:S(2)}) collective-permute-start(bf16[2,32,2048]{2,1,0:T(8,128)(2,1)S(1)} %bitcast.42), channel_id=1, source_target_pairs={{0,16},{8,24},{16,0},{24,8},{1,17},{9,25},{17,1},{25,9},{2,18},{10... | collective-permute-start | bytes 786440 | tf_op jit(solution)/shard_map/ppermute | solution.py:438
  30.2 10.8 %collective-permute-start.28 = (bf16[2,32,2048]{2,1,0:T(8,128)(2,1)S(1)}, bf16[2,32,2048]{2,1,0:T(8,128)(2,1)S(1)}, u32[]{:S(2)}, u32[]{:S(2)}) collective-permute-start(bf16[2,32,2048]{2,1,0:T(8,128)(2,1)S(1)} %bitcast.41), channel_id=1, source_target_pairs={{0,24},{8,16},{16,8},{24,0},{1,25},{9,17},{17,9},{25,1},{2,26},{10... | collective-permute-start | bytes 786440 | tf_op jit(solution)/shard_map/ppermute | solution.py:438
  30.4 11.1 %collective-permute-start.29 = (bf16[2,32,2048]{2,1,0:T(8,128)(2,1)S(1)}, bf16[2,32,2048]{2,1,0:T(8,128)(2,1)S(1)}, u32[]{:S(2)}, u32[]{:S(2)}) collective-permute-start(bf16[2,32,2048]{2,1,0:T(8,128)(2,1)S(1)} %bitcast.33), channel_id=1, source_target_pairs={{0,1},{1,0},{2,3},{3,2},{4,5},{5,4},{6,7},{7,6},{8,9},{9,8},{10,11... | collective-permute-start | bytes 786440 | tf_op jit(solution)/shard_map/ppermute | solution.py:442
  34.0 7.6 %collective-permute-start.30 = (bf16[2,32,2048]{2,1,0:T(8,128)(2,1)S(1)}, bf16[2,32,2048]{2,1,0:T(8,128)(2,1)S(1)}, u32[]{:S(2)}, u32[]{:S(2)}) collective-permute-start(bf16[2,32,2048]{2,1,0:T(8,128)(2,1)S(1)} %collective-permute-done.26.refs_1_), channel_id=1, source_target_pairs={{0,1},{1,0},{2,3},{3,2},{4,5},{5,4},{6,7},{7,6},{8,9},{9,8},{10,11... | collective-permute-start | bytes 786440 | tf_op jit(solution)/shard_map/ppermute | solution.py:442
  41.0 1.5 %collective-permute-start.31 = (bf16[2,32,2048]{2,1,0:T(8,128)(2,1)S(1)}, bf16[2,32,2048]{2,1,0:T(8,128)(2,1)S(1)}, u32[]{:S(2)}, u32[]{:S(2)}) collective-permute-start(bf16[2,32,2048]{2,1,0:T(8,128)(2,1)S(1)} %collective-permute-done.27.refs_2_), channel_id=1, source_target_pairs={{0,1},{1,0},{2,3},{3,2},{4,5},{5,4},{6,7},{7,6},{8,9},{9,8},{10,11... | collective-permute-start | bytes 786440 | tf_op jit(solution)/shard_map/ppermute | solution.py:442
  41.0 1.9 %collective-permute-start.32 = (bf16[2,32,2048]{2,1,0:T(8,128)(2,1)S(1)}, bf16[2,32,2048]{2,1,0:T(8,128)(2,1)S(1)}, u32[]{:S(2)}, u32[]{:S(2)}) collective-permute-start(bf16[2,32,2048]{2,1,0:T(8,128)(2,1)S(1)} %collective-permute-done.28.refs_3_), channel_id=1, source_target_pairs={{0,1},{1,0},{2,3},{3,2},{4,5},{5,4},{6,7},{7,6},{8,9},{9,8},{10,11... | collective-permute-start | bytes 786440 | tf_op jit(solution)/shard_map/ppermute | solution.py:442
  41.5 9.9 %collective-permute-start.6 = (bf16[2,384,128]{2,1,0:T(8,128)(2,1)S(1)}, bf16[2,384,128]{2,1,0:T(8,128)(2,1)S(1)}, u32[]{:S(2)}, u32[]{:S(2)}) collective-permute-start(bf16[2,384,128]{2,1,0:T(8,128)(2,1)S(1)} %collective-permute-done.2.refs_12_), channel_id=1, source_target_pairs={{0,1},{1,0},{2,3},{3,2},{4,5},{5,4},{6,7},{7,6},{8,9},{9,8},{10,11... | collective-permute-start | bytes 589832 | tf_op jit(solution)/shard_map/ppermute | solution.py:442
  41.6 10.2 %collective-permute-start.7 = (bf16[2,384,128]{2,1,0:T(8,128)(2,1)S(1)}, bf16[2,384,128]{2,1,0:T(8,128)(2,1)S(1)}, u32[]{:S(2)}, u32[]{:S(2)}) collective-permute-start(bf16[2,384,128]{2,1,0:T(8,128)(2,1)S(1)} %collective-permute-done.3.refs_13_), channel_id=1, source_target_pairs={{0,1},{1,0},{2,3},{3,2},{4,5},{5,4},{6,7},{7,6},{8,9},{9,8},{10,11... | collective-permute-start | bytes 589832 | tf_op jit(solution)/shard_map/ppermute | solution.py:442
  42.5 9.8 %collective-permute-start.16 = (bf16[2,32,2048]{2,1,0:T(8,128)(2,1)S(1)}, bf16[2,32,2048]{2,1,0:T(8,128)(2,1)S(1)}, u32[]{:S(2)}, u32[]{:S(2)}) collective-permute-start(bf16[2,32,2048]{2,1,0:T(8,128)(2,1)S(1)} %collective-permute-done.12.refs_1_), channel_id=1, source_target_pairs={{0,1},{1,0},{2,3},{3,2},{4,5},{5,4},{6,7},{7,6},{8,9},{9,8},{10,11... | collective-permute-start | bytes 786440 | tf_op jit(solution)/shard_map/ppermute | solution.py:442
  42.9 9.1 %collective-permute-start.8 = (bf16[2,384,128]{2,1,0:T(8,128)(2,1)S(1)}, bf16[2,384,128]{2,1,0:T(8,128)(2,1)S(1)}, u32[]{:S(2)}, u32[]{:S(2)}) collective-permute-start(bf16[2,384,128]{2,1,0:T(8,128)(2,1)S(1)} %collective-permute-done.4.refs_14_), channel_id=1, source_target_pairs={{0,1},{1,0},{2,3},{3,2},{4,5},{5,4},{6,7},{7,6},{8,9},{9,8},{10,11... | collective-permute-start | bytes 589832 | tf_op jit(solution)/shard_map/ppermute | solution.py:442
  51.4 1.6 %collective-permute-start.34 = (bf16[2,32,2048]{2,1,0:T(8,128)(2,1)S(1)}, bf16[2,32,2048]{2,1,0:T(8,128)(2,1)S(1)}, u32[]{:S(2)}, u32[]{:S(2)}) collective-permute-start(bf16[2,32,2048]{2,1,0:T(8,128)(2,1)S(1)} %get-tuple-element.77), channel_id=1, source_target_pairs={{0,1},{1,0},{2,3},{3,2},{4,5},{5,4},{6,7},{7,6},{8,9},{9,8},{10,11... | collective-permute-start | bytes 786440 | tf_op jit(solution)/shard_map/ppermute | solution.py:442
  51.8 1.6 %collective-permute-start.17 = (bf16[2,32,2048]{2,1,0:T(8,128)(2,1)S(1)}, bf16[2,32,2048]{2,1,0:T(8,128)(2,1)S(1)}, u32[]{:S(2)}, u32[]{:S(2)}) collective-permute-start(bf16[2,32,2048]{2,1,0:T(8,128)(2,1)S(1)} %collective-permute-done.13.refs_2_), channel_id=1, source_target_pairs={{0,1},{1,0},{2,3},{3,2},{4,5},{5,4},{6,7},{7,6},{8,9},{9,8},{10,11... | collective-permute-start | bytes 786440 | tf_op jit(solution)/shard_map/ppermute | solution.py:442
  52.0 12.5 %collective-permute-start.18 = (bf16[2,32,2048]{2,1,0:T(8,128)(2,1)S(1)}, bf16[2,32,2048]{2,1,0:T(8,128)(2,1)S(1)}, u32[]{:S(2)}, u32[]{:S(2)}) collective-permute-start(bf16[2,32,2048]{2,1,0:T(8,128)(2,1)S(1)} %collective-permute-done.14.refs_3_), channel_id=1, source_target_pairs={{0,1},{1,0},{2,3},{3,2},{4,5},{5,4},{6,7},{7,6},{8,9},{9,8},{10,11... | collective-permute-start | bytes 786440 | tf_op jit(solution)/shard_map/ppermute | solution.py:442
  52.3 16.1 %collective-permute-start.36 = (bf16[2,32,2048]{2,1,0:T(8,128)(2,1)S(1)}, bf16[2,32,2048]{2,1,0:T(8,128)(2,1)S(1)}, u32[]{:S(2)}, u32[]{:S(2)}) collective-permute-start(bf16[2,32,2048]{2,1,0:T(8,128)(2,1)S(1)} %get-tuple-element.79), channel_id=1, source_target_pairs={{0,1},{1,0},{2,3},{3,2},{4,5},{5,4},{6,7},{7,6},{8,9},{9,8},{10,11... | collective-permute-start | bytes 786440 | tf_op jit(solution)/shard_map/ppermute | solution.py:442
  53.0 15.7 %collective-permute-start.38 = (bf16[2,32,2048]{2,1,0:T(8,128)(2,1)S(1)}, bf16[2,32,2048]{2,1,0:T(8,128)(2,1)S(1)}, u32[]{:S(2)}, u32[]{:S(2)}) collective-permute-start(bf16[2,32,2048]{2,1,0:T(8,128)(2,1)S(1)} %get-tuple-element.81), channel_id=1, source_target_pairs={{0,1},{1,0},{2,3},{3,2},{4,5},{5,4},{6,7},{7,6},{8,9},{9,8},{10,11... | collective-permute-start | bytes 786440 | tf_op jit(solution)/shard_map/ppermute | solution.py:442
  53.4 15.7 %collective-permute-start.33 = (bf16[2,32,2048]{2,1,0:T(8,128)(2,1)S(1)}, bf16[2,32,2048]{2,1,0:T(8,128)(2,1)S(1)}, u32[]{:S(2)}, u32[]{:S(2)}) collective-permute-start(bf16[2,32,2048]{2,1,0:T(8,128)(2,1)S(1)} %get-tuple-element.75), channel_id=1, source_target_pairs={{0,1},{1,0},{2,3},{3,2},{4,5},{5,4},{6,7},{7,6},{8,9},{9,8},{10,11... | collective-permute-start | bytes 786440 | tf_op jit(solution)/shard_map/ppermute | solution.py:442
  53.7 17.2 %collective-permute-start.35 = (bf16[2,32,2048]{2,1,0:T(8,128)(2,1)S(1)}, bf16[2,32,2048]{2,1,0:T(8,128)(2,1)S(1)}, u32[]{:S(2)}, u32[]{:S(2)}) collective-permute-start(bf16[2,32,2048]{2,1,0:T(8,128)(2,1)S(1)} %add.141), channel_id=1, source_target_pairs={{0,8},{8,0},{16,24},{24,16},{1,9},{9,1},{17,25},{25,17},{2,10},{10... | collective-permute-start | bytes 786440 | tf_op jit(solution)/shard_map/ppermute | solution.py:438
  68.1 4.4 %collective-permute-start.20 = (bf16[2,32,2048]{2,1,0:T(8,128)(2,1)S(1)}, bf16[2,32,2048]{2,1,0:T(8,128)(2,1)S(1)}, u32[]{:S(2)}, u32[]{:S(2)}) collective-permute-start(bf16[2,32,2048]{2,1,0:T(8,128)(2,1)S(1)} %get-tuple-element.62), channel_id=1, source_target_pairs={{0,1},{1,0},{2,3},{3,2},{4,5},{5,4},{6,7},{7,6},{8,9},{9,8},{10,11... | collective-permute-start | bytes 786440 | tf_op jit(solution)/shard_map/ppermute | solution.py:442
  68.4 4.1 %collective-permute-start.22 = (bf16[2,32,2048]{2,1,0:T(8,128)(2,1)S(1)}, bf16[2,32,2048]{2,1,0:T(8,128)(2,1)S(1)}, u32[]{:S(2)}, u32[]{:S(2)}) collective-permute-start(bf16[2,32,2048]{2,1,0:T(8,128)(2,1)S(1)} %get-tuple-element.64), channel_id=1, source_target_pairs={{0,1},{1,0},{2,3},{3,2},{4,5},{5,4},{6,7},{7,6},{8,9},{9,8},{10,11... | collective-permute-start | bytes 786440 | tf_op jit(solution)/shard_map/ppermute | solution.py:442
  68.7 4.4 %collective-permute-start.24 = (bf16[2,32,2048]{2,1,0:T(8,128)(2,1)S(1)}, bf16[2,32,2048]{2,1,0:T(8,128)(2,1)S(1)}, u32[]{:S(2)}, u32[]{:S(2)}) collective-permute-start(bf16[2,32,2048]{2,1,0:T(8,128)(2,1)S(1)} %get-tuple-element.66), channel_id=1, source_target_pairs={{0,1},{1,0},{2,3},{3,2},{4,5},{5,4},{6,7},{7,6},{8,9},{9,8},{10,11... | collective-permute-start | bytes 786440 | tf_op jit(solution)/shard_map/ppermute | solution.py:442
  69.1 14.1 %collective-permute-start.37 = (bf16[2,32,2048]{2,1,0:T(8,128)(2,1)S(1)}, bf16[2,32,2048]{2,1,0:T(8,128)(2,1)S(1)}, u32[]{:S(2)}, u32[]{:S(2)}) collective-permute-start(bf16[2,32,2048]{2,1,0:T(8,128)(2,1)S(1)} %add.142), channel_id=1, source_target_pairs={{0,16},{8,24},{16,0},{24,8},{1,17},{9,25},{17,1},{25,9},{2,18},{10... | collective-permute-start | bytes 786440 | tf_op jit(solution)/shard_map/ppermute | solution.py:438
  70.9 14.1 %collective-permute-start.39 = (bf16[2,32,2048]{2,1,0:T(8,128)(2,1)S(1)}, bf16[2,32,2048]{2,1,0:T(8,128)(2,1)S(1)}, u32[]{:S(2)}, u32[]{:S(2)}) collective-permute-start(bf16[2,32,2048]{2,1,0:T(8,128)(2,1)S(1)} %add.143), channel_id=1, source_target_pairs={{0,24},{8,16},{16,8},{24,0},{1,25},{9,17},{17,9},{25,1},{2,26},{10... | collective-permute-start | bytes 786440 | tf_op jit(solution)/shard_map/ppermute | solution.py:438
  72.5 14.3 %collective-permute-start.19 = (bf16[2,32,2048]{2,1,0:T(8,128)(2,1)S(1)}, bf16[2,32,2048]{2,1,0:T(8,128)(2,1)S(1)}, u32[]{:S(2)}, u32[]{:S(2)}) collective-permute-start(bf16[2,32,2048]{2,1,0:T(8,128)(2,1)S(1)} %get-tuple-element.60), channel_id=1, source_target_pairs={{0,1},{1,0},{2,3},{3,2},{4,5},{5,4},{6,7},{7,6},{8,9},{9,8},{10,11... | collective-permute-start | bytes 786440 | tf_op jit(solution)/shard_map/ppermute | solution.py:442
  72.5 16.8 %collective-permute-start.21 = (bf16[2,32,2048]{2,1,0:T(8,128)(2,1)S(1)}, bf16[2,32,2048]{2,1,0:T(8,128)(2,1)S(1)}, u32[]{:S(2)}, u32[]{:S(2)}) collective-permute-start(bf16[2,32,2048]{2,1,0:T(8,128)(2,1)S(1)} %add.137), channel_id=1, source_target_pairs={{0,8},{8,0},{16,24},{24,16},{1,9},{9,1},{17,25},{25,17},{2,10},{10... | collective-permute-start | bytes 786440 | tf_op jit(solution)/shard_map/ppermute | solution.py:438
  73.1 28.8 %collective-permute-start.9 = (bf16[96,2048]{1,0:T(8,128)(2,1)S(1)}, bf16[96,2048]{1,0:T(8,128)(2,1)S(1)}, u32[]{:S(2)}, u32[]{:S(2)}) collective-permute-start(bf16[96,2048]{1,0:T(8,128)(2,1)S(1)} %get-tuple-element.48), channel_id=1, source_target_pairs={{0,2},{2,0},{4,6},{6,4},{1,3},{3,1},{5,7},{7,5},{8,10},{10,8},{12,... | collective-permute-start | bytes 1179656 | tf_op jit(solution)/shard_map/ppermute | solution.py:438
  83.2 13.2 %collective-permute-start.23 = (bf16[2,32,2048]{2,1,0:T(8,128)(2,1)S(1)}, bf16[2,32,2048]{2,1,0:T(8,128)(2,1)S(1)}, u32[]{:S(2)}, u32[]{:S(2)}) collective-permute-start(bf16[2,32,2048]{2,1,0:T(8,128)(2,1)S(1)} %add.138), channel_id=1, source_target_pairs={{0,16},{8,24},{16,0},{24,8},{1,17},{9,25},{17,1},{25,9},{2,18},{10... | collective-permute-start | bytes 786440 | tf_op jit(solution)/shard_map/ppermute | solution.py:438
  85.0 11.5 %collective-permute-start.25 = (bf16[2,32,2048]{2,1,0:T(8,128)(2,1)S(1)}, bf16[2,32,2048]{2,1,0:T(8,128)(2,1)S(1)}, u32[]{:S(2)}, u32[]{:S(2)}) collective-permute-start(bf16[2,32,2048]{2,1,0:T(8,128)(2,1)S(1)} %add.139), channel_id=1, source_target_pairs={{0,24},{8,16},{16,8},{24,0},{1,25},{9,17},{17,9},{25,1},{2,26},{10... | collective-permute-start | bytes 786440 | tf_op jit(solution)/shard_map/ppermute | solution.py:438
  86.7 37.4 %collective-permute-start.10 = (bf16[96,2048]{1,0:T(8,128)(2,1)S(1)}, bf16[96,2048]{1,0:T(8,128)(2,1)S(1)}, u32[]{:S(2)}, u32[]{:S(2)}) collective-permute-start(bf16[96,2048]{1,0:T(8,128)(2,1)S(1)} %get-tuple-element.49), channel_id=1, source_target_pairs={{0,4},{2,6},{4,0},{6,2},{1,5},{3,7},{5,1},{7,3},{8,12},{10,14},{12... | collective-permute-start | bytes 1179656 | tf_op jit(solution)/shard_map/ppermute | solution.py:438
  89.3 34.8 %collective-permute-start.11 = (bf16[96,2048]{1,0:T(8,128)(2,1)S(1)}, bf16[96,2048]{1,0:T(8,128)(2,1)S(1)}, u32[]{:S(2)}, u32[]{:S(2)}) collective-permute-start(bf16[96,2048]{1,0:T(8,128)(2,1)S(1)} %get-tuple-element.50), channel_id=1, source_target_pairs={{0,6},{2,4},{4,2},{6,0},{1,7},{3,5},{5,3},{7,1},{8,14},{10,12},{12... | collective-permute-start | bytes 1179656 | tf_op jit(solution)/shard_map/ppermute | solution.py:438
  97.6 27.4 %collective-permute-start.40 = (bf16[48,2048]{1,0:T(8,128)(2,1)S(1)}, bf16[48,2048]{1,0:T(8,128)(2,1)S(1)}, u32[]{:S(2)}, u32[]{:S(2)}) collective-permute-start(bf16[48,2048]{1,0:T(8,128)(2,1)S(1)} %get-tuple-element.83), channel_id=1, source_target_pairs={{0,2},{2,0},{4,6},{6,4},{1,3},{3,1},{5,7},{7,5},{8,10},{10,8},{12,... | collective-permute-start | bytes 589832 | tf_op jit(solution)/shard_map/ppermute | solution.py:438
  99.3 37.4 %collective-permute-start.41 = (bf16[48,2048]{1,0:T(8,128)(2,1)S(1)}, bf16[48,2048]{1,0:T(8,128)(2,1)S(1)}, u32[]{:S(2)}, u32[]{:S(2)}) collective-permute-start(bf16[48,2048]{1,0:T(8,128)(2,1)S(1)} %get-tuple-element.84), channel_id=1, source_target_pairs={{0,4},{2,6},{4,0},{6,2},{1,5},{3,7},{5,1},{7,3},{8,12},{10,14},{12... | collective-permute-start | bytes 589832 | tf_op jit(solution)/shard_map/ppermute | solution.py:438
  101.9 34.8 %collective-permute-start.42 = (bf16[48,2048]{1,0:T(8,128)(2,1)S(1)}, bf16[48,2048]{1,0:T(8,128)(2,1)S(1)}, u32[]{:S(2)}, u32[]{:S(2)}) collective-permute-start(bf16[48,2048]{1,0:T(8,128)(2,1)S(1)} %get-tuple-element.85), channel_id=1, source_target_pairs={{0,6},{2,4},{4,2},{6,0},{1,7},{3,5},{5,3},{7,1},{8,14},{10,12},{12... | collective-permute-start | bytes 589832 | tf_op jit(solution)/shard_map/ppermute | solution.py:438

commit v7 on v6

--- a/solution.py
+++ b/solution.py
@@ -100,22 +100,51 @@
     )
 
 
-def add_kernel(*refs):
-    total = refs[0][...].astype(F32)
-    for ref in refs[1:-1]:
+def add_kernel(n_out, *refs):
+    ins, outs = refs[:-n_out], refs[-n_out:]
+    total = ins[0][...].astype(F32)
+    for ref in ins[1:]:
         total = total + ref[...].astype(F32)
-    refs[-1][...] = total.astype(BF16)
-
-
-def add(*arrays):
+    width = outs[0].shape[-1]
+    for n, ref in enumerate(outs):
+        ref[...] = total[..., n * width : (n + 1) * width].astype(BF16)
+
+
+def add(*arrays, halves=1):
+    *lead, width = arrays[0].shape
+    out = jax.ShapeDtypeStruct((*lead, width // halves), BF16)
     return pl.pallas_call(
-        add_kernel,
+        lambda *refs: add_kernel(halves, *refs),
         in_specs=[IN_VMEM] * len(arrays),
-        out_specs=IN_VMEM,
-        out_shape=jax.ShapeDtypeStruct(arrays[0].shape, BF16),
+        out_specs=[IN_VMEM] * halves,
+        out_shape=[out] * halves,
         compiler_params=pltpu.CompilerParams(vmem_limit_bytes=8 * MIB),
         name="add",
     )(*arrays)
+
+
+def join_kernel(*refs):
+    ins, out_ref = refs[:-1], refs[-1]
+    width = ins[0].shape[-1]
+    count = out_ref.shape[-1] // width
+    for n in range(count):
+        total = ins[n][...].astype(F32)
+        for ref in ins[n + count :: count]:
+            total = total + ref[...].astype(F32)
+        out_ref[:, n * width : (n + 1) * width] = total.astype(BF16)
+
+
+def join(parts):
+    flat = [h for part in parts for h in part]
+    rows, width = flat[0].shape
+    return pl.pallas_call(
+        join_kernel,
+        in_specs=[IN_VMEM] * len(flat),
+        out_specs=IN_VMEM,
+        out_shape=jax.ShapeDtypeStruct((rows, width * len(parts[0])), BF16),
+        compiler_params=pltpu.CompilerParams(vmem_limit_bytes=8 * MIB),
+        name="join",
+    )(*flat)
 
 
 def weight_copies(sources, targets, first, sems, sem):
@@ -157,25 +186,34 @@
     )(after, *in_hbm(weights))
 
 
-def mix_kernel(n_pieces, n_z, z_ref, q_own, q_other, gain_hbm, cos_ref, sin_ref, w_other, *rest):
-    pieces = rest[4 : 4 + n_pieces]
-    outs = rest[4 + n_pieces : 4 + n_pieces + n_z]
-    loaded = rest[4 + n_pieces + n_z : 7 + n_pieces + n_z]
-    keys_ref, vals_ref, mixed_ref, w_own, gain_ref, sems = rest[7 + n_pieces + n_z :]
+def mix_kernel(n_pieces, steps, n_loads, z_ref, q_own, q_other, gain_hbm, cos_ref, sin_ref, *rest):
+    n_z = q_own.shape[0]
+    w_other, w_hbm = rest[:2]
+    pieces = rest[2 : 2 + n_pieces]
+    sources = rest[2 + n_pieces : 2 + n_pieces + n_loads]
+    outs = rest[2 + n_pieces + n_loads : -4]
+    mixed_ref, w_own, gain_ref, sems = rest[-4:]
+    n_out = len(steps)
+    loaded = outs[n_out : n_out + n_loads]
     copies = [
         pltpu.make_async_copy(gain_hbm, gain_ref, sems.at[0]),
-        pltpu.make_async_copy(rest[0], w_own, sems.at[1]),
-        *weight_copies(rest[1:4], loaded, 0, sems, 2),
+        pltpu.make_async_copy(w_hbm, w_own, sems.at[1]),
+        *weight_copies(sources, loaded, 0, sems, 2),
     ]
     for copy in copies:
         copy.start()
-    row = 0
-    for piece in pieces:
-        rows = piece.shape[1]
-        keys_ref[row : row + rows] = piece[0]
-        vals_ref[row : row + rows, :HD] = piece[1]
-        row += rows
-    vals_ref[:, HD:] = jnp.ones((row, HD), BF16)
+    if len(outs) > n_out + n_loads:
+        keys_ref, vals_ref = outs[n_out + n_loads :]
+        row = 0
+        for piece in pieces:
+            rows = piece.shape[1]
+            keys_ref[row : row + rows] = piece[0]
+            vals_ref[row : row + rows, :HD] = piece[1]
+            row += rows
+        vals_ref[:, HD:] = jnp.ones((row, HD), BF16)
+    else:
+        keys_ref, vals_ref = pieces
+        row = keys_ref.shape[0]
     factor = HD ** (-0.5) * 1.4426950408889634
     part = q_own.shape[1]
     heads = q_own.shape[-1] // HD
@@ -187,7 +225,7 @@
     copies[1].wait()
 
     def one(n, carry):
-        block = peer(z_ref[0], n, n_z)
+        block = peer(z_ref[0], n + steps[0], n_z)
         at = pl.multiple_of(block * part, 16)
         cosine, sine = cos_ref[pl.ds(at, part)], sin_ref[pl.ds(at, part)]
         queries = []
@@ -228,41 +266,42 @@
         mixed_ref[n] = mixed.astype(BF16)
         return carry
 
-    lax.fori_loop(0, n_z, one, 0)
-    for n, out_ref in enumerate(outs):
+    lax.fori_loop(0, n_out, one, 0)
+    for n, out_ref in enumerate(outs[:n_out]):
         out_ref[...] = mixed_ref[n]
     for copy in copies[2:]:
         copy.wait()
 
 
-def mix(z_index, q_own, q_other, gain, cosine, sine, w_own, w_other, weights, per, pieces):
-    n_z, part, _ = q_own.shape
+def mix(z_index, q_own, q_other, gain, cosine, sine, w_own, w_other, pieces, steps, loads, per):
+    _, part, _ = q_own.shape
     d_model = w_own.shape[-1]
-    length = sum(p.shape[1] for p in pieces)
+    joined = len(pieces) == 2
+    length = pieces[0].shape[0] if joined else sum(p.shape[1] for p in pieces)
+    whole = [] if joined else [(length, HD), (length, 2 * HD)]
     any_space = pl.BlockSpec(memory_space=pl.ANY)
+    shapes = [(part, d_model)] * len(steps) + [(per, *w.shape[1:]) for w in loads] + whole
     outs = pl.pallas_call(
-        lambda *refs: mix_kernel(len(pieces), n_z, *refs),
-        in_specs=[IN_SMEM, IN_VMEM, IN_VMEM, any_space, IN_VMEM, IN_VMEM, IN_VMEM]
-        + [any_space] * 4
-        + [IN_VMEM] * len(pieces),
-        out_specs=[IN_VMEM] * (n_z + 3),
-        out_shape=[jax.ShapeDtypeStruct((part, d_model), BF16)] * n_z
-        + [jax.ShapeDtypeStruct((per, *w.shape[1:]), BF16) for w in weights],
+        lambda *refs: mix_kernel(len(pieces), steps, len(loads), *refs),
+        in_specs=[IN_SMEM, IN_VMEM, IN_VMEM, any_space, IN_VMEM, IN_VMEM, IN_VMEM, any_space]
+        + [IN_VMEM] * len(pieces)
+        + [any_space] * len(loads),
+        out_specs=[IN_VMEM] * len(shapes),
+        out_shape=[jax.ShapeDtypeStruct(shape, BF16) for shape in shapes],
         scratch_shapes=[
-            pltpu.VMEM((length, HD), BF16),
-            pltpu.VMEM((length, 2 * HD), BF16),
-            pltpu.VMEM((n_z, part, d_model), BF16),
+            pltpu.VMEM((len(steps), part, d_model), BF16),
             pltpu.VMEM(w_own.shape, BF16),
             pltpu.VMEM(gain.shape, F32),
-            pltpu.SemaphoreType.DMA((2 + 3 * per * SPLIT,)),
+            pltpu.SemaphoreType.DMA((2 + len(loads) * per * SPLIT,)),
         ],
-        compiler_params=pltpu.CompilerParams(vmem_limit_bytes=8 * MIB + length * HD * 6),
+        compiler_params=pltpu.CompilerParams(vmem_limit_bytes=10 * MIB),
         name="mix",
     )(
-        z_index, q_own, q_other, *in_hbm([gain]), cosine, sine, w_other,
-        *in_hbm([w_own, *weights]), *pieces,
+        z_index, q_own, q_other, *in_hbm([gain]), cosine, sine, w_other, *in_hbm([w_own]),
+        *pieces, *in_hbm(loads),
     )
-    return outs[:n_z], outs[n_z:]
+    at = len(steps)
+    return outs[:at], outs[at : at + len(loads)], outs[at + len(loads) :]
 
 
 def block_of(index, block, count):
@@ -393,10 +432,12 @@
     return outs[: len(own)], outs[len(own) :]
 
 
-def combine_kernel(n_back, z_ref, cols_ref, *rest):
+def combine_kernel(n_back, at, z_ref, cols_ref, *rest):
     back_refs, out_refs, total_ref = rest[:n_back], rest[n_back:-1], rest[-1]
     rows = cols_ref.shape[0]
-    back = jnp.concatenate([ref[...] for ref in back_refs], axis=0)
+    width = total_ref.shape[-1]
+    back = [ref[:, at : at + width] if ref.shape[-1] > width else ref[...] for ref in back_refs]
+    back = jnp.concatenate(back, axis=0)
     slot = lax.broadcasted_iota(jnp.int32, (rows, back.shape[0]), 1)
     matrix = jnp.zeros(slot.shape, F32)
     for k in range(TOPK):
@@ -412,17 +453,21 @@
         out_ref[...] = total_ref[peer(z_ref[0], n, n_z)].astype(BF16)
 
 
-def combine(z_index, cols, backs, n_z):
-    rows, d_model = cols.shape[0], backs[0].shape[-1]
+def combine(z_index, cols, backs, n_z, at, width):
+    rows = cols.shape[0]
     return pl.pallas_call(
-        lambda *refs: combine_kernel(len(backs), *refs),
+        lambda *refs: combine_kernel(len(backs), at, *refs),
         in_specs=[IN_SMEM] + [IN_VMEM] * (1 + len(backs)),
         out_specs=[IN_VMEM] * n_z,
-        out_shape=[jax.ShapeDtypeStruct((rows // n_z, d_model), BF16)] * n_z,
-        scratch_shapes=[pltpu.VMEM((n_z, rows // n_z, d_model), F32)],
+        out_shape=[jax.ShapeDtypeStruct((rows // n_z, width), BF16)] * n_z,
+        scratch_shapes=[pltpu.VMEM((n_z, rows // n_z, width), F32)],
         compiler_params=pltpu.CompilerParams(vmem_limit_bytes=24 * MIB),
         name="combine",
     )(z_index, cols, *backs)
+
+
+def chunks_of(n_local):
+    return 2 if n_local % 2 == 0 else 1
 
 
 def peer(own, step, n):
@@ -486,7 +531,7 @@
     w_other = swap_cores(out_weight)
 
     n_local = gate_weight.shape[0]
-    chunks = 2 if n_local % 2 == 0 else 1
+    chunks = chunks_of(n_local)
     per = n_local // chunks
     ep_arg = lax.axis_index("ep").reshape(1).astype(jnp.int32)
     outgoing, cols = dispatch(
@@ -503,29 +548,35 @@
 
     all_weights = [gate_weight, up_weight, down_weight]
     weights = [load(all_weights, chunk * per, per, cols) for chunk in range(1, chunks)]
-    mixed, first_weights = mix(
-        z_arg, q_own, q_other, query_gain[None], cosine, sine, out_weight, w_other,
-        all_weights, per, pieces,
-    )
-    weights = [first_weights, *weights]
-    gathered = [mixed[0]]
-    for step in range(1, n_z):
-        gathered.append(shift(mixed[step], "z", step))
-    mixed_out = add(*gathered)
-
-    backs = []
+    steps = list(range(n_z))
+    far, near = steps[n_z // 2 :], steps[: n_z // 2]
+    own = (z_arg, q_own, q_other, query_gain[None], cosine, sine, out_weight, w_other)
+    far_rows, first_part, joined = mix(*own, pieces, far, all_weights[:2], per)
+    near_rows, last_part, _ = mix(*own, joined, near, all_weights[2:], per)
+    weights = [[*first_part, *last_part], *weights]
+    gathered = []
+    for step, rows in zip(near + far, [*near_rows, *far_rows]):
+        gathered.append(shift(rows, "z", step) if step else rows)
+    mixed_out = add(*gathered)[0]
+
+    backs = [[], []]
     for chunk in range(chunks):
+        halves = 2 if chunk == chunks - 1 else 1
         keep, send = experts(*arrived[chunk], weights[chunk])
         for step in range(n_ep):
-            result = add(keep[step], swap_cores(send[step]))
-            result = shift(result, "ep", step, back=True) if step else result
-            backs.append(result.reshape(-1, d_model))
-    rows = combine(z_arg, cols, backs, n_z)
-    gathered = [rows[0]]
-    for step in range(1, n_z):
-        gathered.append(shift(rows[step], "z", step))
-    expert_out = add(*gathered)
-    return (mixed_out, expert_out)
+            result = add(keep[step], swap_cores(send[step]), halves=halves)
+            for half in range(2):
+                if half < halves:
+                    piece = shift(result[half], "ep", step, back=True) if step else result[half]
+                    piece = piece.reshape(-1, piece.shape[-1])
+                backs[half].append(piece)
+    parts = [[] for _ in range(n_z)]
+    for half in range(2):
+        width = d_model // 2
+        rows = combine(z_arg, cols, backs[half], n_z, half * width, width)
+        for step in range(n_z):
+            parts[step].append(shift(rows[step], "z", step) if step else rows[step])
+    return (mixed_out, join(parts))
 
 
 def solution(mesh):

time: 140 us -> 143 us (1.021)
  starting transfers between devices: 35.9 us -> 44.1 us
  waiting for transfers between devices: 69.4 us -> 63.2 us
  Pallas kernels: 30.3 us -> 32.4 us
    ppermute x21 -> x27, starting transfers between devices: 30.9 us -> 39.1 us  [shift(): return lax.ppermute(a, axis, pairs)]
    ppermute x21 -> x27, waiting for transfers between devices: 68.1 us -> 62 us  [shift(): return lax.ppermute(a, axis, pairs)]
    pallas_call x12 -> x14, Pallas kernels: 14.1 us -> 16.3 us  [the longest x2 12.5 us: mix(): pl.pallas_call(lambda *refs: mix_kernel(len(pieces), steps, len(loads), *...]
  transfers between devices with their start and end apart: 43 -> 49, of which waited for: 12 -> 15; matrix products, arithmetic and copies ran while one was open for 0% -> 0% of each run, Pallas kernels for 20% -> 21%
where the time goes in v7:
time: 143 us; the launch traced here: 142 us
  waiting for transfers between devices  63.2 us (44%)
  starting transfers between devices  44.1 us (31%)
  Pallas kernels  32.4 us (23%)
    ppermute x27, waiting for transfers between devices, shift(): return lax.ppermute(a, axis, pairs)  62 us
    ppermute x27, starting transfers between devices, shift(): return lax.ppermute(a, axis, pairs)  39.1 us
    pallas_call x2, Pallas kernels, mix(): pl.pallas_call(lambda *refs: mix_kernel(len(pieces), steps, len(loads), *...  12.5 us
    pallas_call x2, Pallas kernels, experts(): pl.pallas_call(lambda *refs: expert_kernel(len(pieces), group, *refs), in...  7.18 us
    ppermute x22, starting transfers between devices, swap_cores(): return lax.ppermute(a, 'core', [(i, CORES - 1 - i) for i in range(CORES)])  5.07 us
    pallas_call x1, Pallas kernels, load(): pl.pallas_call(lambda *refs: load_kernel(first, *refs), in_specs=[any_spa...  4.7 us
  transfers between devices with their start and end apart: 49, of which 15 were waited for; matrix products, arithmetic and copies ran while one was open for 0% of the time, Pallas kernels for 21%

profile of v7, /device:TPU:0, one launch (start us, length us, event | category | flops | bytes accessed | tf_op | source)
XLA Modules:
  0.0 141.7 jit_solution(4580451250494904562)
XLA Ops:
  0.9 0.8 sine_multiply_fusion
  1.7 1.4 %prepare.1 = (bf16[2,384,128]{2,1,0:T(8,128)(2,1)S(1)}, bf16[4,96,256]{2,1,0:T(8,128)(2,1)S(1)}, bf16[4,96,256]{2,1,0:T(8,128)(2,1)S(1)}) custom-call(s32[1]{0:T(128)} %bitcast.1.core_ref.refs_0_, s32[1]{0:T(128)} %bitcast.2.head_ref, bf16[4,2,96,512]{3,2,1,0:T(8,128)(2,1)} %bitcast.62, bf16[4,2,96,512]{3,2,1,0:T(8,128)(2,1)} %bitcast.63, ...), custom_call_target="tpu_custom_call" | custom-call | tf_op jit(solution)/shard_map/prepare/pallas_call | solution.py:74
  3.1 0.6 collective-permute-start
  3.7 2.6 %collective-permute-start.2 = (bf16[2,384,128]{2,1,0:T(8,128)(2,1)S(1)}, bf16[2,384,128]{2,1,0:T(8,128)(2,1)S(1)}, u32[]{:S(2)}, u32[]{:S(2)}) collective-permute-start(bf16[2,384,128]{2,1,0:T(8,128)(2,1)S(1)} %get-tuple-element.60.refs_8_), channel_id=1, source_target_pairs={{0,8},{8,0},{16,24},{24,16},{1,9},{9,1},{17,25},{25,17},{2,10},{10... | collective-permute-start | bytes 589832 | tf_op jit(solution)/shard_map/ppermute | solution.py:483
  6.2 1.5 %collective-permute-start.3 = (bf16[2,384,128]{2,1,0:T(8,128)(2,1)S(1)}, bf16[2,384,128]{2,1,0:T(8,128)(2,1)S(1)}, u32[]{:S(2)}, u32[]{:S(2)}) collective-permute-start(bf16[2,384,128]{2,1,0:T(8,128)(2,1)S(1)} %get-tuple-element.60.refs_8_), channel_id=1, source_target_pairs={{0,16},{8,24},{16,0},{24,8},{1,17},{9,25},{17,1},{25,9},{2,18},{10... | collective-permute-start | bytes 589832 | tf_op jit(solution)/shard_map/ppermute | solution.py:483
  7.8 2.8 %dispatch.1 = (bf16[64,2048]{1,0:T(8,128)(2,1)S(1)}, bf16[64,2048]{1,0:T(8,128)(2,1)S(1)}, bf16[64,2048]{1,0:T(8,128)(2,1)S(1)}, bf16[64,2048]{1,0:T(8,128)(2,1)...) custom-call(s32[1]{0:T(128)} %bitcast.1.core_ref.refs_0_, ...), custom_call_target="tpu_custom_call" | custom-call | tf_op jit(solution)/shard_map/dispatch/pallas_call | solution.py:382
  10.6 2.0 %collective-permute-start.12 = (bf16[2,32,2048]{2,1,0:T(8,128)(2,1)S(1)}, bf16[2,32,2048]{2,1,0:T(8,128)(2,1)S(1)}, u32[]{:S(2)}, u32[]{:S(2)}) collective-permute-start(bf16[2,32,2048]{2,1,0:T(8,128)(2,1)S(1)} %bitcast.58), channel_id=1, source_target_pairs={{0,8},{8,0},{16,24},{24,16},{1,9},{9,1},{17,25},{25,17},{2,10},{10... | collective-permute-start | bytes 786440 | tf_op jit(solution)/shard_map/ppermute | solution.py:483
  12.6 1.5 %collective-permute-start.13 = (bf16[2,32,2048]{2,1,0:T(8,128)(2,1)S(1)}, bf16[2,32,2048]{2,1,0:T(8,128)(2,1)S(1)}, u32[]{:S(2)}, u32[]{:S(2)}) collective-permute-start(bf16[2,32,2048]{2,1,0:T(8,128)(2,1)S(1)} %bitcast.57), channel_id=1, source_target_pairs={{0,16},{8,24},{16,0},{24,8},{1,17},{9,25},{17,1},{25,9},{2,18},{10... | collective-permute-start | bytes 786440 | tf_op jit(solution)/shard_map/ppermute | solution.py:483
  14.2 3.2 %collective-permute-done.3.refs_10_ = bf16[2,384,128]{2,1,0:T(8,128)(2,1)S(1)} collective-permute-done((bf16[2,384,128]{2,1,0:T(8,128)(2,1)S(1)}, bf16[2,384,128]{2,1,0:T(8,128)(2,1)S(1)}, u32[]{:S(2)}, u32[]{:S(2)}) %collective-permute-start.3) | collective-permute-done | bytes 196640 | tf_op jit(solution)/shard_map/ppermute | solution.py:483
  17.4 1.7 %collective-permute-start.14 = (bf16[2,32,2048]{2,1,0:T(8,128)(2,1)S(1)}, bf16[2,32,2048]{2,1,0:T(8,128)(2,1)S(1)}, u32[]{:S(2)}, u32[]{:S(2)}) collective-permute-start(bf16[2,32,2048]{2,1,0:T(8,128)(2,1)S(1)} %bitcast.56), channel_id=1, source_target_pairs={{0,24},{8,16},{16,8},{24,0},{1,25},{9,17},{17,9},{25,1},{2,26},{10... | collective-permute-start | bytes 786440 | tf_op jit(solution)/shard_map/ppermute | solution.py:483
  19.0 0.5 collective-permute-start.1
  19.5 2.3 %collective-permute-done.12.refs_1_ = bf16[2,32,2048]{2,1,0:T(8,128)(2,1)S(1)} collective-permute-done((bf16[2,32,2048]{2,1,0:T(8,128)(2,1)S(1)}, bf16[2,32,2048]{2,1,0:T(8,128)(2,1)S(1)}, u32[]{:S(2)}, u32[]{:S(2)}) %collective-permute-start.12) | collective-permute-done | bytes 262176 | tf_op jit(solution)/shard_map/ppermute | solution.py:483
  21.9 2.0 %collective-permute-start.26 = (bf16[2,32,2048]{2,1,0:T(8,128)(2,1)S(1)}, bf16[2,32,2048]{2,1,0:T(8,128)(2,1)S(1)}, u32[]{:S(2)}, u32[]{:S(2)}) collective-permute-start(bf16[2,32,2048]{2,1,0:T(8,128)(2,1)S(1)} %bitcast.55), channel_id=1, source_target_pairs={{0,8},{8,0},{16,24},{24,16},{1,9},{9,1},{17,25},{25,17},{2,10},{10... | collective-permute-start | bytes 786440 | tf_op jit(solution)/shard_map/ppermute | solution.py:483
  23.9 4.4 %collective-permute-done.13.refs_2_ = bf16[2,32,2048]{2,1,0:T(8,128)(2,1)S(1)} collective-permute-done((bf16[2,32,2048]{2,1,0:T(8,128)(2,1)S(1)}, bf16[2,32,2048]{2,1,0:T(8,128)(2,1)S(1)}, u32[]{:S(2)}, u32[]{:S(2)}) %collective-permute-start.13) | collective-permute-done | bytes 262176 | tf_op jit(solution)/shard_map/ppermute | solution.py:483
  28.3 1.9 %collective-permute-start.27 = (bf16[2,32,2048]{2,1,0:T(8,128)(2,1)S(1)}, bf16[2,32,2048]{2,1,0:T(8,128)(2,1)S(1)}, u32[]{:S(2)}, u32[]{:S(2)}) collective-permute-start(bf16[2,32,2048]{2,1,0:T(8,128)(2,1)S(1)} %bitcast.54), channel_id=1, source_target_pairs={{0,16},{8,24},{16,0},{24,8},{1,17},{9,25},{17,1},{25,9},{2,18},{10... | collective-permute-start | bytes 786440 | tf_op jit(solution)/shard_map/ppermute | solution.py:483
  30.4 3.6 %collective-permute-done.26.refs_1_ = bf16[2,32,2048]{2,1,0:T(8,128)(2,1)S(1)} collective-permute-done((bf16[2,32,2048]{2,1,0:T(8,128)(2,1)S(1)}, bf16[2,32,2048]{2,1,0:T(8,128)(2,1)S(1)}, u32[]{:S(2)}, u32[]{:S(2)}) %collective-permute-start.26) | collective-permute-done | bytes 262176 | tf_op jit(solution)/shard_map/ppermute | solution.py:483
  34.0 7.0 %collective-permute-done.27.refs_2_ = bf16[2,32,2048]{2,1,0:T(8,128)(2,1)S(1)} collective-permute-done((bf16[2,32,2048]{2,1,0:T(8,128)(2,1)S(1)}, bf16[2,32,2048]{2,1,0:T(8,128)(2,1)S(1)}, u32[]{:S(2)}, u32[]{:S(2)}) %collective-permute-start.27) | collective-permute-done | bytes 262176 | tf_op jit(solution)/shard_map/ppermute | solution.py:483
  41.0 0.5 collective-permute-start.31
  41.6 0.4 collective-permute-start.32
  42.0 1.2 collective-permute-done.7.refs_14_
  44.2 4.7 %load.1 = (bf16[2,2048,512]{2,1,0:T(8,128)(2,1)S(1)}, bf16[2,2048,512]{2,1,0:T(8,128)(2,1)S(1)}, bf16[2,512,2048]{2,1,0:T(8,128)(2,1)S(1)}) custom-call(f32[192,8]{1,0:T(8,128)S(1)} %get-tuple-element.67.refs_0_.refs_1_, bf16[4,2048,512]{2,1,0:T(8,128)(2,1)} %refs_1_.1, bf16[4,2048,512]{2,1,0:T(8,128)(2,1)} %refs_2_.1, bf16[4,512,2048]{2,1,0:T(8,128)(2,1)} %refs_3_.1), custom_call_target="tpu_custom_call" | custom-call | tf_op jit(solution)/shard_map/load/pallas_call | solution.py:178
  48.9 3.6 %experts.3 = (bf16[2,32,2048]{2,1,0:T(8,128)(2,1)S(1)}, bf16[2,32,2048]{2,1,0:T(8,128)(2,1)S(1)}, bf16[2,32,2048]{2,1,0:T(8,128)(2,1)S(1)}, bf16[2,32,2048]{2,1,...) custom-call(bf16[2,32,2048]{2,1,0:T(8,128)(2,1)S(1)} %bitcast.44, ...), custom_call_target="tpu_custom_call" | custom-call | tf_op jit(solution)/shard_map/experts/pallas_call | solution.py:424
  53.6 6.3 %mix.2 = (bf16[96,2048]{1,0:T(8,128)(2,1)S(1)}, bf16[96,2048]{1,0:T(8,128)(2,1)S(1)}, bf16[2,2048,512]{2,1,0:T(8,128)(2,1)S(1)}, bf16[2,2048,512]{2,1,0:T(8,128)...) custom-call(s32[1]{0:T(128)} %bitcast.refs_0_, ...), custom_call_target="tpu_custom_call" | custom-call | tf_op jit(solution)/shard_map/mix/pallas_call | solution.py:284
  59.9 6.2 %mix.3 = (bf16[96,2048]{1,0:T(8,128)(2,1)S(1)}, bf16[96,2048]{1,0:T(8,128)(2,1)S(1)}, bf16[2,512,2048]{2,1,0:T(8,128)(2,1)S(1)}) custom-call(s32[1]{0:T(128)} %bitcast.refs_0_, bf16[4,96,256]{2,1,0:T(8,128)(2,1)S(1)} %get-tuple-element.58.refs_1_, bf16[4,96,256]{2,1,0:T(8,128)(2,1)S(1)} %collective-permute-done.refs_2_, f32[1,128]{1,0:T(1,128)} %bitcast.68, ...), custom_call_target="tpu_custom_call" | custom-call | tf_op jit(solution)/shard_map/mix/pallas_call | solution.py:284
  66.2 3.6 %experts.2 = (bf16[2,32,2048]{2,1,0:T(8,128)(2,1)S(1)}, bf16[2,32,2048]{2,1,0:T(8,128)(2,1)S(1)}, bf16[2,32,2048]{2,1,0:T(8,128)(2,1)S(1)}, bf16[2,32,2048]{2,1,...) custom-call(bf16[2,32,2048]{2,1,0:T(8,128)(2,1)S(1)} %bitcast.42, ...), custom_call_target="tpu_custom_call" | custom-call | tf_op jit(solution)/shard_map/experts/pallas_call | solution.py:424
  70.8 1.8 %collective-permute-start.37 = (bf16[2,32,1024]{2,1,0:T(8,128)(2,1)S(1)}, bf16[2,32,1024]{2,1,0:T(8,128)(2,1)S(1)}, u32[]{:S(2)}, u32[]{:S(2)}) collective-permute-start(bf16[2,32,1024]{2,1,0:T(8,128)(2,1)S(1)} %get-tuple-element.98), channel_id=1, source_target_pairs={{0,16},{8,24},{16,0},{24,8},{1,17},{9,25},{17,1},{25,9},{2,18},{10... | collective-permute-start | bytes 393224 | tf_op jit(solution)/shard_map/ppermute | solution.py:483
  72.8 3.3 %collective-permute-done.35 = bf16[2,32,1024]{2,1,0:T(8,128)(2,1)S(1)} collective-permute-done((bf16[2,32,1024]{2,1,0:T(8,128)(2,1)S(1)}, bf16[2,32,1024]{2,1,0:T(8,128)(2,1)S(1)}, u32[]{:S(2)}, u32[]{:S(2)}) %collective-permute-start.35) | collective-permute-done | bytes 131104 | tf_op jit(solution)/shard_map/ppermute | solution.py:483
  76.7 3.1 %collective-permute-start.39 = (bf16[2,32,1024]{2,1,0:T(8,128)(2,1)S(1)}, bf16[2,32,1024]{2,1,0:T(8,128)(2,1)S(1)}, u32[]{:S(2)}, u32[]{:S(2)}) collective-permute-start(bf16[2,32,1024]{2,1,0:T(8,128)(2,1)S(1)} %get-tuple-element.101), channel_id=1, source_target_pairs={{0,24},{8,16},{16,8},{24,0},{1,25},{9,17},{17,9},{25,1},{2,26},{10... | collective-permute-start | bytes 393224 | tf_op jit(solution)/shard_map/ppermute | solution.py:483
  79.9 0.5 collective-permute-start.23
  80.5 8.5 %collective-permute-done.39 = bf16[2,32,1024]{2,1,0:T(8,128)(2,1)S(1)} collective-permute-done((bf16[2,32,1024]{2,1,0:T(8,128)(2,1)S(1)}, bf16[2,32,1024]{2,1,0:T(8,128)(2,1)S(1)}, u32[]{:S(2)}, u32[]{:S(2)}) %collective-permute-start.39) | collective-permute-done | bytes 131104 | tf_op jit(solution)/shard_map/ppermute | solution.py:483
  89.2 1.1 collective-permute-done.40
  90.3 1.6 %collective-permute-start.9 = (bf16[96,2048]{1,0:T(8,128)(2,1)S(1)}, bf16[96,2048]{1,0:T(8,128)(2,1)S(1)}, u32[]{:S(2)}, u32[]{:S(2)}) collective-permute-start(bf16[96,2048]{1,0:T(8,128)(2,1)S(1)} %get-tuple-element.64), channel_id=1, source_target_pairs={{0,2},{2,0},{4,6},{6,4},{1,3},{3,1},{5,7},{7,5},{8,10},{10,8},{12,... | collective-permute-start | bytes 1179656 | tf_op jit(solution)/shard_map/ppermute | solution.py:483
  91.9 2.6 %collective-permute-start.10 = (bf16[96,2048]{1,0:T(8,128)(2,1)S(1)}, bf16[96,2048]{1,0:T(8,128)(2,1)S(1)}, u32[]{:S(2)}, u32[]{:S(2)}) collective-permute-start(bf16[96,2048]{1,0:T(8,128)(2,1)S(1)} %get-tuple-element.65), channel_id=1, source_target_pairs={{0,4},{2,6},{4,0},{6,2},{1,5},{3,7},{5,1},{7,3},{8,12},{10,14},{12... | collective-permute-start | bytes 1179656 | tf_op jit(solution)/shard_map/ppermute | solution.py:483
  94.7 1.7 %collective-permute-start.41 = (bf16[2,32,1024]{2,1,0:T(8,128)(2,1)S(1)}, bf16[2,32,1024]{2,1,0:T(8,128)(2,1)S(1)}, u32[]{:S(2)}, u32[]{:S(2)}) collective-permute-start(bf16[2,32,1024]{2,1,0:T(8,128)(2,1)S(1)} %get-tuple-element.105), channel_id=1, source_target_pairs={{0,16},{8,24},{16,0},{24,8},{1,17},{9,25},{17,1},{25,9},{2,18},{10... | collective-permute-start | bytes 393224 | tf_op jit(solution)/shard_map/ppermute | solution.py:483
  96.5 5.0 %collective-permute-start.42 = (bf16[2,32,1024]{2,1,0:T(8,128)(2,1)S(1)}, bf16[2,32,1024]{2,1,0:T(8,128)(2,1)S(1)}, u32[]{:S(2)}, u32[]{:S(2)}) collective-permute-start(bf16[2,32,1024]{2,1,0:T(8,128)(2,1)S(1)} %get-tuple-element.106), channel_id=1, source_target_pairs={{0,24},{8,16},{16,8},{24,0},{1,25},{9,17},{17,9},{25,1},{2,26},{10... | collective-permute-start | bytes 393224 | tf_op jit(solution)/shard_map/ppermute | solution.py:483
  101.6 0.8 combine.2
  102.3 1.6 %collective-permute-start.43 = (bf16[48,1024]{1,0:T(8,128)(2,1)S(1)}, bf16[48,1024]{1,0:T(8,128)(2,1)S(1)}, u32[]{:S(2)}, u32[]{:S(2)}) collective-permute-start(bf16[48,1024]{1,0:T(8,128)(2,1)S(1)} %get-tuple-element.108), channel_id=1, source_target_pairs={{0,2},{2,0},{4,6},{6,4},{1,3},{3,1},{5,7},{7,5},{8,10},{10,8},{12,... | collective-permute-start | bytes 294920 | tf_op jit(solution)/shard_map/ppermute | solution.py:483
  104.0 0.4 collective-permute-done.42
  104.4 0.8 combine.3
  105.1 1.6 %collective-permute-start.44 = (bf16[48,1024]{1,0:T(8,128)(2,1)S(1)}, bf16[48,1024]{1,0:T(8,128)(2,1)S(1)}, u32[]{:S(2)}, u32[]{:S(2)}) collective-permute-start(bf16[48,1024]{1,0:T(8,128)(2,1)S(1)} %get-tuple-element.109), channel_id=1, source_target_pairs={{0,2},{2,0},{4,6},{6,4},{1,3},{3,1},{5,7},{7,5},{8,10},{10,8},{12,... | collective-permute-start | bytes 294920 | tf_op jit(solution)/shard_map/ppermute | solution.py:483
  106.8 1.5 %collective-permute-done.9.refs_1_ = bf16[96,2048]{1,0:T(8,128)(2,1)S(1)} collective-permute-done((bf16[96,2048]{1,0:T(8,128)(2,1)S(1)}, bf16[96,2048]{1,0:T(8,128)(2,1)S(1)}, u32[]{:S(2)}, u32[]{:S(2)}) %collective-permute-start.9) | collective-permute-done | bytes 393248 | tf_op jit(solution)/shard_map/ppermute | solution.py:483
  108.3 1.2 collective-permute-start.45
  109.5 15.8 %collective-permute-done.10.refs_2_ = bf16[96,2048]{1,0:T(8,128)(2,1)S(1)} collective-permute-done((bf16[96,2048]{1,0:T(8,128)(2,1)S(1)}, bf16[96,2048]{1,0:T(8,128)(2,1)S(1)}, u32[]{:S(2)}, u32[]{:S(2)}) %collective-permute-start.10) | collective-permute-done | bytes 393248 | tf_op jit(solution)/shard_map/ppermute | solution.py:483
  125.3 3.8 %collective-permute-start.47 = (bf16[48,1024]{1,0:T(8,128)(2,1)S(1)}, bf16[48,1024]{1,0:T(8,128)(2,1)S(1)}, u32[]{:S(2)}, u32[]{:S(2)}) collective-permute-start(bf16[48,1024]{1,0:T(8,128)(2,1)S(1)} %get-tuple-element.112), channel_id=1, source_target_pairs={{0,6},{2,4},{4,2},{6,0},{1,7},{3,5},{5,3},{7,1},{8,14},{10,12},{12... | collective-permute-start | bytes 294920 | tf_op jit(solution)/shard_map/ppermute | solution.py:483
  129.2 1.0 add.134
  130.2 9.6 %collective-permute-done.45.refs_4_ = bf16[48,1024]{1,0:T(8,128)(2,1)S(1)} collective-permute-done((bf16[48,1024]{1,0:T(8,128)(2,1)S(1)}, bf16[48,1024]{1,0:T(8,128)(2,1)S(1)}, u32[]{:S(2)}, u32[]{:S(2)}) %collective-permute-start.45) | collective-permute-done | bytes 98336 | tf_op jit(solution)/shard_map/ppermute | solution.py:483
  139.8 1.1 collective-permute-done.46.refs_5_
  140.9 0.8 join.1
  (78 shorter events, 5.4 us)
Async XLA Ops:
  3.1 7.5 %collective-permute-start = (bf16[4,96,256]{2,1,0:T(8,128)(2,1)S(1)}, bf16[4,96,256]{2,1,0:T(8,128)(2,1)S(1)}, u32[]{:S(2)}, u32[]{:S(2)}) collective-permute-start(bf16[4,96,256]{2,1,0:T(8,128)(2,1)S(1)} %get-tuple-element.59), channel_id=1, source_target_pairs={{0,1},{1,0},{2,3},{3,2},{4,5},{5,4},{6,7},{7,6},{8,9},{9,8},{10,11... | collective-permute-start | bytes 589832 | tf_op jit(solution)/shard_map/ppermute | solution.py:487
  3.7 9.0 %collective-permute-start.2 = (bf16[2,384,128]{2,1,0:T(8,128)(2,1)S(1)}, bf16[2,384,128]{2,1,0:T(8,128)(2,1)S(1)}, u32[]{:S(2)}, u32[]{:S(2)}) collective-permute-start(bf16[2,384,128]{2,1,0:T(8,128)(2,1)S(1)} %get-tuple-element.60.refs_8_), channel_id=1, source_target_pairs={{0,8},{8,0},{16,24},{24,16},{1,9},{9,1},{17,25},{25,17},{2,10},{10... | collective-permute-start | bytes 589832 | tf_op jit(solution)/shard_map/ppermute | solution.py:483
  6.2 11.1 %collective-permute-start.3 = (bf16[2,384,128]{2,1,0:T(8,128)(2,1)S(1)}, bf16[2,384,128]{2,1,0:T(8,128)(2,1)S(1)}, u32[]{:S(2)}, u32[]{:S(2)}) collective-permute-start(bf16[2,384,128]{2,1,0:T(8,128)(2,1)S(1)} %get-tuple-element.60.refs_8_), channel_id=1, source_target_pairs={{0,16},{8,24},{16,0},{24,8},{1,17},{9,25},{17,1},{25,9},{2,18},{10... | collective-permute-start | bytes 589832 | tf_op jit(solution)/shard_map/ppermute | solution.py:483
  7.7 11.3 %collective-permute-start.4 = (bf16[2,384,128]{2,1,0:T(8,128)(2,1)S(1)}, bf16[2,384,128]{2,1,0:T(8,128)(2,1)S(1)}, u32[]{:S(2)}, u32[]{:S(2)}) collective-permute-start(bf16[2,384,128]{2,1,0:T(8,128)(2,1)S(1)} %get-tuple-element.60.refs_8_), channel_id=1, source_target_pairs={{0,24},{8,16},{16,8},{24,0},{1,25},{9,17},{17,9},{25,1},{2,26},{10... | collective-permute-start | bytes 589832 | tf_op jit(solution)/shard_map/ppermute | solution.py:483
  7.8 11.3 %collective-permute-start.5 = (bf16[2,384,128]{2,1,0:T(8,128)(2,1)S(1)}, bf16[2,384,128]{2,1,0:T(8,128)(2,1)S(1)}, u32[]{:S(2)}, u32[]{:S(2)}) collective-permute-start(bf16[2,384,128]{2,1,0:T(8,128)(2,1)S(1)} %get-tuple-element.60.refs_8_), channel_id=1, source_target_pairs={{0,1},{1,0},{2,3},{3,2},{4,5},{5,4},{6,7},{7,6},{8,9},{9,8},{10,11... | collective-permute-start | bytes 589832 | tf_op jit(solution)/shard_map/ppermute | solution.py:487
  10.6 11.2 %collective-permute-start.12 = (bf16[2,32,2048]{2,1,0:T(8,128)(2,1)S(1)}, bf16[2,32,2048]{2,1,0:T(8,128)(2,1)S(1)}, u32[]{:S(2)}, u32[]{:S(2)}) collective-permute-start(bf16[2,32,2048]{2,1,0:T(8,128)(2,1)S(1)} %bitcast.58), channel_id=1, source_target_pairs={{0,8},{8,0},{16,24},{24,16},{1,9},{9,1},{17,25},{25,17},{2,10},{10... | collective-permute-start | bytes 786440 | tf_op jit(solution)/shard_map/ppermute | solution.py:483
  12.6 15.6 %collective-permute-start.13 = (bf16[2,32,2048]{2,1,0:T(8,128)(2,1)S(1)}, bf16[2,32,2048]{2,1,0:T(8,128)(2,1)S(1)}, u32[]{:S(2)}, u32[]{:S(2)}) collective-permute-start(bf16[2,32,2048]{2,1,0:T(8,128)(2,1)S(1)} %bitcast.57), channel_id=1, source_target_pairs={{0,16},{8,24},{16,0},{24,8},{1,17},{9,25},{17,1},{25,9},{2,18},{10... | collective-permute-start | bytes 786440 | tf_op jit(solution)/shard_map/ppermute | solution.py:483
  17.4 12.8 %collective-permute-start.14 = (bf16[2,32,2048]{2,1,0:T(8,128)(2,1)S(1)}, bf16[2,32,2048]{2,1,0:T(8,128)(2,1)S(1)}, u32[]{:S(2)}, u32[]{:S(2)}) collective-permute-start(bf16[2,32,2048]{2,1,0:T(8,128)(2,1)S(1)} %bitcast.56), channel_id=1, source_target_pairs={{0,24},{8,16},{16,8},{24,0},{1,25},{9,17},{17,9},{25,1},{2,26},{10... | collective-permute-start | bytes 786440 | tf_op jit(solution)/shard_map/ppermute | solution.py:483
  19.0 11.4 %collective-permute-start.15 = (bf16[2,32,2048]{2,1,0:T(8,128)(2,1)S(1)}, bf16[2,32,2048]{2,1,0:T(8,128)(2,1)S(1)}, u32[]{:S(2)}, u32[]{:S(2)}) collective-permute-start(bf16[2,32,2048]{2,1,0:T(8,128)(2,1)S(1)} %bitcast.41), channel_id=1, source_target_pairs={{0,1},{1,0},{2,3},{3,2},{4,5},{5,4},{6,7},{7,6},{8,9},{9,8},{10,11... | collective-permute-start | bytes 786440 | tf_op jit(solution)/shard_map/ppermute | solution.py:487
  19.0 34.2 %collective-permute-start.1 = (bf16[256,2048]{1,0:T(8,128)(2,1)S(1)}, bf16[256,2048]{1,0:T(8,128)(2,1)S(1)}, u32[]{:S(2)}, u32[]{:S(2)}) collective-permute-start(bf16[256,2048]{1,0:T(8,128)(2,1)S(1)} %copy-done), channel_id=1, source_target_pairs={{0,1},{1,0},{2,3},{3,2},{4,5},{5,4},{6,7},{7,6},{8,9},{9,8},{10,11... | collective-permute-start | bytes 3145736 | tf_op jit(solution)/shard_map/ppermute | solution.py:487
  21.9 12.2 %collective-permute-start.26 = (bf16[2,32,2048]{2,1,0:T(8,128)(2,1)S(1)}, bf16[2,32,2048]{2,1,0:T(8,128)(2,1)S(1)}, u32[]{:S(2)}, u32[]{:S(2)}) collective-permute-start(bf16[2,32,2048]{2,1,0:T(8,128)(2,1)S(1)} %bitcast.55), channel_id=1, source_target_pairs={{0,8},{8,0},{16,24},{24,16},{1,9},{9,1},{17,25},{25,17},{2,10},{10... | collective-permute-start | bytes 786440 | tf_op jit(solution)/shard_map/ppermute | solution.py:483
  28.3 12.7 %collective-permute-start.27 = (bf16[2,32,2048]{2,1,0:T(8,128)(2,1)S(1)}, bf16[2,32,2048]{2,1,0:T(8,128)(2,1)S(1)}, u32[]{:S(2)}, u32[]{:S(2)}) collective-permute-start(bf16[2,32,2048]{2,1,0:T(8,128)(2,1)S(1)} %bitcast.54), channel_id=1, source_target_pairs={{0,16},{8,24},{16,0},{24,8},{1,17},{9,25},{17,1},{25,9},{2,18},{10... | collective-permute-start | bytes 786440 | tf_op jit(solution)/shard_map/ppermute | solution.py:483
  30.2 10.8 %collective-permute-start.28 = (bf16[2,32,2048]{2,1,0:T(8,128)(2,1)S(1)}, bf16[2,32,2048]{2,1,0:T(8,128)(2,1)S(1)}, u32[]{:S(2)}, u32[]{:S(2)}) collective-permute-start(bf16[2,32,2048]{2,1,0:T(8,128)(2,1)S(1)} %bitcast.53), channel_id=1, source_target_pairs={{0,24},{8,16},{16,8},{24,0},{1,25},{9,17},{17,9},{25,1},{2,26},{10... | collective-permute-start | bytes 786440 | tf_op jit(solution)/shard_map/ppermute | solution.py:483
  30.4 11.1 %collective-permute-start.29 = (bf16[2,32,2048]{2,1,0:T(8,128)(2,1)S(1)}, bf16[2,32,2048]{2,1,0:T(8,128)(2,1)S(1)}, u32[]{:S(2)}, u32[]{:S(2)}) collective-permute-start(bf16[2,32,2048]{2,1,0:T(8,128)(2,1)S(1)} %bitcast.43), channel_id=1, source_target_pairs={{0,1},{1,0},{2,3},{3,2},{4,5},{5,4},{6,7},{7,6},{8,9},{9,8},{10,11... | collective-permute-start | bytes 786440 | tf_op jit(solution)/shard_map/ppermute | solution.py:487
  34.0 7.6 %collective-permute-start.6 = (bf16[2,384,128]{2,1,0:T(8,128)(2,1)S(1)}, bf16[2,384,128]{2,1,0:T(8,128)(2,1)S(1)}, u32[]{:S(2)}, u32[]{:S(2)}) collective-permute-start(bf16[2,384,128]{2,1,0:T(8,128)(2,1)S(1)} %collective-permute-done.2.refs_9_), channel_id=1, source_target_pairs={{0,1},{1,0},{2,3},{3,2},{4,5},{5,4},{6,7},{7,6},{8,9},{9,8},{10,11... | collective-permute-start | bytes 589832 | tf_op jit(solution)/shard_map/ppermute | solution.py:487
  41.0 2.3 %collective-permute-start.30 = (bf16[2,32,2048]{2,1,0:T(8,128)(2,1)S(1)}, bf16[2,32,2048]{2,1,0:T(8,128)(2,1)S(1)}, u32[]{:S(2)}, u32[]{:S(2)}) collective-permute-start(bf16[2,32,2048]{2,1,0:T(8,128)(2,1)S(1)} %collective-permute-done.26.refs_1_), channel_id=1, source_target_pairs={{0,1},{1,0},{2,3},{3,2},{4,5},{5,4},{6,7},{7,6},{8,9},{9,8},{10,11... | collective-permute-start | bytes 786440 | tf_op jit(solution)/shard_map/ppermute | solution.py:487
  41.0 2.7 %collective-permute-start.31 = (bf16[2,32,2048]{2,1,0:T(8,128)(2,1)S(1)}, bf16[2,32,2048]{2,1,0:T(8,128)(2,1)S(1)}, u32[]{:S(2)}, u32[]{:S(2)}) collective-permute-start(bf16[2,32,2048]{2,1,0:T(8,128)(2,1)S(1)} %collective-permute-done.27.refs_2_), channel_id=1, source_target_pairs={{0,1},{1,0},{2,3},{3,2},{4,5},{5,4},{6,7},{7,6},{8,9},{9,8},{10,11... | collective-permute-start | bytes 786440 | tf_op jit(solution)/shard_map/ppermute | solution.py:487
  41.6 2.3 %collective-permute-start.32 = (bf16[2,32,2048]{2,1,0:T(8,128)(2,1)S(1)}, bf16[2,32,2048]{2,1,0:T(8,128)(2,1)S(1)}, u32[]{:S(2)}, u32[]{:S(2)}) collective-permute-start(bf16[2,32,2048]{2,1,0:T(8,128)(2,1)S(1)} %collective-permute-done.28.refs_3_), channel_id=1, source_target_pairs={{0,1},{1,0},{2,3},{3,2},{4,5},{5,4},{6,7},{7,6},{8,9},{9,8},{10,11... | collective-permute-start | bytes 786440 | tf_op jit(solution)/shard_map/ppermute | solution.py:487
  43.2 9.6 %collective-permute-start.16 = (bf16[2,32,2048]{2,1,0:T(8,128)(2,1)S(1)}, bf16[2,32,2048]{2,1,0:T(8,128)(2,1)S(1)}, u32[]{:S(2)}, u32[]{:S(2)}) collective-permute-start(bf16[2,32,2048]{2,1,0:T(8,128)(2,1)S(1)} %collective-permute-done.12.refs_1_), channel_id=1, source_target_pairs={{0,1},{1,0},{2,3},{3,2},{4,5},{5,4},{6,7},{7,6},{8,9},{9,8},{10,11... | collective-permute-start | bytes 786440 | tf_op jit(solution)/shard_map/ppermute | solution.py:487
  43.3 9.8 %collective-permute-start.17 = (bf16[2,32,2048]{2,1,0:T(8,128)(2,1)S(1)}, bf16[2,32,2048]{2,1,0:T(8,128)(2,1)S(1)}, u32[]{:S(2)}, u32[]{:S(2)}) collective-permute-start(bf16[2,32,2048]{2,1,0:T(8,128)(2,1)S(1)} %collective-permute-done.13.refs_2_), channel_id=1, source_target_pairs={{0,1},{1,0},{2,3},{3,2},{4,5},{5,4},{6,7},{7,6},{8,9},{9,8},{10,11... | collective-permute-start | bytes 786440 | tf_op jit(solution)/shard_map/ppermute | solution.py:487
  43.7 8.8 %collective-permute-start.8 = (bf16[2,384,128]{2,1,0:T(8,128)(2,1)S(1)}, bf16[2,384,128]{2,1,0:T(8,128)(2,1)S(1)}, u32[]{:S(2)}, u32[]{:S(2)}) collective-permute-start(bf16[2,384,128]{2,1,0:T(8,128)(2,1)S(1)} %collective-permute-done.4.refs_11_), channel_id=1, source_target_pairs={{0,1},{1,0},{2,3},{3,2},{4,5},{5,4},{6,7},{7,6},{8,9},{9,8},{10,11... | collective-permute-start | bytes 589832 | tf_op jit(solution)/shard_map/ppermute | solution.py:487
  43.9 22.3 %collective-permute-start.18 = (bf16[2,32,2048]{2,1,0:T(8,128)(2,1)S(1)}, bf16[2,32,2048]{2,1,0:T(8,128)(2,1)S(1)}, u32[]{:S(2)}, u32[]{:S(2)}) collective-permute-start(bf16[2,32,2048]{2,1,0:T(8,128)(2,1)S(1)} %collective-permute-done.14.refs_3_), channel_id=1, source_target_pairs={{0,1},{1,0},{2,3},{3,2},{4,5},{5,4},{6,7},{7,6},{8,9},{9,8},{10,11... | collective-permute-start | bytes 786440 | tf_op jit(solution)/shard_map/ppermute | solution.py:487
  52.5 17.4 %collective-permute-start.34 = (bf16[2,32,2048]{2,1,0:T(8,128)(2,1)S(1)}, bf16[2,32,2048]{2,1,0:T(8,128)(2,1)S(1)}, u32[]{:S(2)}, u32[]{:S(2)}) collective-permute-start(bf16[2,32,2048]{2,1,0:T(8,128)(2,1)S(1)} %get-tuple-element.94), channel_id=1, source_target_pairs={{0,1},{1,0},{2,3},{3,2},{4,5},{5,4},{6,7},{7,6},{8,9},{9,8},{10,11... | collective-permute-start | bytes 786440 | tf_op jit(solution)/shard_map/ppermute | solution.py:487
  52.8 17.7 %collective-permute-start.33 = (bf16[2,32,2048]{2,1,0:T(8,128)(2,1)S(1)}, bf16[2,32,2048]{2,1,0:T(8,128)(2,1)S(1)}, u32[]{:S(2)}, u32[]{:S(2)}) collective-permute-start(bf16[2,32,2048]{2,1,0:T(8,128)(2,1)S(1)} %get-tuple-element.91), channel_id=1, source_target_pairs={{0,1},{1,0},{2,3},{3,2},{4,5},{5,4},{6,7},{7,6},{8,9},{9,8},{10,11... | collective-permute-start | bytes 786440 | tf_op jit(solution)/shard_map/ppermute | solution.py:487
  53.1 17.4 %collective-permute-start.36 = (bf16[2,32,2048]{2,1,0:T(8,128)(2,1)S(1)}, bf16[2,32,2048]{2,1,0:T(8,128)(2,1)S(1)}, u32[]{:S(2)}, u32[]{:S(2)}) collective-permute-start(bf16[2,32,2048]{2,1,0:T(8,128)(2,1)S(1)} %get-tuple-element.97), channel_id=1, source_target_pairs={{0,1},{1,0},{2,3},{3,2},{4,5},{5,4},{6,7},{7,6},{8,9},{9,8},{10,11... | collective-permute-start | bytes 786440 | tf_op jit(solution)/shard_map/ppermute | solution.py:487
  53.3 17.5 %collective-permute-start.38 = (bf16[2,32,2048]{2,1,0:T(8,128)(2,1)S(1)}, bf16[2,32,2048]{2,1,0:T(8,128)(2,1)S(1)}, u32[]{:S(2)}, u32[]{:S(2)}) collective-permute-start(bf16[2,32,2048]{2,1,0:T(8,128)(2,1)S(1)} %get-tuple-element.100), channel_id=1, source_target_pairs={{0,1},{1,0},{2,3},{3,2},{4,5},{5,4},{6,7},{7,6},{8,9},{9,8},{10,11... | collective-permute-start | bytes 786440 | tf_op jit(solution)/shard_map/ppermute | solution.py:487
  69.8 2.8 %collective-permute-start.20 = (bf16[2,32,2048]{2,1,0:T(8,128)(2,1)S(1)}, bf16[2,32,2048]{2,1,0:T(8,128)(2,1)S(1)}, u32[]{:S(2)}, u32[]{:S(2)}) collective-permute-start(bf16[2,32,2048]{2,1,0:T(8,128)(2,1)S(1)} %get-tuple-element.78), channel_id=1, source_target_pairs={{0,1},{1,0},{2,3},{3,2},{4,5},{5,4},{6,7},{7,6},{8,9},{9,8},{10,11... | collective-permute-start | bytes 786440 | tf_op jit(solution)/shard_map/ppermute | solution.py:487
  70.0 9.8 %collective-permute-start.22 = (bf16[2,32,2048]{2,1,0:T(8,128)(2,1)S(1)}, bf16[2,32,2048]{2,1,0:T(8,128)(2,1)S(1)}, u32[]{:S(2)}, u32[]{:S(2)}) collective-permute-start(bf16[2,32,2048]{2,1,0:T(8,128)(2,1)S(1)} %get-tuple-element.80), channel_id=1, source_target_pairs={{0,1},{1,0},{2,3},{3,2},{4,5},{5,4},{6,7},{7,6},{8,9},{9,8},{10,11... | collective-permute-start | bytes 786440 | tf_op jit(solution)/shard_map/ppermute | solution.py:487
  70.4 5.6 %collective-permute-start.35 = (bf16[2,32,1024]{2,1,0:T(8,128)(2,1)S(1)}, bf16[2,32,1024]{2,1,0:T(8,128)(2,1)S(1)}, u32[]{:S(2)}, u32[]{:S(2)}) collective-permute-start(bf16[2,32,1024]{2,1,0:T(8,128)(2,1)S(1)} %get-tuple-element.95), channel_id=1, source_target_pairs={{0,8},{8,0},{16,24},{24,16},{1,9},{9,1},{17,25},{25,17},{2,10},{10... | collective-permute-start | bytes 393224 | tf_op jit(solution)/shard_map/ppermute | solution.py:483
  70.5 9.4 %collective-permute-start.24 = (bf16[2,32,2048]{2,1,0:T(8,128)(2,1)S(1)}, bf16[2,32,2048]{2,1,0:T(8,128)(2,1)S(1)}, u32[]{:S(2)}, u32[]{:S(2)}) collective-permute-start(bf16[2,32,2048]{2,1,0:T(8,128)(2,1)S(1)} %get-tuple-element.82), channel_id=1, source_target_pairs={{0,1},{1,0},{2,3},{3,2},{4,5},{5,4},{6,7},{7,6},{8,9},{9,8},{10,11... | collective-permute-start | bytes 786440 | tf_op jit(solution)/shard_map/ppermute | solution.py:487
  70.8 5.8 %collective-permute-start.37 = (bf16[2,32,1024]{2,1,0:T(8,128)(2,1)S(1)}, bf16[2,32,1024]{2,1,0:T(8,128)(2,1)S(1)}, u32[]{:S(2)}, u32[]{:S(2)}) collective-permute-start(bf16[2,32,1024]{2,1,0:T(8,128)(2,1)S(1)} %get-tuple-element.98), channel_id=1, source_target_pairs={{0,16},{8,24},{16,0},{24,8},{1,17},{9,25},{17,1},{25,9},{2,18},{10... | collective-permute-start | bytes 393224 | tf_op jit(solution)/shard_map/ppermute | solution.py:483
  72.6 19.3 %collective-permute-start.19 = (bf16[2,32,2048]{2,1,0:T(8,128)(2,1)S(1)}, bf16[2,32,2048]{2,1,0:T(8,128)(2,1)S(1)}, u32[]{:S(2)}, u32[]{:S(2)}) collective-permute-start(bf16[2,32,2048]{2,1,0:T(8,128)(2,1)S(1)} %get-tuple-element.76), channel_id=1, source_target_pairs={{0,1},{1,0},{2,3},{3,2},{4,5},{5,4},{6,7},{7,6},{8,9},{9,8},{10,11... | collective-permute-start | bytes 786440 | tf_op jit(solution)/shard_map/ppermute | solution.py:487
  76.0 18.5 %collective-permute-start.21 = (bf16[2,32,2048]{2,1,0:T(8,128)(2,1)S(1)}, bf16[2,32,2048]{2,1,0:T(8,128)(2,1)S(1)}, u32[]{:S(2)}, u32[]{:S(2)}) collective-permute-start(bf16[2,32,2048]{2,1,0:T(8,128)(2,1)S(1)} %add.136), channel_id=1, source_target_pairs={{0,8},{8,0},{16,24},{24,16},{1,9},{9,1},{17,25},{25,17},{2,10},{10... | collective-permute-start | bytes 786440 | tf_op jit(solution)/shard_map/ppermute | solution.py:483
  76.7 12.4 %collective-permute-start.39 = (bf16[2,32,1024]{2,1,0:T(8,128)(2,1)S(1)}, bf16[2,32,1024]{2,1,0:T(8,128)(2,1)S(1)}, u32[]{:S(2)}, u32[]{:S(2)}) collective-permute-start(bf16[2,32,1024]{2,1,0:T(8,128)(2,1)S(1)} %get-tuple-element.101), channel_id=1, source_target_pairs={{0,24},{8,16},{16,8},{24,0},{1,25},{9,17},{17,9},{25,1},{2,26},{10... | collective-permute-start | bytes 393224 | tf_op jit(solution)/shard_map/ppermute | solution.py:483
  79.8 10.6 %collective-permute-start.40 = (bf16[2,32,1024]{2,1,0:T(8,128)(2,1)S(1)}, bf16[2,32,1024]{2,1,0:T(8,128)(2,1)S(1)}, u32[]{:S(2)}, u32[]{:S(2)}) collective-permute-start(bf16[2,32,1024]{2,1,0:T(8,128)(2,1)S(1)} %get-tuple-element.104), channel_id=1, source_target_pairs={{0,8},{8,0},{16,24},{24,16},{1,9},{9,1},{17,25},{25,17},{2,10},{10... | collective-permute-start | bytes 393224 | tf_op jit(solution)/shard_map/ppermute | solution.py:483
  79.9 14.8 %collective-permute-start.23 = (bf16[2,32,2048]{2,1,0:T(8,128)(2,1)S(1)}, bf16[2,32,2048]{2,1,0:T(8,128)(2,1)S(1)}, u32[]{:S(2)}, u32[]{:S(2)}) collective-permute-start(bf16[2,32,2048]{2,1,0:T(8,128)(2,1)S(1)} %add.137), channel_id=1, source_target_pairs={{0,16},{8,24},{16,0},{24,8},{1,17},{9,25},{17,1},{25,9},{2,18},{10... | collective-permute-start | bytes 786440 | tf_op jit(solution)/shard_map/ppermute | solution.py:483
  89.0 7.4 %collective-permute-start.25 = (bf16[2,32,2048]{2,1,0:T(8,128)(2,1)S(1)}, bf16[2,32,2048]{2,1,0:T(8,128)(2,1)S(1)}, u32[]{:S(2)}, u32[]{:S(2)}) collective-permute-start(bf16[2,32,2048]{2,1,0:T(8,128)(2,1)S(1)} %add.138), channel_id=1, source_target_pairs={{0,24},{8,16},{16,8},{24,0},{1,25},{9,17},{17,9},{25,1},{2,26},{10... | collective-permute-start | bytes 786440 | tf_op jit(solution)/shard_map/ppermute | solution.py:483
  90.3 17.9 %collective-permute-start.9 = (bf16[96,2048]{1,0:T(8,128)(2,1)S(1)}, bf16[96,2048]{1,0:T(8,128)(2,1)S(1)}, u32[]{:S(2)}, u32[]{:S(2)}) collective-permute-start(bf16[96,2048]{1,0:T(8,128)(2,1)S(1)} %get-tuple-element.64), channel_id=1, source_target_pairs={{0,2},{2,0},{4,6},{6,4},{1,3},{3,1},{5,7},{7,5},{8,10},{10,8},{12,... | collective-permute-start | bytes 1179656 | tf_op jit(solution)/shard_map/ppermute | solution.py:483
  91.9 33.4 %collective-permute-start.10 = (bf16[96,2048]{1,0:T(8,128)(2,1)S(1)}, bf16[96,2048]{1,0:T(8,128)(2,1)S(1)}, u32[]{:S(2)}, u32[]{:S(2)}) collective-permute-start(bf16[96,2048]{1,0:T(8,128)(2,1)S(1)} %get-tuple-element.65), channel_id=1, source_target_pairs={{0,4},{2,6},{4,0},{6,2},{1,5},{3,7},{5,1},{7,3},{8,12},{10,14},{12... | collective-permute-start | bytes 1179656 | tf_op jit(solution)/shard_map/ppermute | solution.py:483
  94.5 30.8 %collective-permute-start.11 = (bf16[96,2048]{1,0:T(8,128)(2,1)S(1)}, bf16[96,2048]{1,0:T(8,128)(2,1)S(1)}, u32[]{:S(2)}, u32[]{:S(2)}) collective-permute-start(bf16[96,2048]{1,0:T(8,128)(2,1)S(1)} %get-tuple-element.66), channel_id=1, source_target_pairs={{0,6},{2,4},{4,2},{6,0},{1,7},{3,5},{5,3},{7,1},{8,14},{10,12},{12... | collective-permute-start | bytes 1179656 | tf_op jit(solution)/shard_map/ppermute | solution.py:483
  94.7 7.6 %collective-permute-start.41 = (bf16[2,32,1024]{2,1,0:T(8,128)(2,1)S(1)}, bf16[2,32,1024]{2,1,0:T(8,128)(2,1)S(1)}, u32[]{:S(2)}, u32[]{:S(2)}) collective-permute-start(bf16[2,32,1024]{2,1,0:T(8,128)(2,1)S(1)} %get-tuple-element.105), channel_id=1, source_target_pairs={{0,16},{8,24},{16,0},{24,8},{1,17},{9,25},{17,1},{25,9},{2,18},{10... | collective-permute-start | bytes 393224 | tf_op jit(solution)/shard_map/ppermute | solution.py:483
  96.5 7.9 %collective-permute-start.42 = (bf16[2,32,1024]{2,1,0:T(8,128)(2,1)S(1)}, bf16[2,32,1024]{2,1,0:T(8,128)(2,1)S(1)}, u32[]{:S(2)}, u32[]{:S(2)}) collective-permute-start(bf16[2,32,1024]{2,1,0:T(8,128)(2,1)S(1)} %get-tuple-element.106), channel_id=1, source_target_pairs={{0,24},{8,16},{16,8},{24,0},{1,25},{9,17},{17,9},{25,1},{2,26},{10... | collective-permute-start | bytes 393224 | tf_op jit(solution)/shard_map/ppermute | solution.py:483
  102.3 26.8 %collective-permute-start.43 = (bf16[48,1024]{1,0:T(8,128)(2,1)S(1)}, bf16[48,1024]{1,0:T(8,128)(2,1)S(1)}, u32[]{:S(2)}, u32[]{:S(2)}) collective-permute-start(bf16[48,1024]{1,0:T(8,128)(2,1)S(1)} %get-tuple-element.108), channel_id=1, source_target_pairs={{0,2},{2,0},{4,6},{6,4},{1,3},{3,1},{5,7},{7,5},{8,10},{10,8},{12,... | collective-permute-start | bytes 294920 | tf_op jit(solution)/shard_map/ppermute | solution.py:483
  105.1 25.0 %collective-permute-start.44 = (bf16[48,1024]{1,0:T(8,128)(2,1)S(1)}, bf16[48,1024]{1,0:T(8,128)(2,1)S(1)}, u32[]{:S(2)}, u32[]{:S(2)}) collective-permute-start(bf16[48,1024]{1,0:T(8,128)(2,1)S(1)} %get-tuple-element.109), channel_id=1, source_target_pairs={{0,2},{2,0},{4,6},{6,4},{1,3},{3,1},{5,7},{7,5},{8,10},{10,8},{12,... | collective-permute-start | bytes 294920 | tf_op jit(solution)/shard_map/ppermute | solution.py:483
  108.3 31.5 %collective-permute-start.45 = (bf16[48,1024]{1,0:T(8,128)(2,1)S(1)}, bf16[48,1024]{1,0:T(8,128)(2,1)S(1)}, u32[]{:S(2)}, u32[]{:S(2)}) collective-permute-start(bf16[48,1024]{1,0:T(8,128)(2,1)S(1)} %get-tuple-element.110), channel_id=1, source_target_pairs={{0,4},{2,6},{4,0},{6,2},{1,5},{3,7},{5,1},{7,3},{8,12},{10,14},{12... | collective-permute-start | bytes 294920 | tf_op jit(solution)/shard_map/ppermute | solution.py:483
  125.3 15.6 %collective-permute-start.46 = (bf16[48,1024]{1,0:T(8,128)(2,1)S(1)}, bf16[48,1024]{1,0:T(8,128)(2,1)S(1)}, u32[]{:S(2)}, u32[]{:S(2)}) collective-permute-start(bf16[48,1024]{1,0:T(8,128)(2,1)S(1)} %get-tuple-element.111), channel_id=1, source_target_pairs={{0,4},{2,6},{4,0},{6,2},{1,5},{3,7},{5,1},{7,3},{8,12},{10,14},{12... | collective-permute-start | bytes 294920 | tf_op jit(solution)/shard_map/ppermute | solution.py:483
  125.3 15.6 %collective-permute-start.47 = (bf16[48,1024]{1,0:T(8,128)(2,1)S(1)}, bf16[48,1024]{1,0:T(8,128)(2,1)S(1)}, u32[]{:S(2)}, u32[]{:S(2)}) collective-permute-start(bf16[48,1024]{1,0:T(8,128)(2,1)S(1)} %get-tuple-element.112), channel_id=1, source_target_pairs={{0,6},{2,4},{4,2},{6,0},{1,7},{3,5},{5,3},{7,1},{8,14},{10,12},{12... | collective-permute-start | bytes 294920 | tf_op jit(solution)/shard_map/ppermute | solution.py:483
  129.1 11.7 %collective-permute-start.48 = (bf16[48,1024]{1,0:T(8,128)(2,1)S(1)}, bf16[48,1024]{1,0:T(8,128)(2,1)S(1)}, u32[]{:S(2)}, u32[]{:S(2)}) collective-permute-start(bf16[48,1024]{1,0:T(8,128)(2,1)S(1)} %get-tuple-element.113), channel_id=1, source_target_pairs={{0,6},{2,4},{4,2},{6,0},{1,7},{3,5},{5,3},{7,1},{8,14},{10,12},{12... | collective-permute-start | bytes 294920 | tf_op jit(solution)/shard_map/ppermute | solution.py:483
  (2 other events, 20.1 us)

commit v8 on v7

--- a/solution.py
+++ b/solution.py
@@ -165,7 +165,8 @@
 
 
 def load_kernel(first, after_ref, *refs):
-    sources, targets, sems = refs[:3], refs[3:6], refs[6]
+    count = len(refs) // 2
+    sources, targets, sems = refs[:count], refs[count:-1], refs[-1]
     copies = weight_copies(sources, targets, first, sems, 0)
     for copy in copies:
         copy.start()
@@ -177,10 +178,10 @@
     any_space = pl.BlockSpec(memory_space=pl.ANY)
     return pl.pallas_call(
         lambda *refs: load_kernel(first, *refs),
-        in_specs=[any_space] * 4,
-        out_specs=[IN_VMEM] * 3,
+        in_specs=[any_space] * (1 + len(weights)),
+        out_specs=[IN_VMEM] * len(weights),
         out_shape=[jax.ShapeDtypeStruct((per, *w.shape[1:]), BF16) for w in weights],
-        scratch_shapes=[pltpu.SemaphoreType.DMA((3 * per * SPLIT,))],
+        scratch_shapes=[pltpu.SemaphoreType.DMA((len(weights) * per * SPLIT,))],
         compiler_params=pltpu.CompilerParams(vmem_limit_bytes=2 * MIB),
         name="load",
     )(after, *in_hbm(weights))
@@ -548,11 +549,12 @@
 
     all_weights = [gate_weight, up_weight, down_weight]
     weights = [load(all_weights, chunk * per, per, cols) for chunk in range(1, chunks)]
+    last_part = load(all_weights[2:], 0, per, cols)
     steps = list(range(n_z))
     far, near = steps[n_z // 2 :], steps[: n_z // 2]
     own = (z_arg, q_own, q_other, query_gain[None], cosine, sine, out_weight, w_other)
     far_rows, first_part, joined = mix(*own, pieces, far, all_weights[:2], per)
-    near_rows, last_part, _ = mix(*own, joined, near, all_weights[2:], per)
+    near_rows, _, _ = mix(*own, joined, near, [], per)
     weights = [[*first_part, *last_part], *weights]
     gathered = []
     for step, rows in zip(near + far, [*near_rows, *far_rows]):

time: 143 us -> 144 us (level)
  starting transfers between devices: 44.1 us -> 38.6 us
  waiting for transfers between devices: 63.2 us -> 67.2 us
  Pallas kernels: 32.4 us -> 34.5 us
    ppermute x27, starting transfers between devices: 39.1 us -> 33.5 us  [shift(): return lax.ppermute(a, axis, pairs)]
    ppermute x27, waiting for transfers between devices: 62 us -> 66 us  [shift(): return lax.ppermute(a, axis, pairs)]
    pallas_call x1 -> x2, Pallas kernels: 4.7 us -> 6.9 us  [load(): pl.pallas_call(lambda *refs: load_kernel(first, *refs), in_specs=[any_spa...]
  transfers between devices with their start and end apart: 49 -> 49, of which waited for: 15 -> 15; matrix products, arithmetic and copies ran while one was open for 0% -> 0% of each run, Pallas kernels for 21% -> 23%
where the time goes in v8:
time: 144 us; the launch traced here: 142 us
  waiting for transfers between devices  67.2 us (47%)
  starting transfers between devices  38.6 us (27%)
  Pallas kernels  34.5 us (24%)
    ppermute x27, waiting for transfers between devices, shift(): return lax.ppermute(a, axis, pairs)  66 us
    ppermute x27, starting transfers between devices, shift(): return lax.ppermute(a, axis, pairs)  33.5 us
    pallas_call x2, Pallas kernels, mix(): pl.pallas_call(lambda *refs: mix_kernel(len(pieces), steps, len(loads), *...  12.5 us
    pallas_call x2, Pallas kernels, experts(): pl.pallas_call(lambda *refs: expert_kernel(len(pieces), group, *refs), in...  7.19 us
    pallas_call x2, Pallas kernels, load(): pl.pallas_call(lambda *refs: load_kernel(first, *refs), in_specs=[any_spa...  6.9 us
    ppermute x22, starting transfers between devices, swap_cores(): return lax.ppermute(a, 'core', [(i, CORES - 1 - i) for i in range(CORES)])  5.07 us
  transfers between devices with their start and end apart: 49, of which 15 were waited for; matrix products, arithmetic and copies ran while one was open for 0% of the time, Pallas kernels for 23%

profile of v8, /device:TPU:0, one launch (start us, length us, event | category | flops | bytes accessed | tf_op | source)
XLA Modules:
  0.0 142.3 jit_solution(745729277175236534)
XLA Ops:
  0.9 0.8 sine_multiply_fusion
  1.7 1.4 %prepare.1 = (bf16[2,384,128]{2,1,0:T(8,128)(2,1)S(1)}, bf16[4,96,256]{2,1,0:T(8,128)(2,1)S(1)}, bf16[4,96,256]{2,1,0:T(8,128)(2,1)S(1)}) custom-call(s32[1]{0:T(128)} %bitcast.1.core_ref.refs_0_, s32[1]{0:T(128)} %bitcast.2.head_ref, bf16[4,2,96,512]{3,2,1,0:T(8,128)(2,1)} %bitcast.62, bf16[4,2,96,512]{3,2,1,0:T(8,128)(2,1)} %bitcast.63, ...), custom_call_target="tpu_custom_call" | custom-call | tf_op jit(solution)/shard_map/prepare/pallas_call | solution.py:74
  3.1 0.6 collective-permute-start
  3.7 2.6 %collective-permute-start.2 = (bf16[2,384,128]{2,1,0:T(8,128)(2,1)S(1)}, bf16[2,384,128]{2,1,0:T(8,128)(2,1)S(1)}, u32[]{:S(2)}, u32[]{:S(2)}) collective-permute-start(bf16[2,384,128]{2,1,0:T(8,128)(2,1)S(1)} %get-tuple-element.59.refs_8_), channel_id=1, source_target_pairs={{0,8},{8,0},{16,24},{24,16},{1,9},{9,1},{17,25},{25,17},{2,10},{10... | collective-permute-start | bytes 589832 | tf_op jit(solution)/shard_map/ppermute | solution.py:484
  6.2 1.5 %collective-permute-start.3 = (bf16[2,384,128]{2,1,0:T(8,128)(2,1)S(1)}, bf16[2,384,128]{2,1,0:T(8,128)(2,1)S(1)}, u32[]{:S(2)}, u32[]{:S(2)}) collective-permute-start(bf16[2,384,128]{2,1,0:T(8,128)(2,1)S(1)} %get-tuple-element.59.refs_8_), channel_id=1, source_target_pairs={{0,16},{8,24},{16,0},{24,8},{1,17},{9,25},{17,1},{25,9},{2,18},{10... | collective-permute-start | bytes 589832 | tf_op jit(solution)/shard_map/ppermute | solution.py:484
  7.8 2.8 %dispatch.1 = (bf16[64,2048]{1,0:T(8,128)(2,1)S(1)}, bf16[64,2048]{1,0:T(8,128)(2,1)S(1)}, bf16[64,2048]{1,0:T(8,128)(2,1)S(1)}, bf16[64,2048]{1,0:T(8,128)(2,1)...) custom-call(s32[1]{0:T(128)} %bitcast.1.core_ref.refs_0_, ...), custom_call_target="tpu_custom_call" | custom-call | tf_op jit(solution)/shard_map/dispatch/pallas_call | solution.py:383
  10.6 2.0 %collective-permute-start.12 = (bf16[2,32,2048]{2,1,0:T(8,128)(2,1)S(1)}, bf16[2,32,2048]{2,1,0:T(8,128)(2,1)S(1)}, u32[]{:S(2)}, u32[]{:S(2)}) collective-permute-start(bf16[2,32,2048]{2,1,0:T(8,128)(2,1)S(1)} %bitcast.58), channel_id=1, source_target_pairs={{0,8},{8,0},{16,24},{24,16},{1,9},{9,1},{17,25},{25,17},{2,10},{10... | collective-permute-start | bytes 786440 | tf_op jit(solution)/shard_map/ppermute | solution.py:484
  12.6 1.5 %collective-permute-start.13 = (bf16[2,32,2048]{2,1,0:T(8,128)(2,1)S(1)}, bf16[2,32,2048]{2,1,0:T(8,128)(2,1)S(1)}, u32[]{:S(2)}, u32[]{:S(2)}) collective-permute-start(bf16[2,32,2048]{2,1,0:T(8,128)(2,1)S(1)} %bitcast.57), channel_id=1, source_target_pairs={{0,16},{8,24},{16,0},{24,8},{1,17},{9,25},{17,1},{25,9},{2,18},{10... | collective-permute-start | bytes 786440 | tf_op jit(solution)/shard_map/ppermute | solution.py:484
  14.2 3.2 %collective-permute-done.3.refs_10_ = bf16[2,384,128]{2,1,0:T(8,128)(2,1)S(1)} collective-permute-done((bf16[2,384,128]{2,1,0:T(8,128)(2,1)S(1)}, bf16[2,384,128]{2,1,0:T(8,128)(2,1)S(1)}, u32[]{:S(2)}, u32[]{:S(2)}) %collective-permute-start.3) | collective-permute-done | bytes 196640 | tf_op jit(solution)/shard_map/ppermute | solution.py:484
  17.4 1.7 %collective-permute-start.14 = (bf16[2,32,2048]{2,1,0:T(8,128)(2,1)S(1)}, bf16[2,32,2048]{2,1,0:T(8,128)(2,1)S(1)}, u32[]{:S(2)}, u32[]{:S(2)}) collective-permute-start(bf16[2,32,2048]{2,1,0:T(8,128)(2,1)S(1)} %bitcast.56), channel_id=1, source_target_pairs={{0,24},{8,16},{16,8},{24,0},{1,25},{9,17},{17,9},{25,1},{2,26},{10... | collective-permute-start | bytes 786440 | tf_op jit(solution)/shard_map/ppermute | solution.py:484
  19.5 2.3 %collective-permute-done.12.refs_1_ = bf16[2,32,2048]{2,1,0:T(8,128)(2,1)S(1)} collective-permute-done((bf16[2,32,2048]{2,1,0:T(8,128)(2,1)S(1)}, bf16[2,32,2048]{2,1,0:T(8,128)(2,1)S(1)}, u32[]{:S(2)}, u32[]{:S(2)}) %collective-permute-start.12) | collective-permute-done | bytes 262176 | tf_op jit(solution)/shard_map/ppermute | solution.py:484
  21.9 2.0 %collective-permute-start.26 = (bf16[2,32,2048]{2,1,0:T(8,128)(2,1)S(1)}, bf16[2,32,2048]{2,1,0:T(8,128)(2,1)S(1)}, u32[]{:S(2)}, u32[]{:S(2)}) collective-permute-start(bf16[2,32,2048]{2,1,0:T(8,128)(2,1)S(1)} %bitcast.55), channel_id=1, source_target_pairs={{0,8},{8,0},{16,24},{24,16},{1,9},{9,1},{17,25},{25,17},{2,10},{10... | collective-permute-start | bytes 786440 | tf_op jit(solution)/shard_map/ppermute | solution.py:484
  23.9 4.4 %collective-permute-done.13.refs_2_ = bf16[2,32,2048]{2,1,0:T(8,128)(2,1)S(1)} collective-permute-done((bf16[2,32,2048]{2,1,0:T(8,128)(2,1)S(1)}, bf16[2,32,2048]{2,1,0:T(8,128)(2,1)S(1)}, u32[]{:S(2)}, u32[]{:S(2)}) %collective-permute-start.13) | collective-permute-done | bytes 262176 | tf_op jit(solution)/shard_map/ppermute | solution.py:484
  28.3 1.9 %collective-permute-start.27 = (bf16[2,32,2048]{2,1,0:T(8,128)(2,1)S(1)}, bf16[2,32,2048]{2,1,0:T(8,128)(2,1)S(1)}, u32[]{:S(2)}, u32[]{:S(2)}) collective-permute-start(bf16[2,32,2048]{2,1,0:T(8,128)(2,1)S(1)} %bitcast.54), channel_id=1, source_target_pairs={{0,16},{8,24},{16,0},{24,8},{1,17},{9,25},{17,1},{25,9},{2,18},{10... | collective-permute-start | bytes 786440 | tf_op jit(solution)/shard_map/ppermute | solution.py:484
  30.4 3.6 %collective-permute-done.26.refs_1_ = bf16[2,32,2048]{2,1,0:T(8,128)(2,1)S(1)} collective-permute-done((bf16[2,32,2048]{2,1,0:T(8,128)(2,1)S(1)}, bf16[2,32,2048]{2,1,0:T(8,128)(2,1)S(1)}, u32[]{:S(2)}, u32[]{:S(2)}) %collective-permute-start.26) | collective-permute-done | bytes 262176 | tf_op jit(solution)/shard_map/ppermute | solution.py:484
  34.0 7.0 %collective-permute-done.27.refs_2_ = bf16[2,32,2048]{2,1,0:T(8,128)(2,1)S(1)} collective-permute-done((bf16[2,32,2048]{2,1,0:T(8,128)(2,1)S(1)}, bf16[2,32,2048]{2,1,0:T(8,128)(2,1)S(1)}, u32[]{:S(2)}, u32[]{:S(2)}) %collective-permute-start.27) | collective-permute-done | bytes 262176 | tf_op jit(solution)/shard_map/ppermute | solution.py:484
  41.0 0.5 collective-permute-start.31
  42.0 1.2 collective-permute-done.7.refs_14_
  44.2 4.7 %load.3 = (bf16[2,2048,512]{2,1,0:T(8,128)(2,1)S(1)}, bf16[2,2048,512]{2,1,0:T(8,128)(2,1)S(1)}, bf16[2,512,2048]{2,1,0:T(8,128)(2,1)S(1)}) custom-call(f32[192,8]{1,0:T(8,128)S(1)} %get-tuple-element.66.refs_0_.refs_1_, bf16[4,2048,512]{2,1,0:T(8,128)(2,1)} %refs_1_.3, bf16[4,2048,512]{2,1,0:T(8,128)(2,1)} %refs_2_.1, bf16[4,512,2048]{2,1,0:T(8,128)(2,1)} %refs_3_.1), custom_call_target="tpu_custom_call" | custom-call | tf_op jit(solution)/shard_map/load/pallas_call | solution.py:179
  48.9 3.6 %experts.3 = (bf16[2,32,2048]{2,1,0:T(8,128)(2,1)S(1)}, bf16[2,32,2048]{2,1,0:T(8,128)(2,1)S(1)}, bf16[2,32,2048]{2,1,0:T(8,128)(2,1)S(1)}, bf16[2,32,2048]{2,1,...) custom-call(bf16[2,32,2048]{2,1,0:T(8,128)(2,1)S(1)} %bitcast.44, ...), custom_call_target="tpu_custom_call" | custom-call | tf_op jit(solution)/shard_map/experts/pallas_call | solution.py:425
  53.6 2.2 %load.2.refs_10_ = bf16[2,512,2048]{2,1,0:T(8,128)(2,1)S(1)} custom-call(f32[192,8]{1,0:T(8,128)S(1)} %get-tuple-element.66.refs_0_.refs_1_, bf16[4,512,2048]{2,1,0:T(8,128)(2,1)} %refs_3_.1), custom_call_target="tpu_custom_call" | custom-call | tf_op jit(solution)/shard_map/load/pallas_call | solution.py:179
  55.9 6.3 %mix.2 = (bf16[96,2048]{1,0:T(8,128)(2,1)S(1)}, bf16[96,2048]{1,0:T(8,128)(2,1)S(1)}, bf16[2,2048,512]{2,1,0:T(8,128)(2,1)S(1)}, bf16[2,2048,512]{2,1,0:T(8,128)...) custom-call(s32[1]{0:T(128)} %bitcast.refs_0_, ...), custom_call_target="tpu_custom_call" | custom-call | tf_op jit(solution)/shard_map/mix/pallas_call | solution.py:285
  62.1 3.6 %experts.2 = (bf16[2,32,2048]{2,1,0:T(8,128)(2,1)S(1)}, bf16[2,32,2048]{2,1,0:T(8,128)(2,1)S(1)}, bf16[2,32,2048]{2,1,0:T(8,128)(2,1)S(1)}, bf16[2,32,2048]{2,1,...) custom-call(bf16[2,32,2048]{2,1,0:T(8,128)(2,1)S(1)} %bitcast.42, ...), custom_call_target="tpu_custom_call" | custom-call | tf_op jit(solution)/shard_map/experts/pallas_call | solution.py:425
  66.8 1.8 %collective-permute-start.37 = (bf16[2,32,1024]{2,1,0:T(8,128)(2,1)S(1)}, bf16[2,32,1024]{2,1,0:T(8,128)(2,1)S(1)}, u32[]{:S(2)}, u32[]{:S(2)}) collective-permute-start(bf16[2,32,1024]{2,1,0:T(8,128)(2,1)S(1)} %get-tuple-element.96), channel_id=1, source_target_pairs={{0,16},{8,24},{16,0},{24,8},{1,17},{9,25},{17,1},{25,9},{2,18},{10... | collective-permute-start | bytes 393224 | tf_op jit(solution)/shard_map/ppermute | solution.py:484
  68.8 3.3 %collective-permute-done.35 = bf16[2,32,1024]{2,1,0:T(8,128)(2,1)S(1)} collective-permute-done((bf16[2,32,1024]{2,1,0:T(8,128)(2,1)S(1)}, bf16[2,32,1024]{2,1,0:T(8,128)(2,1)S(1)}, u32[]{:S(2)}, u32[]{:S(2)}) %collective-permute-start.35) | collective-permute-done | bytes 131104 | tf_op jit(solution)/shard_map/ppermute | solution.py:484
  72.6 3.1 %collective-permute-start.39 = (bf16[2,32,1024]{2,1,0:T(8,128)(2,1)S(1)}, bf16[2,32,1024]{2,1,0:T(8,128)(2,1)S(1)}, u32[]{:S(2)}, u32[]{:S(2)}) collective-permute-start(bf16[2,32,1024]{2,1,0:T(8,128)(2,1)S(1)} %get-tuple-element.99), channel_id=1, source_target_pairs={{0,24},{8,16},{16,8},{24,0},{1,25},{9,17},{17,9},{25,1},{2,26},{10... | collective-permute-start | bytes 393224 | tf_op jit(solution)/shard_map/ppermute | solution.py:484
  75.9 0.5 collective-permute-start.23
  76.5 8.5 %collective-permute-done.39 = bf16[2,32,1024]{2,1,0:T(8,128)(2,1)S(1)} collective-permute-done((bf16[2,32,1024]{2,1,0:T(8,128)(2,1)S(1)}, bf16[2,32,1024]{2,1,0:T(8,128)(2,1)S(1)}, u32[]{:S(2)}, u32[]{:S(2)}) %collective-permute-start.39) | collective-permute-done | bytes 131104 | tf_op jit(solution)/shard_map/ppermute | solution.py:484
  85.2 6.2 %mix.3 = (bf16[96,2048]{1,0:T(8,128)(2,1)S(1)}, bf16[96,2048]{1,0:T(8,128)(2,1)S(1)}) custom-call(s32[1]{0:T(128)} %bitcast.refs_0_, bf16[4,96,256]{2,1,0:T(8,128)(2,1)S(1)} %get-tuple-element.57.refs_1_, bf16[4,96,256]{2,1,0:T(8,128)(2,1)S(1)} %collective-permute-done.refs_2_, f32[1,128]{1,0:T(1,128)} %bitcast.68, ...), custom_call_target="tpu_custom_call" | custom-call | tf_op jit(solution)/shard_map/mix/pallas_call | solution.py:285
  91.4 1.7 %collective-permute-start.9 = (bf16[96,2048]{1,0:T(8,128)(2,1)S(1)}, bf16[96,2048]{1,0:T(8,128)(2,1)S(1)}, u32[]{:S(2)}, u32[]{:S(2)}) collective-permute-start(bf16[96,2048]{1,0:T(8,128)(2,1)S(1)} %get-tuple-element.63), channel_id=1, source_target_pairs={{0,2},{2,0},{4,6},{6,4},{1,3},{3,1},{5,7},{7,5},{8,10},{10,8},{12,... | collective-permute-start | bytes 1179656 | tf_op jit(solution)/shard_map/ppermute | solution.py:484
  93.1 2.6 %collective-permute-start.10 = (bf16[96,2048]{1,0:T(8,128)(2,1)S(1)}, bf16[96,2048]{1,0:T(8,128)(2,1)S(1)}, u32[]{:S(2)}, u32[]{:S(2)}) collective-permute-start(bf16[96,2048]{1,0:T(8,128)(2,1)S(1)} %get-tuple-element.64), channel_id=1, source_target_pairs={{0,4},{2,6},{4,0},{6,2},{1,5},{3,7},{5,1},{7,3},{8,12},{10,14},{12... | collective-permute-start | bytes 1179656 | tf_op jit(solution)/shard_map/ppermute | solution.py:484
  95.9 1.8 %collective-permute-start.41 = (bf16[2,32,1024]{2,1,0:T(8,128)(2,1)S(1)}, bf16[2,32,1024]{2,1,0:T(8,128)(2,1)S(1)}, u32[]{:S(2)}, u32[]{:S(2)}) collective-permute-start(bf16[2,32,1024]{2,1,0:T(8,128)(2,1)S(1)} %get-tuple-element.103), channel_id=1, source_target_pairs={{0,16},{8,24},{16,0},{24,8},{1,17},{9,25},{17,1},{25,9},{2,18},{10... | collective-permute-start | bytes 393224 | tf_op jit(solution)/shard_map/ppermute | solution.py:484
  97.6 1.3 collective-permute-start.42
  99.0 0.8 combine.2
  99.8 1.0 collective-permute-done.41
  100.8 0.7 collective-permute-start.43
  101.5 2.0 %collective-permute-done.42 = bf16[2,32,1024]{2,1,0:T(8,128)(2,1)S(1)} collective-permute-done((bf16[2,32,1024]{2,1,0:T(8,128)(2,1)S(1)}, bf16[2,32,1024]{2,1,0:T(8,128)(2,1)S(1)}, u32[]{:S(2)}, u32[]{:S(2)}) %collective-permute-start.42) | collective-permute-done | bytes 131104 | tf_op jit(solution)/shard_map/ppermute | solution.py:484
  103.5 0.7 combine.3
  104.2 0.7 collective-permute-start.44
  105.0 4.6 %collective-permute-done.9.refs_1_ = bf16[96,2048]{1,0:T(8,128)(2,1)S(1)} collective-permute-done((bf16[96,2048]{1,0:T(8,128)(2,1)S(1)}, bf16[96,2048]{1,0:T(8,128)(2,1)S(1)}, u32[]{:S(2)}, u32[]{:S(2)}) %collective-permute-start.9) | collective-permute-done | bytes 393248 | tf_op jit(solution)/shard_map/ppermute | solution.py:484
  109.6 1.2 collective-permute-start.45
  110.8 17.0 %collective-permute-done.10.refs_2_ = bf16[96,2048]{1,0:T(8,128)(2,1)S(1)} collective-permute-done((bf16[96,2048]{1,0:T(8,128)(2,1)S(1)}, bf16[96,2048]{1,0:T(8,128)(2,1)S(1)}, u32[]{:S(2)}, u32[]{:S(2)}) %collective-permute-start.10) | collective-permute-done | bytes 393248 | tf_op jit(solution)/shard_map/ppermute | solution.py:484
  127.8 1.9 %collective-permute-start.47 = (bf16[48,1024]{1,0:T(8,128)(2,1)S(1)}, bf16[48,1024]{1,0:T(8,128)(2,1)S(1)}, u32[]{:S(2)}, u32[]{:S(2)}) collective-permute-start(bf16[48,1024]{1,0:T(8,128)(2,1)S(1)} %get-tuple-element.110), channel_id=1, source_target_pairs={{0,6},{2,4},{4,2},{6,0},{1,7},{3,5},{5,3},{7,1},{8,14},{10,12},{12... | collective-permute-start | bytes 294920 | tf_op jit(solution)/shard_map/ppermute | solution.py:484
  129.7 1.9 %collective-permute-start.48 = (bf16[48,1024]{1,0:T(8,128)(2,1)S(1)}, bf16[48,1024]{1,0:T(8,128)(2,1)S(1)}, u32[]{:S(2)}, u32[]{:S(2)}) collective-permute-start(bf16[48,1024]{1,0:T(8,128)(2,1)S(1)} %get-tuple-element.111), channel_id=1, source_target_pairs={{0,6},{2,4},{4,2},{6,0},{1,7},{3,5},{5,3},{7,1},{8,14},{10,12},{12... | collective-permute-start | bytes 294920 | tf_op jit(solution)/shard_map/ppermute | solution.py:484
  131.6 0.9 add.134
  132.6 7.9 %collective-permute-done.45.refs_4_ = bf16[48,1024]{1,0:T(8,128)(2,1)S(1)} collective-permute-done((bf16[48,1024]{1,0:T(8,128)(2,1)S(1)}, bf16[48,1024]{1,0:T(8,128)(2,1)S(1)}, u32[]{:S(2)}, u32[]{:S(2)}) %collective-permute-start.45) | collective-permute-done | bytes 98336 | tf_op jit(solution)/shard_map/ppermute | solution.py:484
  140.4 1.1 collective-permute-done.46.refs_5_
  141.5 0.8 join.1
  (79 shorter events, 6.2 us)
Async XLA Ops:
  3.1 7.5 %collective-permute-start = (bf16[4,96,256]{2,1,0:T(8,128)(2,1)S(1)}, bf16[4,96,256]{2,1,0:T(8,128)(2,1)S(1)}, u32[]{:S(2)}, u32[]{:S(2)}) collective-permute-start(bf16[4,96,256]{2,1,0:T(8,128)(2,1)S(1)} %get-tuple-element.58), channel_id=1, source_target_pairs={{0,1},{1,0},{2,3},{3,2},{4,5},{5,4},{6,7},{7,6},{8,9},{9,8},{10,11... | collective-permute-start | bytes 589832 | tf_op jit(solution)/shard_map/ppermute | solution.py:488
  3.7 9.0 %collective-permute-start.2 = (bf16[2,384,128]{2,1,0:T(8,128)(2,1)S(1)}, bf16[2,384,128]{2,1,0:T(8,128)(2,1)S(1)}, u32[]{:S(2)}, u32[]{:S(2)}) collective-permute-start(bf16[2,384,128]{2,1,0:T(8,128)(2,1)S(1)} %get-tuple-element.59.refs_8_), channel_id=1, source_target_pairs={{0,8},{8,0},{16,24},{24,16},{1,9},{9,1},{17,25},{25,17},{2,10},{10... | collective-permute-start | bytes 589832 | tf_op jit(solution)/shard_map/ppermute | solution.py:484
  6.2 11.1 %collective-permute-start.3 = (bf16[2,384,128]{2,1,0:T(8,128)(2,1)S(1)}, bf16[2,384,128]{2,1,0:T(8,128)(2,1)S(1)}, u32[]{:S(2)}, u32[]{:S(2)}) collective-permute-start(bf16[2,384,128]{2,1,0:T(8,128)(2,1)S(1)} %get-tuple-element.59.refs_8_), channel_id=1, source_target_pairs={{0,16},{8,24},{16,0},{24,8},{1,17},{9,25},{17,1},{25,9},{2,18},{10... | collective-permute-start | bytes 589832 | tf_op jit(solution)/shard_map/ppermute | solution.py:484
  7.7 11.3 %collective-permute-start.4 = (bf16[2,384,128]{2,1,0:T(8,128)(2,1)S(1)}, bf16[2,384,128]{2,1,0:T(8,128)(2,1)S(1)}, u32[]{:S(2)}, u32[]{:S(2)}) collective-permute-start(bf16[2,384,128]{2,1,0:T(8,128)(2,1)S(1)} %get-tuple-element.59.refs_8_), channel_id=1, source_target_pairs={{0,24},{8,16},{16,8},{24,0},{1,25},{9,17},{17,9},{25,1},{2,26},{10... | collective-permute-start | bytes 589832 | tf_op jit(solution)/shard_map/ppermute | solution.py:484
  7.8 11.3 %collective-permute-start.5 = (bf16[2,384,128]{2,1,0:T(8,128)(2,1)S(1)}, bf16[2,384,128]{2,1,0:T(8,128)(2,1)S(1)}, u32[]{:S(2)}, u32[]{:S(2)}) collective-permute-start(bf16[2,384,128]{2,1,0:T(8,128)(2,1)S(1)} %get-tuple-element.59.refs_8_), channel_id=1, source_target_pairs={{0,1},{1,0},{2,3},{3,2},{4,5},{5,4},{6,7},{7,6},{8,9},{9,8},{10,11... | collective-permute-start | bytes 589832 | tf_op jit(solution)/shard_map/ppermute | solution.py:488
  10.6 11.2 %collective-permute-start.12 = (bf16[2,32,2048]{2,1,0:T(8,128)(2,1)S(1)}, bf16[2,32,2048]{2,1,0:T(8,128)(2,1)S(1)}, u32[]{:S(2)}, u32[]{:S(2)}) collective-permute-start(bf16[2,32,2048]{2,1,0:T(8,128)(2,1)S(1)} %bitcast.58), channel_id=1, source_target_pairs={{0,8},{8,0},{16,24},{24,16},{1,9},{9,1},{17,25},{25,17},{2,10},{10... | collective-permute-start | bytes 786440 | tf_op jit(solution)/shard_map/ppermute | solution.py:484
  12.6 15.6 %collective-permute-start.13 = (bf16[2,32,2048]{2,1,0:T(8,128)(2,1)S(1)}, bf16[2,32,2048]{2,1,0:T(8,128)(2,1)S(1)}, u32[]{:S(2)}, u32[]{:S(2)}) collective-permute-start(bf16[2,32,2048]{2,1,0:T(8,128)(2,1)S(1)} %bitcast.57), channel_id=1, source_target_pairs={{0,16},{8,24},{16,0},{24,8},{1,17},{9,25},{17,1},{25,9},{2,18},{10... | collective-permute-start | bytes 786440 | tf_op jit(solution)/shard_map/ppermute | solution.py:484
  17.4 12.8 %collective-permute-start.14 = (bf16[2,32,2048]{2,1,0:T(8,128)(2,1)S(1)}, bf16[2,32,2048]{2,1,0:T(8,128)(2,1)S(1)}, u32[]{:S(2)}, u32[]{:S(2)}) collective-permute-start(bf16[2,32,2048]{2,1,0:T(8,128)(2,1)S(1)} %bitcast.56), channel_id=1, source_target_pairs={{0,24},{8,16},{16,8},{24,0},{1,25},{9,17},{17,9},{25,1},{2,26},{10... | collective-permute-start | bytes 786440 | tf_op jit(solution)/shard_map/ppermute | solution.py:484
  19.0 11.4 %collective-permute-start.15 = (bf16[2,32,2048]{2,1,0:T(8,128)(2,1)S(1)}, bf16[2,32,2048]{2,1,0:T(8,128)(2,1)S(1)}, u32[]{:S(2)}, u32[]{:S(2)}) collective-permute-start(bf16[2,32,2048]{2,1,0:T(8,128)(2,1)S(1)} %bitcast.41), channel_id=1, source_target_pairs={{0,1},{1,0},{2,3},{3,2},{4,5},{5,4},{6,7},{7,6},{8,9},{9,8},{10,11... | collective-permute-start | bytes 786440 | tf_op jit(solution)/shard_map/ppermute | solution.py:488
  19.0 34.2 %collective-permute-start.1 = (bf16[256,2048]{1,0:T(8,128)(2,1)S(1)}, bf16[256,2048]{1,0:T(8,128)(2,1)S(1)}, u32[]{:S(2)}, u32[]{:S(2)}) collective-permute-start(bf16[256,2048]{1,0:T(8,128)(2,1)S(1)} %copy-done), channel_id=1, source_target_pairs={{0,1},{1,0},{2,3},{3,2},{4,5},{5,4},{6,7},{7,6},{8,9},{9,8},{10,11... | collective-permute-start | bytes 3145736 | tf_op jit(solution)/shard_map/ppermute | solution.py:488
  21.9 12.2 %collective-permute-start.26 = (bf16[2,32,2048]{2,1,0:T(8,128)(2,1)S(1)}, bf16[2,32,2048]{2,1,0:T(8,128)(2,1)S(1)}, u32[]{:S(2)}, u32[]{:S(2)}) collective-permute-start(bf16[2,32,2048]{2,1,0:T(8,128)(2,1)S(1)} %bitcast.55), channel_id=1, source_target_pairs={{0,8},{8,0},{16,24},{24,16},{1,9},{9,1},{17,25},{25,17},{2,10},{10... | collective-permute-start | bytes 786440 | tf_op jit(solution)/shard_map/ppermute | solution.py:484
  28.3 12.7 %collective-permute-start.27 = (bf16[2,32,2048]{2,1,0:T(8,128)(2,1)S(1)}, bf16[2,32,2048]{2,1,0:T(8,128)(2,1)S(1)}, u32[]{:S(2)}, u32[]{:S(2)}) collective-permute-start(bf16[2,32,2048]{2,1,0:T(8,128)(2,1)S(1)} %bitcast.54), channel_id=1, source_target_pairs={{0,16},{8,24},{16,0},{24,8},{1,17},{9,25},{17,1},{25,9},{2,18},{10... | collective-permute-start | bytes 786440 | tf_op jit(solution)/shard_map/ppermute | solution.py:484
  30.2 10.8 %collective-permute-start.28 = (bf16[2,32,2048]{2,1,0:T(8,128)(2,1)S(1)}, bf16[2,32,2048]{2,1,0:T(8,128)(2,1)S(1)}, u32[]{:S(2)}, u32[]{:S(2)}) collective-permute-start(bf16[2,32,2048]{2,1,0:T(8,128)(2,1)S(1)} %bitcast.53), channel_id=1, source_target_pairs={{0,24},{8,16},{16,8},{24,0},{1,25},{9,17},{17,9},{25,1},{2,26},{10... | collective-permute-start | bytes 786440 | tf_op jit(solution)/shard_map/ppermute | solution.py:484
  30.4 11.1 %collective-permute-start.29 = (bf16[2,32,2048]{2,1,0:T(8,128)(2,1)S(1)}, bf16[2,32,2048]{2,1,0:T(8,128)(2,1)S(1)}, u32[]{:S(2)}, u32[]{:S(2)}) collective-permute-start(bf16[2,32,2048]{2,1,0:T(8,128)(2,1)S(1)} %bitcast.43), channel_id=1, source_target_pairs={{0,1},{1,0},{2,3},{3,2},{4,5},{5,4},{6,7},{7,6},{8,9},{9,8},{10,11... | collective-permute-start | bytes 786440 | tf_op jit(solution)/shard_map/ppermute | solution.py:488
  34.0 7.6 %collective-permute-start.6 = (bf16[2,384,128]{2,1,0:T(8,128)(2,1)S(1)}, bf16[2,384,128]{2,1,0:T(8,128)(2,1)S(1)}, u32[]{:S(2)}, u32[]{:S(2)}) collective-permute-start(bf16[2,384,128]{2,1,0:T(8,128)(2,1)S(1)} %collective-permute-done.2.refs_9_), channel_id=1, source_target_pairs={{0,1},{1,0},{2,3},{3,2},{4,5},{5,4},{6,7},{7,6},{8,9},{9,8},{10,11... | collective-permute-start | bytes 589832 | tf_op jit(solution)/shard_map/ppermute | solution.py:488
  41.0 2.3 %collective-permute-start.30 = (bf16[2,32,2048]{2,1,0:T(8,128)(2,1)S(1)}, bf16[2,32,2048]{2,1,0:T(8,128)(2,1)S(1)}, u32[]{:S(2)}, u32[]{:S(2)}) collective-permute-start(bf16[2,32,2048]{2,1,0:T(8,128)(2,1)S(1)} %collective-permute-done.26.refs_1_), channel_id=1, source_target_pairs={{0,1},{1,0},{2,3},{3,2},{4,5},{5,4},{6,7},{7,6},{8,9},{9,8},{10,11... | collective-permute-start | bytes 786440 | tf_op jit(solution)/shard_map/ppermute | solution.py:488
  41.0 2.7 %collective-permute-start.31 = (bf16[2,32,2048]{2,1,0:T(8,128)(2,1)S(1)}, bf16[2,32,2048]{2,1,0:T(8,128)(2,1)S(1)}, u32[]{:S(2)}, u32[]{:S(2)}) collective-permute-start(bf16[2,32,2048]{2,1,0:T(8,128)(2,1)S(1)} %collective-permute-done.27.refs_2_), channel_id=1, source_target_pairs={{0,1},{1,0},{2,3},{3,2},{4,5},{5,4},{6,7},{7,6},{8,9},{9,8},{10,11... | collective-permute-start | bytes 786440 | tf_op jit(solution)/shard_map/ppermute | solution.py:488
  41.6 2.3 %collective-permute-start.32 = (bf16[2,32,2048]{2,1,0:T(8,128)(2,1)S(1)}, bf16[2,32,2048]{2,1,0:T(8,128)(2,1)S(1)}, u32[]{:S(2)}, u32[]{:S(2)}) collective-permute-start(bf16[2,32,2048]{2,1,0:T(8,128)(2,1)S(1)} %collective-permute-done.28.refs_3_), channel_id=1, source_target_pairs={{0,1},{1,0},{2,3},{3,2},{4,5},{5,4},{6,7},{7,6},{8,9},{9,8},{10,11... | collective-permute-start | bytes 786440 | tf_op jit(solution)/shard_map/ppermute | solution.py:488
  43.2 9.6 %collective-permute-start.16 = (bf16[2,32,2048]{2,1,0:T(8,128)(2,1)S(1)}, bf16[2,32,2048]{2,1,0:T(8,128)(2,1)S(1)}, u32[]{:S(2)}, u32[]{:S(2)}) collective-permute-start(bf16[2,32,2048]{2,1,0:T(8,128)(2,1)S(1)} %collective-permute-done.12.refs_1_), channel_id=1, source_target_pairs={{0,1},{1,0},{2,3},{3,2},{4,5},{5,4},{6,7},{7,6},{8,9},{9,8},{10,11... | collective-permute-start | bytes 786440 | tf_op jit(solution)/shard_map/ppermute | solution.py:488
  43.3 9.8 %collective-permute-start.17 = (bf16[2,32,2048]{2,1,0:T(8,128)(2,1)S(1)}, bf16[2,32,2048]{2,1,0:T(8,128)(2,1)S(1)}, u32[]{:S(2)}, u32[]{:S(2)}) collective-permute-start(bf16[2,32,2048]{2,1,0:T(8,128)(2,1)S(1)} %collective-permute-done.13.refs_2_), channel_id=1, source_target_pairs={{0,1},{1,0},{2,3},{3,2},{4,5},{5,4},{6,7},{7,6},{8,9},{9,8},{10,11... | collective-permute-start | bytes 786440 | tf_op jit(solution)/shard_map/ppermute | solution.py:488
  43.7 8.8 %collective-permute-start.8 = (bf16[2,384,128]{2,1,0:T(8,128)(2,1)S(1)}, bf16[2,384,128]{2,1,0:T(8,128)(2,1)S(1)}, u32[]{:S(2)}, u32[]{:S(2)}) collective-permute-start(bf16[2,384,128]{2,1,0:T(8,128)(2,1)S(1)} %collective-permute-done.4.refs_11_), channel_id=1, source_target_pairs={{0,1},{1,0},{2,3},{3,2},{4,5},{5,4},{6,7},{7,6},{8,9},{9,8},{10,11... | collective-permute-start | bytes 589832 | tf_op jit(solution)/shard_map/ppermute | solution.py:488
  43.9 18.3 %collective-permute-start.18 = (bf16[2,32,2048]{2,1,0:T(8,128)(2,1)S(1)}, bf16[2,32,2048]{2,1,0:T(8,128)(2,1)S(1)}, u32[]{:S(2)}, u32[]{:S(2)}) collective-permute-start(bf16[2,32,2048]{2,1,0:T(8,128)(2,1)S(1)} %collective-permute-done.14.refs_3_), channel_id=1, source_target_pairs={{0,1},{1,0},{2,3},{3,2},{4,5},{5,4},{6,7},{7,6},{8,9},{9,8},{10,11... | collective-permute-start | bytes 786440 | tf_op jit(solution)/shard_map/ppermute | solution.py:488
  52.5 13.4 %collective-permute-start.34 = (bf16[2,32,2048]{2,1,0:T(8,128)(2,1)S(1)}, bf16[2,32,2048]{2,1,0:T(8,128)(2,1)S(1)}, u32[]{:S(2)}, u32[]{:S(2)}) collective-permute-start(bf16[2,32,2048]{2,1,0:T(8,128)(2,1)S(1)} %get-tuple-element.92), channel_id=1, source_target_pairs={{0,1},{1,0},{2,3},{3,2},{4,5},{5,4},{6,7},{7,6},{8,9},{9,8},{10,11... | collective-permute-start | bytes 786440 | tf_op jit(solution)/shard_map/ppermute | solution.py:488
  52.8 13.7 %collective-permute-start.33 = (bf16[2,32,2048]{2,1,0:T(8,128)(2,1)S(1)}, bf16[2,32,2048]{2,1,0:T(8,128)(2,1)S(1)}, u32[]{:S(2)}, u32[]{:S(2)}) collective-permute-start(bf16[2,32,2048]{2,1,0:T(8,128)(2,1)S(1)} %get-tuple-element.89), channel_id=1, source_target_pairs={{0,1},{1,0},{2,3},{3,2},{4,5},{5,4},{6,7},{7,6},{8,9},{9,8},{10,11... | collective-permute-start | bytes 786440 | tf_op jit(solution)/shard_map/ppermute | solution.py:488
  53.1 13.4 %collective-permute-start.36 = (bf16[2,32,2048]{2,1,0:T(8,128)(2,1)S(1)}, bf16[2,32,2048]{2,1,0:T(8,128)(2,1)S(1)}, u32[]{:S(2)}, u32[]{:S(2)}) collective-permute-start(bf16[2,32,2048]{2,1,0:T(8,128)(2,1)S(1)} %get-tuple-element.95), channel_id=1, source_target_pairs={{0,1},{1,0},{2,3},{3,2},{4,5},{5,4},{6,7},{7,6},{8,9},{9,8},{10,11... | collective-permute-start | bytes 786440 | tf_op jit(solution)/shard_map/ppermute | solution.py:488
  53.3 13.5 %collective-permute-start.38 = (bf16[2,32,2048]{2,1,0:T(8,128)(2,1)S(1)}, bf16[2,32,2048]{2,1,0:T(8,128)(2,1)S(1)}, u32[]{:S(2)}, u32[]{:S(2)}) collective-permute-start(bf16[2,32,2048]{2,1,0:T(8,128)(2,1)S(1)} %get-tuple-element.98), channel_id=1, source_target_pairs={{0,1},{1,0},{2,3},{3,2},{4,5},{5,4},{6,7},{7,6},{8,9},{9,8},{10,11... | collective-permute-start | bytes 786440 | tf_op jit(solution)/shard_map/ppermute | solution.py:488
  65.8 2.9 %collective-permute-start.20 = (bf16[2,32,2048]{2,1,0:T(8,128)(2,1)S(1)}, bf16[2,32,2048]{2,1,0:T(8,128)(2,1)S(1)}, u32[]{:S(2)}, u32[]{:S(2)}) collective-permute-start(bf16[2,32,2048]{2,1,0:T(8,128)(2,1)S(1)} %get-tuple-element.76), channel_id=1, source_target_pairs={{0,1},{1,0},{2,3},{3,2},{4,5},{5,4},{6,7},{7,6},{8,9},{9,8},{10,11... | collective-permute-start | bytes 786440 | tf_op jit(solution)/shard_map/ppermute | solution.py:488
  66.0 9.8 %collective-permute-start.22 = (bf16[2,32,2048]{2,1,0:T(8,128)(2,1)S(1)}, bf16[2,32,2048]{2,1,0:T(8,128)(2,1)S(1)}, u32[]{:S(2)}, u32[]{:S(2)}) collective-permute-start(bf16[2,32,2048]{2,1,0:T(8,128)(2,1)S(1)} %get-tuple-element.78), channel_id=1, source_target_pairs={{0,1},{1,0},{2,3},{3,2},{4,5},{5,4},{6,7},{7,6},{8,9},{9,8},{10,11... | collective-permute-start | bytes 786440 | tf_op jit(solution)/shard_map/ppermute | solution.py:488
  66.4 5.6 %collective-permute-start.35 = (bf16[2,32,1024]{2,1,0:T(8,128)(2,1)S(1)}, bf16[2,32,1024]{2,1,0:T(8,128)(2,1)S(1)}, u32[]{:S(2)}, u32[]{:S(2)}) collective-permute-start(bf16[2,32,1024]{2,1,0:T(8,128)(2,1)S(1)} %get-tuple-element.93), channel_id=1, source_target_pairs={{0,8},{8,0},{16,24},{24,16},{1,9},{9,1},{17,25},{25,17},{2,10},{10... | collective-permute-start | bytes 393224 | tf_op jit(solution)/shard_map/ppermute | solution.py:484
  66.5 9.4 %collective-permute-start.24 = (bf16[2,32,2048]{2,1,0:T(8,128)(2,1)S(1)}, bf16[2,32,2048]{2,1,0:T(8,128)(2,1)S(1)}, u32[]{:S(2)}, u32[]{:S(2)}) collective-permute-start(bf16[2,32,2048]{2,1,0:T(8,128)(2,1)S(1)} %get-tuple-element.80), channel_id=1, source_target_pairs={{0,1},{1,0},{2,3},{3,2},{4,5},{5,4},{6,7},{7,6},{8,9},{9,8},{10,11... | collective-permute-start | bytes 786440 | tf_op jit(solution)/shard_map/ppermute | solution.py:488
  66.8 5.8 %collective-permute-start.37 = (bf16[2,32,1024]{2,1,0:T(8,128)(2,1)S(1)}, bf16[2,32,1024]{2,1,0:T(8,128)(2,1)S(1)}, u32[]{:S(2)}, u32[]{:S(2)}) collective-permute-start(bf16[2,32,1024]{2,1,0:T(8,128)(2,1)S(1)} %get-tuple-element.96), channel_id=1, source_target_pairs={{0,16},{8,24},{16,0},{24,8},{1,17},{9,25},{17,1},{25,9},{2,18},{10... | collective-permute-start | bytes 393224 | tf_op jit(solution)/shard_map/ppermute | solution.py:484
  68.6 24.4 %collective-permute-start.19 = (bf16[2,32,2048]{2,1,0:T(8,128)(2,1)S(1)}, bf16[2,32,2048]{2,1,0:T(8,128)(2,1)S(1)}, u32[]{:S(2)}, u32[]{:S(2)}) collective-permute-start(bf16[2,32,2048]{2,1,0:T(8,128)(2,1)S(1)} %get-tuple-element.74), channel_id=1, source_target_pairs={{0,1},{1,0},{2,3},{3,2},{4,5},{5,4},{6,7},{7,6},{8,9},{9,8},{10,11... | collective-permute-start | bytes 786440 | tf_op jit(solution)/shard_map/ppermute | solution.py:488
  72.0 23.6 %collective-permute-start.21 = (bf16[2,32,2048]{2,1,0:T(8,128)(2,1)S(1)}, bf16[2,32,2048]{2,1,0:T(8,128)(2,1)S(1)}, u32[]{:S(2)}, u32[]{:S(2)}) collective-permute-start(bf16[2,32,2048]{2,1,0:T(8,128)(2,1)S(1)} %add.136), channel_id=1, source_target_pairs={{0,8},{8,0},{16,24},{24,16},{1,9},{9,1},{17,25},{25,17},{2,10},{10... | collective-permute-start | bytes 786440 | tf_op jit(solution)/shard_map/ppermute | solution.py:484
  72.6 12.4 %collective-permute-start.39 = (bf16[2,32,1024]{2,1,0:T(8,128)(2,1)S(1)}, bf16[2,32,1024]{2,1,0:T(8,128)(2,1)S(1)}, u32[]{:S(2)}, u32[]{:S(2)}) collective-permute-start(bf16[2,32,1024]{2,1,0:T(8,128)(2,1)S(1)} %get-tuple-element.99), channel_id=1, source_target_pairs={{0,24},{8,16},{16,8},{24,0},{1,25},{9,17},{17,9},{25,1},{2,26},{10... | collective-permute-start | bytes 393224 | tf_op jit(solution)/shard_map/ppermute | solution.py:484
  75.8 15.6 %collective-permute-start.40 = (bf16[2,32,1024]{2,1,0:T(8,128)(2,1)S(1)}, bf16[2,32,1024]{2,1,0:T(8,128)(2,1)S(1)}, u32[]{:S(2)}, u32[]{:S(2)}) collective-permute-start(bf16[2,32,1024]{2,1,0:T(8,128)(2,1)S(1)} %get-tuple-element.102), channel_id=1, source_target_pairs={{0,8},{8,0},{16,24},{24,16},{1,9},{9,1},{17,25},{25,17},{2,10},{10... | collective-permute-start | bytes 393224 | tf_op jit(solution)/shard_map/ppermute | solution.py:484
  75.9 19.9 %collective-permute-start.23 = (bf16[2,32,2048]{2,1,0:T(8,128)(2,1)S(1)}, bf16[2,32,2048]{2,1,0:T(8,128)(2,1)S(1)}, u32[]{:S(2)}, u32[]{:S(2)}) collective-permute-start(bf16[2,32,2048]{2,1,0:T(8,128)(2,1)S(1)} %add.137), channel_id=1, source_target_pairs={{0,16},{8,24},{16,0},{24,8},{1,17},{9,25},{17,1},{25,9},{2,18},{10... | collective-permute-start | bytes 786440 | tf_op jit(solution)/shard_map/ppermute | solution.py:484
  85.0 12.6 %collective-permute-start.25 = (bf16[2,32,2048]{2,1,0:T(8,128)(2,1)S(1)}, bf16[2,32,2048]{2,1,0:T(8,128)(2,1)S(1)}, u32[]{:S(2)}, u32[]{:S(2)}) collective-permute-start(bf16[2,32,2048]{2,1,0:T(8,128)(2,1)S(1)} %add.138), channel_id=1, source_target_pairs={{0,24},{8,16},{16,8},{24,0},{1,25},{9,17},{17,9},{25,1},{2,26},{10... | collective-permute-start | bytes 786440 | tf_op jit(solution)/shard_map/ppermute | solution.py:484
  91.4 18.2 %collective-permute-start.9 = (bf16[96,2048]{1,0:T(8,128)(2,1)S(1)}, bf16[96,2048]{1,0:T(8,128)(2,1)S(1)}, u32[]{:S(2)}, u32[]{:S(2)}) collective-permute-start(bf16[96,2048]{1,0:T(8,128)(2,1)S(1)} %get-tuple-element.63), channel_id=1, source_target_pairs={{0,2},{2,0},{4,6},{6,4},{1,3},{3,1},{5,7},{7,5},{8,10},{10,8},{12,... | collective-permute-start | bytes 1179656 | tf_op jit(solution)/shard_map/ppermute | solution.py:484
  93.1 34.7 %collective-permute-start.10 = (bf16[96,2048]{1,0:T(8,128)(2,1)S(1)}, bf16[96,2048]{1,0:T(8,128)(2,1)S(1)}, u32[]{:S(2)}, u32[]{:S(2)}) collective-permute-start(bf16[96,2048]{1,0:T(8,128)(2,1)S(1)} %get-tuple-element.64), channel_id=1, source_target_pairs={{0,4},{2,6},{4,0},{6,2},{1,5},{3,7},{5,1},{7,3},{8,12},{10,14},{12... | collective-permute-start | bytes 1179656 | tf_op jit(solution)/shard_map/ppermute | solution.py:484
  95.6 32.2 %collective-permute-start.11 = (bf16[96,2048]{1,0:T(8,128)(2,1)S(1)}, bf16[96,2048]{1,0:T(8,128)(2,1)S(1)}, u32[]{:S(2)}, u32[]{:S(2)}) collective-permute-start(bf16[96,2048]{1,0:T(8,128)(2,1)S(1)} %get-tuple-element.65), channel_id=1, source_target_pairs={{0,6},{2,4},{4,2},{6,0},{1,7},{3,5},{5,3},{7,1},{8,14},{10,12},{12... | collective-permute-start | bytes 1179656 | tf_op jit(solution)/shard_map/ppermute | solution.py:484
  95.9 5.0 %collective-permute-start.41 = (bf16[2,32,1024]{2,1,0:T(8,128)(2,1)S(1)}, bf16[2,32,1024]{2,1,0:T(8,128)(2,1)S(1)}, u32[]{:S(2)}, u32[]{:S(2)}) collective-permute-start(bf16[2,32,1024]{2,1,0:T(8,128)(2,1)S(1)} %get-tuple-element.103), channel_id=1, source_target_pairs={{0,16},{8,24},{16,0},{24,8},{1,17},{9,25},{17,1},{25,9},{2,18},{10... | collective-permute-start | bytes 393224 | tf_op jit(solution)/shard_map/ppermute | solution.py:484
  97.6 5.9 %collective-permute-start.42 = (bf16[2,32,1024]{2,1,0:T(8,128)(2,1)S(1)}, bf16[2,32,1024]{2,1,0:T(8,128)(2,1)S(1)}, u32[]{:S(2)}, u32[]{:S(2)}) collective-permute-start(bf16[2,32,1024]{2,1,0:T(8,128)(2,1)S(1)} %get-tuple-element.104), channel_id=1, source_target_pairs={{0,24},{8,16},{16,8},{24,0},{1,25},{9,17},{17,9},{25,1},{2,26},{10... | collective-permute-start | bytes 393224 | tf_op jit(solution)/shard_map/ppermute | solution.py:484
  100.8 28.9 %collective-permute-start.43 = (bf16[48,1024]{1,0:T(8,128)(2,1)S(1)}, bf16[48,1024]{1,0:T(8,128)(2,1)S(1)}, u32[]{:S(2)}, u32[]{:S(2)}) collective-permute-start(bf16[48,1024]{1,0:T(8,128)(2,1)S(1)} %get-tuple-element.106), channel_id=1, source_target_pairs={{0,2},{2,0},{4,6},{6,4},{1,3},{3,1},{5,7},{7,5},{8,10},{10,8},{12,... | collective-permute-start | bytes 294920 | tf_op jit(solution)/shard_map/ppermute | solution.py:484
  104.2 28.3 %collective-permute-start.44 = (bf16[48,1024]{1,0:T(8,128)(2,1)S(1)}, bf16[48,1024]{1,0:T(8,128)(2,1)S(1)}, u32[]{:S(2)}, u32[]{:S(2)}) collective-permute-start(bf16[48,1024]{1,0:T(8,128)(2,1)S(1)} %get-tuple-element.107), channel_id=1, source_target_pairs={{0,2},{2,0},{4,6},{6,4},{1,3},{3,1},{5,7},{7,5},{8,10},{10,8},{12,... | collective-permute-start | bytes 294920 | tf_op jit(solution)/shard_map/ppermute | solution.py:484
  109.6 30.8 %collective-permute-start.45 = (bf16[48,1024]{1,0:T(8,128)(2,1)S(1)}, bf16[48,1024]{1,0:T(8,128)(2,1)S(1)}, u32[]{:S(2)}, u32[]{:S(2)}) collective-permute-start(bf16[48,1024]{1,0:T(8,128)(2,1)S(1)} %get-tuple-element.108), channel_id=1, source_target_pairs={{0,4},{2,6},{4,0},{6,2},{1,5},{3,7},{5,1},{7,3},{8,12},{10,14},{12... | collective-permute-start | bytes 294920 | tf_op jit(solution)/shard_map/ppermute | solution.py:484
  127.8 13.7 %collective-permute-start.46 = (bf16[48,1024]{1,0:T(8,128)(2,1)S(1)}, bf16[48,1024]{1,0:T(8,128)(2,1)S(1)}, u32[]{:S(2)}, u32[]{:S(2)}) collective-permute-start(bf16[48,1024]{1,0:T(8,128)(2,1)S(1)} %get-tuple-element.109), channel_id=1, source_target_pairs={{0,4},{2,6},{4,0},{6,2},{1,5},{3,7},{5,1},{7,3},{8,12},{10,14},{12... | collective-permute-start | bytes 294920 | tf_op jit(solution)/shard_map/ppermute | solution.py:484
  127.8 13.7 %collective-permute-start.47 = (bf16[48,1024]{1,0:T(8,128)(2,1)S(1)}, bf16[48,1024]{1,0:T(8,128)(2,1)S(1)}, u32[]{:S(2)}, u32[]{:S(2)}) collective-permute-start(bf16[48,1024]{1,0:T(8,128)(2,1)S(1)} %get-tuple-element.110), channel_id=1, source_target_pairs={{0,6},{2,4},{4,2},{6,0},{1,7},{3,5},{5,3},{7,1},{8,14},{10,12},{12... | collective-permute-start | bytes 294920 | tf_op jit(solution)/shard_map/ppermute | solution.py:484
  129.7 11.8 %collective-permute-start.48 = (bf16[48,1024]{1,0:T(8,128)(2,1)S(1)}, bf16[48,1024]{1,0:T(8,128)(2,1)S(1)}, u32[]{:S(2)}, u32[]{:S(2)}) collective-permute-start(bf16[48,1024]{1,0:T(8,128)(2,1)S(1)} %get-tuple-element.111), channel_id=1, source_target_pairs={{0,6},{2,4},{4,2},{6,0},{1,7},{3,5},{5,3},{7,1},{8,14},{10,12},{12... | collective-permute-start | bytes 294920 | tf_op jit(solution)/shard_map/ppermute | solution.py:484
  (2 other events, 20.1 us)
